TPU v7x, 128 devices: a 2x2x16 block of a 8x8x16 slice. The times are simulated.
128 devices in a mesh: grp: 4 (over y, x), ep: 32 (over z, core).
Axes of the slice: x: 2, y: 2, z: 16, core: 2. Of those that a mesh axis runs over, the one named last changes fastest.
The devices are a block of a 8x8x16 slice.
Arguments:
- resid: bfloat16 [1536, 2048], P(('grp', 'ep')), parts along dimension 0, may hold values from -6 to 6
- norm_gains: float32 [4, 2048], replicated, may hold values from 0.1 to 1.9
- w_query: bfloat16 [2048, 1024], P(None, 'ep'), may hold values from -0.125 to 0.125
- w_key: bfloat16 [2048, 1024], P(None, 'ep'), may hold values from -0.125 to 0.125
- w_value: bfloat16 [2048, 1024], P(None, 'ep'), may hold values from -0.125 to 0.125
- w_outgate: bfloat16 [2048, 1024], P(None, 'ep'), may hold values from -0.125 to 0.125
- w_igate: bfloat16 [2048, 8], replicated, may hold values from -0.125 to 0.125
- w_fgate: bfloat16 [2048, 8], replicated, may hold values from -0.125 to 0.125
- igate_bias: float32 [8], replicated, may hold values from -1 to 1
- fgate_bias: float32 [8], replicated, may hold values from -1 to 5
- state_matrix: float32 [1536, 8, 128, 128], P(('grp', 'ep')), parts along dimension 0, may hold values from -0.8 to 0.8
- state_norm: float32 [1536, 8, 128], P(('grp', 'ep')), parts along dimension 0, may hold values from -2.4 to 2.4
- state_max: float32 [1536, 8], P(('grp', 'ep')), parts along dimension 0, may hold values from -1 to 1
- w_mix_out: bfloat16 [1024, 2048], replicated, may hold values from -0.1875 to 0.1875
- routes: int32 [1536, 2], P(('grp', 'ep')), parts along dimension 0, may hold values from 0 to 31, all different within a row; in each aligned block of 12 rows (0 to 11, 12 to 23, ...) at most 2 rows name the same one
- route_scores: bfloat16 [1536, 2], P(('grp', 'ep')), parts along dimension 0, may hold values from 0.099609375 to 1
- expert_gate: bfloat16 [32, 2048, 512], P('ep'), may hold values from -0.125 to 0.125
- expert_up: bfloat16 [32, 2048, 512], P('ep'), may hold values from -0.125 to 0.125
- expert_down: bfloat16 [32, 512, 2048], P('ep'), may hold values from -0.25 to 0.25
- dense_gate: bfloat16 [2048, 8192], P(None, 'ep'), may hold values from -0.125 to 0.125
- dense_up: bfloat16 [2048, 8192], P(None, 'ep'), may hold values from -0.125 to 0.125
- dense_down: bfloat16 [8192, 2048], P('ep'), may hold values from -0.0625 to 0.0625
- branch_weight: bfloat16 [2048], replicated, may hold values from -0.125 to 0.125
Outputs:
- out_stream: bfloat16 [1536, 2048], P(('grp', 'ep')), parts along dimension 0
- new_matrix: float32 [1536, 8, 128, 128], P(('grp', 'ep')), parts along dimension 0
- new_norm: float32 [1536, 8, 128], P(('grp', 'ep')), parts along dimension 0
- new_max: float32 [1536, 8], P(('grp', 'ep')), parts along dimension 0
There are 4 independent parts, one for each index of `grp`. A program takes and returns all parts, laid end to end along the dimension named above; an argument that names none is the same for every part. Nothing has to cross between parts.
Inputs may be any that keep to these rules, and one draw needn't show every extreme that they name: `routes`: each row names 2 different experts. In each aligned block of 12 rows (the rows of one device) no expert is named by more than 2 rows, a bound that some block reaches.
All inputs are finite; a program needn't handle non-finite values.
Results may differ from a plain program's by a relative error of at most 0.015.
Values may be sent and summed in bfloat16 or wider, within the bound.
No kernel may reach another device: no remote copies, remote signals or barrier semaphores. Data moves between devices by JAX's collectives and lax.ppermute only.
A program may use at most 128 MiB of HBM per device.

v0:
```python
import jax
import jax.numpy as jnp
from jax import lax
from jax.sharding import PartitionSpec as P

CAP = 2


def rms_scale(values, gains):
    return values * lax.rsqrt(jnp.mean(values * values, axis=-1, keepdims=True) + 1e-06) * gains


def expert_batch(picked, gate_matrix, up_matrix, down_matrix):
    gate_out = jnp.einsum("jrd,jdf->jrf", picked, gate_matrix, preferred_element_type=jnp.float32)
    up_out = jnp.einsum("jrd,jdf->jrf", picked, up_matrix, preferred_element_type=jnp.float32)
    hidden = (jax.nn.silu(gate_out) * up_out).astype(jnp.bfloat16)
    return jnp.einsum(
        "jrf,jfd->jrd", hidden, down_matrix, preferred_element_type=jnp.float32
    ).astype(jnp.bfloat16)


def route_tables(routes, route_scores, expert_ids):
    onehot = (routes[:, :, None] == expert_ids[None, None, :]).astype(jnp.float32)
    scores = route_scores.astype(jnp.float32)
    shares = scores / jnp.sum(scores, axis=-1, keepdims=True)
    weights = jnp.sum(shares[:, :, None] * onehot, axis=1)
    hit_count = jnp.sum(onehot, axis=1)
    return (weights, hit_count)


def exchanged_experts(
    branch_in, routes, route_scores, expert_gate, expert_up, expert_down, devices_ep
):
    experts = expert_gate.shape[0] * devices_ep
    weights, hit_count = route_tables(routes, route_scores, jnp.arange(experts, dtype=jnp.int32))
    hit_int = hit_count.astype(jnp.int32)
    rank_index = jnp.cumsum(hit_int, axis=0) - hit_int
    slot_range = jnp.arange(CAP, dtype=jnp.int32)
    chosen = (
        (rank_index.T[:, None, :] == slot_range[None, :, None]) & (hit_count.T[:, None, :] > 0.5)
    ).astype(jnp.float32)
    outgoing = jnp.einsum(
        "ect,td->ecd", chosen.astype(jnp.bfloat16), branch_in, preferred_element_type=jnp.float32
    ).astype(jnp.bfloat16)
    incoming = lax.all_to_all(outgoing, "ep", split_axis=0, concat_axis=1, tiled=True)
    produced = expert_batch(incoming, expert_gate, expert_up, expert_down)
    returned = lax.all_to_all(produced, "ep", split_axis=1, concat_axis=0, tiled=True)
    weighted = chosen * weights.T[:, None, :]
    each_expert = jnp.einsum("ect,ecd->etd", weighted, returned.astype(jnp.float32))
    return jnp.sum(each_expert.astype(jnp.bfloat16).astype(jnp.float32), axis=0)


def local(
    resid,
    norm_gains,
    w_query,
    w_key,
    w_value,
    w_outgate,
    w_igate,
    w_fgate,
    igate_bias,
    fgate_bias,
    state_matrix,
    state_norm,
    state_max,
    w_mix_out,
    routes,
    route_scores,
    expert_gate,
    expert_up,
    expert_down,
    dense_gate,
    dense_up,
    dense_down,
    branch_weight,
):
    seqs_local = resid.shape[0]
    heads = state_matrix.shape[1]
    head_size = state_matrix.shape[2]
    devices_ep = lax.axis_size("ep")
    resid32 = resid.astype(jnp.float32)
    normed = rms_scale(resid32, norm_gains[0]).astype(jnp.bfloat16)
    row_piece = lax.all_gather(normed, "ep", axis=0, tiled=True)
    projected = jnp.stack(
        [
            jnp.dot(row_piece, matrix, preferred_element_type=jnp.float32).astype(jnp.bfloat16)
            for matrix in (w_query, w_key, w_value, w_outgate)
        ],
        axis=1,
    )
    own_proj = lax.all_to_all(projected, "ep", split_axis=0, concat_axis=2, tiled=True)
    head_shape = (seqs_local, heads, head_size)
    query = own_proj[:, 0].astype(jnp.float32).reshape(head_shape)
    key_heads = own_proj[:, 1].astype(jnp.float32).reshape(head_shape) * head_size ** (-0.5)
    value_heads = own_proj[:, 2].astype(jnp.float32).reshape(head_shape)
    outgate = own_proj[:, 3].astype(jnp.float32).reshape(head_shape)
    ipre = jnp.dot(normed, w_igate, preferred_element_type=jnp.float32) + igate_bias
    fpre = jnp.dot(normed, w_fgate, preferred_element_type=jnp.float32) + fgate_bias
    logf = jax.nn.log_sigmoid(fpre)
    new_max = jnp.maximum(ipre, logf + state_max)
    keep_gain = jnp.exp(logf + state_max - new_max)
    write_gain = jnp.exp(ipre - new_max)
    new_matrix = (
        keep_gain[:, :, None, None] * state_matrix
        + write_gain[:, :, None, None] * value_heads[:, :, :, None] * key_heads[:, :, None, :]
    )
    new_norm = keep_gain[:, :, None] * state_norm + write_gain[:, :, None] * key_heads
    numer = jnp.einsum("shed,shd->she", new_matrix, query)
    denom = jnp.sum(new_norm * query, axis=-1)
    cell = numer / jnp.maximum(jnp.abs(denom), 1.0)[:, :, None]
    gated = (
        (jax.nn.sigmoid(outgate) * cell).reshape(seqs_local, heads * head_size).astype(jnp.bfloat16)
    )
    mixed = jnp.dot(gated, w_mix_out, preferred_element_type=jnp.float32)
    middle = resid32 + rms_scale(mixed, norm_gains[1])
    branch_in = rms_scale(middle, norm_gains[2]).astype(jnp.bfloat16)
    all_rows = lax.all_gather(branch_in, "ep", axis=0, tiled=True)
    moe_own = exchanged_experts(
        branch_in, routes, route_scores, expert_gate, expert_up, expert_down, devices_ep
    )
    gate_out = jnp.dot(all_rows, dense_gate, preferred_element_type=jnp.float32)
    up_out = jnp.dot(all_rows, dense_up, preferred_element_type=jnp.float32)
    hidden = (jax.nn.silu(gate_out) * up_out).astype(jnp.bfloat16)
    logit = jnp.dot(all_rows, branch_weight, preferred_element_type=jnp.float32)
    summed = lax.psum_scatter(
        (
            jnp.dot(hidden, dense_down, preferred_element_type=jnp.float32)
            * jax.nn.sigmoid(logit)[:, None]
        ).astype(jnp.bfloat16),
        "ep",
        scatter_dimension=0,
        tiled=True,
    ).astype(jnp.float32)
    combined = moe_own + summed
    out_stream = (middle + rms_scale(combined, norm_gains[3])).astype(jnp.bfloat16)
    return (out_stream, new_matrix, new_norm, new_max)


def solution(mesh):
    placed = (
        P(("grp", "ep"), None),
        P(),
        P(None, "ep"),
        P(None, "ep"),
        P(None, "ep"),
        P(None, "ep"),
        P(),
        P(),
        P(),
        P(),
        P(("grp", "ep"), None, None, None),
        P(("grp", "ep"), None, None),
        P(("grp", "ep"), None),
        P(),
        P(("grp", "ep"), None),
        P(("grp", "ep"), None),
        P("ep", None, None),
        P("ep", None, None),
        P("ep", None, None),
        P(None, "ep"),
        P(None, "ep"),
        P("ep", None),
        P(),
    )
    return jax.shard_map(
        local,
        mesh=mesh,
        in_specs=placed,
        out_specs=(
            P(("grp", "ep"), None),
            P(("grp", "ep"), None, None, None),
            P(("grp", "ep"), None, None),
            P(("grp", "ep"), None),
        ),
        check_vma=False,
    )
```

profile of v0, /device:TPU:69, one launch (start us, length us, event | category | flops | bytes accessed | tf_op | source)
XLA Modules:
  0.0 311.6 jit_solution(119060778574030641)
XLA Ops:
  7.3 1.0 fusion.59
  8.2 1.0 fusion.27
  9.2 1.6 fusion.58
  10.9 1.1 fusion.51
  12.0 1.1 broadcast_multiply_fusion.2
  13.3 0.7 convert_reduce_fusion.2
  14.0 0.7 convert_divide_fusion
  14.8 0.8 copy.82
  15.7 70.9 %all-gather.5.cloned.1.call-done = bf16[32,12,2048]{2,1,0:T(8,128)(2,1)} async-done(((bf16[1,12,2048]{2,1,0:T(8,128)(2,1)}), bf16[32,12,2048]{2,1,0:T(8,128)(2,1)}) %all-gather.5.cloned.1.call-update) | async-done | bytes 1572880 | tf_op jit(solution)/shard_map/all_gather | solution.py:84
  86.6 3.6 %reshape.139 = bf16[384,2048]{1,0:T(8,128)(2,1)} reshape(bf16[32,12,2048]{2,1,0:T(8,128)(2,1)} %all-gather.5.cloned.1.call-done) | data formatting | bytes 3145728
  90.2 2.1 fusion.14
  92.3 2.0 fusion.15
  95.8 0.9 reshape.152
  96.7 8.5 %all-to-all-start = ((bf16[32,2,768]{2,1,0:T(2,128)(2,1)}), bf16[32,2,768]{2,1,0:T(2,128)(2,1)S(1)}, u32[]{:S(2)}, u32[]{:S(2)}) async-start(bf16[32,2,768]{2,1,0:T(2,128)(2,1)} %reshape.152), calls=%async_computation | async-start | bytes 196608 | tf_op jit(solution)/shard_map/all_to_all | solution.py:92
  105.5 14.2 %all-to-all-done = bf16[32,2,768]{2,1,0:T(2,128)(2,1)S(1)} async-done(((bf16[32,2,768]{2,1,0:T(2,128)(2,1)}), bf16[32,2,768]{2,1,0:T(2,128)(2,1)S(1)}, u32[]{:S(2)}, u32[]{:S(2)}) %all-to-all-start) | async-done | bytes 98336 | tf_op jit(solution)/shard_map/all_to_all | solution.py:92
  120.8 0.7 multiply_reduce_fusion.3
  121.5 4.5 %multiply_add_fusion = f32[12,8,128,128]{3,2,1,0:T(8,128)S(1)} fusion(f32[12,8,128,128]{3,2,1,0:T(8,128)} %param.33, f32[12,8,128]{2,1,0:T(8,128)S(1)} %get-tuple-element.14, f32[12,8,128]{2,1,0:T(8,128)S(1)} %get-tuple-element.21, f32[12,8]{1,0:T(8,128)S(1)} %copy.78), kind=kLoop, calls=%fused_computation | loop fusion | flops 4718592 | bytes 12681600 | tf_op jit(solution)/shard_map/add | solution.py:105
  126.0 1.7 fusion.41
  127.7 1.5 copy-done.2
  129.3 1.1 copy-done.4
  130.5 0.8 multiply_reduce_fusion.2
  131.5 0.7 fusion.55
  132.9 29.4 %all_to_all.39 = bf16[32,2,2048]{2,1,0:T(2,128)(2,1)S(1)} all-to-all(bf16[32,2,2048]{2,1,0:T(2,128)(2,1)S(1)} %copy.88), channel_id=1, replica_groups=mesh['grp'=4,'ep'=32] {'ep'}, dimensions={0} | all-to-all | bytes 524288 | tf_op jit(solution)/shard_map/all_to_all | solution.py:45
  162.5 2.1 fusion.5
  164.6 2.5 fusion.1
  167.5 0.6 broadcast.130
  168.1 2.2 reduce.6
  170.3 0.9 reshape.154
  171.2 4.4 %all-to-all-start.2 = ((bf16[32,2,2048]{2,1,0:T(2,128)(2,1)}), bf16[32,2,2048]{2,1,0:T(2,128)(2,1)S(1)}, u32[]{:S(2)}, u32[]{:S(2)}) async-start(bf16[32,2,2048]{2,1,0:T(2,128)(2,1)} %reshape.154), calls=%async_computation.2 | async-start | bytes 524288 | tf_op jit(solution)/shard_map/all_to_all | solution.py:47
  175.7 0.7 copy.86
  176.4 0.6 dynamic-slice.4
  177.5 21.2 %all-to-all-done.2 = bf16[32,2,2048]{2,1,0:T(2,128)(2,1)S(1)} async-done(((bf16[32,2,2048]{2,1,0:T(2,128)(2,1)}), bf16[32,2,2048]{2,1,0:T(2,128)(2,1)S(1)}, u32[]{:S(2)}, u32[]{:S(2)}) %all-to-all-start.2) | async-done | bytes 262176 | tf_op jit(solution)/shard_map/all_to_all | solution.py:47
  199.4 3.6 %reshape.141 = bf16[384,2048]{1,0:T(8,128)(2,1)} reshape(bf16[32,12,2048]{2,1,0:T(8,128)(2,1)} %all-gather.7.cloned.1.call-done) | data formatting | bytes 3145728
  203.0 2.4 fusion.60
  205.9 5.0 %multiply_convert_fusion = bf16[384,2048]{1,0:T(8,128)(2,1)} fusion(bf16[256,2048]{1,0:T(8,128)(2,1)} %param.44, f32[384]{0:T(512)S(1)} %add_divide_fusion, bf16[384,2048]{1,0:T(8,128)(2,1)} %reshape.141, bf16[2048,256]{1,0:T(8,128)(2,1)} %param.43, f32[384,256]{1,0:T(8,128)S(1)} %fusion.60), kind=kOutput, calls=%fused_computation.2 | convolution fusion | flops 807469056 | bytes 5637632 | tf_op jit(solution)/shard_map/dot_general | solution.py:128
  210.9 57.9 %fusion = bf16[16,2048]{1,0:T(8,128)(2,1)S(1)} fusion(bf16[384,2048]{1,0:T(8,128)(2,1)} %multiply_convert_fusion), kind=kCustom, calls=%all-reduce-scatter | all-reduce-scatter fusion | flops 1048577 | bytes 1638912
  268.8 2.0 collective-permute-start
  270.9 1.3 collective-permute-start.1
  272.2 4.9 %collective-permute-start.7 = (bf16[12,2048]{1,0:T(8,128)(2,1)S(1)}, bf16[12,2048]{1,0:T(8,128)(2,1)S(1)}, u32[]{:S(2)}, u32[]{:S(2)}) collective-permute-start(bf16[12,2048]{1,0:T(8,128)(2,1)S(1)} %slice.36), channel_id=1, source_target_pairs={{0,8},{1,9},{2,10},{3,11},{4,12},{5,13},{6,14},{7,15},{8,16},{9,17... | collective-permute-start | bytes 147464
  277.2 1.4 bitcast_reduce_fusion
  278.8 5.3 %collective-permute-start.2 = (bf16[16,2048]{1,0:T(8,128)(2,1)S(1)}, bf16[16,2048]{1,0:T(8,128)(2,1)S(1)}, u32[]{:S(2)}, u32[]{:S(2)}) collective-permute-start(bf16[16,2048]{1,0:T(8,128)(2,1)S(1)} %fusion), channel_id=1, source_target_pairs={{0,3},{1,4},{2,5},{3,6},{4,7},{5,8},{6,9},{7,10},{8,11},{9,12},{10... | collective-permute-start | bytes 196616
  284.1 4.6 %collective-permute-start.3 = (bf16[16,2048]{1,0:T(8,128)(2,1)S(1)}, bf16[16,2048]{1,0:T(8,128)(2,1)S(1)}, u32[]{:S(2)}, u32[]{:S(2)}) collective-permute-start(bf16[16,2048]{1,0:T(8,128)(2,1)S(1)} %fusion), channel_id=1, source_target_pairs={{0,4},{1,5},{2,6},{3,7},{4,8},{5,9},{6,10},{7,11},{8,12},{9,13},{1... | collective-permute-start | bytes 196616
  288.7 5.3 %collective-permute-start.4 = (bf16[16,2048]{1,0:T(8,128)(2,1)S(1)}, bf16[16,2048]{1,0:T(8,128)(2,1)S(1)}, u32[]{:S(2)}, u32[]{:S(2)}) collective-permute-start(bf16[16,2048]{1,0:T(8,128)(2,1)S(1)} %fusion), channel_id=1, source_target_pairs={{0,5},{1,6},{2,7},{3,8},{4,9},{5,10},{6,11},{7,12},{8,13},{9,14},{... | collective-permute-start | bytes 196616
  294.0 1.7 collective-permute-start.5
  295.7 3.7 %collective-permute-start.6 = (bf16[16,2048]{1,0:T(8,128)(2,1)S(1)}, bf16[16,2048]{1,0:T(8,128)(2,1)}, u32[]{:S(2)}, u32[]{:S(2)}) collective-permute-start(bf16[16,2048]{1,0:T(8,128)(2,1)S(1)} %fusion), channel_id=1, source_target_pairs={{0,7},{1,8},{2,9},{3,10},{4,11},{5,12},{6,13},{7,14},{8,15},{9,16}... | collective-permute-start | bytes 196616
  299.5 1.5 convert_reduce_fusion
  301.0 2.2 concatenate
  303.4 1.3 add_convert_fusion
  (88 shorter events, 6.5 us)
Async XLA Ops:
  7.2 157.4 %copy-start = (bf16[1,512,2048]{2,1,0:T(8,128)(2,1)S(1)}, bf16[1,512,2048]{2,1,0:T(8,128)(2,1)}, u32[]{:S(2)}) copy-start(bf16[1,512,2048]{2,1,0:T(8,128)(2,1)} %param.41) | copy-start | bytes 6291460
  7.2 79.4 %all-gather.5.cloned.1.call-start = ((), (), s32[]{:S(2)}) async-start(), calls=%async_computation.3 | async-start | bytes 2162688 | tf_op jit(solution)/shard_map/all_gather | solution.py:84
  10.8 79.3 %copy-start.6 = (bf16[2048,32]{0,1:T(8,128)(2,1)S(1)}, bf16[2048,32]{0,1:T(8,128)(2,1)}, u32[]{:S(2)}) copy-start(bf16[2048,32]{0,1:T(8,128)(2,1)} %param.25) | copy-start | bytes 393220
  13.1 1.0 copy-start.15
  15.7 76.6 %copy-start.7 = (bf16[2048,32]{0,1:T(8,128)(2,1)S(1)}, bf16[2048,32]{0,1:T(8,128)(2,1)}, u32[]{:S(2)}) copy-start(bf16[2048,32]{0,1:T(8,128)(2,1)} %param.26) | copy-start | bytes 393220
  90.2 4.1 %copy-start.1 = (bf16[384,2048]{1,0:T(8,128)(2,1)S(1)}, bf16[384,2048]{1,0:T(8,128)(2,1)}, u32[]{:S(2)}) copy-start(bf16[384,2048]{1,0:T(8,128)(2,1)} %reshape.139) | copy-start | bytes 4718596
  90.2 4.2 %copy-start.8 = (bf16[2048,32]{0,1:T(8,128)(2,1)S(1)}, bf16[2048,32]{0,1:T(8,128)(2,1)}, u32[]{:S(2)}) copy-start(bf16[2048,32]{0,1:T(8,128)(2,1)} %param.27) | copy-start | bytes 393220
  92.3 2.6 copy-start.9
  95.5 25.3 %copy-start.11 = (f32[12,8,128]{2,1,0:T(8,128)S(1)}, f32[12,8,128]{2,1,0:T(8,128)}, u32[]{:S(2)}) copy-start(f32[12,8,128]{2,1,0:T(8,128)} %param.34) | copy-start | bytes 147460
  96.7 23.0 %all-to-all-start = ((bf16[32,2,768]{2,1,0:T(2,128)(2,1)}), bf16[32,2,768]{2,1,0:T(2,128)(2,1)S(1)}, u32[]{:S(2)}, u32[]{:S(2)}) async-start(bf16[32,2,768]{2,1,0:T(2,128)(2,1)} %reshape.152), calls=%async_computation | async-start | bytes 196608 | tf_op jit(solution)/shard_map/all_to_all | solution.py:92
  105.2 94.1 %all-gather.7.cloned.1.call-start = ((), (), s32[]{:S(2)}) async-start(), calls=%async_computation.4 | async-start | bytes 2162688 | tf_op jit(solution)/shard_map/all_gather | solution.py:118
  105.4 26.9 %copy-start.10 = (s32[32,12]{1,0:T(8,128)}, s32[32,12]{1,0:T(8,128)S(1)}, u32[]{:S(2)}) copy-start(s32[32,12]{1,0:T(8,128)S(1)} %copy.83) | copy-start | bytes 4612
  105.5 26.8 %copy-start.12 = (pred[32,12]{1,0:T(8,128)(4,1)}, pred[32,12]{1,0:T(8,128)(4,1)S(1)}, u32[]{:S(2)}) copy-start(pred[32,12]{1,0:T(8,128)(4,1)S(1)} %copy.84) | copy-start | bytes 1156
  126.0 3.2 %copy-start.2 = (f32[12,8,128,128]{3,2,1,0:T(8,128)}, f32[12,8,128,128]{3,2,1,0:T(8,128)S(1)}, u32[]{:S(2)}) copy-start(f32[12,8,128,128]{3,2,1,0:T(8,128)S(1)} %multiply_add_fusion) | copy-start | bytes 18874372
  126.0 4.5 %copy-start.4 = (bf16[1024,2048]{1,0:T(8,128)(2,1)S(1)}, bf16[1024,2048]{1,0:T(8,128)(2,1)}, u32[]{:S(2)}) copy-start(bf16[1024,2048]{1,0:T(8,128)(2,1)} %param.36) | copy-start | bytes 12582916
  130.4 0.8 copy-start.5
  131.2 33.3 %copy-start.13 = (f32[12]{0:T(128)}, f32[12]{0:T(128)S(1)}, u32[]{:S(2)}) copy-start(f32[12]{0:T(128)S(1)} %add_rsqrt_fusion.2) | copy-start | bytes 148
  167.1 8.6 %copy-start.14 = (bf16[2048]{0:T(1024)(128)(2,1)S(1)}, bf16[2048]{0:T(1024)(128)(2,1)}, u32[]{:S(2)}) copy-start(bf16[2048]{0:T(1024)(128)(2,1)} %param.45) | copy-start | bytes 12292
  167.1 9.3 %copy-start.16 = (u32[128]{0:T(128)S(1)}, u32[128]{0:T(128)}, u32[]{:S(2)}) copy-start(u32[128]{0:T(128)} %constant.42) | copy-start | bytes 1540
  171.2 27.5 %all-to-all-start.2 = ((bf16[32,2,2048]{2,1,0:T(2,128)(2,1)}), bf16[32,2,2048]{2,1,0:T(2,128)(2,1)S(1)}, u32[]{:S(2)}, u32[]{:S(2)}) async-start(bf16[32,2,2048]{2,1,0:T(2,128)(2,1)} %reshape.154), calls=%async_computation.2 | async-start | bytes 524288 | tf_op jit(solution)/shard_map/all_to_all | solution.py:47
  203.0 2.4 copy-start.3
  268.8 25.2 %collective-permute-start = (bf16[16,2048]{1,0:T(8,128)(2,1)S(1)}, bf16[16,2048]{1,0:T(8,128)(2,1)S(1)}, u32[]{:S(2)}, u32[]{:S(2)}) collective-permute-start(bf16[16,2048]{1,0:T(8,128)(2,1)S(1)} %fusion), channel_id=1, source_target_pairs={{0,1},{1,2},{2,3},{3,4},{4,5},{5,6},{6,7},{7,8},{8,9},{9,10},{10,1... | collective-permute-start | bytes 196616
  270.9 24.8 %collective-permute-start.1 = (bf16[16,2048]{1,0:T(8,128)(2,1)S(1)}, bf16[16,2048]{1,0:T(8,128)(2,1)S(1)}, u32[]{:S(2)}, u32[]{:S(2)}) collective-permute-start(bf16[16,2048]{1,0:T(8,128)(2,1)S(1)} %fusion), channel_id=1, source_target_pairs={{0,2},{1,3},{2,4},{3,5},{4,6},{5,7},{6,8},{7,9},{8,10},{9,11},{10,... | collective-permute-start | bytes 196616
  272.2 16.5 %collective-permute-start.7 = (bf16[12,2048]{1,0:T(8,128)(2,1)S(1)}, bf16[12,2048]{1,0:T(8,128)(2,1)S(1)}, u32[]{:S(2)}, u32[]{:S(2)}) collective-permute-start(bf16[12,2048]{1,0:T(8,128)(2,1)S(1)} %slice.36), channel_id=1, source_target_pairs={{0,8},{1,9},{2,10},{3,11},{4,12},{5,13},{6,14},{7,15},{8,16},{9,17... | collective-permute-start | bytes 147464
  278.8 22.2 %collective-permute-start.2 = (bf16[16,2048]{1,0:T(8,128)(2,1)S(1)}, bf16[16,2048]{1,0:T(8,128)(2,1)S(1)}, u32[]{:S(2)}, u32[]{:S(2)}) collective-permute-start(bf16[16,2048]{1,0:T(8,128)(2,1)S(1)} %fusion), channel_id=1, source_target_pairs={{0,3},{1,4},{2,5},{3,6},{4,7},{5,8},{6,9},{7,10},{8,11},{9,12},{10... | collective-permute-start | bytes 196616
  284.1 16.9 %collective-permute-start.3 = (bf16[16,2048]{1,0:T(8,128)(2,1)S(1)}, bf16[16,2048]{1,0:T(8,128)(2,1)S(1)}, u32[]{:S(2)}, u32[]{:S(2)}) collective-permute-start(bf16[16,2048]{1,0:T(8,128)(2,1)S(1)} %fusion), channel_id=1, source_target_pairs={{0,4},{1,5},{2,6},{3,7},{4,8},{5,9},{6,10},{7,11},{8,12},{9,13},{1... | collective-permute-start | bytes 196616
  288.7 12.3 %collective-permute-start.4 = (bf16[16,2048]{1,0:T(8,128)(2,1)S(1)}, bf16[16,2048]{1,0:T(8,128)(2,1)S(1)}, u32[]{:S(2)}, u32[]{:S(2)}) collective-permute-start(bf16[16,2048]{1,0:T(8,128)(2,1)S(1)} %fusion), channel_id=1, source_target_pairs={{0,5},{1,6},{2,7},{3,8},{4,9},{5,10},{6,11},{7,12},{8,13},{9,14},{... | collective-permute-start | bytes 196616
  294.0 7.0 %collective-permute-start.5 = (bf16[16,2048]{1,0:T(8,128)(2,1)S(1)}, bf16[16,2048]{1,0:T(8,128)(2,1)S(1)}, u32[]{:S(2)}, u32[]{:S(2)}) collective-permute-start(bf16[16,2048]{1,0:T(8,128)(2,1)S(1)} %fusion), channel_id=1, source_target_pairs={{0,6},{1,7},{2,8},{3,9},{4,10},{5,11},{6,12},{7,13},{8,14},{9,15},... | collective-permute-start | bytes 196616
  295.7 5.3 %collective-permute-start.6 = (bf16[16,2048]{1,0:T(8,128)(2,1)S(1)}, bf16[16,2048]{1,0:T(8,128)(2,1)}, u32[]{:S(2)}, u32[]{:S(2)}) collective-permute-start(bf16[16,2048]{1,0:T(8,128)(2,1)S(1)} %fusion), channel_id=1, source_target_pairs={{0,7},{1,8},{2,9},{3,10},{4,11},{5,12},{6,13},{7,14},{8,15},{9,16}... | collective-permute-start | bytes 196616
Sparse Core Ops, SparseCore 0:
  11.0 75.5 all-gather.4
  132.4 66.8 all-gather.6
where the time goes:
time: 314 us; the launch traced here: 312 us
  waiting for transfers between devices  107 us (34%)
  blocking collectives  87.3 us (28%)
  starting transfers between devices  41.9 us (13%)
  matrix products  24.1 us (8%)
  local copies, waits for them, and re-layouts  21.9 us (7%)
  between operations  15.2 us (5%)
  other arithmetic  14.4 us (5%)
    all_gather x1, waiting for transfers between devices, local(): row_piece = lax.all_gather(normed, 'ep', axis=0, tiled=True)  70.9 us
    unnamed x1, blocking collectives  57.9 us
    all_to_all x1, blocking collectives, exchanged_experts(): lax.all_to_all(outgoing, 'ep', split_axis=0, concat_axis=1, tiled=True)  29.4 us
    unnamed x8, starting transfers between devices  28.9 us
    all_to_all x1, waiting for transfers between devices, exchanged_experts(): lax.all_to_all(produced, 'ep', split_axis=1, concat_axis=0, tiled=True)  21.2 us
    unnamed x49, local copies, waits for them, and re-layouts  16.5 us
    all_to_all x1, waiting for transfers between devices, local(): lax.all_to_all(projected, 'ep', split_axis=0, concat_axis=2, tiled=True)  14.2 us
    all_to_all x1, starting transfers between devices, local(): lax.all_to_all(projected, 'ep', split_axis=0, concat_axis=2, tiled=True)  8.52 us
  transfers between devices with their start and end apart: 12, of which 4 were waited for; matrix products, arithmetic and copies ran while one was open for 6% of the time, Pallas kernels for 0%

commit v1 on v0

v1 whole, which is shorter than its diff:
```python
import functools

import jax
import jax.numpy as jnp
from jax import lax
from jax.experimental import pallas as pl
from jax.experimental.pallas import tpu as pltpu
from jax.sharding import PartitionSpec as P

CAP = 2
INTERPRET = False
F32 = jnp.float32
BF16 = jnp.bfloat16


def call(kernel, outs, args, scratch=(), vmem=16, flops=1000000, name=None):
    single = not isinstance(outs, (list, tuple))
    shapes = [outs] if single else list(outs)
    result = pl.pallas_call(
        kernel,
        out_shape=[jax.ShapeDtypeStruct(s, d) for s, d in shapes] if not single
        else None,
        scratch_shapes=[pltpu.VMEM(s, d) for s, d in scratch],
        compiler_params=pltpu.CompilerParams(vmem_limit_bytes=vmem << 20),
        cost_estimate=pl.CostEstimate(flops=flops, bytes_accessed=1000000, transcendentals=0),
        interpret=INTERPRET,
        name=name,
    )(*args)
    return result


def rms(values, gains):
    return values * lax.rsqrt(jnp.mean(values * values, axis=-1, keepdims=True) + 1e-06) * gains


def core():
    return lax.rem(lax.axis_index("ep"), 2)


def dot(a, b):
    return jnp.dot(a, b, preferred_element_type=F32)


def half_of(c, values):
    h = values.shape[-1] // 2
    return jnp.where(c == 0, values[:, :h], values[:, h:])


def norm_kernel(own_ref, other_ref, gains_ref, out_ref, rows):
    c = core()
    r = own_ref.shape[0]
    own, other = own_ref[...].astype(F32), other_ref[...].astype(F32)
    rows[:r] = jnp.where(c == 0, own, other)
    rows[r : 2 * r] = jnp.where(c == 0, other, own)
    normed = rms(rows[...], gains_ref[0:1, :])
    half = half_of(c, normed).astype(BF16)
    for z in range(out_ref.shape[0]):
        out_ref[z] = half


def gates_kernel(
    resid_ref, gains_ref, wi_ref, wf_ref, bi_ref, bf_ref, max_ref, routes_ref, scores_ref,
    keep_ref, write_ref, newmax_ref, info_ref,
):
    r = resid_ref.shape[0]
    normed = rms(resid_ref[...].astype(F32), gains_ref[0:1, :]).astype(BF16)
    ipre = dot(normed, wi_ref[...]) + bi_ref[...]
    fpre = dot(normed, wf_ref[...]) + bf_ref[...]
    logf = jnp.minimum(fpre, 0.0) - jnp.log1p(jnp.exp(-jnp.abs(fpre)))
    decayed = logf + max_ref[...]
    new_max = jnp.maximum(ipre, decayed)
    keep_ref[...] = jnp.exp(decayed - new_max)
    write_ref[...] = jnp.exp(ipre - new_max)
    newmax_ref[...] = new_max
    lanes = lax.broadcasted_iota(jnp.int32, (r, 128), 1)
    row = lax.broadcasted_iota(jnp.int32, (r, 128), 0)
    total = jnp.zeros((r, 128), F32)
    columns = (routes_ref[:, 0:1].astype(F32), routes_ref[:, 1:2].astype(F32),
               scores_ref[:, 0:1].astype(F32), scores_ref[:, 1:2].astype(F32))
    for k, column in enumerate(columns):
        total = total + jnp.where(lanes == row + k * r, column, 0.0)
    info = jnp.sum(total, axis=0, keepdims=True)
    info_ref[...] = jnp.broadcast_to(info, info_ref.shape).astype(BF16)


def proj_kernel(x_ref, y_ref, w_ref, info_ref, out_ref):
    c = core()
    nz, r2, h = x_ref.shape
    x = x_ref[...].reshape(nz * r2, h)
    y = y_ref[...].reshape(nz * r2, h)
    wx = w_ref[pl.ds(pl.multiple_of(c * h, h), h), :]
    wy = w_ref[pl.ds(pl.multiple_of((1 - c) * h, h), h), :]
    p = (dot(x, wx) + dot(y, wy)).astype(BF16).reshape(nz, r2, w_ref.shape[1])
    out_ref[:, :r2, :] = p
    for z in range(nz):
        out_ref[z, r2 : r2 + 8, :] = info_ref[...]


def cell_kernel(
    a_ref, b_ref, keep_ref, write_ref, m_ref, norm_ref, mix_ref, resid_ref, gains_ref,
    middle_ref, mine_ref, send_ref, newnorm_ref, keys_ref, wvt_ref,
    p0, p1, q_scr, wv_scr, gated,
):
    c = core()
    r, heads, dh = norm_ref.shape
    nz = a_ref.shape[0]
    cols = heads * dh // (2 * nz)
    per = dh // cols
    p0[...] = jnp.zeros_like(p0)
    p1[...] = jnp.zeros_like(p1)
    for z in range(nz):
        a, b = a_ref[z].astype(F32), b_ref[z].astype(F32)
        a = jnp.where(c == 0, a[:r], a[r : 2 * r])
        b = jnp.where(c == 0, b[:r], b[r : 2 * r])
        p0[z, :r] = jnp.where(c == 0, a, b)
        p1[z, :r] = jnp.where(c == 0, b, a)
    lanes = lax.broadcasted_iota(jnp.int32, (16, dh), 1)

    def gather(h, kind):
        total = jnp.zeros((16, dh), F32)
        for p in range(per):
            ep = h * per + p
            piece = (p0 if ep % 2 == 0 else p1)[ep // 2]
            shift = ((p - kind) * cols) % dh
            piece = pltpu.roll(piece, shift, 1) if shift else piece
            total = jnp.where((lanes >= p * cols) & (lanes < (p + 1) * cols), piece, total)
        return total

    wv_scr[...] = jnp.zeros_like(wv_scr)
    for h in range(heads):
        q_scr[h] = gather(h, 0)
        keys_ref[h] = gather(h, 1) * dh ** (-0.5)
        wv_scr[h * 16 : h * 16 + r] = gather(h, 2)[:r] * write_ref[:, h : h + 1]
    wvt_ref[...] = wv_scr[...].T
    lane128 = lax.broadcasted_iota(jnp.int32, (dh, 128), 1)

    def step(s, acc):
        for h in range(heads):
            prod = m_ref[s, h] * q_scr[h, pl.ds(s, 1), :]
            red = jnp.sum(prod, axis=1, keepdims=True)
            acc = jnp.where(lane128 == h * 16 + s, red, acc)
        return acc

    numer = lax.fori_loop(0, r, step, jnp.zeros((dh, 128), F32)).T
    for h in range(heads):
        query, key = q_scr[h][:r], keys_ref[h][:r]
        outgate = gather(h, 3)[:r]
        keep, write = keep_ref[:, h : h + 1], write_ref[:, h : h + 1]
        new_norm = keep * norm_ref[:, h, :] + write * key
        newnorm_ref[:, h, :] = new_norm
        denom = jnp.sum(new_norm * query, axis=1, keepdims=True)
        kq = jnp.sum(key * query, axis=1, keepdims=True)
        top = keep * numer[h * 16 : h * 16 + r] + wv_scr[h * 16 : h * 16 + r] * kq
        cell = top / jnp.maximum(jnp.abs(denom), 1.0)
        gated[:, h * dh : (h + 1) * dh] = (jax.nn.sigmoid(outgate) * cell).astype(BF16)
    mixed = dot(gated[...], mix_ref[...])
    middle = resid_ref[...].astype(F32) + rms(mixed, gains_ref[1:2, :])
    middle_ref[...] = middle
    branch = rms(middle, gains_ref[2:3, :])
    mine_ref[...] = half_of(c, branch).astype(BF16)
    send_ref[...] = half_of(1 - c, branch).astype(BF16)


def update_kernel(keep_ref, keys_ref, wvt_ref, m_ref, out_ref):
    r, heads, dh, _ = m_ref.shape

    def step(s, carry):
        rolled = pltpu.roll(wvt_ref[...], lax.rem(128 - s, 128), 1)
        for h in range(heads):
            keep = keep_ref[pl.ds(s, 1), h : h + 1]
            key = keys_ref[h, pl.ds(s, 1), :]
            out_ref[s, h] = keep * m_ref[s, h] + rolled[:, h * 16 : h * 16 + 1] * key
        return carry

    lax.fori_loop(0, r, step, 0)


def pair_kernel(mine_ref, got_ref, out_ref, rows):
    c = core()
    r = mine_ref.shape[0]
    mine, got = mine_ref[...].astype(F32), got_ref[...].astype(F32)
    rows[:r] = jnp.where(c == 0, mine, got)
    rows[r : 2 * r] = jnp.where(c == 0, got, mine)
    both = rows[...].astype(BF16)
    for z in range(out_ref.shape[0]):
        out_ref[z] = both


def silu_mul(gate, up):
    return (gate * jax.nn.sigmoid(gate) * up).astype(BF16)


def branch_kernel(
    x_ref, y_ref, a_ref, b_ref, eg_ref, eu_ref, ed_ref, dg_ref, du_ref, dd_ref, bw_ref,
    keep_ref, send_ref, info, made,
):
    c = core()
    me = lax.axis_index("ep").astype(F32)
    nz, r2, h = x_ref.shape
    r = r2 // 2
    rows = nz * r2
    slots = 2 * nz * CAP
    at = pl.ds(pl.multiple_of(c * h, h), h)
    to = pl.ds(pl.multiple_of((1 - c) * h, h), h)
    x = x_ref[...].reshape(rows, h)
    y = y_ref[...].reshape(rows, h)
    low = lax.broadcasted_iota(jnp.int32, (r2, 128), 0) < r
    for z in range(nz):
        a, b = a_ref[z, r2 : r2 + 8, :].astype(F32)[0:1], b_ref[z, r2 : r2 + 8, :].astype(F32)[0:1]
        first, second = jnp.where(c == 0, a, b), jnp.where(c == 0, b, a)
        info[z * r2 : (z + 1) * r2] = jnp.where(low, first, second)
    lane = lax.broadcasted_iota(jnp.int32, (rows, 128), 1)
    token = lax.broadcasted_iota(jnp.int32, (rows, 128), 0)
    block = lax.div(token, r)
    inner = token - block * r
    table = info[...]

    def column(k):
        return jnp.sum(jnp.where(lane == inner + k * r, table, 0.0), axis=1, keepdims=True)

    e0, e1, s0, s1 = column(0), column(1), column(2), column(3)
    hit0, hit1 = e0 == me, e1 == me
    hit = jnp.where(hit0 | hit1, 1.0, 0.0)
    weight = jnp.where(hit0, s0, jnp.where(hit1, s1, 0.0)) / (s0 + s1)
    row_i = lax.broadcasted_iota(jnp.int32, (rows, rows), 0)
    col_i = lax.broadcasted_iota(jnp.int32, (rows, rows), 1)
    earlier = (col_i < row_i) & (lax.div(row_i, r) == lax.div(col_i, r))
    earlier = jnp.where(earlier, 1.0, 0.0).astype(BF16)
    rank = dot(earlier, jnp.broadcast_to(hit, (rows, 128)).astype(BF16))
    slot = block.astype(F32) * CAP + rank
    chosen = jnp.where((slot == lane.astype(F32)) & (hit > 0.5), 1.0, 0.0)
    picker = chosen.T[:slots].astype(BF16)
    placer = chosen[:, :slots].astype(BF16)
    px = dot(picker, x).astype(BF16)
    py = dot(picker, y).astype(BF16)
    gate = dot(px, eg_ref[0, at, :]) + dot(py, eg_ref[0, to, :])
    up = dot(px, eu_ref[0, at, :]) + dot(py, eu_ref[0, to, :])
    made[...] = dot(silu_mul(gate, up), ed_ref[0]).astype(BF16)

    gate = dot(x, dg_ref[at, :]) + dot(y, dg_ref[to, :])
    up = dot(x, du_ref[at, :]) + dot(y, du_ref[to, :])
    hidden = silu_mul(gate, up)
    logit = jnp.sum(x.astype(F32) * bw_ref[:, at].astype(F32), axis=1, keepdims=True)
    logit = logit + jnp.sum(y.astype(F32) * bw_ref[:, to].astype(F32), axis=1, keepdims=True)
    sig = jax.nn.sigmoid(logit)
    for where, ref in ((at, keep_ref), (to, send_ref)):
        part = dot(hidden, dd_ref[:, where]) * sig
        part = part + dot(placer, made[:, where]) * weight
        ref[...] = part.astype(ref.dtype)


def add_kernel(keep_ref, got_ref, out_ref):
    total = keep_ref[...] + got_ref[...].astype(F32)
    out_ref[...] = total.astype(BF16).reshape(out_ref.shape)


def sum_kernel(x_ref, mine_ref, send_ref):
    c = core()
    r = mine_ref.shape[0]
    total = x_ref[0].astype(F32)
    for z in range(1, x_ref.shape[0]):
        total = total + x_ref[z].astype(F32)
    mine_ref[...] = jnp.where(c == 0, total[:r], total[r:])
    send_ref[...] = jnp.where(c == 0, total[r:], total[:r])


def final_kernel(mine_ref, got_ref, middle_ref, gains_ref, out_ref):
    c = core()
    h = mine_ref.shape[1]
    mine, got = mine_ref[...], got_ref[...]
    low, high = jnp.where(c == 0, mine, got), jnp.where(c == 0, got, mine)
    square = jnp.sum(low * low, axis=1, keepdims=True) + jnp.sum(high * high, axis=1, keepdims=True)
    scale = lax.rsqrt(square / (2 * h) + 1e-06)
    gains = gains_ref[3:4, :]
    out_ref[:, :h] = (middle_ref[:, :h] + low * scale * gains[:, :h]).astype(BF16)
    out_ref[:, h:] = (middle_ref[:, h:] + high * scale * gains[:, h:]).astype(BF16)


def local(
    resid, norm_gains, w_query, w_key, w_value, w_outgate, w_igate, w_fgate, igate_bias,
    fgate_bias, state_matrix, state_norm, state_max, w_mix_out, routes, route_scores,
    expert_gate, expert_up, expert_down, dense_gate, dense_up, dense_down, branch_weight,
):
    n = lax.axis_size("ep")
    nz = n // 2
    r, d = resid.shape
    h = d // 2
    heads, dh = state_matrix.shape[1:3]
    inner = heads * dh
    groups = [[2 * z + c for z in range(nz)] for c in range(2)]
    pairs = [(i, i ^ 1) for i in range(n)]

    def swap(x):
        return lax.ppermute(x, "ep", pairs)

    def exchange(x):
        return lax.all_to_all(x, "ep", 0, 0, axis_index_groups=groups)

    other = swap(resid)
    chunk, = call(norm_kernel, [((nz, 2 * r, h), BF16)], (resid, other, norm_gains),
                  scratch=[((2 * r, d), F32)], name="norm")
    x = exchange(chunk)
    keep, write, new_max, info = call(
        gates_kernel,
        [((r, heads), F32), ((r, heads), F32), ((r, heads), F32), ((8, 128), BF16)],
        (resid, norm_gains, w_igate, w_fgate, igate_bias.reshape(1, heads),
         fgate_bias.reshape(1, heads), state_max, routes, route_scores), name="gates")
    w_all = jnp.concatenate([w_query, w_key, w_value, w_outgate], axis=1)
    y = swap(x)
    projected, = call(proj_kernel, [((nz, 2 * r + 8, w_all.shape[1]), BF16)],
                      (x, y, w_all, info), name="proj")
    a = exchange(projected)
    b = swap(a)
    middle, mine, send, new_norm, keys, wvt = call(
        cell_kernel,
        [((r, d), F32), ((r, h), BF16), ((r, h), BF16), ((r, heads, dh), F32),
         ((heads, 16, dh), F32), ((dh, 128), F32)],
        (a, b, keep, write, state_matrix, state_norm, w_mix_out, resid, norm_gains),
        scratch=[((nz, 16, dh), F32), ((nz, 16, dh), F32), ((heads, 16, dh), F32),
                 ((128, dh), F32), ((r, inner), BF16)],
        vmem=24, name="cell")
    got = swap(send)
    chunk, = call(pair_kernel, [((nz, 2 * r, h), BF16)], (mine, got),
                  scratch=[((2 * r, h), F32)], name="pair")
    x = exchange(chunk)
    new_matrix, = call(update_kernel, [(state_matrix.shape, F32)],
                       (keep, keys, wvt, state_matrix), vmem=24, flops=100000000, name="update")
    y = swap(x)
    part, send = call(
        branch_kernel, [((n * r, h), F32), ((n * r, h), BF16)],
        (x, y, a, b, expert_gate, expert_up, expert_down, dense_gate, dense_up, dense_down,
         branch_weight.reshape(1, d)),
        scratch=[((n * r, 128), F32), ((n * CAP, d), BF16)], vmem=32, name="branch")
    got = swap(send)
    chunk, = call(add_kernel, [((nz, 2 * r, h), BF16)], (part, got), name="add")
    x = exchange(chunk)
    mine, send = call(sum_kernel, [((r, h), F32), ((r, h), F32)], (x,), name="sum")
    got = swap(send)
    out, = call(final_kernel, [((r, d), BF16)], (mine, got, middle, norm_gains), name="final")
    return (out, new_matrix, new_norm, new_max)


def solution(mesh):
    placed = (
        P(("grp", "ep"), None), P(), P(None, "ep"), P(None, "ep"), P(None, "ep"), P(None, "ep"),
        P(), P(), P(), P(), P(("grp", "ep"), None, None, None), P(("grp", "ep"), None, None),
        P(("grp", "ep"), None), P(), P(("grp", "ep"), None), P(("grp", "ep"), None),
        P("ep", None, None), P("ep", None, None), P("ep", None, None), P(None, "ep"),
        P(None, "ep"), P("ep", None), P(),
    )
    return jax.shard_map(
        local,
        mesh=mesh,
        in_specs=placed,
        out_specs=(
            P(("grp", "ep"), None),
            P(("grp", "ep"), None, None, None),
            P(("grp", "ep"), None, None),
            P(("grp", "ep"), None),
        ),
        check_vma=False,
    )
```

time: 314 us -> 213 us (0.68)
  waiting for transfers between devices: 107 us -> 6.78 us
  blocking collectives: 87.3 us -> 142 us
  matrix products: 24.1 us -> 0 us
  Pallas kernels: 0 us -> 17 us
  between operations: 15.2 us -> 0.88 us
  other arithmetic: 14.4 us -> 2.23 us
  local copies, waits for them, and re-layouts: 21.9 us -> 11.5 us
  starting transfers between devices: 41.9 us -> 32.3 us
    all_to_all x1 -> x4, blocking collectives: 29.4 us -> 142 us  [exchange(): return lax.all_to_all(x, 'ep', 0, 0, axis_index_groups=groups)]
    all_gather x2 -> x0, waiting for transfers between devices: 71.2 us -> none  [the longest x1 70.9 us: local(): row_piece = lax.all_gather(normed, 'ep', axis=0, tiled=True)]
    unnamed x1 -> x0, blocking collectives: 57.9 us -> none
    all_to_all x2 -> x0, waiting for transfers between devices: 35.4 us -> none  [the longest x1 21.2 us: exchanged_experts(): lax.all_to_all(produced, 'ep', split_axis=1, concat_axis=0, tiled=True)]
    ppermute x0 -> x7, starting transfers between devices: none -> 32.3 us  [swap(): return lax.ppermute(x, 'ep', pairs)]
    unnamed x8 -> x0, starting transfers between devices: 28.9 us -> none
    dot_general x15 -> x0, matrix products: 24.1 us -> none  [the longest x4 5.2 us: local(): jnp.dot(row_piece, matrix, preferred_element_type=jnp.float32)]
    pallas_call x0 -> x10, Pallas kernels: none -> 17 us  [call(): pl.pallas_call(kernel, out_shape=[jax.ShapeDtypeStruct(s, d) for s, d in...]
  transfers between devices with their start and end apart: 12 -> 7, of which waited for: 4 -> 5; matrix products, arithmetic and copies ran while one was open for 6% -> 3% of each run, Pallas kernels for 0% -> 3%
where the time goes in v1:
time: 213 us
  blocking collectives  142 us (67%)
  starting transfers between devices  32.3 us (15%)
  Pallas kernels  17 us (8%)
  local copies, waits for them, and re-layouts  11.5 us (5%)
  waiting for transfers between devices  6.78 us (3%)
  other arithmetic  2.23 us (1%)
    all_to_all x4, blocking collectives, exchange(): return lax.all_to_all(x, 'ep', 0, 0, axis_index_groups=groups)  142 us
    ppermute x7, starting transfers between devices, swap(): return lax.ppermute(x, 'ep', pairs)  32.3 us
    pallas_call x10, Pallas kernels, call(): pl.pallas_call(kernel, out_shape=[jax.ShapeDtypeStruct(s, d) for s, d in...  17 us
    unnamed x62, local copies, waits for them, and re-layouts  11.5 us
    ppermute x7, waiting for transfers between devices, swap(): return lax.ppermute(x, 'ep', pairs)  6.78 us
  transfers between devices with their start and end apart: 7, of which 5 were waited for; matrix products, arithmetic and copies ran while one was open for 3% of the time, Pallas kernels for 3%

profile of v1, /device:TPU:69, one launch (start us, length us, event | category | flops | bytes accessed | tf_op | source)
XLA Modules:
  0.0 212.9 jit_solution(16222679699110434506)
XLA Ops:
  0.6 10.0 %collective-permute-start = (bf16[12,2048]{1,0:T(8,128)(2,1)}, bf16[12,2048]{1,0:T(8,128)(2,1)S(1)}, u32[]{:S(2)}, u32[]{:S(2)}) collective-permute-start(bf16[12,2048]{1,0:T(8,128)(2,1)} %resid_ref.3), channel_id=1, source_target_pairs={{0,1},{1,0},{2,3},{3,2},{4,5},{5,4},{6,7},{7,6},{8,9},{9,8},{10,11... | collective-permute-start | bytes 147464 | tf_op jit(solution)/shard_map/ppermute | solution.py:294
  10.7 1.1 collective-permute-done.other_ref
  11.8 0.8 copy-done.9
  12.6 0.8 copy-done.11
  13.4 0.2 norm.1
  13.6 0.0 copy-start.20
  13.6 0.0 copy-start.21
  13.6 43.9 %all_to_all.20.x_ref = bf16[16,24,1024]{2,1,0:T(8,128)(2,1)S(1)} all-to-all(bf16[16,24,1024]{2,1,0:T(8,128)(2,1)S(1)} %norm.1), channel_id=1, replica_groups={{0,2,4,6,8,10,12,14,16,18,20,22,24,26,28,30},{1,3,5,7,9,11,13,15,17,19,..., dimensions={0} | all-to-all | bytes 1572864 | tf_op jit(solution)/shard_map/all_to_all | solution.py:297
  57.6 6.4 %collective-permute-start.1 = (bf16[16,24,1024]{2,1,0:T(8,128)(2,1)S(1)}, bf16[16,24,1024]{2,1,0:T(8,128)(2,1)S(1)}, u32[]{:S(2)}, u32[]{:S(2)}) collective-permute-start(bf16[16,24,1024]{2,1,0:T(8,128)(2,1)S(1)} %all_to_all.20.x_ref), channel_id=1, source_target_pairs={{0,1},{1,0},{2,3},{3,2},{4,5},{5,4},{6,7},{7,6},{8,9},{9,8},{10,11... | collective-permute-start | bytes 2359304 | tf_op jit(solution)/shard_map/ppermute | solution.py:294
  63.9 0.1 copy.35.scores_ref
  64.0 0.1 copy.33.max_ref
  64.1 0.1 copy.34.routes_ref
  64.2 0.3 copy.27
  64.5 1.0 copy.28
  65.5 1.0 copy.29
  66.6 1.0 copy.30
  67.6 0.3 copy.31.wi_ref
  67.9 0.0 copy-start.13
  67.9 0.3 copy.32.wf_ref
  68.1 0.0 copy-start
  68.2 0.4 gates.1
  68.6 2.2 %pad_maximum_fusion.w_ref = bf16[2048,128]{1,0:T(8,128)(2,1)S(1)} fusion(bf16[2048,32]{1,0:T(8,128)(2,1)} %copy.30, bf16[2048,32]{1,0:T(8,128)(2,1)} %copy.29, bf16[2048,32]{1,0:T(8,128)(2,1)} %copy.28, bf16[2048,32]{1,0:T(8,128)(2,1)S(1)} %copy.27), kind=kLoop, calls=%fused_computation | loop fusion | flops 2097152 | bytes 1048576 | tf_op jit(solution)/shard_map/concatenate | solution.py:308
  70.8 0.0 collective-permute-done.1.y_ref
  70.8 0.6 proj.1
  71.4 17.3 %all_to_all.21.a_ref = bf16[16,32,128]{2,1,0:T(8,128)(2,1)S(1)} all-to-all(bf16[16,32,128]{2,1,0:T(8,128)(2,1)S(1)} %proj.1), channel_id=1, replica_groups={{0,2,4,6,8,10,12,14,16,18,20,22,24,26,28,30},{1,3,5,7,9,11,13,15,17,19,..., dimensions={0} | all-to-all | bytes 262144 | tf_op jit(solution)/shard_map/all_to_all | solution.py:297
  88.7 2.2 %collective-permute-start.2 = (bf16[16,32,128]{2,1,0:T(8,128)(2,1)S(1)}, bf16[16,32,128]{2,1,0:T(8,128)(2,1)S(1)}, u32[]{:S(2)}, u32[]{:S(2)}) collective-permute-start(bf16[16,32,128]{2,1,0:T(8,128)(2,1)S(1)} %all_to_all.21.a_ref), channel_id=1, source_target_pairs={{0,1},{1,0},{2,3},{3,2},{4,5},{5,4},{6,7},{7,6},{8,9},{9,8},{10,11... | collective-permute-start | bytes 393224 | tf_op jit(solution)/shard_map/ppermute | solution.py:294
  90.9 1.0 collective-permute-done.2.b_ref
  91.9 2.2 %copy-done.2 = bf16[1024,2048]{1,0:T(8,128)(2,1)S(1)} copy-done((bf16[1024,2048]{1,0:T(8,128)(2,1)S(1)}, bf16[1024,2048]{1,0:T(8,128)(2,1)}, u32[]{:S(2)}) %copy-start.2) | copy-done | bytes 4194328
  94.1 0.0 copy-start.8
  94.1 4.5 %cell.1 = (f32[12,2048]{1,0:T(8,128)S(1)}, bf16[12,1024]{1,0:T(8,128)(2,1)S(1)}, bf16[12,1024]{1,0:T(8,128)(2,1)S(1)}, f32[12,8,128]{2,1,0:T(8,128)}, f32[8,16,128]{2,1,0:T(8,128)S(1)}, /*index=5*/f32[128,128]{1,0:T(8,128)S(1)}) custom-call(bf16[16,32,128]{2,1,0:T(8,128)(2,1)S(1)} %all_to_all.21.a_ref, ...), custom_call_target="tpu_custom_call" | custom-call | flops 1000000 | bytes 1000000 | tf_op jit(solution)/shard_map/cell/pallas_call | solution.py:19
  98.6 0.4 collective-permute-start.3
  99.0 0.9 collective-permute-done.3.got_ref
  99.9 0.1 pair.1
  99.9 40.4 %all_to_all.22.x_ref = bf16[16,24,1024]{2,1,0:T(8,128)(2,1)S(1)} all-to-all(bf16[16,24,1024]{2,1,0:T(8,128)(2,1)S(1)} %pair.1), channel_id=1, replica_groups={{0,2,4,6,8,10,12,14,16,18,20,22,24,26,28,30},{1,3,5,7,9,11,13,15,17,19,..., dimensions={0} | all-to-all | bytes 1572864 | tf_op jit(solution)/shard_map/all_to_all | solution.py:297
  140.3 6.2 %collective-permute-start.4 = (bf16[16,24,1024]{2,1,0:T(8,128)(2,1)S(1)}, bf16[16,24,1024]{2,1,0:T(8,128)(2,1)S(1)}, u32[]{:S(2)}, u32[]{:S(2)}) collective-permute-start(bf16[16,24,1024]{2,1,0:T(8,128)(2,1)S(1)} %all_to_all.22.x_ref), channel_id=1, source_target_pairs={{0,1},{1,0},{2,3},{3,2},{4,5},{5,4},{6,7},{7,6},{8,9},{9,8},{10,11... | collective-permute-start | bytes 2359304 | tf_op jit(solution)/shard_map/ppermute | solution.py:294
  146.6 1.9 collective-permute-done.4.y_ref
  148.5 3.8 %branch.1 = (f32[384,1024]{1,0:T(8,128)S(1)}, bf16[384,1024]{1,0:T(8,128)(2,1)S(1)}) custom-call(bf16[16,24,1024]{2,1,0:T(8,128)(2,1)S(1)} %all_to_all.22.x_ref, bf16[16,24,1024]{2,1,0:T(8,128)(2,1)S(1)} %collective-permute-done.4.y_ref, bf16[16,32,128]{2,1,0:T(8,128)(2,1)S(1)} %all_to_all.21.a_ref, bf16[16,32,128]{2,1,0:T(8,128)(2,1)S(1)} %collective-permute-done.2.b_ref, ...), custom_call_target="tpu_custom_call" | custom-call | flops 1000000 | bytes 1000000 | tf_op jit(solution)/shard_map/branch/pallas_call | solution.py:19
  152.3 0.5 collective-permute-start.5
  152.8 1.9 collective-permute-done.5.got_ref
  154.8 0.2 add.1
  154.9 40.7 %all_to_all.23.x_ref = bf16[16,24,1024]{2,1,0:T(8,128)(2,1)S(1)} all-to-all(bf16[16,24,1024]{2,1,0:T(8,128)(2,1)S(1)} %add.1), channel_id=1, replica_groups={{0,2,4,6,8,10,12,14,16,18,20,22,24,26,28,30},{1,3,5,7,9,11,13,15,17,19,..., dimensions={0} | all-to-all | bytes 1572864 | tf_op jit(solution)/shard_map/all_to_all | solution.py:297
  195.6 0.1 sum.1
  195.7 6.6 %collective-permute-start.6 = (f32[12,1024]{1,0:T(8,128)S(1)}, f32[12,1024]{1,0:T(8,128)S(1)}, u32[]{:S(2)}, u32[]{:S(2)}) collective-permute-start(f32[12,1024]{1,0:T(8,128)S(1)} %get-tuple-element.26), channel_id=1, source_target_pairs={{0,1},{1,0},{2,3},{3,2},{4,5},{5,4},{6,7},{7,6},{8,9},{9,8},{10,11... | collective-permute-start | bytes 147464 | tf_op jit(solution)/shard_map/ppermute | solution.py:294
  202.3 0.7 copy.36
  203.0 2.8 %copy-done.1 = f32[12,8,128,128]{3,2,1,0:T(8,128)S(1)} copy-done((f32[12,8,128,128]{3,2,1,0:T(8,128)S(1)}, f32[12,8,128,128]{3,2,1,0:T(8,128)}, u32[]{:S(2)}) %copy-start.1) | copy-done | bytes 6291480
  205.7 6.5 %update.1 = f32[12,8,128,128]{3,2,1,0:T(8,128)} custom-call(f32[12,8]{1,0:T(8,128)S(1)} %get-tuple-element.19.keep_ref, f32[8,16,128]{2,1,0:T(8,128)S(1)} %get-tuple-element.28.keys_ref, f32[128,128]{1,0:T(8,128)S(1)} %get-tuple-element.29.wvt_ref, f32[12,8,128,128]{3,2,1,0:T(8,128)S(1)} %copy-done.1), custom_call_target="tpu_custom_call" | custom-call | flops 100000000 | bytes 1000000 | tf_op jit(solution)/shard_map/update/pallas_call | solution.py:19
  212.2 0.0 collective-permute-done.6.got_ref
  212.2 0.7 final.1
  (44 shorter events, 0.1 us)
Async XLA Ops:
  0.6 11.1 %collective-permute-start = (bf16[12,2048]{1,0:T(8,128)(2,1)}, bf16[12,2048]{1,0:T(8,128)(2,1)S(1)}, u32[]{:S(2)}, u32[]{:S(2)}) collective-permute-start(bf16[12,2048]{1,0:T(8,128)(2,1)} %resid_ref.3), channel_id=1, source_target_pairs={{0,1},{1,0},{2,3},{3,2},{4,5},{5,4},{6,7},{7,6},{8,9},{9,8},{10,11... | collective-permute-start | bytes 147464 | tf_op jit(solution)/shard_map/ppermute | solution.py:294
  11.8 0.8 copy-start.9
  12.6 0.8 copy-start.11
  13.4 50.6 %copy-start.25 = (bf16[12,2]{0,1:T(2,128)(2,1)S(1)}, bf16[12,2]{0,1:T(2,128)(2,1)}, u32[]{:S(2)}) copy-start(bf16[12,2]{0,1:T(2,128)(2,1)} %param.38) | copy-start | bytes 148
  13.4 50.7 %copy-start.22 = (f32[12,8]{0,1:T(8,128)S(1)}, f32[12,8]{0,1:T(8,128)}, u32[]{:S(2)}) copy-start(f32[12,8]{0,1:T(8,128)} %param.35) | copy-start | bytes 1156
  13.4 50.8 %copy-start.24 = (s32[12,2]{0,1:T(2,128)S(1)}, s32[12,2]{0,1:T(2,128)}, u32[]{:S(2)}) copy-start(s32[12,2]{0,1:T(2,128)} %param.37) | copy-start | bytes 292
  13.4 50.9 %copy-start.16 = (bf16[2048,32]{0,1:T(8,128)(2,1)S(1)}, bf16[2048,32]{0,1:T(8,128)(2,1)}, u32[]{:S(2)}) copy-start(bf16[2048,32]{0,1:T(8,128)(2,1)} %param.25) | copy-start | bytes 393220
  13.4 51.1 %copy-start.17 = (bf16[2048,32]{0,1:T(8,128)(2,1)S(1)}, bf16[2048,32]{0,1:T(8,128)(2,1)}, u32[]{:S(2)}) copy-start(bf16[2048,32]{0,1:T(8,128)(2,1)} %param.26) | copy-start | bytes 393220
  13.4 52.2 %copy-start.18 = (bf16[2048,32]{0,1:T(8,128)(2,1)S(1)}, bf16[2048,32]{0,1:T(8,128)(2,1)}, u32[]{:S(2)}) copy-start(bf16[2048,32]{0,1:T(8,128)(2,1)} %param.27) | copy-start | bytes 393220
  13.4 53.2 %copy-start.19 = (bf16[2048,32]{0,1:T(8,128)(2,1)S(1)}, bf16[2048,32]{0,1:T(8,128)(2,1)}, u32[]{:S(2)}) copy-start(bf16[2048,32]{0,1:T(8,128)(2,1)} %param.28) | copy-start | bytes 393220
  13.6 54.0 %copy-start.20 = (bf16[2048,8]{0,1:T(8,128)(2,1)S(1)}, bf16[2048,8]{0,1:T(8,128)(2,1)}, u32[]{:S(2)}) copy-start(bf16[2048,8]{0,1:T(8,128)(2,1)} %param.29) | copy-start | bytes 98308
  13.6 54.2 %copy-start.21 = (bf16[2048,8]{0,1:T(8,128)(2,1)S(1)}, bf16[2048,8]{0,1:T(8,128)(2,1)}, u32[]{:S(2)}) copy-start(bf16[2048,8]{0,1:T(8,128)(2,1)} %param.30) | copy-start | bytes 98308
  57.5 10.6 %copy-start.10 = (bf16[12,2048]{1,0:T(8,128)(2,1)S(1)}, bf16[12,2048]{1,0:T(8,128)(2,1)}, u32[]{:S(2)}) copy-start(bf16[12,2048]{1,0:T(8,128)(2,1)} %resid_ref.3) | copy-start | bytes 147460
  57.5 10.6 %copy-start.12 = (f32[4,2048]{1,0:T(4,128)S(1)}, f32[4,2048]{1,0:T(4,128)}, u32[]{:S(2)}) copy-start(f32[4,2048]{1,0:T(4,128)} %gains_ref.7) | copy-start | bytes 98308
  57.6 10.6 %copy-start.14 = (f32[8]{0:T(128)S(1)}, f32[8]{0:T(128)}, u32[]{:S(2)}) copy-start(f32[8]{0:T(128)} %param.31) | copy-start | bytes 100
  57.6 10.6 %copy-start.15 = (f32[8]{0:T(128)S(1)}, f32[8]{0:T(128)}, u32[]{:S(2)}) copy-start(f32[8]{0:T(128)} %param.32) | copy-start | bytes 100
  57.6 13.2 %collective-permute-start.1 = (bf16[16,24,1024]{2,1,0:T(8,128)(2,1)S(1)}, bf16[16,24,1024]{2,1,0:T(8,128)(2,1)S(1)}, u32[]{:S(2)}, u32[]{:S(2)}) collective-permute-start(bf16[16,24,1024]{2,1,0:T(8,128)(2,1)S(1)} %all_to_all.20.x_ref), channel_id=1, source_target_pairs={{0,1},{1,0},{2,3},{3,2},{4,5},{5,4},{6,7},{7,6},{8,9},{9,8},{10,11... | collective-permute-start | bytes 2359304 | tf_op jit(solution)/shard_map/ppermute | solution.py:294
  67.9 24.1 %copy-start.13 = (f32[12,8,128]{2,1,0:T(8,128)S(1)}, f32[12,8,128]{2,1,0:T(8,128)}, u32[]{:S(2)}) copy-start(f32[12,8,128]{2,1,0:T(8,128)} %norm_ref.1) | copy-start | bytes 147460
  68.1 23.8 %copy-start = (f32[12,8,128,128]{3,2,1,0:T(8,128)S(1)}, f32[12,8,128,128]{3,2,1,0:T(8,128)}, u32[]{:S(2)}) copy-start(f32[12,8,128,128]{3,2,1,0:T(8,128)} %m_ref.3) | copy-start | bytes 18874372
  88.7 3.2 %collective-permute-start.2 = (bf16[16,32,128]{2,1,0:T(8,128)(2,1)S(1)}, bf16[16,32,128]{2,1,0:T(8,128)(2,1)S(1)}, u32[]{:S(2)}, u32[]{:S(2)}) collective-permute-start(bf16[16,32,128]{2,1,0:T(8,128)(2,1)S(1)} %all_to_all.21.a_ref), channel_id=1, source_target_pairs={{0,1},{1,0},{2,3},{3,2},{4,5},{5,4},{6,7},{7,6},{8,9},{9,8},{10,11... | collective-permute-start | bytes 393224 | tf_op jit(solution)/shard_map/ppermute | solution.py:294
  91.9 2.2 %copy-start.2 = (bf16[1024,2048]{1,0:T(8,128)(2,1)S(1)}, bf16[1024,2048]{1,0:T(8,128)(2,1)}, u32[]{:S(2)}) copy-start(bf16[1024,2048]{1,0:T(8,128)(2,1)} %mix_ref.1) | copy-start | bytes 12582916
  94.1 54.4 %copy-start.4 = (bf16[1,2048,512]{2,1,0:T(8,128)(2,1)S(1)}, bf16[1,2048,512]{2,1,0:T(8,128)(2,1)}, u32[]{:S(2)}) copy-start(bf16[1,2048,512]{2,1,0:T(8,128)(2,1)} %eu_ref.1) | copy-start | bytes 6291460
  94.1 54.4 %copy-start.5 = (bf16[1,512,2048]{2,1,0:T(8,128)(2,1)S(1)}, bf16[1,512,2048]{2,1,0:T(8,128)(2,1)}, u32[]{:S(2)}) copy-start(bf16[1,512,2048]{2,1,0:T(8,128)(2,1)} %ed_ref.1) | copy-start | bytes 6291460
  94.1 54.4 %copy-start.6 = (bf16[2048,256]{1,0:T(8,128)(2,1)S(1)}, bf16[2048,256]{1,0:T(8,128)(2,1)}, u32[]{:S(2)}) copy-start(bf16[2048,256]{1,0:T(8,128)(2,1)} %dg_ref.1) | copy-start | bytes 3145732
  94.1 54.4 %copy-start.7 = (bf16[2048,256]{1,0:T(8,128)(2,1)S(1)}, bf16[2048,256]{1,0:T(8,128)(2,1)}, u32[]{:S(2)}) copy-start(bf16[2048,256]{1,0:T(8,128)(2,1)} %du_ref.1) | copy-start | bytes 3145732
  94.1 54.4 %copy-start.8 = (bf16[256,2048]{1,0:T(8,128)(2,1)S(1)}, bf16[256,2048]{1,0:T(8,128)(2,1)}, u32[]{:S(2)}) copy-start(bf16[256,2048]{1,0:T(8,128)(2,1)} %dd_ref.1) | copy-start | bytes 3145732
  98.6 47.9 %copy-start.23 = (bf16[2048]{0:T(1024)(128)(2,1)S(1)}, bf16[2048]{0:T(1024)(128)(2,1)}, u32[]{:S(2)}) copy-start(bf16[2048]{0:T(1024)(128)(2,1)} %param.45) | copy-start | bytes 12292
  98.6 49.9 %copy-start.3 = (bf16[1,2048,512]{2,1,0:T(8,128)(2,1)S(1)}, bf16[1,2048,512]{2,1,0:T(8,128)(2,1)}, u32[]{:S(2)}) copy-start(bf16[1,2048,512]{2,1,0:T(8,128)(2,1)} %eg_ref.1) | copy-start | bytes 6291460
  98.6 1.2 collective-permute-start.3
  140.3 8.2 %collective-permute-start.4 = (bf16[16,24,1024]{2,1,0:T(8,128)(2,1)S(1)}, bf16[16,24,1024]{2,1,0:T(8,128)(2,1)S(1)}, u32[]{:S(2)}, u32[]{:S(2)}) collective-permute-start(bf16[16,24,1024]{2,1,0:T(8,128)(2,1)S(1)} %all_to_all.22.x_ref), channel_id=1, source_target_pairs={{0,1},{1,0},{2,3},{3,2},{4,5},{5,4},{6,7},{7,6},{8,9},{9,8},{10,11... | collective-permute-start | bytes 2359304 | tf_op jit(solution)/shard_map/ppermute | solution.py:294
  152.3 2.4 %collective-permute-start.5 = (bf16[384,1024]{1,0:T(8,128)(2,1)S(1)}, bf16[384,1024]{1,0:T(8,128)(2,1)S(1)}, u32[]{:S(2)}, u32[]{:S(2)}) collective-permute-start(bf16[384,1024]{1,0:T(8,128)(2,1)S(1)} %get-tuple-element.24), channel_id=1, source_target_pairs={{0,1},{1,0},{2,3},{3,2},{4,5},{5,4},{6,7},{7,6},{8,9},{9,8},{10,11... | collective-permute-start | bytes 2359304 | tf_op jit(solution)/shard_map/ppermute | solution.py:294
  195.7 16.5 %collective-permute-start.6 = (f32[12,1024]{1,0:T(8,128)S(1)}, f32[12,1024]{1,0:T(8,128)S(1)}, u32[]{:S(2)}, u32[]{:S(2)}) collective-permute-start(f32[12,1024]{1,0:T(8,128)S(1)} %get-tuple-element.26), channel_id=1, source_target_pairs={{0,1},{1,0},{2,3},{3,2},{4,5},{5,4},{6,7},{7,6},{8,9},{9,8},{10,11... | collective-permute-start | bytes 147464 | tf_op jit(solution)/shard_map/ppermute | solution.py:294
  203.0 2.8 %copy-start.1 = (f32[12,8,128,128]{3,2,1,0:T(8,128)S(1)}, f32[12,8,128,128]{3,2,1,0:T(8,128)}, u32[]{:S(2)}) copy-start(f32[12,8,128,128]{3,2,1,0:T(8,128)} %m_ref.3) | copy-start | bytes 18874372

commit v2 on v1

--- a/solution.py
+++ b/solution.py
@@ -13,14 +13,20 @@
 BF16 = jnp.bfloat16
 
 
-def call(kernel, outs, args, scratch=(), vmem=16, flops=1000000, name=None):
-    single = not isinstance(outs, (list, tuple))
-    shapes = [outs] if single else list(outs)
+def call(kernel, outs, args, scratch=(), vmem=16, flops=1000000, name=None, hbm=(), sems=0, **grid):
+    if hbm:
+        if not INTERPRET:
+            args = [pltpu.with_memory_space_constraint(x, pltpu.HBM) if i in hbm else x
+                    for i, x in enumerate(args)]
+        grid["in_specs"] = [
+            pl.BlockSpec(memory_space=pltpu.HBM if i in hbm else pltpu.VMEM)
+            for i in range(len(args))]
     result = pl.pallas_call(
         kernel,
-        out_shape=[jax.ShapeDtypeStruct(s, d) for s, d in shapes] if not single
-        else None,
-        scratch_shapes=[pltpu.VMEM(s, d) for s, d in scratch],
+        out_shape=[jax.ShapeDtypeStruct(s, d) for s, d in outs],
+        scratch_shapes=[pltpu.VMEM(s, d) for s, d in scratch]
+        + ([pltpu.SemaphoreType.DMA((sems,))] if sems else []),
+        **grid,
         compiler_params=pltpu.CompilerParams(vmem_limit_bytes=vmem << 20),
         cost_estimate=pl.CostEstimate(flops=flops, bytes_accessed=1000000, transcendentals=0),
         interpret=INTERPRET,
@@ -37,6 +43,10 @@
     return lax.rem(lax.axis_index("ep"), 2)
 
 
+def dot_t(a, b):
+    return lax.dot_general(a, b, (((1,), (1,)), ((), ())), preferred_element_type=F32)
+
+
 def dot(a, b):
     return jnp.dot(a, b, preferred_element_type=F32)
 
@@ -53,25 +63,35 @@
     rows[:r] = jnp.where(c == 0, own, other)
     rows[r : 2 * r] = jnp.where(c == 0, other, own)
     normed = rms(rows[...], gains_ref[0:1, :])
-    half = half_of(c, normed).astype(BF16)
-    for z in range(out_ref.shape[0]):
-        out_ref[z] = half
+    out_ref[...] = half_of(c, normed).astype(BF16)
 
 
 def gates_kernel(
-    resid_ref, gains_ref, wi_ref, wf_ref, bi_ref, bf_ref, max_ref, routes_ref, scores_ref,
-    keep_ref, write_ref, newmax_ref, info_ref,
+    resid_ref, gains_ref, wi_ref, wf_ref, bi_ref, bf_ref, bit_ref, bft_ref, max_ref, maxt_ref,
+    routes_ref, scores_ref, wq_ref, wk_ref, wv_ref, wo_ref,
+    keep_ref, write_ref, newmax_ref, info_ref, weights_ref, sems,
 ):
     r = resid_ref.shape[0]
+    cols = wq_ref.shape[0]
+    copies = [
+        pltpu.make_async_copy(w, weights_ref.at[pl.ds(k * cols, cols)], sems.at[k])
+        for k, w in enumerate((wq_ref, wk_ref, wv_ref, wo_ref))]
+    for copy in copies:
+        copy.start()
     normed = rms(resid_ref[...].astype(F32), gains_ref[0:1, :]).astype(BF16)
-    ipre = dot(normed, wi_ref[...]) + bi_ref[...]
-    fpre = dot(normed, wf_ref[...]) + bf_ref[...]
-    logf = jnp.minimum(fpre, 0.0) - jnp.log1p(jnp.exp(-jnp.abs(fpre)))
-    decayed = logf + max_ref[...]
-    new_max = jnp.maximum(ipre, decayed)
+
+    def gates(ipre, fpre, old):
+        logf = jnp.minimum(fpre, 0.0) - jnp.log1p(jnp.exp(-jnp.abs(fpre)))
+        return ipre, logf + old, jnp.maximum(ipre, logf + old)
+
+    ipre, decayed, new_max = gates(
+        dot_t(normed, wi_ref[...]) + bi_ref[...], dot_t(normed, wf_ref[...]) + bf_ref[...],
+        max_ref[...])
     keep_ref[...] = jnp.exp(decayed - new_max)
     write_ref[...] = jnp.exp(ipre - new_max)
-    newmax_ref[...] = new_max
+    newmax_ref[...] = gates(
+        dot_t(wi_ref[...], normed) + bit_ref[...], dot_t(wf_ref[...], normed) + bft_ref[...],
+        maxt_ref[...])[2]
     lanes = lax.broadcasted_iota(jnp.int32, (r, 128), 1)
     row = lax.broadcasted_iota(jnp.int32, (r, 128), 0)
     total = jnp.zeros((r, 128), F32)
@@ -81,6 +101,8 @@
         total = total + jnp.where(lanes == row + k * r, column, 0.0)
     info = jnp.sum(total, axis=0, keepdims=True)
     info_ref[...] = jnp.broadcast_to(info, info_ref.shape).astype(BF16)
+    for copy in copies:
+        copy.wait()
 
 
 def proj_kernel(x_ref, y_ref, w_ref, info_ref, out_ref):
@@ -88,10 +110,10 @@
     nz, r2, h = x_ref.shape
     x = x_ref[...].reshape(nz * r2, h)
     y = y_ref[...].reshape(nz * r2, h)
-    wx = w_ref[pl.ds(pl.multiple_of(c * h, h), h), :]
-    wy = w_ref[pl.ds(pl.multiple_of((1 - c) * h, h), h), :]
-    p = (dot(x, wx) + dot(y, wy)).astype(BF16).reshape(nz, r2, w_ref.shape[1])
-    out_ref[:, :r2, :] = p
+    at = pl.ds(pl.multiple_of(c * h, h), h)
+    to = pl.ds(pl.multiple_of((1 - c) * h, h), h)
+    p = (dot_t(x, w_ref[:, at]) + dot_t(y, w_ref[:, to])).astype(BF16)
+    out_ref[:, :r2, :] = p.reshape(nz, r2, p.shape[1])
     for z in range(nz):
         out_ref[z, r2 : r2 + 8, :] = info_ref[...]
 
@@ -99,10 +121,18 @@
 def cell_kernel(
     a_ref, b_ref, keep_ref, write_ref, m_ref, norm_ref, mix_ref, resid_ref, gains_ref,
     middle_ref, mine_ref, send_ref, newnorm_ref, keys_ref, wvt_ref,
-    p0, p1, q_scr, wv_scr, gated,
+    p0, p1, q_scr, wv_scr, gated, m_scr, mix_scr, sems,
 ):
     c = core()
     r, heads, dh = norm_ref.shape
+
+    def state_copy(s):
+        return pltpu.make_async_copy(m_ref.at[s], m_scr.at[s], sems.at[s])
+
+    mix_copy = pltpu.make_async_copy(mix_ref, mix_scr, sems.at[r])
+    for s in range(r):
+        state_copy(s).start()
+    mix_copy.start()
     nz = a_ref.shape[0]
     cols = heads * dh // (2 * nz)
     per = dh // cols
@@ -135,8 +165,9 @@
     lane128 = lax.broadcasted_iota(jnp.int32, (dh, 128), 1)
 
     def step(s, acc):
+        state_copy(s).wait()
         for h in range(heads):
-            prod = m_ref[s, h] * q_scr[h, pl.ds(s, 1), :]
+            prod = m_scr[s, h] * q_scr[h, pl.ds(s, 1), :]
             red = jnp.sum(prod, axis=1, keepdims=True)
             acc = jnp.where(lane128 == h * 16 + s, red, acc)
         return acc
@@ -153,7 +184,8 @@
         top = keep * numer[h * 16 : h * 16 + r] + wv_scr[h * 16 : h * 16 + r] * kq
         cell = top / jnp.maximum(jnp.abs(denom), 1.0)
         gated[:, h * dh : (h + 1) * dh] = (jax.nn.sigmoid(outgate) * cell).astype(BF16)
-    mixed = dot(gated[...], mix_ref[...])
+    mix_copy.wait()
+    mixed = dot(gated[...], mix_scr[...])
     middle = resid_ref[...].astype(F32) + rms(mixed, gains_ref[1:2, :])
     middle_ref[...] = middle
     branch = rms(middle, gains_ref[2:3, :])
@@ -161,18 +193,15 @@
     send_ref[...] = half_of(1 - c, branch).astype(BF16)
 
 
-def update_kernel(keep_ref, keys_ref, wvt_ref, m_ref, out_ref):
-    r, heads, dh, _ = m_ref.shape
-
-    def step(s, carry):
-        rolled = pltpu.roll(wvt_ref[...], lax.rem(128 - s, 128), 1)
-        for h in range(heads):
-            keep = keep_ref[pl.ds(s, 1), h : h + 1]
-            key = keys_ref[h, pl.ds(s, 1), :]
-            out_ref[s, h] = keep * m_ref[s, h] + rolled[:, h * 16 : h * 16 + 1] * key
-        return carry
-
-    lax.fori_loop(0, r, step, 0)
+def update_kernel(keep_ref, keys_ref, wvt_ref, after_ref, m_ref, out_ref, token_ref):
+    token_ref[...] = jnp.zeros_like(token_ref)
+    heads = m_ref.shape[1]
+    s = pl.program_id(0)
+    rolled = pltpu.roll(wvt_ref[...], lax.rem(128 - s, 128), 1)
+    for h in range(heads):
+        keep = keep_ref[pl.ds(s, 1), h : h + 1]
+        key = keys_ref[h, pl.ds(s, 1), :]
+        out_ref[0, h] = keep * m_ref[0, h] + rolled[:, h * 16 : h * 16 + 1] * key
 
 
 def pair_kernel(mine_ref, got_ref, out_ref, rows):
@@ -181,9 +210,7 @@
     mine, got = mine_ref[...].astype(F32), got_ref[...].astype(F32)
     rows[:r] = jnp.where(c == 0, mine, got)
     rows[r : 2 * r] = jnp.where(c == 0, got, mine)
-    both = rows[...].astype(BF16)
-    for z in range(out_ref.shape[0]):
-        out_ref[z] = both
+    out_ref[...] = rows[...].astype(BF16)
 
 
 def silu_mul(gate, up):
@@ -249,17 +276,42 @@
         ref[...] = part.astype(ref.dtype)
 
 
-def add_kernel(keep_ref, got_ref, out_ref):
-    total = keep_ref[...] + got_ref[...].astype(F32)
-    out_ref[...] = total.astype(BF16).reshape(out_ref.shape)
-
-
-def sum_kernel(x_ref, mine_ref, send_ref):
+NEAR = (1, -1, 2, -2)
+FAR = 5
+
+
+def spread_kernel(keep_ref, got_ref, *out_refs):
+    z = lax.div(lax.axis_index("ep"), 2)
+    own_ref, near_refs, last_ref = out_refs[0], out_refs[1:-1], out_refs[-1]
+    nz = keep_ref.shape[0]
+
+    def term(offset):
+        at = lax.rem(z + offset + nz, nz)
+        return keep_ref[at] + got_ref[at].astype(F32)
+
+    for i, far in enumerate((0, FAR, -FAR)):
+        own_ref[i] = term(far)
+        for near, ref in zip(NEAR, near_refs):
+            ref[i] = term(near + far).astype(BF16)
+    last_ref[...] = term(nz // 2).astype(BF16)
+
+
+def fold_kernel(
+    own_ref, a_ref, b_ref, c_ref, d_ref, last_ref, token_ref, own_out, plus_ref, minus_ref,
+):
+    def total(i):
+        t = own_ref[i] + a_ref[i].astype(F32) + b_ref[i].astype(F32)
+        return t + c_ref[i].astype(F32) + d_ref[i].astype(F32)
+
+    own_out[...] = total(0)
+    plus_ref[...] = (total(1) + last_ref[...].astype(F32)).astype(BF16)
+    minus_ref[...] = total(2).astype(BF16)
+
+
+def sum_kernel(own_ref, a_ref, b_ref, mine_ref, send_ref):
     c = core()
     r = mine_ref.shape[0]
-    total = x_ref[0].astype(F32)
-    for z in range(1, x_ref.shape[0]):
-        total = total + x_ref[z].astype(F32)
+    total = own_ref[...] + a_ref[...].astype(F32) + b_ref[...].astype(F32)
     mine_ref[...] = jnp.where(c == 0, total[:r], total[r:])
     send_ref[...] = jnp.where(c == 0, total[r:], total[:r])
 
@@ -296,19 +348,30 @@
     def exchange(x):
         return lax.all_to_all(x, "ep", 0, 0, axis_index_groups=groups)
 
+    def shift(x, offset):
+        return lax.ppermute(
+            x, "ep", [(2 * z + c, 2 * ((z + offset) % nz) + c) for z in range(nz) for c in range(2)])
+
+    def gather(x):
+        return lax.all_gather(x, "ep", axis=0, axis_index_groups=groups)
+
     other = swap(resid)
-    chunk, = call(norm_kernel, [((nz, 2 * r, h), BF16)], (resid, other, norm_gains),
+    chunk, = call(norm_kernel, [((2 * r, h), BF16)], (resid, other, norm_gains),
                   scratch=[((2 * r, d), F32)], name="norm")
-    x = exchange(chunk)
-    keep, write, new_max, info = call(
+    x = gather(chunk)
+    keep, write, new_max, info, w_all = call(
         gates_kernel,
-        [((r, heads), F32), ((r, heads), F32), ((r, heads), F32), ((8, 128), BF16)],
-        (resid, norm_gains, w_igate, w_fgate, igate_bias.reshape(1, heads),
-         fgate_bias.reshape(1, heads), state_max, routes, route_scores), name="gates")
-    w_all = jnp.concatenate([w_query, w_key, w_value, w_outgate], axis=1)
+        [((r, heads), F32), ((r, heads), F32), ((heads, r), F32), ((8, 128), BF16),
+         ((4 * inner // n, d), BF16)],
+        (resid, norm_gains, w_igate.T, w_fgate.T, igate_bias.reshape(1, heads),
+         fgate_bias.reshape(1, heads), igate_bias.reshape(heads, 1),
+         fgate_bias.reshape(heads, 1), state_max, state_max.T, routes, route_scores,
+         w_query.T, w_key.T, w_value.T, w_outgate.T),
+        hbm=(12, 13, 14, 15), sems=4, name="gates")
     y = swap(x)
-    projected, = call(proj_kernel, [((nz, 2 * r + 8, w_all.shape[1]), BF16)],
-                      (x, y, w_all, info), name="proj")
+    projected, = call(
+        proj_kernel, [((nz, 2 * r + 8, 4 * inner // n), BF16)],
+        (x, y, w_all, info), name="proj")
     a = exchange(projected)
     b = swap(a)
     middle, mine, send, new_norm, keys, wvt = call(
@@ -317,14 +380,13 @@
          ((heads, 16, dh), F32), ((dh, 128), F32)],
         (a, b, keep, write, state_matrix, state_norm, w_mix_out, resid, norm_gains),
         scratch=[((nz, 16, dh), F32), ((nz, 16, dh), F32), ((heads, 16, dh), F32),
-                 ((128, dh), F32), ((r, inner), BF16)],
-        vmem=24, name="cell")
+                 ((128, dh), F32), ((r, inner), BF16), (state_matrix.shape, F32),
+                 (w_mix_out.shape, BF16)],
+        hbm=(4, 6), sems=r + 1, vmem=24, name="cell")
     got = swap(send)
-    chunk, = call(pair_kernel, [((nz, 2 * r, h), BF16)], (mine, got),
+    chunk, = call(pair_kernel, [((2 * r, h), BF16)], (mine, got),
                   scratch=[((2 * r, h), F32)], name="pair")
-    x = exchange(chunk)
-    new_matrix, = call(update_kernel, [(state_matrix.shape, F32)],
-                       (keep, keys, wvt, state_matrix), vmem=24, flops=100000000, name="update")
+    x = gather(chunk)
     y = swap(x)
     part, send = call(
         branch_kernel, [((n * r, h), F32), ((n * r, h), BF16)],
@@ -332,12 +394,31 @@
          branch_weight.reshape(1, d)),
         scratch=[((n * r, 128), F32), ((n * CAP, d), BF16)], vmem=32, name="branch")
     got = swap(send)
-    chunk, = call(add_kernel, [((nz, 2 * r, h), BF16)], (part, got), name="add")
-    x = exchange(chunk)
-    mine, send = call(sum_kernel, [((r, h), F32), ((r, h), F32)], (x,), name="sum")
+    tile = (2 * r, h)
+    own, *near, last = call(
+        spread_kernel, [((3,) + tile, F32)] + [((3,) + tile, BF16)] * 4 + [(tile, BF16)],
+        (part.reshape((nz,) + tile), got.reshape((nz,) + tile)), name="spread")
+    near = [shift(x, offset) for x, offset in zip(near, NEAR)]
+    tail, last = last, shift(last, nz // 2 - FAR)
+    new_matrix, token = call(
+        update_kernel, [(state_matrix.shape, F32), ((8, 128), F32)],
+        (keep, keys, wvt, tail, state_matrix),
+        grid=(r,),
+        in_specs=[pl.BlockSpec(keep.shape, lambda s: (0, 0)),
+                  pl.BlockSpec(keys.shape, lambda s: (0, 0, 0)),
+                  pl.BlockSpec(wvt.shape, lambda s: (0, 0)),
+                  pl.BlockSpec((8, 128), lambda s: (0, 0)),
+                  pl.BlockSpec((1, heads, dh, dh), lambda s: (s, 0, 0, 0))],
+        out_specs=[pl.BlockSpec((1, heads, dh, dh), lambda s: (s, 0, 0, 0)),
+                   pl.BlockSpec((8, 128), lambda s: (0, 0))],
+        vmem=8, flops=500000000, name="update")
+    own, plus, minus = call(fold_kernel, [(tile, F32), (tile, BF16), (tile, BF16)],
+                            (own, *near, last, token), name="fold")
+    plus, minus = shift(plus, FAR), shift(minus, -FAR)
+    mine, send = call(sum_kernel, [((r, h), F32), ((r, h), F32)], (own, plus, minus), name="sum")
     got = swap(send)
     out, = call(final_kernel, [((r, d), BF16)], (mine, got, middle, norm_gains), name="final")
-    return (out, new_matrix, new_norm, new_max)
+    return (out, new_matrix, new_norm, new_max.T)
 
 
 def solution(mesh):

time: 213 us -> 162 us (0.76)
  blocking collectives: 142 us -> 72.3 us
  starting transfers between devices: 32.3 us -> 45.4 us
  waiting for transfers between devices: 6.78 us -> 11.8 us
  Pallas kernels: 17 us -> 20.3 us
  other arithmetic: 2.23 us -> 0.01 us
    all_to_all x4 -> x1, blocking collectives: 142 us -> 17.6 us  [exchange(): return lax.all_to_all(x, 'ep', 0, 0, axis_index_groups=groups)]
    all_gather x0 -> x2, blocking collectives: none -> 54.7 us  [gather(): return lax.all_gather(x, 'ep', axis=0, axis_index_groups=groups)]
    ppermute x0 -> x7, starting transfers between devices: none -> 13.9 us  [shift(): lax.ppermute(x, 'ep', [(2 * z + c, 2 * ((z + offset) % nz) + c) for z in...]
    ppermute x0 -> x7, waiting for transfers between devices: none -> 4.17 us  [shift(): lax.ppermute(x, 'ep', [(2 * z + c, 2 * ((z + offset) % nz) + c) for z in...]
    pallas_call x10 -> x11, Pallas kernels: 17 us -> 20.3 us  [call(): pl.pallas_call(kernel, out_shape=[jax.ShapeDtypeStruct(s, d) for s, d in...]
    unnamed x62 -> x45, local copies, waits for them, and re-layouts: 11.5 us -> 9.05 us
    concatenate x1 -> x0, other arithmetic: 2.23 us -> none  [local(): w_all = jnp.concatenate([w_query, w_key, w_value, w_outgate], axis=1)]
  transfers between devices with their start and end apart: 7 -> 14, of which waited for: 5 -> 8; matrix products, arithmetic and copies ran while one was open for 3% -> 2% of each run, Pallas kernels for 3% -> 5%
where the time goes in v2:
time: 162 us; the launch traced here: 161 us
  blocking collectives  72.3 us (45%)
  starting transfers between devices  45.4 us (28%)
  Pallas kernels  20.3 us (13%)
  waiting for transfers between devices  11.8 us (7%)
  local copies, waits for them, and re-layouts  10.5 us (6%)
    all_gather x2, blocking collectives, gather(): return lax.all_gather(x, 'ep', axis=0, axis_index_groups=groups)  54.7 us
    ppermute x7, starting transfers between devices, swap(): return lax.ppermute(x, 'ep', pairs)  31.5 us
    pallas_call x11, Pallas kernels, call(): pl.pallas_call(kernel, out_shape=[jax.ShapeDtypeStruct(s, d) for s, d in...  20.3 us
    all_to_all x1, blocking collectives, exchange(): return lax.all_to_all(x, 'ep', 0, 0, axis_index_groups=groups)  17.6 us
    ppermute x7, starting transfers between devices, shift(): lax.ppermute(x, 'ep', [(2 * z + c, 2 * ((z + offset) % nz) + c) for z in...  13.9 us
    unnamed x45, local copies, waits for them, and re-layouts  9.05 us
    ppermute x7, waiting for transfers between devices, swap(): return lax.ppermute(x, 'ep', pairs)  7.66 us
    ppermute x7, waiting for transfers between devices, shift(): lax.ppermute(x, 'ep', [(2 * z + c, 2 * ((z + offset) % nz) + c) for z in...  4.17 us
  transfers between devices with their start and end apart: 14, of which 8 were waited for; matrix products, arithmetic and copies ran while one was open for 2% of the time, Pallas kernels for 5%

profile of v2, /device:TPU:69, one launch (start us, length us, event | category | flops | bytes accessed | tf_op | source)
XLA Modules:
  0.0 161.2 jit_solution(7546513604810555783)
XLA Ops:
  0.6 10.0 %collective-permute-start = (bf16[12,2048]{1,0:T(8,128)(2,1)}, bf16[12,2048]{1,0:T(8,128)(2,1)S(1)}, u32[]{:S(2)}, u32[]{:S(2)}) collective-permute-start(bf16[12,2048]{1,0:T(8,128)(2,1)} %resid_ref.3), channel_id=1, source_target_pairs={{0,1},{1,0},{2,3},{3,2},{4,5},{5,4},{6,7},{7,6},{8,9},{9,8},{10,11... | collective-permute-start | bytes 147464 | tf_op jit(solution)/shard_map/ppermute | solution.py:346
  10.6 1.1 collective-permute-done.other_ref
  11.8 0.8 copy-done.6
  12.6 0.8 copy-done.9
  13.4 0.2 norm.1
  13.5 0.0 copy-start.8
  13.6 27.5 %all-gather = bf16[384,1024]{1,0:T(8,128)(2,1)S(1)} all-gather(bf16[24,1024]{1,0:T(8,128)(2,1)S(1)} %norm.1), channel_id=2, replica_groups={{0,2,4,6,8,10,12,14,16,18,20,22,24,26,28,30},{1,3,5,7,9,11,13,15,17,19,..., dimensions={0}, use_global_device_ids=true | all-gather | bytes 835584 | tf_op jit(solution)/shard_map/all_gather | solution.py:356
  41.0 7.4 %collective-permute-start.1 = (bf16[16,24,1024]{2,1,0:T(8,128)(2,1)S(1)}, bf16[16,24,1024]{2,1,0:T(8,128)(2,1)S(1)}, u32[]{:S(2)}, u32[]{:S(2)}) collective-permute-start(bf16[16,24,1024]{2,1,0:T(8,128)(2,1)S(1)} %bitcast.18), channel_id=1, source_target_pairs={{0,1},{1,0},{2,3},{3,2},{4,5},{5,4},{6,7},{7,6},{8,9},{9,8},{10,11... | collective-permute-start | bytes 2359304 | tf_op jit(solution)/shard_map/ppermute | solution.py:346
  48.4 0.7 copy.31.scores_ref
  49.2 0.7 copy.28.bft_ref
  49.9 0.7 copy.27.bit_ref
  50.6 0.8 copy.30.routes_ref
  51.4 0.8 copy.29.max_ref
  52.2 0.8 copy-done.7
  53.0 0.8 copy-done.10
  53.8 0.8 copy-done.13
  54.5 0.8 copy-done.14
  55.3 0.7 copy-done.15
  56.0 0.7 copy-done.16
  56.6 0.7 copy-done.17
  57.3 1.8 %gates.1 = (f32[12,8]{1,0:T(8,128)S(1)}, f32[12,8]{1,0:T(8,128)S(1)}, f32[8,12]{1,0:T(8,128)}, bf16[8,128]{1,0:T(8,128)(2,1)S(1)}, bf16[128,2048]{1,0:T(8,128)(2,1)S(1)}) custom-call(bf16[12,2048]{1,0:T(8,128)(2,1)S(1)} %copy-done.7, f32[4,2048]{1,0:T(4,128)S(1)} %copy-done.10, bf16[8,2048]{1,0:T(8,128)(2,1)S(1)} %bitcast.24, bf16[8,2048]{1,0:T(8,128)(2,1)S(1)} %bitcast.25, ...), custom_call_target="tpu_custom_call" | custom-call | flops 1000000 | bytes 1000000 | tf_op jit(solution)/shard_map/gates/pallas_call | solution.py:24
  59.1 0.6 proj.1
  59.7 17.6 %all_to_all.5.a_ref = bf16[16,32,128]{2,1,0:T(8,128)(2,1)S(1)} all-to-all(bf16[16,32,128]{2,1,0:T(8,128)(2,1)S(1)} %proj.1), channel_id=1, replica_groups={{0,2,4,6,8,10,12,14,16,18,20,22,24,26,28,30},{1,3,5,7,9,11,13,15,17,19,..., dimensions={0} | all-to-all | bytes 262144 | tf_op jit(solution)/shard_map/all_to_all | solution.py:349
  77.3 1.9 %collective-permute-start.2 = (bf16[16,32,128]{2,1,0:T(8,128)(2,1)S(1)}, bf16[16,32,128]{2,1,0:T(8,128)(2,1)S(1)}, u32[]{:S(2)}, u32[]{:S(2)}) collective-permute-start(bf16[16,32,128]{2,1,0:T(8,128)(2,1)S(1)} %all_to_all.5.a_ref), channel_id=1, source_target_pairs={{0,1},{1,0},{2,3},{3,2},{4,5},{5,4},{6,7},{7,6},{8,9},{9,8},{10,11... | collective-permute-start | bytes 393224 | tf_op jit(solution)/shard_map/ppermute | solution.py:346
  79.2 1.0 collective-permute-done.2.b_ref
  80.3 5.9 %cell.1 = (f32[12,2048]{1,0:T(8,128)S(1)}, bf16[12,1024]{1,0:T(8,128)(2,1)S(1)}, bf16[12,1024]{1,0:T(8,128)(2,1)S(1)}, f32[12,8,128]{2,1,0:T(8,128)}, f32[8,16,128]{2,1,0:T(8,128)S(1)}, /*index=5*/f32[128,128]{1,0:T(8,128)S(1)}) custom-call(bf16[16,32,128]{2,1,0:T(8,128)(2,1)S(1)} %all_to_all.5.a_ref, bf16[16,32,128]{2,1,0:T(8,128)(2,1)S(1)} %collective-permute-done.2.b_ref, ...), custom_call_target="tpu_custom_call" | custom-call | flops 1000000 | bytes 1000000 | tf_op jit(solution)/shard_map/cell/pallas_call | solution.py:24
  86.2 0.5 collective-permute-start.3
  86.7 0.9 collective-permute-done.3.got_ref
  87.5 27.2 %all-gather.1 = bf16[384,1024]{1,0:T(8,128)(2,1)S(1)} all-gather(bf16[24,1024]{1,0:T(8,128)(2,1)S(1)} %pair.1), channel_id=3, replica_groups={{0,2,4,6,8,10,12,14,16,18,20,22,24,26,28,30},{1,3,5,7,9,11,13,15,17,19,..., dimensions={0}, use_global_device_ids=true | all-gather | bytes 835584 | tf_op jit(solution)/shard_map/all_gather | solution.py:356
  114.8 7.3 %collective-permute-start.4 = (bf16[16,24,1024]{2,1,0:T(8,128)(2,1)S(1)}, bf16[16,24,1024]{2,1,0:T(8,128)(2,1)S(1)}, u32[]{:S(2)}, u32[]{:S(2)}) collective-permute-start(bf16[16,24,1024]{2,1,0:T(8,128)(2,1)S(1)} %bitcast.20), channel_id=1, source_target_pairs={{0,1},{1,0},{2,3},{3,2},{4,5},{5,4},{6,7},{7,6},{8,9},{9,8},{10,11... | collective-permute-start | bytes 2359304 | tf_op jit(solution)/shard_map/ppermute | solution.py:346
  122.1 0.0 slice-start.1
  122.1 1.9 %collective-permute-done.4.y_ref = bf16[16,24,1024]{2,1,0:T(8,128)(2,1)S(1)} collective-permute-done((bf16[16,24,1024]{2,1,0:T(8,128)(2,1)S(1)}, bf16[16,24,1024]{2,1,0:T(8,128)(2,1)S(1)}, u32[]{:S(2)}, u32[]{:S(2)}) %collective-permute-start.4) | collective-permute-done | bytes 786464 | tf_op jit(solution)/shard_map/ppermute | solution.py:346
  124.0 3.9 %branch.1 = (f32[384,1024]{1,0:T(8,128)S(1)}, bf16[384,1024]{1,0:T(8,128)(2,1)S(1)}) custom-call(bf16[16,24,1024]{2,1,0:T(8,128)(2,1)S(1)} %bitcast.21, bf16[16,24,1024]{2,1,0:T(8,128)(2,1)S(1)} %collective-permute-done.4.y_ref, bf16[16,32,128]{2,1,0:T(8,128)(2,1)S(1)} %all_to_all.5.a_ref, bf16[16,32,128]{2,1,0:T(8,128)(2,1)S(1)} %collective-permute-done.2.b_ref, ...), custom_call_target="tpu_custom_call" | custom-call | flops 1000000 | bytes 1000000 | tf_op jit(solution)/shard_map/branch/pallas_call | solution.py:24
  127.9 0.5 collective-permute-start.5
  128.4 1.9 %collective-permute-done.5 = bf16[384,1024]{1,0:T(8,128)(2,1)S(1)} collective-permute-done((bf16[384,1024]{1,0:T(8,128)(2,1)S(1)}, bf16[384,1024]{1,0:T(8,128)(2,1)S(1)}, u32[]{:S(2)}, u32[]{:S(2)}) %collective-permute-start.5) | collective-permute-done | bytes 786464 | tf_op jit(solution)/shard_map/ppermute | solution.py:346
  130.3 0.1 spread.1
  130.4 0.1 collective-permute-start.6
  130.6 2.6 %collective-permute-start.7 = (bf16[3,24,1024]{2,1,0:T(8,128)(2,1)S(1)}, bf16[3,24,1024]{2,1,0:T(8,128)(2,1)S(1)}, u32[]{:S(2)}, u32[]{:S(2)}) collective-permute-start(bf16[3,24,1024]{2,1,0:T(8,128)(2,1)S(1)} %get-tuple-element.40), channel_id=1, source_target_pairs={{0,30},{1,31},{2,0},{3,1},{4,2},{5,3},{6,4},{7,5},{8,6},{9,7},{10,... | collective-permute-start | bytes 442376 | tf_op jit(solution)/shard_map/ppermute | solution.py:352
  133.2 3.6 %collective-permute-start.9 = (bf16[3,24,1024]{2,1,0:T(8,128)(2,1)S(1)}, bf16[3,24,1024]{2,1,0:T(8,128)(2,1)S(1)}, u32[]{:S(2)}, u32[]{:S(2)}) collective-permute-start(bf16[3,24,1024]{2,1,0:T(8,128)(2,1)S(1)} %get-tuple-element.42), channel_id=1, source_target_pairs={{0,28},{1,29},{2,30},{3,31},{4,0},{5,1},{6,2},{7,3},{8,4},{9,5},{1... | collective-permute-start | bytes 442376 | tf_op jit(solution)/shard_map/ppermute | solution.py:352
  136.8 7.0 %update.1 = (f32[12,8,128,128]{3,2,1,0:T(8,128)}, f32[8,128]{1,0:T(8,128)S(1)}) custom-call(f32[12,8]{1,0:T(8,128)S(1)} %get-tuple-element.32.keep_ref, f32[8,16,128]{2,1,0:T(8,128)S(1)} %get-tuple-element.44.keys_ref, f32[128,128]{1,0:T(8,128)S(1)} %get-tuple-element.45.wvt_ref, bf16[24,1024]{1,0:T(8,128)(2,1)S(1)} %get-tuple-element.43.after_ref, ...), custom_call_target="tpu_custom_call" | custom-call | flops 500000000 | bytes 1000000 | tf_op jit(solution)/shard_map/update/pallas_call | solution.py:24
  143.8 1.5 collective-permute-done.10.last_ref
  145.3 0.1 fold.1
  145.4 1.5 collective-permute-start.11
  146.9 6.1 %collective-permute-start.12 = (bf16[24,1024]{1,0:T(8,128)(2,1)S(1)}, bf16[24,1024]{1,0:T(8,128)(2,1)S(1)}, u32[]{:S(2)}, u32[]{:S(2)}) collective-permute-start(bf16[24,1024]{1,0:T(8,128)(2,1)S(1)} %get-tuple-element.49), channel_id=1, source_target_pairs={{0,22},{1,23},{2,24},{3,25},{4,26},{5,27},{6,28},{7,29},{8,30},{9,... | collective-permute-start | bytes 147464 | tf_op jit(solution)/shard_map/ppermute | solution.py:352
  153.0 2.6 %collective-permute-done.11.a_ref = bf16[24,1024]{1,0:T(8,128)(2,1)S(1)} collective-permute-done((bf16[24,1024]{1,0:T(8,128)(2,1)S(1)}, bf16[24,1024]{1,0:T(8,128)(2,1)S(1)}, u32[]{:S(2)}, u32[]{:S(2)}) %collective-permute-start.11) | collective-permute-done | bytes 49184 | tf_op jit(solution)/shard_map/ppermute | solution.py:352
  155.7 3.9 %collective-permute-start.13 = (f32[12,1024]{1,0:T(8,128)S(1)}, f32[12,1024]{1,0:T(8,128)S(1)}, u32[]{:S(2)}, u32[]{:S(2)}) collective-permute-start(f32[12,1024]{1,0:T(8,128)S(1)} %get-tuple-element.51), channel_id=1, source_target_pairs={{0,1},{1,0},{2,3},{3,2},{4,5},{5,4},{6,7},{7,6},{8,9},{9,8},{10,11... | collective-permute-start | bytes 147464 | tf_op jit(solution)/shard_map/ppermute | solution.py:346
  159.6 0.9 collective-permute-done.13.got_ref
  160.5 0.7 final.1
  (43 shorter events, 0.2 us)
Async XLA Ops:
  0.6 11.1 %collective-permute-start = (bf16[12,2048]{1,0:T(8,128)(2,1)}, bf16[12,2048]{1,0:T(8,128)(2,1)S(1)}, u32[]{:S(2)}, u32[]{:S(2)}) collective-permute-start(bf16[12,2048]{1,0:T(8,128)(2,1)} %resid_ref.3), channel_id=1, source_target_pairs={{0,1},{1,0},{2,3},{3,2},{4,5},{5,4},{6,7},{7,6},{8,9},{9,8},{10,11... | collective-permute-start | bytes 147464 | tf_op jit(solution)/shard_map/ppermute | solution.py:346
  11.8 0.8 copy-start.6
  12.6 0.8 copy-start.9
  13.5 66.7 %copy-start.8 = (bf16[12,2048]{1,0:T(8,128)(2,1)S(1)}, bf16[12,2048]{1,0:T(8,128)(2,1)}, u32[]{:S(2)}) copy-start(bf16[12,2048]{1,0:T(8,128)(2,1)} %resid_ref.3) | copy-start | bytes 147460
  13.5 66.7 %copy-start.11 = (f32[4,2048]{1,0:T(4,128)S(1)}, f32[4,2048]{1,0:T(4,128)}, u32[]{:S(2)}) copy-start(f32[4,2048]{1,0:T(4,128)} %gains_ref.7) | copy-start | bytes 98308
  13.5 66.6 %copy-start.12 = (f32[12,8,128]{2,1,0:T(8,128)S(1)}, f32[12,8,128]{2,1,0:T(8,128)}, u32[]{:S(2)}) copy-start(f32[12,8,128]{2,1,0:T(8,128)} %norm_ref.1) | copy-start | bytes 147460
  41.0 18.0 %collective-permute-start.1 = (bf16[16,24,1024]{2,1,0:T(8,128)(2,1)S(1)}, bf16[16,24,1024]{2,1,0:T(8,128)(2,1)S(1)}, u32[]{:S(2)}, u32[]{:S(2)}) collective-permute-start(bf16[16,24,1024]{2,1,0:T(8,128)(2,1)S(1)} %bitcast.18), channel_id=1, source_target_pairs={{0,1},{1,0},{2,3},{3,2},{4,5},{5,4},{6,7},{7,6},{8,9},{9,8},{10,11... | collective-permute-start | bytes 2359304 | tf_op jit(solution)/shard_map/ppermute | solution.py:346
  52.2 0.8 copy-start.7
  53.0 0.8 copy-start.10
  53.8 0.8 copy-start.13
  54.5 0.8 copy-start.14
  55.3 0.7 copy-start.15
  56.0 0.7 copy-start.16
  56.6 0.7 copy-start.17
  77.3 2.9 %collective-permute-start.2 = (bf16[16,32,128]{2,1,0:T(8,128)(2,1)S(1)}, bf16[16,32,128]{2,1,0:T(8,128)(2,1)S(1)}, u32[]{:S(2)}, u32[]{:S(2)}) collective-permute-start(bf16[16,32,128]{2,1,0:T(8,128)(2,1)S(1)} %all_to_all.5.a_ref), channel_id=1, source_target_pairs={{0,1},{1,0},{2,3},{3,2},{4,5},{5,4},{6,7},{7,6},{8,9},{9,8},{10,11... | collective-permute-start | bytes 393224 | tf_op jit(solution)/shard_map/ppermute | solution.py:346
  80.2 41.9 %copy-start.18 = (bf16[2048]{0:T(1024)(128)(2,1)S(1)}, bf16[2048]{0:T(1024)(128)(2,1)}, u32[]{:S(2)}) copy-start(bf16[2048]{0:T(1024)(128)(2,1)} %param.45) | copy-start | bytes 12292
  80.2 43.8 %copy-start = (bf16[1,2048,512]{2,1,0:T(8,128)(2,1)S(1)}, bf16[1,2048,512]{2,1,0:T(8,128)(2,1)}, u32[]{:S(2)}) copy-start(bf16[1,2048,512]{2,1,0:T(8,128)(2,1)} %eg_ref.1) | copy-start | bytes 6291460
  80.2 43.8 %copy-start.1 = (bf16[1,2048,512]{2,1,0:T(8,128)(2,1)S(1)}, bf16[1,2048,512]{2,1,0:T(8,128)(2,1)}, u32[]{:S(2)}) copy-start(bf16[1,2048,512]{2,1,0:T(8,128)(2,1)} %eu_ref.1) | copy-start | bytes 6291460
  80.2 43.8 %copy-start.2 = (bf16[1,512,2048]{2,1,0:T(8,128)(2,1)S(1)}, bf16[1,512,2048]{2,1,0:T(8,128)(2,1)}, u32[]{:S(2)}) copy-start(bf16[1,512,2048]{2,1,0:T(8,128)(2,1)} %ed_ref.1) | copy-start | bytes 6291460
  80.2 43.8 %copy-start.3 = (bf16[2048,256]{1,0:T(8,128)(2,1)S(1)}, bf16[2048,256]{1,0:T(8,128)(2,1)}, u32[]{:S(2)}) copy-start(bf16[2048,256]{1,0:T(8,128)(2,1)} %dg_ref.1) | copy-start | bytes 3145732
  80.2 43.8 %copy-start.4 = (bf16[2048,256]{1,0:T(8,128)(2,1)S(1)}, bf16[2048,256]{1,0:T(8,128)(2,1)}, u32[]{:S(2)}) copy-start(bf16[2048,256]{1,0:T(8,128)(2,1)} %du_ref.1) | copy-start | bytes 3145732
  80.3 43.8 %copy-start.5 = (bf16[256,2048]{1,0:T(8,128)(2,1)S(1)}, bf16[256,2048]{1,0:T(8,128)(2,1)}, u32[]{:S(2)}) copy-start(bf16[256,2048]{1,0:T(8,128)(2,1)} %dd_ref.1) | copy-start | bytes 3145732
  86.2 1.3 collective-permute-start.3
  114.8 9.2 %collective-permute-start.4 = (bf16[16,24,1024]{2,1,0:T(8,128)(2,1)S(1)}, bf16[16,24,1024]{2,1,0:T(8,128)(2,1)S(1)}, u32[]{:S(2)}, u32[]{:S(2)}) collective-permute-start(bf16[16,24,1024]{2,1,0:T(8,128)(2,1)S(1)} %bitcast.20), channel_id=1, source_target_pairs={{0,1},{1,0},{2,3},{3,2},{4,5},{5,4},{6,7},{7,6},{8,9},{9,8},{10,11... | collective-permute-start | bytes 2359304 | tf_op jit(solution)/shard_map/ppermute | solution.py:346
  122.1 14.7 %slice-start = ((s8[6291456]{0:T(1024)(128)(4,1)}), s8[4194304]{0:T(1024)(128)(4,1)S(1)}, s32[]{:S(2)}) async-start(s8[6291456]{0:T(1024)(128)(4,1)} %bitcast.16), calls=%async_computation.1 | async-start | bytes 8388608
  122.1 14.7 %slice-start.1 = ((s8[6291456]{0:T(1024)(128)(4,1)}), s8[2097152]{0:T(1024)(128)(4,1)S(1)}, s32[]{:S(2)}) async-start(s8[6291456]{0:T(1024)(128)(4,1)} %bitcast.16), calls=%async_computation.2 | async-start | bytes 4194304
  127.9 2.4 %collective-permute-start.5 = (bf16[384,1024]{1,0:T(8,128)(2,1)S(1)}, bf16[384,1024]{1,0:T(8,128)(2,1)S(1)}, u32[]{:S(2)}, u32[]{:S(2)}) collective-permute-start(bf16[384,1024]{1,0:T(8,128)(2,1)S(1)} %get-tuple-element.37), channel_id=1, source_target_pairs={{0,1},{1,0},{2,3},{3,2},{4,5},{5,4},{6,7},{7,6},{8,9},{9,8},{10,11... | collective-permute-start | bytes 2359304 | tf_op jit(solution)/shard_map/ppermute | solution.py:346
  130.4 14.9 %collective-permute-start.6 = (bf16[3,24,1024]{2,1,0:T(8,128)(2,1)S(1)}, bf16[3,24,1024]{2,1,0:T(8,128)(2,1)S(1)}, u32[]{:S(2)}, u32[]{:S(2)}) collective-permute-start(bf16[3,24,1024]{2,1,0:T(8,128)(2,1)S(1)} %get-tuple-element.39), channel_id=1, source_target_pairs={{0,2},{1,3},{2,4},{3,5},{4,6},{5,7},{6,8},{7,9},{8,10},{9,11},{10,... | collective-permute-start | bytes 442376 | tf_op jit(solution)/shard_map/ppermute | solution.py:352
  130.6 14.8 %collective-permute-start.7 = (bf16[3,24,1024]{2,1,0:T(8,128)(2,1)S(1)}, bf16[3,24,1024]{2,1,0:T(8,128)(2,1)S(1)}, u32[]{:S(2)}, u32[]{:S(2)}) collective-permute-start(bf16[3,24,1024]{2,1,0:T(8,128)(2,1)S(1)} %get-tuple-element.40), channel_id=1, source_target_pairs={{0,30},{1,31},{2,0},{3,1},{4,2},{5,3},{6,4},{7,5},{8,6},{9,7},{10,... | collective-permute-start | bytes 442376 | tf_op jit(solution)/shard_map/ppermute | solution.py:352
  133.2 12.1 %collective-permute-start.8 = (bf16[3,24,1024]{2,1,0:T(8,128)(2,1)S(1)}, bf16[3,24,1024]{2,1,0:T(8,128)(2,1)S(1)}, u32[]{:S(2)}, u32[]{:S(2)}) collective-permute-start(bf16[3,24,1024]{2,1,0:T(8,128)(2,1)S(1)} %get-tuple-element.41), channel_id=1, source_target_pairs={{0,4},{1,5},{2,6},{3,7},{4,8},{5,9},{6,10},{7,11},{8,12},{9,13},{1... | collective-permute-start | bytes 442376 | tf_op jit(solution)/shard_map/ppermute | solution.py:352
  133.2 12.1 %collective-permute-start.9 = (bf16[3,24,1024]{2,1,0:T(8,128)(2,1)S(1)}, bf16[3,24,1024]{2,1,0:T(8,128)(2,1)S(1)}, u32[]{:S(2)}, u32[]{:S(2)}) collective-permute-start(bf16[3,24,1024]{2,1,0:T(8,128)(2,1)S(1)} %get-tuple-element.42), channel_id=1, source_target_pairs={{0,28},{1,29},{2,30},{3,31},{4,0},{5,1},{6,2},{7,3},{8,4},{9,5},{1... | collective-permute-start | bytes 442376 | tf_op jit(solution)/shard_map/ppermute | solution.py:352
  136.8 8.5 %collective-permute-start.10 = (bf16[24,1024]{1,0:T(8,128)(2,1)S(1)}, bf16[24,1024]{1,0:T(8,128)(2,1)S(1)}, u32[]{:S(2)}, u32[]{:S(2)}) collective-permute-start(bf16[24,1024]{1,0:T(8,128)(2,1)S(1)} %get-tuple-element.43.after_ref), channel_id=1, source_target_pairs={{0,6},{1,7},{2,8},{3,9},{4,10},{5,11},{6,12},{7,13},{8,14},{9,15},... | collective-permute-start | bytes 147464 | tf_op jit(solution)/shard_map/ppermute | solution.py:352
  145.4 10.2 %collective-permute-start.11 = (bf16[24,1024]{1,0:T(8,128)(2,1)S(1)}, bf16[24,1024]{1,0:T(8,128)(2,1)S(1)}, u32[]{:S(2)}, u32[]{:S(2)}) collective-permute-start(bf16[24,1024]{1,0:T(8,128)(2,1)S(1)} %get-tuple-element.48), channel_id=1, source_target_pairs={{0,10},{1,11},{2,12},{3,13},{4,14},{5,15},{6,16},{7,17},{8,18},{9,... | collective-permute-start | bytes 147464 | tf_op jit(solution)/shard_map/ppermute | solution.py:352
  146.9 8.8 %collective-permute-start.12 = (bf16[24,1024]{1,0:T(8,128)(2,1)S(1)}, bf16[24,1024]{1,0:T(8,128)(2,1)S(1)}, u32[]{:S(2)}, u32[]{:S(2)}) collective-permute-start(bf16[24,1024]{1,0:T(8,128)(2,1)S(1)} %get-tuple-element.49), channel_id=1, source_target_pairs={{0,22},{1,23},{2,24},{3,25},{4,26},{5,27},{6,28},{7,29},{8,30},{9,... | collective-permute-start | bytes 147464 | tf_op jit(solution)/shard_map/ppermute | solution.py:352
  155.7 4.8 %collective-permute-start.13 = (f32[12,1024]{1,0:T(8,128)S(1)}, f32[12,1024]{1,0:T(8,128)S(1)}, u32[]{:S(2)}, u32[]{:S(2)}) collective-permute-start(f32[12,1024]{1,0:T(8,128)S(1)} %get-tuple-element.51), channel_id=1, source_target_pairs={{0,1},{1,0},{2,3},{3,2},{4,5},{5,4},{6,7},{7,6},{8,9},{9,8},{10,11... | collective-permute-start | bytes 147464 | tf_op jit(solution)/shard_map/ppermute | solution.py:346

commit v3 on v2

v3 whole, which is shorter than its diff:
```python
import functools

import jax
import jax.numpy as jnp
from jax import lax
from jax.experimental import pallas as pl
from jax.experimental.pallas import tpu as pltpu
from jax.sharding import PartitionSpec as P

CAP = 2
INTERPRET = False
F32 = jnp.float32
BF16 = jnp.bfloat16


def in_hbm(x):
    return x if INTERPRET else pltpu.with_memory_space_constraint(x, pltpu.HBM)


def call(kernel, outs, args, scratch=(), vmem=16, flops=1000000, name=None, hbm=(), sems=0, held=(), **grid):
    if hbm:
        args = [in_hbm(x) if i in hbm else x for i, x in enumerate(args)]
        grid["in_specs"] = [
            pl.BlockSpec(memory_space=pltpu.HBM if i in hbm else pltpu.VMEM)
            for i in range(len(args))]
    result = pl.pallas_call(
        kernel,
        out_shape=[pltpu.VMEM(s, d) if i in held and not INTERPRET else jax.ShapeDtypeStruct(s, d)
                   for i, (s, d) in enumerate(outs)],
        scratch_shapes=[pltpu.VMEM(s, d) for s, d in scratch]
        + ([pltpu.SemaphoreType.DMA((sems,))] if sems else []),
        **grid,
        compiler_params=pltpu.CompilerParams(vmem_limit_bytes=vmem << 20),
        cost_estimate=pl.CostEstimate(flops=flops, bytes_accessed=1000000, transcendentals=0),
        interpret=INTERPRET,
        name=name,
    )(*args)
    return result


def rms(values, gains):
    return values * lax.rsqrt(jnp.mean(values * values, axis=-1, keepdims=True) + 1e-06) * gains


def core():
    return lax.rem(lax.axis_index("ep"), 2)


def dot_t(a, b):
    return lax.dot_general(a, b, (((1,), (1,)), ((), ())), preferred_element_type=F32)


def dot(a, b):
    return jnp.dot(a, b, preferred_element_type=F32)


def half_of(c, values):
    h = values.shape[-1] // 2
    return jnp.where(c == 0, values[:, :h], values[:, h:])


FAR = 5


def offsets(nz):
    ring = [0, -FAR, FAR]
    near = [n + o for n in (-1, 1, -2, 2) for o in ring]
    return [o % nz for o in ring + near + [-8]]


def own_kernel(resid_hbm, gains_hbm, out_ref, gains_ref, resid, sems):
    copies = [pltpu.make_async_copy(resid_hbm, resid, sems.at[0]),
              pltpu.make_async_copy(gains_hbm, gains_ref, sems.at[1])]
    for copy in copies:
        copy.start()
    for copy in copies:
        copy.wait()
    out_ref[...] = rms(resid[...].astype(F32), gains_ref[0:1, :]).astype(BF16)


def norm_kernel(own_ref, other_ref, gains_ref, out_ref, rows):
    c = core()
    r = own_ref.shape[0]
    own = half_of(c, own_ref[...].astype(F32))
    other = half_of(c, rms(other_ref[...].astype(F32), gains_ref[0:1, :]))
    rows[:r] = jnp.where(c == 0, own, other)
    rows[r : 2 * r] = jnp.where(c == 0, other, own)
    out_ref[...] = rows[...].astype(BF16)


def relay_kernel(x_ref, after_ref, out_ref):
    out_ref[...] = x_ref[...]


def stack_kernel(a_ref, b_ref, c_ref, after_ref, out_ref):
    out_ref[0] = a_ref[...]
    out_ref[1] = b_ref[...]
    out_ref[2] = c_ref[...]


def gates_kernel(
    normed_ref, wi_hbm, wf_hbm, bi_hbm, bf_hbm, max_hbm, routes_hbm, scores_hbm,
    wq_ref, wk_ref, wv_ref, wo_ref, state_ref, mix_ref,
    keep_ref, write_ref, newmax_ref, info_ref, weights_ref, state_out, mix_out,
    wi_ref, wf_ref, bi_ref, bf_ref, max_ref, routes_ref, scores_ref, turn_ref, info_scr, sems,
):
    heads, r = max_ref.shape
    cols = wq_ref.shape[0]
    small = [(wi_hbm, wi_ref), (wf_hbm, wf_ref), (max_hbm, max_ref), (routes_hbm, routes_ref),
             (scores_hbm, scores_ref), (bi_hbm, bi_ref), (bf_hbm, bf_ref)]
    small = [pltpu.make_async_copy(x, y, sems.at[k]) for k, (x, y) in enumerate(small)]
    copies = [
        pltpu.make_async_copy(w, weights_ref.at[pl.ds(k * cols, cols)], sems.at[7 + k])
        for k, w in enumerate((wq_ref, wk_ref, wv_ref, wo_ref))]
    copies.append(pltpu.make_async_copy(mix_ref, mix_out, sems.at[11]))
    for k in range(state_ref.shape[0]):
        copies.append(pltpu.make_async_copy(state_ref.at[k], state_out.at[k], sems.at[12 + k]))
    for copy in small + copies:
        copy.start()
    for copy in small:
        copy.wait()
    diagonal = lax.broadcasted_iota(jnp.int32, (heads, heads), 0) == lax.broadcasted_iota(
        jnp.int32, (heads, heads), 1)

    def column(bias):
        return jnp.sum(jnp.where(diagonal, bias, 0.0), axis=1, keepdims=True)

    normed = normed_ref[...]
    ipre = dot_t(wi_ref[...], normed) + column(bi_ref[...])
    fpre = dot_t(wf_ref[...], normed) + column(bf_ref[...])
    logf = jnp.minimum(fpre, 0.0) - jnp.log1p(jnp.exp(-jnp.abs(fpre)))
    decayed = logf + max_ref[...]
    new_max = jnp.maximum(ipre, decayed)
    newmax_ref[...] = new_max
    turn_ref[...] = jnp.zeros_like(turn_ref)
    turn_ref[0:heads, :r] = jnp.exp(decayed - new_max)
    keep_ref[...] = turn_ref[...].T[:r, :heads]
    turn_ref[0:heads, :r] = jnp.exp(ipre - new_max)
    write_ref[...] = turn_ref[...].T[:r, :heads]
    info_scr[...] = jnp.zeros_like(info_scr)
    info_scr[0:2, :r] = routes_ref[...].astype(F32)
    info_scr[2:4, :r] = scores_ref[...].astype(F32)
    info_ref[...] = info_scr[...].astype(BF16)
    for copy in copies:
        copy.wait()


def collect(refs, out):
    at = 0
    for ref in refs:
        size = 1
        for extent in ref.shape[:-1]:
            size *= extent
        out[at : at + size] = ref[...].reshape(size, ref.shape[-1])
        at += size


def proj_kernel(*refs):
    xs, ys, (w_ref, info_ref, out_ref, x, y) = refs[:6], refs[6:12], refs[12:]
    c = core()
    z = lax.div(lax.axis_index("ep"), 2)
    nz = out_ref.shape[0]
    h = x.shape[1]
    r2 = x.shape[0] // nz
    collect(xs, x)
    collect(ys, y)
    at = pl.ds(pl.multiple_of(c * h, h), h)
    to = pl.ds(pl.multiple_of((1 - c) * h, h), h)
    p = (dot_t(x[...], w_ref[:, at]) + dot_t(y[...], w_ref[:, to])).astype(BF16)
    for k, offset in enumerate(offsets(nz)):
        where = lax.rem(z + offset, nz)
        out_ref[where, :r2, :] = p[k * r2 : (k + 1) * r2]
        out_ref[k, r2 : r2 + 8, :] = info_ref[...]


def cell_kernel(
    a_ref, b_ref, keep_ref, write_ref, m_ref, norm_ref, mix_ref, resid_ref, gains_ref,
    middle_ref, mine_ref, send_ref, newnorm_ref, keys_ref, wvt_ref,
    p0, p1, q_scr, wv_scr, gated,
):
    c = core()
    r, heads, dh = norm_ref.shape
    nz = a_ref.shape[0]
    cols = heads * dh // (2 * nz)
    per = dh // cols
    p0[...] = jnp.zeros_like(p0)
    p1[...] = jnp.zeros_like(p1)
    for z in range(nz):
        a, b = a_ref[z].astype(F32), b_ref[z].astype(F32)
        a = jnp.where(c == 0, a[:r], a[r : 2 * r])
        b = jnp.where(c == 0, b[:r], b[r : 2 * r])
        p0[z, :r] = jnp.where(c == 0, a, b)
        p1[z, :r] = jnp.where(c == 0, b, a)
    lanes = lax.broadcasted_iota(jnp.int32, (16, dh), 1)

    def gather(h, kind):
        total = jnp.zeros((16, dh), F32)
        for p in range(per):
            ep = h * per + p
            piece = (p0 if ep % 2 == 0 else p1)[ep // 2]
            shift = ((p - kind) * cols) % dh
            piece = pltpu.roll(piece, shift, 1) if shift else piece
            total = jnp.where((lanes >= p * cols) & (lanes < (p + 1) * cols), piece, total)
        return total

    wv_scr[...] = jnp.zeros_like(wv_scr)
    for h in range(heads):
        q_scr[h] = gather(h, 0)
        keys_ref[h] = gather(h, 1) * dh ** (-0.5)
        wv_scr[h * 16 : h * 16 + r] = gather(h, 2)[:r] * write_ref[:, h : h + 1]
    wvt_ref[...] = wv_scr[...].T
    lane128 = lax.broadcasted_iota(jnp.int32, (dh, 128), 1)

    def step(s, acc):
        for h in range(heads):
            prod = m_ref[s, h] * q_scr[h, pl.ds(s, 1), :]
            red = jnp.sum(prod, axis=1, keepdims=True)
            acc = jnp.where(lane128 == h * 16 + s, red, acc)
        return acc

    numer = lax.fori_loop(0, r, step, jnp.zeros((dh, 128), F32)).T
    for h in range(heads):
        query, key = q_scr[h][:r], keys_ref[h][:r]
        outgate = gather(h, 3)[:r]
        keep, write = keep_ref[:, h : h + 1], write_ref[:, h : h + 1]
        new_norm = keep * norm_ref[:, h, :] + write * key
        newnorm_ref[:, h, :] = new_norm
        denom = jnp.sum(new_norm * query, axis=1, keepdims=True)
        kq = jnp.sum(key * query, axis=1, keepdims=True)
        top = keep * numer[h * 16 : h * 16 + r] + wv_scr[h * 16 : h * 16 + r] * kq
        cell = top / jnp.maximum(jnp.abs(denom), 1.0)
        gated[:, h * dh : (h + 1) * dh] = (jax.nn.sigmoid(outgate) * cell).astype(BF16)
    mixed = dot(gated[...], mix_ref[...])
    middle = resid_ref[...].astype(F32) + rms(mixed, gains_ref[1:2, :])
    middle_ref[...] = middle
    branch = rms(middle, gains_ref[2:3, :])
    mine_ref[...] = half_of(c, branch).astype(BF16)
    send_ref[...] = half_of(1 - c, branch).astype(BF16)


def update_kernel(keep_ref, keys_ref, wvt_ref, m_ref, out_ref, token_ref, new, sems):
    r, heads = m_ref.shape[:2]
    token_ref[...] = jnp.zeros_like(token_ref)

    def put(s):
        return pltpu.make_async_copy(new.at[s], out_ref.at[s], sems.at[s])

    def step(s, carry):
        rolled = pltpu.roll(wvt_ref[...], lax.rem(128 - s, 128), 1)
        for h in range(heads):
            keep = keep_ref[pl.ds(s, 1), h : h + 1]
            key = keys_ref[h, pl.ds(s, 1), :]
            new[s, h] = keep * m_ref[s, h] + rolled[:, h * 16 : h * 16 + 1] * key
        put(s).start()
        return carry

    lax.fori_loop(0, r, step, 0)
    for s in range(r):
        put(s).wait()


def pair_kernel(mine_ref, got_ref, out_ref, rows):
    c = core()
    r = mine_ref.shape[0]
    mine, got = mine_ref[...].astype(F32), got_ref[...].astype(F32)
    rows[:r] = jnp.where(c == 0, mine, got)
    rows[r : 2 * r] = jnp.where(c == 0, got, mine)
    out_ref[...] = rows[...].astype(BF16)


def silu_mul(gate, up):
    return (gate * jax.nn.sigmoid(gate) * up).astype(BF16)


def branch_kernel(*refs):
    xs, ys = refs[:6], refs[6:12]
    (a_ref, b_ref, eg_ref, eu_ref, ed_ref, dg_ref, du_ref, dd_ref, bw_ref,
     keep_ref, send_ref, table, made, x_scr, y_scr) = refs[12:]
    c = core()
    me = lax.axis_index("ep").astype(F32)
    home = lax.div(lax.axis_index("ep"), 2)
    nz = a_ref.shape[0]
    rows, h = x_scr.shape
    r2 = rows // nz
    r = r2 // 2
    slots = 2 * nz * CAP
    at = pl.ds(pl.multiple_of(c * h, h), h)
    to = pl.ds(pl.multiple_of((1 - c) * h, h), h)
    collect(xs, x_scr)
    collect(ys, y_scr)
    x, y = x_scr[...], y_scr[...]
    low = lax.broadcasted_iota(jnp.int32, (r2, 128), 0) < r
    for k, offset in enumerate(offsets(nz)):
        z = lax.rem(home + offset, nz)
        a, b = a_ref[z, r2 : r2 + 8, :].astype(F32), b_ref[z, r2 : r2 + 8, :].astype(F32)
        first, second = jnp.where(c == 0, a, b), jnp.where(c == 0, b, a)
        for j in range(4):
            table[j, k * r2 : (k + 1) * r2] = jnp.where(low, first[j : j + 1], second[j : j + 1])
    lane = lax.broadcasted_iota(jnp.int32, (rows, 128), 1)
    token = lax.broadcasted_iota(jnp.int32, (rows, 128), 0)
    block = lax.div(token, r)
    inner = token - block * r

    def column(k):
        return jnp.sum(jnp.where(lane == inner, table[k], 0.0), axis=1, keepdims=True)

    e0, e1, s0, s1 = column(0), column(1), column(2), column(3)
    hit0, hit1 = e0 == me, e1 == me
    hit = jnp.where(hit0 | hit1, 1.0, 0.0)
    weight = jnp.where(hit0, s0, jnp.where(hit1, s1, 0.0)) / (s0 + s1)
    row_i = lax.broadcasted_iota(jnp.int32, (rows, rows), 0)
    col_i = lax.broadcasted_iota(jnp.int32, (rows, rows), 1)
    earlier = (col_i < row_i) & (lax.div(row_i, r) == lax.div(col_i, r))
    earlier = jnp.where(earlier, 1.0, 0.0).astype(BF16)
    rank = dot(earlier, jnp.broadcast_to(hit, (rows, 128)).astype(BF16))
    slot = block.astype(F32) * CAP + rank
    chosen = jnp.where((slot == lane.astype(F32)) & (hit > 0.5), 1.0, 0.0)
    picker = chosen.T[:slots].astype(BF16)
    placer = chosen[:, :slots].astype(BF16)
    px = dot(picker, x).astype(BF16)
    py = dot(picker, y).astype(BF16)
    gate = dot(px, eg_ref[0, at, :]) + dot(py, eg_ref[0, to, :])
    up = dot(px, eu_ref[0, at, :]) + dot(py, eu_ref[0, to, :])
    made[...] = dot(silu_mul(gate, up), ed_ref[0]).astype(BF16)

    gate = dot(x, dg_ref[at, :]) + dot(y, dg_ref[to, :])
    up = dot(x, du_ref[at, :]) + dot(y, du_ref[to, :])
    hidden = silu_mul(gate, up)
    logit = jnp.sum(x.astype(F32) * bw_ref[:, at].astype(F32), axis=1, keepdims=True)
    logit = logit + jnp.sum(y.astype(F32) * bw_ref[:, to].astype(F32), axis=1, keepdims=True)
    sig = jax.nn.sigmoid(logit)
    for where, ref in ((at, keep_ref), (to, send_ref)):
        part = dot(hidden, dd_ref[:, where]) * sig
        part = part + dot(placer, made[:, where]) * weight
        ref[...] = part.astype(ref.dtype)


NEAR = (1, -1, 2, -2)


def spread_kernel(keep_ref, got_ref, *out_refs):
    own_ref, near_refs, last_ref = out_refs[0], out_refs[1:-1], out_refs[-1]
    nz = keep_ref.shape[0]
    order = offsets(nz)

    def term(offset):
        at = order.index(offset % nz)
        return keep_ref[at] + got_ref[at].astype(F32)

    for i, far in enumerate((0, FAR, -FAR)):
        own_ref[i] = term(far)
        for near, ref in zip(NEAR, near_refs):
            ref[i] = term(near + far).astype(BF16)
    last_ref[...] = term(8).astype(BF16)


def fold_kernel(
    own_ref, a_ref, b_ref, c_ref, d_ref, last_ref, own_out, plus_ref, minus_ref,
):
    def total(i):
        t = own_ref[i] + a_ref[i].astype(F32) + b_ref[i].astype(F32)
        return t + c_ref[i].astype(F32) + d_ref[i].astype(F32)

    own_out[...] = total(0)
    plus_ref[...] = (total(1) + last_ref[...].astype(F32)).astype(BF16)
    minus_ref[...] = total(2).astype(BF16)


def sum_kernel(own_ref, a_ref, b_ref, mine_ref, send_ref):
    c = core()
    r = mine_ref.shape[0]
    total = own_ref[...] + a_ref[...].astype(F32) + b_ref[...].astype(F32)
    mine_ref[...] = jnp.where(c == 0, total[:r], total[r:])
    send_ref[...] = jnp.where(c == 0, total[r:], total[:r])


def final_kernel(mine_ref, got_ref, middle_ref, gains_ref, out_ref):
    c = core()
    h = mine_ref.shape[1]
    mine, got = mine_ref[...], got_ref[...]
    low, high = jnp.where(c == 0, mine, got), jnp.where(c == 0, got, mine)
    square = jnp.sum(low * low, axis=1, keepdims=True) + jnp.sum(high * high, axis=1, keepdims=True)
    scale = lax.rsqrt(square / (2 * h) + 1e-06)
    gains = gains_ref[3:4, :]
    out_ref[:, :h] = (middle_ref[:, :h] + low * scale * gains[:, :h]).astype(BF16)
    out_ref[:, h:] = (middle_ref[:, h:] + high * scale * gains[:, h:]).astype(BF16)


def local(
    resid, norm_gains, w_query, w_key, w_value, w_outgate, w_igate, w_fgate, igate_bias,
    fgate_bias, state_matrix, state_norm, state_max, w_mix_out, routes, route_scores,
    expert_gate, expert_up, expert_down, dense_gate, dense_up, dense_down, branch_weight,
):
    n = lax.axis_size("ep")
    nz = n // 2
    r, d = resid.shape
    h = d // 2
    heads, dh = state_matrix.shape[1:3]
    inner = heads * dh
    groups = [[2 * z + c for z in range(nz)] for c in range(2)]
    pairs = [(i, i ^ 1) for i in range(n)]

    def swap(x):
        return lax.ppermute(x, "ep", pairs)

    def exchange(x):
        return lax.all_to_all(x, "ep", 0, 0, axis_index_groups=groups)

    def shift(x, offset):
        return lax.ppermute(
            x, "ep", [(2 * z + c, 2 * ((z + offset) % nz) + c) for z in range(nz) for c in range(2)])

    tile = (2 * r, h)

    def gather(own, after):
        plus, minus = shift(own, FAR), shift(own, -FAR)
        ring, = call(stack_kernel, [((3,) + tile, BF16)], (own, plus, minus, after), name="stack")
        last = shift(plus, 8 - FAR)
        up, down = shift(ring, 1), shift(ring, -1)
        relay, = call(relay_kernel, [((3,) + tile, BF16)], (up, last), name="relay")
        pieces = (ring, up, down, shift(relay, 1), shift(down, -1), last)
        return pieces, [swap(piece) for piece in pieces]

    other = swap(resid)
    normed, gains = call(
        own_kernel, [((r, d), BF16), (norm_gains.shape, F32)], (resid, norm_gains),
        scratch=[((r, d), BF16)], hbm=(0, 1), sems=2, name="own")
    keep, write, new_max, info, w_all, state, mix = call(
        gates_kernel,
        [((r, heads), F32), ((r, heads), F32), ((heads, r), F32), ((8, 128), BF16),
         ((4 * inner // n, d), BF16), (state_matrix.shape, F32), (w_mix_out.shape, BF16)],
        (normed, w_igate.T, w_fgate.T, igate_bias.reshape(1, heads),
         fgate_bias.reshape(1, heads), state_max.T, routes.T, route_scores.T,
         w_query.T, w_key.T, w_value.T, w_outgate.T, state_matrix, w_mix_out),
        scratch=[((heads, d), BF16), ((heads, d), BF16), ((1, heads), F32), ((1, heads), F32),
                 ((heads, r), F32), ((2, r), jnp.int32),
                 ((2, r), BF16), ((128, 128), F32), ((8, 128), F32)],
        hbm=tuple(range(1, 14)), sems=12 + r, held=(4, 5, 6), name="gates")
    chunk, = call(norm_kernel, [(tile, BF16)], (normed, other, gains),
                  scratch=[(tile, F32)], name="norm")
    xs, ys = gather(chunk, info)
    projected, = call(
        proj_kernel, [((nz, 2 * r + 8, 4 * inner // n), BF16)],
        (*xs, *ys, w_all, info), scratch=[((n * r, h), BF16)] * 2, name="proj")
    a = exchange(projected)
    b = swap(a)
    middle, mine, send, new_norm, keys, wvt = call(
        cell_kernel,
        [((r, d), F32), ((r, h), BF16), ((r, h), BF16), ((r, heads, dh), F32),
         ((heads, 16, dh), F32), ((dh, 128), F32)],
        (a, b, keep, write, state, state_norm, mix, resid, gains),
        scratch=[((nz, 16, dh), F32), ((nz, 16, dh), F32), ((heads, 16, dh), F32),
                 ((128, dh), F32), ((r, inner), BF16)], name="cell")
    got = swap(send)
    chunk, = call(pair_kernel, [((2 * r, h), BF16)], (mine, got),
                  scratch=[((2 * r, h), F32)], name="pair")
    new_matrix, token = call(
        update_kernel, [(state_matrix.shape, F32), ((8, 128), F32)], (keep, keys, wvt, state),
        scratch=[(state_matrix.shape, F32)], sems=r, name="update",
        out_specs=[pl.BlockSpec(memory_space=pltpu.HBM), pl.BlockSpec(memory_space=pltpu.VMEM)])
    xs, ys = gather(chunk, token)
    part, send = call(
        branch_kernel, [((n * r, h), F32), ((n * r, h), BF16)],
        (*xs, *ys, a, b, expert_gate, expert_up, expert_down, dense_gate, dense_up, dense_down,
         branch_weight.reshape(1, d)),
        scratch=[((4, n * r, 128), F32), ((n * CAP, d), BF16), ((n * r, h), BF16),
                 ((n * r, h), BF16)], vmem=32, name="branch")
    got = swap(send)
    own, *near, last = call(
        spread_kernel, [((3,) + tile, F32)] + [((3,) + tile, BF16)] * 4 + [(tile, BF16)],
        (part.reshape((nz,) + tile), got.reshape((nz,) + tile)), name="spread")
    near = [shift(x, offset) for x, offset in zip(near, NEAR)]
    last = shift(last, 8 - FAR)
    own, plus, minus = call(fold_kernel, [(tile, F32), (tile, BF16), (tile, BF16)],
                            (own, *near, last), name="fold")
    plus, minus = shift(plus, FAR), shift(minus, -FAR)
    mine, send = call(sum_kernel, [((r, h), F32), ((r, h), F32)], (own, plus, minus), name="sum")
    got = swap(send)
    out, = call(final_kernel, [((r, d), BF16)], (mine, got, middle, gains), name="final")
    return (out, new_matrix, new_norm, new_max.T)


def solution(mesh):
    placed = (
        P(("grp", "ep"), None), P(), P(None, "ep"), P(None, "ep"), P(None, "ep"), P(None, "ep"),
        P(), P(), P(), P(), P(("grp", "ep"), None, None, None), P(("grp", "ep"), None, None),
        P(("grp", "ep"), None), P(), P(("grp", "ep"), None), P(("grp", "ep"), None),
        P("ep", None, None), P("ep", None, None), P("ep", None, None), P(None, "ep"),
        P(None, "ep"), P("ep", None), P(),
    )
    return jax.shard_map(
        local,
        mesh=mesh,
        in_specs=placed,
        out_specs=(
            P(("grp", "ep"), None),
            P(("grp", "ep"), None, None, None),
            P(("grp", "ep"), None, None),
            P(("grp", "ep"), None),
        ),
        check_vma=False,
    )
```

time: 162 us -> 151 us (0.932)
  blocking collectives: 72.3 us -> 22.6 us
  starting transfers between devices: 45.4 us -> 72.7 us
  waiting for transfers between devices: 11.8 us -> 34.1 us
  local copies, waits for them, and re-layouts: 10.5 us -> 0.04 us
    all_gather x2 -> x0, blocking collectives: 54.7 us -> none  [gather(): return lax.all_gather(x, 'ep', axis=0, axis_index_groups=groups)]
    ppermute x7 -> x21, starting transfers between devices: 13.9 us -> 45.6 us  [shift(): lax.ppermute(x, 'ep', [(2 * z + c, 2 * ((z + offset) % nz) + c) for z in...]
    ppermute x7 -> x21, waiting for transfers between devices: 4.17 us -> 25.9 us  [shift(): lax.ppermute(x, 'ep', [(2 * z + c, 2 * ((z + offset) % nz) + c) for z in...]
    unnamed x45 -> x18, local copies, waits for them, and re-layouts: 9.05 us -> 0.04 us
    all_to_all x1, blocking collectives: 17.6 us -> 22.6 us  [exchange(): return lax.all_to_all(x, 'ep', 0, 0, axis_index_groups=groups)]
    ppermute x7 -> x17, starting transfers between devices: 31.5 us -> 27.2 us  [swap(): return lax.ppermute(x, 'ep', pairs)]
    pallas_call x11 -> x16, Pallas kernels: 20.3 us -> 20.9 us  [call(): pl.pallas_call(kernel, out_shape=[pltpu.VMEM(s, d) if i in held and (not...]
    ppermute x7 -> x17, waiting for transfers between devices: 7.66 us -> 8.17 us  [swap(): return lax.ppermute(x, 'ep', pairs)]
  transfers between devices with their start and end apart: 14 -> 38, of which waited for: 8 -> 20; matrix products, arithmetic and copies ran while one was open for 2% -> 0% of each run, Pallas kernels for 5% -> 7%
where the time goes in v3:
time: 151 us
  starting transfers between devices  72.7 us (48%)
  waiting for transfers between devices  34.1 us (23%)
  blocking collectives  22.6 us (15%)
  Pallas kernels  20.9 us (14%)
    ppermute x21, starting transfers between devices, shift(): lax.ppermute(x, 'ep', [(2 * z + c, 2 * ((z + offset) % nz) + c) for z in...  45.6 us
    ppermute x17, starting transfers between devices, swap(): return lax.ppermute(x, 'ep', pairs)  27.2 us
    ppermute x21, waiting for transfers between devices, shift(): lax.ppermute(x, 'ep', [(2 * z + c, 2 * ((z + offset) % nz) + c) for z in...  25.9 us
    all_to_all x1, blocking collectives, exchange(): return lax.all_to_all(x, 'ep', 0, 0, axis_index_groups=groups)  22.6 us
    pallas_call x16, Pallas kernels, call(): pl.pallas_call(kernel, out_shape=[pltpu.VMEM(s, d) if i in held and (not...  20.9 us
    ppermute x17, waiting for transfers between devices, swap(): return lax.ppermute(x, 'ep', pairs)  8.17 us
  transfers between devices with their start and end apart: 38, of which 20 were waited for; matrix products, arithmetic and copies ran while one was open for 0% of the time, Pallas kernels for 7%

profile of v3, /device:TPU:69, one launch (start us, length us, event | category | flops | bytes accessed | tf_op | source)
XLA Modules:
  0.0 151.2 jit_solution(10848337890280149645)
XLA Ops:
  0.6 10.0 %collective-permute-start = (bf16[12,2048]{1,0:T(8,128)(2,1)}, bf16[12,2048]{1,0:T(8,128)(2,1)S(1)}, u32[]{:S(2)}, u32[]{:S(2)}) collective-permute-start(bf16[12,2048]{1,0:T(8,128)(2,1)} %resid_ref.1), channel_id=1, source_target_pairs={{0,1},{1,0},{2,3},{3,2},{4,5},{5,4},{6,7},{7,6},{8,9},{9,8},{10,11... | collective-permute-start | bytes 147464 | tf_op jit(solution)/shard_map/ppermute | solution.py:404
  10.6 1.0 own.1
  11.9 0.9 collective-permute-start.1
  12.8 6.7 %collective-permute-start.2 = (bf16[24,1024]{1,0:T(8,128)(2,1)S(1)}, bf16[24,1024]{1,0:T(8,128)(2,1)S(1)}, u32[]{:S(2)}, u32[]{:S(2)}) collective-permute-start(bf16[24,1024]{1,0:T(8,128)(2,1)S(1)} %norm.1.a_ref), channel_id=1, source_target_pairs={{0,22},{1,23},{2,24},{3,25},{4,26},{5,27},{6,28},{7,29},{8,30},{9,... | collective-permute-start | bytes 147464 | tf_op jit(solution)/shard_map/ppermute | solution.py:410
  19.5 5.1 %gates.1 = (f32[12,8]{1,0:T(8,128)S(1)}, f32[12,8]{1,0:T(8,128)S(1)}, f32[8,12]{1,0:T(8,128)}, bf16[8,128]{1,0:T(8,128)(2,1)S(1)}, bf16[128,2048]{1,0:T(8,128)(2...) custom-call(bf16[12,2048]{1,0:T(8,128)(2,1)S(1)} %get-tuple-element.34.own_ref.normed_ref, ...), custom_call_target="tpu_custom_call" | custom-call | flops 1000000 | bytes 1000000 | tf_op jit(solution)/shard_map/gates/pallas_call | solution.py:26
  24.8 3.6 %collective-permute-start.4 = (bf16[3,24,1024]{2,1,0:T(8,128)(2,1)S(1)}, bf16[3,24,1024]{2,1,0:T(8,128)(2,1)S(1)}, u32[]{:S(2)}, u32[]{:S(2)}) collective-permute-start(bf16[3,24,1024]{2,1,0:T(8,128)(2,1)S(1)} %stack.2.refs_0_), channel_id=1, source_target_pairs={{0,30},{1,31},{2,0},{3,1},{4,2},{5,3},{6,4},{7,5},{8,6},{9,7},{10,... | collective-permute-start | bytes 442376 | tf_op jit(solution)/shard_map/ppermute | solution.py:410
  28.4 4.3 %collective-permute-start.5 = (bf16[24,1024]{1,0:T(8,128)(2,1)S(1)}, bf16[24,1024]{1,0:T(8,128)(2,1)S(1)}, u32[]{:S(2)}, u32[]{:S(2)}) collective-permute-start(bf16[24,1024]{1,0:T(8,128)(2,1)S(1)} %collective-permute-done.1.b_ref), channel_id=1, source_target_pairs={{0,6},{1,7},{2,8},{3,9},{4,10},{5,11},{6,12},{7,13},{8,14},{9,15},... | collective-permute-start | bytes 147464 | tf_op jit(solution)/shard_map/ppermute | solution.py:410
  32.7 3.6 %collective-permute-done.5.after_ref.refs_5_ = bf16[24,1024]{1,0:T(8,128)(2,1)S(1)} collective-permute-done((bf16[24,1024]{1,0:T(8,128)(2,1)S(1)}, bf16[24,1024]{1,0:T(8,128)(2,1)S(1)}, u32[]{:S(2)}, u32[]{:S(2)}) %collective-permute-start.5) | collective-permute-done | bytes 49184 | tf_op jit(solution)/shard_map/ppermute | solution.py:410
  36.5 2.6 %collective-permute-start.7 = (bf16[3,24,1024]{2,1,0:T(8,128)(2,1)S(1)}, bf16[3,24,1024]{2,1,0:T(8,128)(2,1)S(1)}, u32[]{:S(2)}, u32[]{:S(2)}) collective-permute-start(bf16[3,24,1024]{2,1,0:T(8,128)(2,1)S(1)} %collective-permute-done.4.refs_2_), channel_id=1, source_target_pairs={{0,30},{1,31},{2,0},{3,1},{4,2},{5,3},{6,4},{7,5},{8,6},{9,7},{10,... | collective-permute-start | bytes 442376 | tf_op jit(solution)/shard_map/ppermute | solution.py:410
  39.1 1.4 collective-permute-start.13
  40.6 0.5 collective-permute-start.10
  41.1 0.4 collective-permute-done.13.refs_11_
  41.8 0.4 collective-permute-done.6.refs_3_
  42.2 1.7 %collective-permute-start.11 = (bf16[3,24,1024]{2,1,0:T(8,128)(2,1)S(1)}, bf16[3,24,1024]{2,1,0:T(8,128)(2,1)S(1)}, u32[]{:S(2)}, u32[]{:S(2)}) collective-permute-start(bf16[3,24,1024]{2,1,0:T(8,128)(2,1)S(1)} %collective-permute-done.6.refs_3_), channel_id=1, source_target_pairs={{0,1},{1,0},{2,3},{3,2},{4,5},{5,4},{6,7},{7,6},{8,9},{9,8},{10,11... | collective-permute-start | bytes 442376 | tf_op jit(solution)/shard_map/ppermute | solution.py:404
  44.2 0.8 collective-permute-done.11.refs_9_
  45.3 0.6 proj.1
  45.9 22.6 %all_to_all.5.a_ref.refs_12_ = bf16[16,32,128]{2,1,0:T(8,128)(2,1)S(1)} all-to-all(bf16[16,32,128]{2,1,0:T(8,128)(2,1)S(1)} %proj.1), channel_id=1, replica_groups={{0,2,4,6,8,10,12,14,16,18,20,22,24,26,28,30},{1,3,5,7,9,11,13,15,17,19,..., dimensions={0} | all-to-all | bytes 262144 | tf_op jit(solution)/shard_map/all_to_all | solution.py:407
  68.5 3.3 %collective-permute-start.14 = (bf16[16,32,128]{2,1,0:T(8,128)(2,1)S(1)}, bf16[16,32,128]{2,1,0:T(8,128)(2,1)S(1)}, u32[]{:S(2)}, u32[]{:S(2)}) collective-permute-start(bf16[16,32,128]{2,1,0:T(8,128)(2,1)S(1)} %all_to_all.5.a_ref.refs_12_), channel_id=1, source_target_pairs={{0,1},{1,0},{2,3},{3,2},{4,5},{5,4},{6,7},{7,6},{8,9},{9,8},{10,11... | collective-permute-start | bytes 393224 | tf_op jit(solution)/shard_map/ppermute | solution.py:404
  71.7 1.0 collective-permute-done.14.b_ref.refs_13_
  72.7 4.5 %cell.1 = (f32[12,2048]{1,0:T(8,128)S(1)}, bf16[12,1024]{1,0:T(8,128)(2,1)S(1)}, bf16[12,1024]{1,0:T(8,128)(2,1)S(1)}, f32[12,8,128]{2,1,0:T(8,128)}, f32[8,16,128]{2,1,0:T(8,128)S(1)}, /*index=5*/f32[128,128]{1,0:T(8,128)S(1)}) custom-call(bf16[16,32,128]{2,1,0:T(8,128)(2,1)S(1)} %all_to_all.5.a_ref.refs_12_, ...), custom_call_target="tpu_custom_call" | custom-call | flops 1000000 | bytes 1000000 | tf_op jit(solution)/shard_map/cell/pallas_call | solution.py:26
  77.3 0.5 collective-permute-start.15
  77.7 0.9 collective-permute-done.15.got_ref
  78.6 2.4 %collective-permute-start.16 = (bf16[24,1024]{1,0:T(8,128)(2,1)S(1)}, bf16[24,1024]{1,0:T(8,128)(2,1)S(1)}, u32[]{:S(2)}, u32[]{:S(2)}) collective-permute-start(bf16[24,1024]{1,0:T(8,128)(2,1)S(1)} %pair.1.a_ref), channel_id=1, source_target_pairs={{0,10},{1,11},{2,12},{3,13},{4,14},{5,15},{6,16},{7,17},{8,18},{9,... | collective-permute-start | bytes 147464 | tf_op jit(solution)/shard_map/ppermute | solution.py:410
  81.0 5.2 %collective-permute-start.17 = (bf16[24,1024]{1,0:T(8,128)(2,1)S(1)}, bf16[24,1024]{1,0:T(8,128)(2,1)S(1)}, u32[]{:S(2)}, u32[]{:S(2)}) collective-permute-start(bf16[24,1024]{1,0:T(8,128)(2,1)S(1)} %pair.1.a_ref), channel_id=1, source_target_pairs={{0,22},{1,23},{2,24},{3,25},{4,26},{5,27},{6,28},{7,29},{8,30},{9,... | collective-permute-start | bytes 147464 | tf_op jit(solution)/shard_map/ppermute | solution.py:410
  86.2 4.7 %update.1 = (f32[12,8,128,128]{3,2,1,0:T(8,128)}, f32[8,128]{1,0:T(8,128)S(1)}) custom-call(f32[12,8]{1,0:T(8,128)S(1)} %get-tuple-element.38.keep_ref, f32[8,16,128]{2,1,0:T(8,128)S(1)} %get-tuple-element.44.keys_ref, f32[128,128]{1,0:T(8,128)S(1)} %get-tuple-element.45.wvt_ref, f32[12,8,128,128]{3,2,1,0:T(8,128)S(1)} %get-tuple-element.40.m_ref), custom_call_target="tpu_custom_call" | custom-call | flops 1000000 | bytes 1000000 | tf_op jit(solution)/shard_map/update/pallas_call | solution.py:26
  90.9 0.8 collective-permute-done.16.b_ref
  92.2 2.7 %collective-permute-start.19 = (bf16[3,24,1024]{2,1,0:T(8,128)(2,1)S(1)}, bf16[3,24,1024]{2,1,0:T(8,128)(2,1)S(1)}, u32[]{:S(2)}, u32[]{:S(2)}) collective-permute-start(bf16[3,24,1024]{2,1,0:T(8,128)(2,1)S(1)} %stack.3.refs_0_), channel_id=1, source_target_pairs={{0,30},{1,31},{2,0},{3,1},{4,2},{5,3},{6,4},{7,5},{8,6},{9,7},{10,... | collective-permute-start | bytes 442376 | tf_op jit(solution)/shard_map/ppermute | solution.py:410
  94.9 7.3 %collective-permute-done.20.after_ref.refs_5_ = bf16[24,1024]{1,0:T(8,128)(2,1)S(1)} collective-permute-done((bf16[24,1024]{1,0:T(8,128)(2,1)S(1)}, bf16[24,1024]{1,0:T(8,128)(2,1)S(1)}, u32[]{:S(2)}, u32[]{:S(2)}) %collective-permute-start.20) | collective-permute-done | bytes 49184 | tf_op jit(solution)/shard_map/ppermute | solution.py:410
  102.4 2.6 %collective-permute-start.22 = (bf16[3,24,1024]{2,1,0:T(8,128)(2,1)S(1)}, bf16[3,24,1024]{2,1,0:T(8,128)(2,1)S(1)}, u32[]{:S(2)}, u32[]{:S(2)}) collective-permute-start(bf16[3,24,1024]{2,1,0:T(8,128)(2,1)S(1)} %collective-permute-done.19.refs_2_), channel_id=1, source_target_pairs={{0,30},{1,31},{2,0},{3,1},{4,2},{5,3},{6,4},{7,5},{8,6},{9,7},{10,... | collective-permute-start | bytes 442376 | tf_op jit(solution)/shard_map/ppermute | solution.py:410
  105.0 1.8 %collective-permute-start.28 = (bf16[24,1024]{1,0:T(8,128)(2,1)S(1)}, bf16[24,1024]{1,0:T(8,128)(2,1)S(1)}, u32[]{:S(2)}, u32[]{:S(2)}) collective-permute-start(bf16[24,1024]{1,0:T(8,128)(2,1)S(1)} %collective-permute-done.20.after_ref.refs_5_), channel_id=1, source_target_pairs={{0,1},{1,0},{2,3},{3,2},{4,5},{5,4},{6,7},{7,6},{8,9},{9,8},{10,11... | collective-permute-start | bytes 147464 | tf_op jit(solution)/shard_map/ppermute | solution.py:404
  106.8 0.5 collective-permute-start.24
  107.3 0.4 collective-permute-done.28.refs_11_
  108.1 1.9 %collective-permute-start.26 = (bf16[3,24,1024]{2,1,0:T(8,128)(2,1)S(1)}, bf16[3,24,1024]{2,1,0:T(8,128)(2,1)S(1)}, u32[]{:S(2)}, u32[]{:S(2)}) collective-permute-start(bf16[3,24,1024]{2,1,0:T(8,128)(2,1)S(1)} %collective-permute-done.21.refs_3_), channel_id=1, source_target_pairs={{0,1},{1,0},{2,3},{3,2},{4,5},{5,4},{6,7},{7,6},{8,9},{9,8},{10,11... | collective-permute-start | bytes 442376 | tf_op jit(solution)/shard_map/ppermute | solution.py:404
  110.0 0.9 collective-permute-done.26.refs_9_
  111.3 3.8 %branch.1 = (f32[384,1024]{1,0:T(8,128)S(1)}, bf16[384,1024]{1,0:T(8,128)(2,1)S(1)}) custom-call(bf16[3,24,1024]{2,1,0:T(8,128)(2,1)S(1)} %stack.3.refs_0_, bf16[3,24,1024]{2,1,0:T(8,128)(2,1)S(1)} %collective-permute-done.18.x_ref.refs_1_, bf16[3,24,1024]{2,1,0:T(8,128)(2,1)S(1)} %collective-permute-done.19.refs_2_, ...), custom_call_target="tpu_custom_call" | custom-call | flops 1000000 | bytes 1000000 | tf_op jit(solution)/shard_map/branch/pallas_call | solution.py:26
  115.5 2.1 %collective-permute-done.29 = bf16[384,1024]{1,0:T(8,128)(2,1)S(1)} collective-permute-done((bf16[384,1024]{1,0:T(8,128)(2,1)S(1)}, bf16[384,1024]{1,0:T(8,128)(2,1)S(1)}, u32[]{:S(2)}, u32[]{:S(2)}) %collective-permute-start.29) | collective-permute-done | bytes 786464 | tf_op jit(solution)/shard_map/ppermute | solution.py:404
  117.8 1.4 collective-permute-start.30
  119.2 1.4 collective-permute-start.31
  120.7 3.5 %collective-permute-start.33 = (bf16[3,24,1024]{2,1,0:T(8,128)(2,1)S(1)}, bf16[3,24,1024]{2,1,0:T(8,128)(2,1)S(1)}, u32[]{:S(2)}, u32[]{:S(2)}) collective-permute-start(bf16[3,24,1024]{2,1,0:T(8,128)(2,1)S(1)} %get-tuple-element.53), channel_id=1, source_target_pairs={{0,28},{1,29},{2,30},{3,31},{4,0},{5,1},{6,2},{7,3},{8,4},{9,5},{1... | collective-permute-start | bytes 442376 | tf_op jit(solution)/shard_map/ppermute | solution.py:410
  124.2 7.4 %collective-permute-done.34.last_ref = bf16[24,1024]{1,0:T(8,128)(2,1)S(1)} collective-permute-done((bf16[24,1024]{1,0:T(8,128)(2,1)S(1)}, bf16[24,1024]{1,0:T(8,128)(2,1)S(1)}, u32[]{:S(2)}, u32[]{:S(2)}) %collective-permute-start.34) | collective-permute-done | bytes 49184 | tf_op jit(solution)/shard_map/ppermute | solution.py:410
  131.6 1.0 collective-permute-done.32.c_ref
  132.6 4.6 %collective-permute-start.35 = (bf16[24,1024]{1,0:T(8,128)(2,1)S(1)}, bf16[24,1024]{1,0:T(8,128)(2,1)S(1)}, u32[]{:S(2)}, u32[]{:S(2)}) collective-permute-start(bf16[24,1024]{1,0:T(8,128)(2,1)S(1)} %get-tuple-element.56), channel_id=1, source_target_pairs={{0,10},{1,11},{2,12},{3,13},{4,14},{5,15},{6,16},{7,17},{8,18},{9,... | collective-permute-start | bytes 147464 | tf_op jit(solution)/shard_map/ppermute | solution.py:410
  137.3 3.0 %collective-permute-start.36 = (bf16[24,1024]{1,0:T(8,128)(2,1)S(1)}, bf16[24,1024]{1,0:T(8,128)(2,1)S(1)}, u32[]{:S(2)}, u32[]{:S(2)}) collective-permute-start(bf16[24,1024]{1,0:T(8,128)(2,1)S(1)} %get-tuple-element.57), channel_id=1, source_target_pairs={{0,22},{1,23},{2,24},{3,25},{4,26},{5,27},{6,28},{7,29},{8,30},{9,... | collective-permute-start | bytes 147464 | tf_op jit(solution)/shard_map/ppermute | solution.py:410
  140.2 1.7 %collective-permute-done.35.a_ref = bf16[24,1024]{1,0:T(8,128)(2,1)S(1)} collective-permute-done((bf16[24,1024]{1,0:T(8,128)(2,1)S(1)}, bf16[24,1024]{1,0:T(8,128)(2,1)S(1)}, u32[]{:S(2)}, u32[]{:S(2)}) %collective-permute-start.35) | collective-permute-done | bytes 49184 | tf_op jit(solution)/shard_map/ppermute | solution.py:410
  141.9 3.3 %collective-permute-done.36.b_ref = bf16[24,1024]{1,0:T(8,128)(2,1)S(1)} collective-permute-done((bf16[24,1024]{1,0:T(8,128)(2,1)S(1)}, bf16[24,1024]{1,0:T(8,128)(2,1)S(1)}, u32[]{:S(2)}, u32[]{:S(2)}) %collective-permute-start.36) | collective-permute-done | bytes 49184 | tf_op jit(solution)/shard_map/ppermute | solution.py:410
  145.3 4.3 %collective-permute-start.37 = (f32[12,1024]{1,0:T(8,128)S(1)}, f32[12,1024]{1,0:T(8,128)S(1)}, u32[]{:S(2)}, u32[]{:S(2)}) collective-permute-start(f32[12,1024]{1,0:T(8,128)S(1)} %get-tuple-element.59), channel_id=1, source_target_pairs={{0,1},{1,0},{2,3},{3,2},{4,5},{5,4},{6,7},{7,6},{8,9},{9,8},{10,11... | collective-permute-start | bytes 147464 | tf_op jit(solution)/shard_map/ppermute | solution.py:404
  149.6 0.9 collective-permute-done.37.got_ref
  150.5 0.7 final.1
  (64 shorter events, 3.6 us)
Async XLA Ops:
  0.6 11.1 %collective-permute-start = (bf16[12,2048]{1,0:T(8,128)(2,1)}, bf16[12,2048]{1,0:T(8,128)(2,1)S(1)}, u32[]{:S(2)}, u32[]{:S(2)}) collective-permute-start(bf16[12,2048]{1,0:T(8,128)(2,1)} %resid_ref.1), channel_id=1, source_target_pairs={{0,1},{1,0},{2,3},{3,2},{4,5},{5,4},{6,7},{7,6},{8,9},{9,8},{10,11... | collective-permute-start | bytes 147464 | tf_op jit(solution)/shard_map/ppermute | solution.py:404
  11.9 12.7 %collective-permute-start.1 = (bf16[24,1024]{1,0:T(8,128)(2,1)S(1)}, bf16[24,1024]{1,0:T(8,128)(2,1)S(1)}, u32[]{:S(2)}, u32[]{:S(2)}) collective-permute-start(bf16[24,1024]{1,0:T(8,128)(2,1)S(1)} %norm.1.a_ref), channel_id=1, source_target_pairs={{0,10},{1,11},{2,12},{3,13},{4,14},{5,15},{6,16},{7,17},{8,18},{9,... | collective-permute-start | bytes 147464 | tf_op jit(solution)/shard_map/ppermute | solution.py:410
  12.8 11.9 %collective-permute-start.2 = (bf16[24,1024]{1,0:T(8,128)(2,1)S(1)}, bf16[24,1024]{1,0:T(8,128)(2,1)S(1)}, u32[]{:S(2)}, u32[]{:S(2)}) collective-permute-start(bf16[24,1024]{1,0:T(8,128)(2,1)S(1)} %norm.1.a_ref), channel_id=1, source_target_pairs={{0,22},{1,23},{2,24},{3,25},{4,26},{5,27},{6,28},{7,29},{8,30},{9,... | collective-permute-start | bytes 147464 | tf_op jit(solution)/shard_map/ppermute | solution.py:410
  19.5 53.2 %copy-start.6 = (bf16[12,2048]{1,0:T(8,128)(2,1)S(1)}, bf16[12,2048]{1,0:T(8,128)(2,1)}, u32[]{:S(2)}) copy-start(bf16[12,2048]{1,0:T(8,128)(2,1)} %resid_ref.1) | copy-start | bytes 147460
  19.5 53.2 %copy-start.7 = (f32[12,8,128]{2,1,0:T(8,128)S(1)}, f32[12,8,128]{2,1,0:T(8,128)}, u32[]{:S(2)}) copy-start(f32[12,8,128]{2,1,0:T(8,128)} %norm_ref.1) | copy-start | bytes 147460
  24.7 11.7 %collective-permute-start.3 = (bf16[3,24,1024]{2,1,0:T(8,128)(2,1)S(1)}, bf16[3,24,1024]{2,1,0:T(8,128)(2,1)S(1)}, u32[]{:S(2)}, u32[]{:S(2)}) collective-permute-start(bf16[3,24,1024]{2,1,0:T(8,128)(2,1)S(1)} %stack.2.refs_0_), channel_id=1, source_target_pairs={{0,2},{1,3},{2,4},{3,5},{4,6},{5,7},{6,8},{7,9},{8,10},{9,11},{10,... | collective-permute-start | bytes 442376 | tf_op jit(solution)/shard_map/ppermute | solution.py:410
  24.8 11.7 %collective-permute-start.4 = (bf16[3,24,1024]{2,1,0:T(8,128)(2,1)S(1)}, bf16[3,24,1024]{2,1,0:T(8,128)(2,1)S(1)}, u32[]{:S(2)}, u32[]{:S(2)}) collective-permute-start(bf16[3,24,1024]{2,1,0:T(8,128)(2,1)S(1)} %stack.2.refs_0_), channel_id=1, source_target_pairs={{0,30},{1,31},{2,0},{3,1},{4,2},{5,3},{6,4},{7,5},{8,6},{9,7},{10,... | collective-permute-start | bytes 442376 | tf_op jit(solution)/shard_map/ppermute | solution.py:410
  28.4 7.9 %collective-permute-start.5 = (bf16[24,1024]{1,0:T(8,128)(2,1)S(1)}, bf16[24,1024]{1,0:T(8,128)(2,1)S(1)}, u32[]{:S(2)}, u32[]{:S(2)}) collective-permute-start(bf16[24,1024]{1,0:T(8,128)(2,1)S(1)} %collective-permute-done.1.b_ref), channel_id=1, source_target_pairs={{0,6},{1,7},{2,8},{3,9},{4,10},{5,11},{6,12},{7,13},{8,14},{9,15},... | collective-permute-start | bytes 147464 | tf_op jit(solution)/shard_map/ppermute | solution.py:410
  36.4 5.9 %collective-permute-start.6 = (bf16[3,24,1024]{2,1,0:T(8,128)(2,1)S(1)}, bf16[3,24,1024]{2,1,0:T(8,128)(2,1)S(1)}, u32[]{:S(2)}, u32[]{:S(2)}) collective-permute-start(bf16[3,24,1024]{2,1,0:T(8,128)(2,1)S(1)} %relay.2), channel_id=1, source_target_pairs={{0,2},{1,3},{2,4},{3,5},{4,6},{5,7},{6,8},{7,9},{8,10},{9,11},{10,... | collective-permute-start | bytes 442376 | tf_op jit(solution)/shard_map/ppermute | solution.py:410
  36.5 7.4 %collective-permute-start.7 = (bf16[3,24,1024]{2,1,0:T(8,128)(2,1)S(1)}, bf16[3,24,1024]{2,1,0:T(8,128)(2,1)S(1)}, u32[]{:S(2)}, u32[]{:S(2)}) collective-permute-start(bf16[3,24,1024]{2,1,0:T(8,128)(2,1)S(1)} %collective-permute-done.4.refs_2_), channel_id=1, source_target_pairs={{0,30},{1,31},{2,0},{3,1},{4,2},{5,3},{6,4},{7,5},{8,6},{9,7},{10,... | collective-permute-start | bytes 442376 | tf_op jit(solution)/shard_map/ppermute | solution.py:410
  39.1 2.3 %collective-permute-start.13 = (bf16[24,1024]{1,0:T(8,128)(2,1)S(1)}, bf16[24,1024]{1,0:T(8,128)(2,1)S(1)}, u32[]{:S(2)}, u32[]{:S(2)}) collective-permute-start(bf16[24,1024]{1,0:T(8,128)(2,1)S(1)} %collective-permute-done.5.after_ref.refs_5_), channel_id=1, source_target_pairs={{0,1},{1,0},{2,3},{3,2},{4,5},{5,4},{6,7},{7,6},{8,9},{9,8},{10,11... | collective-permute-start | bytes 147464 | tf_op jit(solution)/shard_map/ppermute | solution.py:404
  40.6 3.6 %collective-permute-start.8 = (bf16[3,24,1024]{2,1,0:T(8,128)(2,1)S(1)}, bf16[3,24,1024]{2,1,0:T(8,128)(2,1)S(1)}, u32[]{:S(2)}, u32[]{:S(2)}) collective-permute-start(bf16[3,24,1024]{2,1,0:T(8,128)(2,1)S(1)} %stack.2.refs_0_), channel_id=1, source_target_pairs={{0,1},{1,0},{2,3},{3,2},{4,5},{5,4},{6,7},{7,6},{8,9},{9,8},{10,11... | collective-permute-start | bytes 442376 | tf_op jit(solution)/shard_map/ppermute | solution.py:404
  40.6 3.6 %collective-permute-start.10 = (bf16[3,24,1024]{2,1,0:T(8,128)(2,1)S(1)}, bf16[3,24,1024]{2,1,0:T(8,128)(2,1)S(1)}, u32[]{:S(2)}, u32[]{:S(2)}) collective-permute-start(bf16[3,24,1024]{2,1,0:T(8,128)(2,1)S(1)} %collective-permute-done.4.refs_2_), channel_id=1, source_target_pairs={{0,1},{1,0},{2,3},{3,2},{4,5},{5,4},{6,7},{7,6},{8,9},{9,8},{10,11... | collective-permute-start | bytes 442376 | tf_op jit(solution)/shard_map/ppermute | solution.py:404
  41.5 2.7 %collective-permute-start.9 = (bf16[3,24,1024]{2,1,0:T(8,128)(2,1)S(1)}, bf16[3,24,1024]{2,1,0:T(8,128)(2,1)S(1)}, u32[]{:S(2)}, u32[]{:S(2)}) collective-permute-start(bf16[3,24,1024]{2,1,0:T(8,128)(2,1)S(1)} %collective-permute-done.3.x_ref.refs_1_), channel_id=1, source_target_pairs={{0,1},{1,0},{2,3},{3,2},{4,5},{5,4},{6,7},{7,6},{8,9},{9,8},{10,11... | collective-permute-start | bytes 442376 | tf_op jit(solution)/shard_map/ppermute | solution.py:404
  42.2 2.7 %collective-permute-start.11 = (bf16[3,24,1024]{2,1,0:T(8,128)(2,1)S(1)}, bf16[3,24,1024]{2,1,0:T(8,128)(2,1)S(1)}, u32[]{:S(2)}, u32[]{:S(2)}) collective-permute-start(bf16[3,24,1024]{2,1,0:T(8,128)(2,1)S(1)} %collective-permute-done.6.refs_3_), channel_id=1, source_target_pairs={{0,1},{1,0},{2,3},{3,2},{4,5},{5,4},{6,7},{7,6},{8,9},{9,8},{10,11... | collective-permute-start | bytes 442376 | tf_op jit(solution)/shard_map/ppermute | solution.py:404
  43.9 1.4 collective-permute-start.12
  68.5 4.3 %collective-permute-start.14 = (bf16[16,32,128]{2,1,0:T(8,128)(2,1)S(1)}, bf16[16,32,128]{2,1,0:T(8,128)(2,1)S(1)}, u32[]{:S(2)}, u32[]{:S(2)}) collective-permute-start(bf16[16,32,128]{2,1,0:T(8,128)(2,1)S(1)} %all_to_all.5.a_ref.refs_12_), channel_id=1, source_target_pairs={{0,1},{1,0},{2,3},{3,2},{4,5},{5,4},{6,7},{7,6},{8,9},{9,8},{10,11... | collective-permute-start | bytes 393224 | tf_op jit(solution)/shard_map/ppermute | solution.py:404
  72.7 38.6 %copy-start.3 = (bf16[2048,256]{1,0:T(8,128)(2,1)S(1)}, bf16[2048,256]{1,0:T(8,128)(2,1)}, u32[]{:S(2)}) copy-start(bf16[2048,256]{1,0:T(8,128)(2,1)} %refs_17_.1) | copy-start | bytes 3145732
  72.7 38.6 %copy-start.4 = (bf16[2048,256]{1,0:T(8,128)(2,1)S(1)}, bf16[2048,256]{1,0:T(8,128)(2,1)}, u32[]{:S(2)}) copy-start(bf16[2048,256]{1,0:T(8,128)(2,1)} %refs_18_.1) | copy-start | bytes 3145732
  72.7 38.6 %copy-start.5 = (bf16[256,2048]{1,0:T(8,128)(2,1)S(1)}, bf16[256,2048]{1,0:T(8,128)(2,1)}, u32[]{:S(2)}) copy-start(bf16[256,2048]{1,0:T(8,128)(2,1)} %refs_19_.1) | copy-start | bytes 3145732
  77.3 32.7 %copy-start.8 = (bf16[2048]{0:T(1024)(128)(2,1)S(1)}, bf16[2048]{0:T(1024)(128)(2,1)}, u32[]{:S(2)}) copy-start(bf16[2048]{0:T(1024)(128)(2,1)} %param.45) | copy-start | bytes 12292
  77.3 34.1 %copy-start = (bf16[1,2048,512]{2,1,0:T(8,128)(2,1)S(1)}, bf16[1,2048,512]{2,1,0:T(8,128)(2,1)}, u32[]{:S(2)}) copy-start(bf16[1,2048,512]{2,1,0:T(8,128)(2,1)} %refs_14_.1) | copy-start | bytes 6291460
  77.3 34.1 %copy-start.1 = (bf16[1,2048,512]{2,1,0:T(8,128)(2,1)S(1)}, bf16[1,2048,512]{2,1,0:T(8,128)(2,1)}, u32[]{:S(2)}) copy-start(bf16[1,2048,512]{2,1,0:T(8,128)(2,1)} %refs_15_.1) | copy-start | bytes 6291460
  77.3 34.1 %copy-start.2 = (bf16[1,512,2048]{2,1,0:T(8,128)(2,1)S(1)}, bf16[1,512,2048]{2,1,0:T(8,128)(2,1)}, u32[]{:S(2)}) copy-start(bf16[1,512,2048]{2,1,0:T(8,128)(2,1)} %refs_16_.1) | copy-start | bytes 6291460
  77.3 1.3 collective-permute-start.15
  78.6 13.1 %collective-permute-start.16 = (bf16[24,1024]{1,0:T(8,128)(2,1)S(1)}, bf16[24,1024]{1,0:T(8,128)(2,1)S(1)}, u32[]{:S(2)}, u32[]{:S(2)}) collective-permute-start(bf16[24,1024]{1,0:T(8,128)(2,1)S(1)} %pair.1.a_ref), channel_id=1, source_target_pairs={{0,10},{1,11},{2,12},{3,13},{4,14},{5,15},{6,16},{7,17},{8,18},{9,... | collective-permute-start | bytes 147464 | tf_op jit(solution)/shard_map/ppermute | solution.py:410
  81.0 11.0 %collective-permute-start.17 = (bf16[24,1024]{1,0:T(8,128)(2,1)S(1)}, bf16[24,1024]{1,0:T(8,128)(2,1)S(1)}, u32[]{:S(2)}, u32[]{:S(2)}) collective-permute-start(bf16[24,1024]{1,0:T(8,128)(2,1)S(1)} %pair.1.a_ref), channel_id=1, source_target_pairs={{0,22},{1,23},{2,24},{3,25},{4,26},{5,27},{6,28},{7,29},{8,30},{9,... | collective-permute-start | bytes 147464 | tf_op jit(solution)/shard_map/ppermute | solution.py:410
  92.0 10.2 %collective-permute-start.18 = (bf16[3,24,1024]{2,1,0:T(8,128)(2,1)S(1)}, bf16[3,24,1024]{2,1,0:T(8,128)(2,1)S(1)}, u32[]{:S(2)}, u32[]{:S(2)}) collective-permute-start(bf16[3,24,1024]{2,1,0:T(8,128)(2,1)S(1)} %stack.3.refs_0_), channel_id=1, source_target_pairs={{0,2},{1,3},{2,4},{3,5},{4,6},{5,7},{6,8},{7,9},{8,10},{9,11},{10,... | collective-permute-start | bytes 442376 | tf_op jit(solution)/shard_map/ppermute | solution.py:410
  92.2 10.2 %collective-permute-start.19 = (bf16[3,24,1024]{2,1,0:T(8,128)(2,1)S(1)}, bf16[3,24,1024]{2,1,0:T(8,128)(2,1)S(1)}, u32[]{:S(2)}, u32[]{:S(2)}) collective-permute-start(bf16[3,24,1024]{2,1,0:T(8,128)(2,1)S(1)} %stack.3.refs_0_), channel_id=1, source_target_pairs={{0,30},{1,31},{2,0},{3,1},{4,2},{5,3},{6,4},{7,5},{8,6},{9,7},{10,... | collective-permute-start | bytes 442376 | tf_op jit(solution)/shard_map/ppermute | solution.py:410
  94.9 7.3 %collective-permute-start.20 = (bf16[24,1024]{1,0:T(8,128)(2,1)S(1)}, bf16[24,1024]{1,0:T(8,128)(2,1)S(1)}, u32[]{:S(2)}, u32[]{:S(2)}) collective-permute-start(bf16[24,1024]{1,0:T(8,128)(2,1)S(1)} %collective-permute-done.16.b_ref), channel_id=1, source_target_pairs={{0,6},{1,7},{2,8},{3,9},{4,10},{5,11},{6,12},{7,13},{8,14},{9,15},... | collective-permute-start | bytes 147464 | tf_op jit(solution)/shard_map/ppermute | solution.py:410
  102.2 5.8 %collective-permute-start.21 = (bf16[3,24,1024]{2,1,0:T(8,128)(2,1)S(1)}, bf16[3,24,1024]{2,1,0:T(8,128)(2,1)S(1)}, u32[]{:S(2)}, u32[]{:S(2)}) collective-permute-start(bf16[3,24,1024]{2,1,0:T(8,128)(2,1)S(1)} %relay.3), channel_id=1, source_target_pairs={{0,2},{1,3},{2,4},{3,5},{4,6},{5,7},{6,8},{7,9},{8,10},{9,11},{10,... | collective-permute-start | bytes 442376 | tf_op jit(solution)/shard_map/ppermute | solution.py:410
  102.4 7.6 %collective-permute-start.22 = (bf16[3,24,1024]{2,1,0:T(8,128)(2,1)S(1)}, bf16[3,24,1024]{2,1,0:T(8,128)(2,1)S(1)}, u32[]{:S(2)}, u32[]{:S(2)}) collective-permute-start(bf16[3,24,1024]{2,1,0:T(8,128)(2,1)S(1)} %collective-permute-done.19.refs_2_), channel_id=1, source_target_pairs={{0,30},{1,31},{2,0},{3,1},{4,2},{5,3},{6,4},{7,5},{8,6},{9,7},{10,... | collective-permute-start | bytes 442376 | tf_op jit(solution)/shard_map/ppermute | solution.py:410
  105.0 2.7 %collective-permute-start.28 = (bf16[24,1024]{1,0:T(8,128)(2,1)S(1)}, bf16[24,1024]{1,0:T(8,128)(2,1)S(1)}, u32[]{:S(2)}, u32[]{:S(2)}) collective-permute-start(bf16[24,1024]{1,0:T(8,128)(2,1)S(1)} %collective-permute-done.20.after_ref.refs_5_), channel_id=1, source_target_pairs={{0,1},{1,0},{2,3},{3,2},{4,5},{5,4},{6,7},{7,6},{8,9},{9,8},{10,11... | collective-permute-start | bytes 147464 | tf_op jit(solution)/shard_map/ppermute | solution.py:404
  106.8 3.1 %collective-permute-start.23 = (bf16[3,24,1024]{2,1,0:T(8,128)(2,1)S(1)}, bf16[3,24,1024]{2,1,0:T(8,128)(2,1)S(1)}, u32[]{:S(2)}, u32[]{:S(2)}) collective-permute-start(bf16[3,24,1024]{2,1,0:T(8,128)(2,1)S(1)} %stack.3.refs_0_), channel_id=1, source_target_pairs={{0,1},{1,0},{2,3},{3,2},{4,5},{5,4},{6,7},{7,6},{8,9},{9,8},{10,11... | collective-permute-start | bytes 442376 | tf_op jit(solution)/shard_map/ppermute | solution.py:404
  106.8 3.1 %collective-permute-start.24 = (bf16[3,24,1024]{2,1,0:T(8,128)(2,1)S(1)}, bf16[3,24,1024]{2,1,0:T(8,128)(2,1)S(1)}, u32[]{:S(2)}, u32[]{:S(2)}) collective-permute-start(bf16[3,24,1024]{2,1,0:T(8,128)(2,1)S(1)} %collective-permute-done.18.x_ref.refs_1_), channel_id=1, source_target_pairs={{0,1},{1,0},{2,3},{3,2},{4,5},{5,4},{6,7},{7,6},{8,9},{9,8},{10,11... | collective-permute-start | bytes 442376 | tf_op jit(solution)/shard_map/ppermute | solution.py:404
  107.7 2.3 %collective-permute-start.25 = (bf16[3,24,1024]{2,1,0:T(8,128)(2,1)S(1)}, bf16[3,24,1024]{2,1,0:T(8,128)(2,1)S(1)}, u32[]{:S(2)}, u32[]{:S(2)}) collective-permute-start(bf16[3,24,1024]{2,1,0:T(8,128)(2,1)S(1)} %collective-permute-done.19.refs_2_), channel_id=1, source_target_pairs={{0,1},{1,0},{2,3},{3,2},{4,5},{5,4},{6,7},{7,6},{8,9},{9,8},{10,11... | collective-permute-start | bytes 442376 | tf_op jit(solution)/shard_map/ppermute | solution.py:404
  108.1 2.9 %collective-permute-start.26 = (bf16[3,24,1024]{2,1,0:T(8,128)(2,1)S(1)}, bf16[3,24,1024]{2,1,0:T(8,128)(2,1)S(1)}, u32[]{:S(2)}, u32[]{:S(2)}) collective-permute-start(bf16[3,24,1024]{2,1,0:T(8,128)(2,1)S(1)} %collective-permute-done.21.refs_3_), channel_id=1, source_target_pairs={{0,1},{1,0},{2,3},{3,2},{4,5},{5,4},{6,7},{7,6},{8,9},{9,8},{10,11... | collective-permute-start | bytes 442376 | tf_op jit(solution)/shard_map/ppermute | solution.py:404
  109.9 1.4 collective-permute-start.27
  115.2 2.4 %collective-permute-start.29 = (bf16[384,1024]{1,0:T(8,128)(2,1)S(1)}, bf16[384,1024]{1,0:T(8,128)(2,1)S(1)}, u32[]{:S(2)}, u32[]{:S(2)}) collective-permute-start(bf16[384,1024]{1,0:T(8,128)(2,1)S(1)} %get-tuple-element.48), channel_id=1, source_target_pairs={{0,1},{1,0},{2,3},{3,2},{4,5},{5,4},{6,7},{7,6},{8,9},{9,8},{10,11... | collective-permute-start | bytes 2359304 | tf_op jit(solution)/shard_map/ppermute | solution.py:404
  117.8 13.8 %collective-permute-start.30 = (bf16[3,24,1024]{2,1,0:T(8,128)(2,1)S(1)}, bf16[3,24,1024]{2,1,0:T(8,128)(2,1)S(1)}, u32[]{:S(2)}, u32[]{:S(2)}) collective-permute-start(bf16[3,24,1024]{2,1,0:T(8,128)(2,1)S(1)} %get-tuple-element.50), channel_id=1, source_target_pairs={{0,2},{1,3},{2,4},{3,5},{4,6},{5,7},{6,8},{7,9},{8,10},{9,11},{10,... | collective-permute-start | bytes 442376 | tf_op jit(solution)/shard_map/ppermute | solution.py:410
  119.2 12.4 %collective-permute-start.31 = (bf16[3,24,1024]{2,1,0:T(8,128)(2,1)S(1)}, bf16[3,24,1024]{2,1,0:T(8,128)(2,1)S(1)}, u32[]{:S(2)}, u32[]{:S(2)}) collective-permute-start(bf16[3,24,1024]{2,1,0:T(8,128)(2,1)S(1)} %get-tuple-element.51), channel_id=1, source_target_pairs={{0,30},{1,31},{2,0},{3,1},{4,2},{5,3},{6,4},{7,5},{8,6},{9,7},{10,... | collective-permute-start | bytes 442376 | tf_op jit(solution)/shard_map/ppermute | solution.py:410
  120.6 11.9 %collective-permute-start.32 = (bf16[3,24,1024]{2,1,0:T(8,128)(2,1)S(1)}, bf16[3,24,1024]{2,1,0:T(8,128)(2,1)S(1)}, u32[]{:S(2)}, u32[]{:S(2)}) collective-permute-start(bf16[3,24,1024]{2,1,0:T(8,128)(2,1)S(1)} %get-tuple-element.52), channel_id=1, source_target_pairs={{0,4},{1,5},{2,6},{3,7},{4,8},{5,9},{6,10},{7,11},{8,12},{9,13},{1... | collective-permute-start | bytes 442376 | tf_op jit(solution)/shard_map/ppermute | solution.py:410
  120.7 11.9 %collective-permute-start.33 = (bf16[3,24,1024]{2,1,0:T(8,128)(2,1)S(1)}, bf16[3,24,1024]{2,1,0:T(8,128)(2,1)S(1)}, u32[]{:S(2)}, u32[]{:S(2)}) collective-permute-start(bf16[3,24,1024]{2,1,0:T(8,128)(2,1)S(1)} %get-tuple-element.53), channel_id=1, source_target_pairs={{0,28},{1,29},{2,30},{3,31},{4,0},{5,1},{6,2},{7,3},{8,4},{9,5},{1... | collective-permute-start | bytes 442376 | tf_op jit(solution)/shard_map/ppermute | solution.py:410
  124.2 7.4 %collective-permute-start.34 = (bf16[24,1024]{1,0:T(8,128)(2,1)S(1)}, bf16[24,1024]{1,0:T(8,128)(2,1)S(1)}, u32[]{:S(2)}, u32[]{:S(2)}) collective-permute-start(bf16[24,1024]{1,0:T(8,128)(2,1)S(1)} %get-tuple-element.54), channel_id=1, source_target_pairs={{0,6},{1,7},{2,8},{3,9},{4,10},{5,11},{6,12},{7,13},{8,14},{9,15},... | collective-permute-start | bytes 147464 | tf_op jit(solution)/shard_map/ppermute | solution.py:410
  132.6 9.3 %collective-permute-start.35 = (bf16[24,1024]{1,0:T(8,128)(2,1)S(1)}, bf16[24,1024]{1,0:T(8,128)(2,1)S(1)}, u32[]{:S(2)}, u32[]{:S(2)}) collective-permute-start(bf16[24,1024]{1,0:T(8,128)(2,1)S(1)} %get-tuple-element.56), channel_id=1, source_target_pairs={{0,10},{1,11},{2,12},{3,13},{4,14},{5,15},{6,16},{7,17},{8,18},{9,... | collective-permute-start | bytes 147464 | tf_op jit(solution)/shard_map/ppermute | solution.py:410
  137.3 8.0 %collective-permute-start.36 = (bf16[24,1024]{1,0:T(8,128)(2,1)S(1)}, bf16[24,1024]{1,0:T(8,128)(2,1)S(1)}, u32[]{:S(2)}, u32[]{:S(2)}) collective-permute-start(bf16[24,1024]{1,0:T(8,128)(2,1)S(1)} %get-tuple-element.57), channel_id=1, source_target_pairs={{0,22},{1,23},{2,24},{3,25},{4,26},{5,27},{6,28},{7,29},{8,30},{9,... | collective-permute-start | bytes 147464 | tf_op jit(solution)/shard_map/ppermute | solution.py:410
  145.3 5.2 %collective-permute-start.37 = (f32[12,1024]{1,0:T(8,128)S(1)}, f32[12,1024]{1,0:T(8,128)S(1)}, u32[]{:S(2)}, u32[]{:S(2)}) collective-permute-start(f32[12,1024]{1,0:T(8,128)S(1)} %get-tuple-element.59), channel_id=1, source_target_pairs={{0,1},{1,0},{2,3},{3,2},{4,5},{5,4},{6,7},{7,6},{8,9},{9,8},{10,11... | collective-permute-start | bytes 147464 | tf_op jit(solution)/shard_map/ppermute | solution.py:404

commit v4 on v3

--- a/solution.py
+++ b/solution.py
@@ -1,5 +1,3 @@
-import functools
-
 import jax
 import jax.numpy as jnp
 from jax import lax
@@ -7,6 +5,7 @@
 from jax.experimental.pallas import tpu as pltpu
 from jax.sharding import PartitionSpec as P
 
+
 CAP = 2
 INTERPRET = False
 F32 = jnp.float32
@@ -17,7 +16,7 @@
     return x if INTERPRET else pltpu.with_memory_space_constraint(x, pltpu.HBM)
 
 
-def call(kernel, outs, args, scratch=(), vmem=16, flops=1000000, name=None, hbm=(), sems=0, held=(), **grid):
+def call(kernel, outs, args, scratch=(), vmem=16, flops=1000000, hbm=(), sems=0, held=(), **grid):
     if hbm:
         args = [in_hbm(x) if i in hbm else x for i, x in enumerate(args)]
         grid["in_specs"] = [
@@ -33,7 +32,6 @@
         compiler_params=pltpu.CompilerParams(vmem_limit_bytes=vmem << 20),
         cost_estimate=pl.CostEstimate(flops=flops, bytes_accessed=1000000, transcendentals=0),
         interpret=INTERPRET,
-        name=name,
     )(*args)
     return result
 
@@ -86,10 +84,6 @@
     rows[:r] = jnp.where(c == 0, own, other)
     rows[r : 2 * r] = jnp.where(c == 0, other, own)
     out_ref[...] = rows[...].astype(BF16)
-
-
-def relay_kernel(x_ref, after_ref, out_ref):
-    out_ref[...] = x_ref[...]
 
 
 def stack_kernel(a_ref, b_ref, c_ref, after_ref, out_ref):
@@ -275,7 +269,7 @@
 def branch_kernel(*refs):
     xs, ys = refs[:6], refs[6:12]
     (a_ref, b_ref, eg_ref, eu_ref, ed_ref, dg_ref, du_ref, dd_ref, bw_ref,
-     keep_ref, send_ref, table, made, x_scr, y_scr) = refs[12:]
+     send_ref, hidden_ref, made, placer_ref, gains_ref, table, x_scr, y_scr) = refs[12:]
     c = core()
     me = lax.axis_index("ep").astype(F32)
     home = lax.div(lax.axis_index("ep"), 2)
@@ -329,17 +323,22 @@
     logit = jnp.sum(x.astype(F32) * bw_ref[:, at].astype(F32), axis=1, keepdims=True)
     logit = logit + jnp.sum(y.astype(F32) * bw_ref[:, to].astype(F32), axis=1, keepdims=True)
     sig = jax.nn.sigmoid(logit)
-    for where, ref in ((at, keep_ref), (to, send_ref)):
-        part = dot(hidden, dd_ref[:, where]) * sig
-        part = part + dot(placer, made[:, where]) * weight
-        ref[...] = part.astype(ref.dtype)
-
-
-NEAR = (1, -1, 2, -2)
-
-
-def spread_kernel(keep_ref, got_ref, *out_refs):
-    own_ref, near_refs, last_ref = out_refs[0], out_refs[1:-1], out_refs[-1]
+    hidden_ref[...] = hidden
+    placer_ref[...] = placer
+    gains_ref[...] = jnp.where(lane == 0, sig, weight)
+    part = dot(hidden, dd_ref[:, to]) * sig
+    send_ref[...] = (part + dot(placer, made[:, to]) * weight).astype(BF16)
+
+
+def rest_kernel(hidden_ref, made_ref, placer_ref, gains_ref, dd_ref, keep_ref):
+    c = core()
+    h = keep_ref.shape[1]
+    at = pl.ds(pl.multiple_of(c * h, h), h)
+    part = dot(hidden_ref[...], dd_ref[:, at]) * gains_ref[:, 0:1]
+    keep_ref[...] = part + dot(placer_ref[...], made_ref[:, at]) * gains_ref[:, 1:2]
+
+
+def spread_kernel(keep_ref, got_ref, zero_ref, one_ref, back_ref, up_ref, down_ref, last_ref):
     nz = keep_ref.shape[0]
     order = offsets(nz)
 
@@ -348,18 +347,21 @@
         return keep_ref[at] + got_ref[at].astype(F32)
 
     for i, far in enumerate((0, FAR, -FAR)):
-        own_ref[i] = term(far)
-        for near, ref in zip(NEAR, near_refs):
-            ref[i] = term(near + far).astype(BF16)
+        zero_ref[i] = term(far)
+        one_ref[i] = term(far + 1)
+        back_ref[i] = term(far - 1)
+        up_ref[i] = term(far + 2).astype(BF16)
+        down_ref[i] = term(far - 2).astype(BF16)
     last_ref[...] = term(8).astype(BF16)
 
 
-def fold_kernel(
-    own_ref, a_ref, b_ref, c_ref, d_ref, last_ref, own_out, plus_ref, minus_ref,
-):
+def relay_kernel(own_ref, got_ref, out_ref):
+    out_ref[...] = (own_ref[...] + got_ref[...].astype(F32)).astype(BF16)
+
+
+def fold_kernel(own_ref, a_ref, b_ref, last_ref, own_out, plus_ref, minus_ref):
     def total(i):
-        t = own_ref[i] + a_ref[i].astype(F32) + b_ref[i].astype(F32)
-        return t + c_ref[i].astype(F32) + d_ref[i].astype(F32)
+        return own_ref[i] + a_ref[i].astype(F32) + b_ref[i].astype(F32)
 
     own_out[...] = total(0)
     plus_ref[...] = (total(1) + last_ref[...].astype(F32)).astype(BF16)
@@ -414,17 +416,16 @@
 
     def gather(own, after):
         plus, minus = shift(own, FAR), shift(own, -FAR)
-        ring, = call(stack_kernel, [((3,) + tile, BF16)], (own, plus, minus, after), name="stack")
+        ring, = call(stack_kernel, [((3,) + tile, BF16)], (own, plus, minus, after))
         last = shift(plus, 8 - FAR)
         up, down = shift(ring, 1), shift(ring, -1)
-        relay, = call(relay_kernel, [((3,) + tile, BF16)], (up, last), name="relay")
-        pieces = (ring, up, down, shift(relay, 1), shift(down, -1), last)
+        pieces = (ring, up, down, shift(up, 1), shift(down, -1), last)
         return pieces, [swap(piece) for piece in pieces]
 
     other = swap(resid)
     normed, gains = call(
         own_kernel, [((r, d), BF16), (norm_gains.shape, F32)], (resid, norm_gains),
-        scratch=[((r, d), BF16)], hbm=(0, 1), sems=2, name="own")
+        scratch=[((r, d), BF16)], hbm=(0, 1), sems=2)
     keep, write, new_max, info, w_all, state, mix = call(
         gates_kernel,
         [((r, heads), F32), ((r, heads), F32), ((heads, r), F32), ((8, 128), BF16),
@@ -435,13 +436,13 @@
         scratch=[((heads, d), BF16), ((heads, d), BF16), ((1, heads), F32), ((1, heads), F32),
                  ((heads, r), F32), ((2, r), jnp.int32),
                  ((2, r), BF16), ((128, 128), F32), ((8, 128), F32)],
-        hbm=tuple(range(1, 14)), sems=12 + r, held=(4, 5, 6), name="gates")
+        hbm=tuple(range(1, 14)), sems=12 + r, held=(4, 5, 6))
     chunk, = call(norm_kernel, [(tile, BF16)], (normed, other, gains),
-                  scratch=[(tile, F32)], name="norm")
+                  scratch=[(tile, F32)])
     xs, ys = gather(chunk, info)
     projected, = call(
         proj_kernel, [((nz, 2 * r + 8, 4 * inner // n), BF16)],
-        (*xs, *ys, w_all, info), scratch=[((n * r, h), BF16)] * 2, name="proj")
+        (*xs, *ys, w_all, info), scratch=[((n * r, h), BF16)] * 2)
     a = exchange(projected)
     b = swap(a)
     middle, mine, send, new_norm, keys, wvt = call(
@@ -450,33 +451,40 @@
          ((heads, 16, dh), F32), ((dh, 128), F32)],
         (a, b, keep, write, state, state_norm, mix, resid, gains),
         scratch=[((nz, 16, dh), F32), ((nz, 16, dh), F32), ((heads, 16, dh), F32),
-                 ((128, dh), F32), ((r, inner), BF16)], name="cell")
+                 ((128, dh), F32), ((r, inner), BF16)])
     got = swap(send)
     chunk, = call(pair_kernel, [((2 * r, h), BF16)], (mine, got),
-                  scratch=[((2 * r, h), F32)], name="pair")
+                  scratch=[((2 * r, h), F32)])
     new_matrix, token = call(
         update_kernel, [(state_matrix.shape, F32), ((8, 128), F32)], (keep, keys, wvt, state),
-        scratch=[(state_matrix.shape, F32)], sems=r, name="update",
+        scratch=[(state_matrix.shape, F32)], sems=r,
         out_specs=[pl.BlockSpec(memory_space=pltpu.HBM), pl.BlockSpec(memory_space=pltpu.VMEM)])
     xs, ys = gather(chunk, token)
-    part, send = call(
-        branch_kernel, [((n * r, h), F32), ((n * r, h), BF16)],
+    send, hidden, made, placer, scales = call(
+        branch_kernel,
+        [((n * r, h), BF16), ((n * r, dense_down.shape[0]), BF16), ((n * CAP, d), BF16),
+         ((n * r, n * CAP), BF16), ((n * r, 128), F32)],
         (*xs, *ys, a, b, expert_gate, expert_up, expert_down, dense_gate, dense_up, dense_down,
          branch_weight.reshape(1, d)),
-        scratch=[((4, n * r, 128), F32), ((n * CAP, d), BF16), ((n * r, h), BF16),
-                 ((n * r, h), BF16)], vmem=32, name="branch")
+        scratch=[((4, n * r, 128), F32), ((n * r, h), BF16), ((n * r, h), BF16)], vmem=32)
     got = swap(send)
-    own, *near, last = call(
-        spread_kernel, [((3,) + tile, F32)] + [((3,) + tile, BF16)] * 4 + [(tile, BF16)],
-        (part.reshape((nz,) + tile), got.reshape((nz,) + tile)), name="spread")
-    near = [shift(x, offset) for x, offset in zip(near, NEAR)]
+    part, = call(rest_kernel, [((n * r, h), F32)], (hidden, made, placer, scales, dense_down),
+                 flops=400000000)
+    three = (3,) + tile
+    own, one, back, up, down, last = call(
+        spread_kernel, [(three, F32)] * 3 + [(three, BF16)] * 2 + [(tile, BF16)],
+        (part.reshape((nz,) + tile), got.reshape((nz,) + tile)))
+    up, down = shift(up, 1), shift(down, -1)
     last = shift(last, 8 - FAR)
+    up, = call(relay_kernel, [(three, BF16)], (one, up))
+    down, = call(relay_kernel, [(three, BF16)], (back, down))
+    up, down = shift(up, 1), shift(down, -1)
     own, plus, minus = call(fold_kernel, [(tile, F32), (tile, BF16), (tile, BF16)],
-                            (own, *near, last), name="fold")
+                            (own, up, down, last))
     plus, minus = shift(plus, FAR), shift(minus, -FAR)
-    mine, send = call(sum_kernel, [((r, h), F32), ((r, h), F32)], (own, plus, minus), name="sum")
+    mine, send = call(sum_kernel, [((r, h), F32), ((r, h), F32)], (own, plus, minus))
     got = swap(send)
-    out, = call(final_kernel, [((r, d), BF16)], (mine, got, middle, gains), name="final")
+    out, = call(final_kernel, [((r, d), BF16)], (mine, got, middle, gains))
     return (out, new_matrix, new_norm, new_max.T)
 
 

time: 151 us -> 151 us (level)
  starting transfers between devices: 72.7 us -> 67.6 us
  waiting for transfers between devices: 34.1 us -> 39.1 us
    ppermute x21, waiting for transfers between devices: 25.9 us -> 32 us  [shift(): lax.ppermute(x, 'ep', [(2 * z + c, 2 * ((z + offset) % nz) + c) for z in...]
    ppermute x21, starting transfers between devices: 45.6 us -> 42.2 us  [shift(): lax.ppermute(x, 'ep', [(2 * z + c, 2 * ((z + offset) % nz) + c) for z in...]
    ppermute x17, starting transfers between devices: 27.2 us -> 25.4 us  [swap(): return lax.ppermute(x, 'ep', pairs)]
    pallas_call x16 -> x17, Pallas kernels: 20.9 us -> 21 us  [call(): pl.pallas_call(kernel, out_shape=[pltpu.VMEM(s, d) if i in held and (not...]
  transfers between devices with their start and end apart: 38 -> 38, of which waited for: 20 -> 24; matrix products, arithmetic and copies ran while one was open for 0% -> 0% of each run, Pallas kernels for 7% -> 8%
where the time goes in v4:
time: 151 us
  starting transfers between devices  67.6 us (45%)
  waiting for transfers between devices  39.1 us (26%)
  blocking collectives  22.4 us (15%)
  Pallas kernels  21 us (14%)
    ppermute x21, starting transfers between devices, shift(): lax.ppermute(x, 'ep', [(2 * z + c, 2 * ((z + offset) % nz) + c) for z in...  42.2 us
    ppermute x21, waiting for transfers between devices, shift(): lax.ppermute(x, 'ep', [(2 * z + c, 2 * ((z + offset) % nz) + c) for z in...  32 us
    ppermute x17, starting transfers between devices, swap(): return lax.ppermute(x, 'ep', pairs)  25.4 us
    all_to_all x1, blocking collectives, exchange(): return lax.all_to_all(x, 'ep', 0, 0, axis_index_groups=groups)  22.4 us
    pallas_call x17, Pallas kernels, call(): pl.pallas_call(kernel, out_shape=[pltpu.VMEM(s, d) if i in held and (not...  21 us
    ppermute x17, waiting for transfers between devices, swap(): return lax.ppermute(x, 'ep', pairs)  7.11 us
  transfers between devices with their start and end apart: 38, of which 24 were waited for; matrix products, arithmetic and copies ran while one was open for 0% of the time, Pallas kernels for 8%

profile of v4, /device:TPU:69, one launch (start us, length us, event | category | flops | bytes accessed | tf_op | source)
XLA Modules:
  0.0 151.0 jit_solution(4344138524425003953)
XLA Ops:
  0.6 10.0 %collective-permute-start = (bf16[12,2048]{1,0:T(8,128)(2,1)}, bf16[12,2048]{1,0:T(8,128)(2,1)S(1)}, u32[]{:S(2)}, u32[]{:S(2)}) collective-permute-start(bf16[12,2048]{1,0:T(8,128)(2,1)} %resid_ref.1), channel_id=1, source_target_pairs={{0,1},{1,0},{2,3},{3,2},{4,5},{5,4},{6,7},{7,6},{8,9},{9,8},{10,11... | collective-permute-start | bytes 147464 | tf_op jit(solution)/shard_map/ppermute | solution.py:406
  10.6 1.0 shard_map.246
  11.9 0.9 collective-permute-start.1
  12.8 6.7 %collective-permute-start.2 = (bf16[24,1024]{1,0:T(8,128)(2,1)S(1)}, bf16[24,1024]{1,0:T(8,128)(2,1)S(1)}, u32[]{:S(2)}, u32[]{:S(2)}) collective-permute-start(bf16[24,1024]{1,0:T(8,128)(2,1)S(1)} %shard_map.247.a_ref), channel_id=1, source_target_pairs={{0,22},{1,23},{2,24},{3,25},{4,26},{5,27},{6,28},{7,29},{8,30},{9,... | collective-permute-start | bytes 147464 | tf_op jit(solution)/shard_map/ppermute | solution.py:412
  19.5 5.1 %shard_map.248 = (f32[12,8]{1,0:T(8,128)S(1)}, f32[12,8]{1,0:T(8,128)S(1)}, f32[8,12]{1,0:T(8,128)}, bf16[8,128]{1,0:T(8,128)(2,1)S(1)}, bf16[128,2048]{1,0:T(8,...) custom-call(bf16[12,2048]{1,0:T(8,128)(2,1)S(1)} %get-tuple-element.37.own_ref.normed_ref, ...), custom_call_target="tpu_custom_call" | custom-call | flops 1000000 | bytes 1000000 | tf_op jit(solution)/shard_map/pallas_call | solution.py:25
  24.8 3.6 %collective-permute-start.4 = (bf16[3,24,1024]{2,1,0:T(8,128)(2,1)S(1)}, bf16[3,24,1024]{2,1,0:T(8,128)(2,1)S(1)}, u32[]{:S(2)}, u32[]{:S(2)}) collective-permute-start(bf16[3,24,1024]{2,1,0:T(8,128)(2,1)S(1)} %shard_map.249.refs_0_), channel_id=1, source_target_pairs={{0,30},{1,31},{2,0},{3,1},{4,2},{5,3},{6,4},{7,5},{8,6},{9,7},{10,... | collective-permute-start | bytes 442376 | tf_op jit(solution)/shard_map/ppermute | solution.py:412
  28.4 3.5 %collective-permute-done.3.refs_1_ = bf16[3,24,1024]{2,1,0:T(8,128)(2,1)S(1)} collective-permute-done((bf16[3,24,1024]{2,1,0:T(8,128)(2,1)S(1)}, bf16[3,24,1024]{2,1,0:T(8,128)(2,1)S(1)}, u32[]{:S(2)}, u32[]{:S(2)}) %collective-permute-start.3) | collective-permute-done | bytes 147488 | tf_op jit(solution)/shard_map/ppermute | solution.py:412
  32.0 2.7 %collective-permute-start.6 = (bf16[3,24,1024]{2,1,0:T(8,128)(2,1)S(1)}, bf16[3,24,1024]{2,1,0:T(8,128)(2,1)S(1)}, u32[]{:S(2)}, u32[]{:S(2)}) collective-permute-start(bf16[3,24,1024]{2,1,0:T(8,128)(2,1)S(1)} %collective-permute-done.4.refs_2_), channel_id=1, source_target_pairs={{0,30},{1,31},{2,0},{3,1},{4,2},{5,3},{6,4},{7,5},{8,6},{9,7},{10,... | collective-permute-start | bytes 442376 | tf_op jit(solution)/shard_map/ppermute | solution.py:412
  34.6 2.9 %collective-permute-start.7 = (bf16[24,1024]{1,0:T(8,128)(2,1)S(1)}, bf16[24,1024]{1,0:T(8,128)(2,1)S(1)}, u32[]{:S(2)}, u32[]{:S(2)}) collective-permute-start(bf16[24,1024]{1,0:T(8,128)(2,1)S(1)} %collective-permute-done.1.b_ref), channel_id=1, source_target_pairs={{0,6},{1,7},{2,8},{3,9},{4,10},{5,11},{6,12},{7,13},{8,14},{9,15},... | collective-permute-start | bytes 147464 | tf_op jit(solution)/shard_map/ppermute | solution.py:412
  37.5 3.5 %collective-permute-done.7.refs_5_ = bf16[24,1024]{1,0:T(8,128)(2,1)S(1)} collective-permute-done((bf16[24,1024]{1,0:T(8,128)(2,1)S(1)}, bf16[24,1024]{1,0:T(8,128)(2,1)S(1)}, u32[]{:S(2)}, u32[]{:S(2)}) %collective-permute-start.7) | collective-permute-done | bytes 49184 | tf_op jit(solution)/shard_map/ppermute | solution.py:412
  41.0 2.8 %collective-permute-start.13 = (bf16[24,1024]{1,0:T(8,128)(2,1)S(1)}, bf16[24,1024]{1,0:T(8,128)(2,1)S(1)}, u32[]{:S(2)}, u32[]{:S(2)}) collective-permute-start(bf16[24,1024]{1,0:T(8,128)(2,1)S(1)} %collective-permute-done.7.refs_5_), channel_id=1, source_target_pairs={{0,1},{1,0},{2,3},{3,2},{4,5},{5,4},{6,7},{7,6},{8,9},{9,8},{10,11... | collective-permute-start | bytes 147464 | tf_op jit(solution)/shard_map/ppermute | solution.py:406
  43.8 0.5 collective-permute-start.10
  44.3 0.4 collective-permute-done.13.refs_11_
  45.6 0.5 collective-permute-done.9.refs_7_
  46.6 0.6 shard_map.250
  47.2 22.4 %all_to_all.5.a_ref.refs_12_ = bf16[16,32,128]{2,1,0:T(8,128)(2,1)S(1)} all-to-all(bf16[16,32,128]{2,1,0:T(8,128)(2,1)S(1)} %shard_map.250), channel_id=1, replica_groups={{0,2,4,6,8,10,12,14,16,18,20,22,24,26,28,30},{1,3,5,7,9,11,13,15,17,19,..., dimensions={0} | all-to-all | bytes 262144 | tf_op jit(solution)/shard_map/all_to_all | solution.py:409
  69.7 3.3 %collective-permute-start.14 = (bf16[16,32,128]{2,1,0:T(8,128)(2,1)S(1)}, bf16[16,32,128]{2,1,0:T(8,128)(2,1)S(1)}, u32[]{:S(2)}, u32[]{:S(2)}) collective-permute-start(bf16[16,32,128]{2,1,0:T(8,128)(2,1)S(1)} %all_to_all.5.a_ref.refs_12_), channel_id=1, source_target_pairs={{0,1},{1,0},{2,3},{3,2},{4,5},{5,4},{6,7},{7,6},{8,9},{9,8},{10,11... | collective-permute-start | bytes 393224 | tf_op jit(solution)/shard_map/ppermute | solution.py:406
  72.9 1.0 collective-permute-done.14.b_ref.refs_13_
  73.9 4.5 %shard_map.251 = (f32[12,2048]{1,0:T(8,128)S(1)}, bf16[12,1024]{1,0:T(8,128)(2,1)S(1)}, bf16[12,1024]{1,0:T(8,128)(2,1)S(1)}, f32[12,8,128]{2,1,0:T(8,128)}, f32...) custom-call(bf16[16,32,128]{2,1,0:T(8,128)(2,1)S(1)} %all_to_all.5.a_ref.refs_12_, ...), custom_call_target="tpu_custom_call" | custom-call | flops 1000000 | bytes 1000000 | tf_op jit(solution)/shard_map/pallas_call | solution.py:25
  78.4 0.5 collective-permute-start.15
  78.9 0.9 collective-permute-done.15.got_ref
  79.8 2.4 %collective-permute-start.16 = (bf16[24,1024]{1,0:T(8,128)(2,1)S(1)}, bf16[24,1024]{1,0:T(8,128)(2,1)S(1)}, u32[]{:S(2)}, u32[]{:S(2)}) collective-permute-start(bf16[24,1024]{1,0:T(8,128)(2,1)S(1)} %shard_map.252.a_ref), channel_id=1, source_target_pairs={{0,10},{1,11},{2,12},{3,13},{4,14},{5,15},{6,16},{7,17},{8,18},{9,... | collective-permute-start | bytes 147464 | tf_op jit(solution)/shard_map/ppermute | solution.py:412
  82.2 5.2 %collective-permute-start.17 = (bf16[24,1024]{1,0:T(8,128)(2,1)S(1)}, bf16[24,1024]{1,0:T(8,128)(2,1)S(1)}, u32[]{:S(2)}, u32[]{:S(2)}) collective-permute-start(bf16[24,1024]{1,0:T(8,128)(2,1)S(1)} %shard_map.252.a_ref), channel_id=1, source_target_pairs={{0,22},{1,23},{2,24},{3,25},{4,26},{5,27},{6,28},{7,29},{8,30},{9,... | collective-permute-start | bytes 147464 | tf_op jit(solution)/shard_map/ppermute | solution.py:412
  87.4 4.7 %shard_map.253 = (f32[12,8,128,128]{3,2,1,0:T(8,128)}, f32[8,128]{1,0:T(8,128)S(1)}) custom-call(f32[12,8]{1,0:T(8,128)S(1)} %get-tuple-element.41.keep_ref, f32[8,16,128]{2,1,0:T(8,128)S(1)} %get-tuple-element.47.keys_ref, f32[128,128]{1,0:T(8,128)S(1)} %get-tuple-element.48.wvt_ref, f32[12,8,128,128]{3,2,1,0:T(8,128)S(1)} %get-tuple-element.43.m_ref), custom_call_target="tpu_custom_call" | custom-call | flops 1000000 | bytes 1000000 | tf_op jit(solution)/shard_map/pallas_call | solution.py:25
  92.1 0.8 collective-permute-done.16.b_ref
  93.3 2.7 %collective-permute-start.19 = (bf16[3,24,1024]{2,1,0:T(8,128)(2,1)S(1)}, bf16[3,24,1024]{2,1,0:T(8,128)(2,1)S(1)}, u32[]{:S(2)}, u32[]{:S(2)}) collective-permute-start(bf16[3,24,1024]{2,1,0:T(8,128)(2,1)S(1)} %shard_map.254.refs_0_), channel_id=1, source_target_pairs={{0,30},{1,31},{2,0},{3,1},{4,2},{5,3},{6,4},{7,5},{8,6},{9,7},{10,... | collective-permute-start | bytes 442376 | tf_op jit(solution)/shard_map/ppermute | solution.py:412
  96.0 3.1 %collective-permute-done.18.refs_1_ = bf16[3,24,1024]{2,1,0:T(8,128)(2,1)S(1)} collective-permute-done((bf16[3,24,1024]{2,1,0:T(8,128)(2,1)S(1)}, bf16[3,24,1024]{2,1,0:T(8,128)(2,1)S(1)}, u32[]{:S(2)}, u32[]{:S(2)}) %collective-permute-start.18) | collective-permute-done | bytes 147488 | tf_op jit(solution)/shard_map/ppermute | solution.py:412
  99.1 2.7 %collective-permute-start.21 = (bf16[3,24,1024]{2,1,0:T(8,128)(2,1)S(1)}, bf16[3,24,1024]{2,1,0:T(8,128)(2,1)S(1)}, u32[]{:S(2)}, u32[]{:S(2)}) collective-permute-start(bf16[3,24,1024]{2,1,0:T(8,128)(2,1)S(1)} %collective-permute-done.19.refs_2_), channel_id=1, source_target_pairs={{0,30},{1,31},{2,0},{3,1},{4,2},{5,3},{6,4},{7,5},{8,6},{9,7},{10,... | collective-permute-start | bytes 442376 | tf_op jit(solution)/shard_map/ppermute | solution.py:412
  101.8 7.2 %collective-permute-done.22.refs_5_ = bf16[24,1024]{1,0:T(8,128)(2,1)S(1)} collective-permute-done((bf16[24,1024]{1,0:T(8,128)(2,1)S(1)}, bf16[24,1024]{1,0:T(8,128)(2,1)S(1)}, u32[]{:S(2)}, u32[]{:S(2)}) %collective-permute-start.22) | collective-permute-done | bytes 49184 | tf_op jit(solution)/shard_map/ppermute | solution.py:412
  108.9 2.6 %collective-permute-start.28 = (bf16[24,1024]{1,0:T(8,128)(2,1)S(1)}, bf16[24,1024]{1,0:T(8,128)(2,1)S(1)}, u32[]{:S(2)}, u32[]{:S(2)}) collective-permute-start(bf16[24,1024]{1,0:T(8,128)(2,1)S(1)} %collective-permute-done.22.refs_5_), channel_id=1, source_target_pairs={{0,1},{1,0},{2,3},{3,2},{4,5},{5,4},{6,7},{7,6},{8,9},{9,8},{10,11... | collective-permute-start | bytes 147464 | tf_op jit(solution)/shard_map/ppermute | solution.py:406
  111.6 0.5 collective-permute-start.24
  113.3 0.5 collective-permute-done.25.refs_8_
  114.4 3.4 %shard_map.255 = (bf16[384,1024]{1,0:T(8,128)(2,1)S(1)}, bf16[384,256]{1,0:T(8,128)(2,1)S(1)}, bf16[64,2048]{1,0:T(8,128)(2,1)S(1)}, bf16[384,64]{1,0:T(8,128)(2,1)S(1)}, f32[384,128]{1,0:T(8,128)S(1)}) custom-call(bf16[3,24,1024]{2,1,0:T(8,128)(2,1)S(1)} %shard_map.254.refs_0_, bf16[3,24,1024]{2,1,0:T(8,128)(2,1)S(1)} %collective-permute-done.18.refs_1_, ...), custom_call_target="tpu_custom_call" | custom-call | flops 1000000 | bytes 1000000 | tf_op jit(solution)/shard_map/pallas_call | solution.py:25
  117.8 0.4 collective-permute-start.29
  118.2 0.6 shard_map.256
  118.8 1.4 collective-permute-done.29
  120.5 1.4 collective-permute-start.30
  121.9 3.6 %collective-permute-done.32.got_ref = bf16[3,24,1024]{2,1,0:T(8,128)(2,1)S(1)} collective-permute-done((bf16[3,24,1024]{2,1,0:T(8,128)(2,1)S(1)}, bf16[3,24,1024]{2,1,0:T(8,128)(2,1)S(1)}, u32[]{:S(2)}, u32[]{:S(2)}) %collective-permute-start.32) | collective-permute-done | bytes 147488 | tf_op jit(solution)/shard_map/ppermute | solution.py:412
  125.6 1.5 %collective-permute-start.33 = (bf16[3,24,1024]{2,1,0:T(8,128)(2,1)S(1)}, bf16[3,24,1024]{2,1,0:T(8,128)(2,1)S(1)}, u32[]{:S(2)}, u32[]{:S(2)}) collective-permute-start(bf16[3,24,1024]{2,1,0:T(8,128)(2,1)S(1)} %shard_map.259), channel_id=1, source_target_pairs={{0,30},{1,31},{2,0},{3,1},{4,2},{5,3},{6,4},{7,5},{8,6},{9,7},{10,... | collective-permute-start | bytes 442376 | tf_op jit(solution)/shard_map/ppermute | solution.py:412
  127.3 1.4 collective-permute-start.34
  128.7 5.2 %collective-permute-done.34.last_ref = bf16[24,1024]{1,0:T(8,128)(2,1)S(1)} collective-permute-done((bf16[24,1024]{1,0:T(8,128)(2,1)S(1)}, bf16[24,1024]{1,0:T(8,128)(2,1)S(1)}, u32[]{:S(2)}, u32[]{:S(2)}) %collective-permute-start.34) | collective-permute-done | bytes 49184 | tf_op jit(solution)/shard_map/ppermute | solution.py:412
  134.3 0.9 collective-permute-start.35
  135.1 6.7 %collective-permute-start.36 = (bf16[24,1024]{1,0:T(8,128)(2,1)S(1)}, bf16[24,1024]{1,0:T(8,128)(2,1)S(1)}, u32[]{:S(2)}, u32[]{:S(2)}) collective-permute-start(bf16[24,1024]{1,0:T(8,128)(2,1)S(1)} %get-tuple-element.63), channel_id=1, source_target_pairs={{0,22},{1,23},{2,24},{3,25},{4,26},{5,27},{6,28},{7,29},{8,30},{9,... | collective-permute-start | bytes 147464 | tf_op jit(solution)/shard_map/ppermute | solution.py:412
  141.9 2.6 %collective-permute-done.35.a_ref = bf16[24,1024]{1,0:T(8,128)(2,1)S(1)} collective-permute-done((bf16[24,1024]{1,0:T(8,128)(2,1)S(1)}, bf16[24,1024]{1,0:T(8,128)(2,1)S(1)}, u32[]{:S(2)}, u32[]{:S(2)}) %collective-permute-start.35) | collective-permute-done | bytes 49184 | tf_op jit(solution)/shard_map/ppermute | solution.py:412
  144.5 1.7 %collective-permute-done.36.b_ref = bf16[24,1024]{1,0:T(8,128)(2,1)S(1)} collective-permute-done((bf16[24,1024]{1,0:T(8,128)(2,1)S(1)}, bf16[24,1024]{1,0:T(8,128)(2,1)S(1)}, u32[]{:S(2)}, u32[]{:S(2)}) %collective-permute-start.36) | collective-permute-done | bytes 49184 | tf_op jit(solution)/shard_map/ppermute | solution.py:412
  146.3 3.1 %collective-permute-start.37 = (f32[12,1024]{1,0:T(8,128)S(1)}, f32[12,1024]{1,0:T(8,128)S(1)}, u32[]{:S(2)}, u32[]{:S(2)}) collective-permute-start(f32[12,1024]{1,0:T(8,128)S(1)} %get-tuple-element.65), channel_id=1, source_target_pairs={{0,1},{1,0},{2,3},{3,2},{4,5},{5,4},{6,7},{7,6},{8,9},{9,8},{10,11... | collective-permute-start | bytes 147464 | tf_op jit(solution)/shard_map/ppermute | solution.py:406
  149.4 0.9 collective-permute-done.37.got_ref
  150.3 0.7 shard_map.262
  (65 shorter events, 5.0 us)
Async XLA Ops:
  0.6 11.1 %collective-permute-start = (bf16[12,2048]{1,0:T(8,128)(2,1)}, bf16[12,2048]{1,0:T(8,128)(2,1)S(1)}, u32[]{:S(2)}, u32[]{:S(2)}) collective-permute-start(bf16[12,2048]{1,0:T(8,128)(2,1)} %resid_ref.1), channel_id=1, source_target_pairs={{0,1},{1,0},{2,3},{3,2},{4,5},{5,4},{6,7},{7,6},{8,9},{9,8},{10,11... | collective-permute-start | bytes 147464 | tf_op jit(solution)/shard_map/ppermute | solution.py:406
  11.9 12.7 %collective-permute-start.1 = (bf16[24,1024]{1,0:T(8,128)(2,1)S(1)}, bf16[24,1024]{1,0:T(8,128)(2,1)S(1)}, u32[]{:S(2)}, u32[]{:S(2)}) collective-permute-start(bf16[24,1024]{1,0:T(8,128)(2,1)S(1)} %shard_map.247.a_ref), channel_id=1, source_target_pairs={{0,10},{1,11},{2,12},{3,13},{4,14},{5,15},{6,16},{7,17},{8,18},{9,... | collective-permute-start | bytes 147464 | tf_op jit(solution)/shard_map/ppermute | solution.py:412
  12.8 11.9 %collective-permute-start.2 = (bf16[24,1024]{1,0:T(8,128)(2,1)S(1)}, bf16[24,1024]{1,0:T(8,128)(2,1)S(1)}, u32[]{:S(2)}, u32[]{:S(2)}) collective-permute-start(bf16[24,1024]{1,0:T(8,128)(2,1)S(1)} %shard_map.247.a_ref), channel_id=1, source_target_pairs={{0,22},{1,23},{2,24},{3,25},{4,26},{5,27},{6,28},{7,29},{8,30},{9,... | collective-permute-start | bytes 147464 | tf_op jit(solution)/shard_map/ppermute | solution.py:412
  19.5 54.4 %copy-start.6 = (bf16[12,2048]{1,0:T(8,128)(2,1)S(1)}, bf16[12,2048]{1,0:T(8,128)(2,1)}, u32[]{:S(2)}) copy-start(bf16[12,2048]{1,0:T(8,128)(2,1)} %resid_ref.1) | copy-start | bytes 147460
  19.5 54.4 %copy-start.7 = (f32[12,8,128]{2,1,0:T(8,128)S(1)}, f32[12,8,128]{2,1,0:T(8,128)}, u32[]{:S(2)}) copy-start(f32[12,8,128]{2,1,0:T(8,128)} %norm_ref.1) | copy-start | bytes 147460
  24.7 7.3 %collective-permute-start.3 = (bf16[3,24,1024]{2,1,0:T(8,128)(2,1)S(1)}, bf16[3,24,1024]{2,1,0:T(8,128)(2,1)S(1)}, u32[]{:S(2)}, u32[]{:S(2)}) collective-permute-start(bf16[3,24,1024]{2,1,0:T(8,128)(2,1)S(1)} %shard_map.249.refs_0_), channel_id=1, source_target_pairs={{0,2},{1,3},{2,4},{3,5},{4,6},{5,7},{6,8},{7,9},{8,10},{9,11},{10,... | collective-permute-start | bytes 442376 | tf_op jit(solution)/shard_map/ppermute | solution.py:412
  24.8 7.2 %collective-permute-start.4 = (bf16[3,24,1024]{2,1,0:T(8,128)(2,1)S(1)}, bf16[3,24,1024]{2,1,0:T(8,128)(2,1)S(1)}, u32[]{:S(2)}, u32[]{:S(2)}) collective-permute-start(bf16[3,24,1024]{2,1,0:T(8,128)(2,1)S(1)} %shard_map.249.refs_0_), channel_id=1, source_target_pairs={{0,30},{1,31},{2,0},{3,1},{4,2},{5,3},{6,4},{7,5},{8,6},{9,7},{10,... | collective-permute-start | bytes 442376 | tf_op jit(solution)/shard_map/ppermute | solution.py:412
  32.0 13.1 %collective-permute-start.5 = (bf16[3,24,1024]{2,1,0:T(8,128)(2,1)S(1)}, bf16[3,24,1024]{2,1,0:T(8,128)(2,1)S(1)}, u32[]{:S(2)}, u32[]{:S(2)}) collective-permute-start(bf16[3,24,1024]{2,1,0:T(8,128)(2,1)S(1)} %collective-permute-done.3.refs_1_), channel_id=1, source_target_pairs={{0,2},{1,3},{2,4},{3,5},{4,6},{5,7},{6,8},{7,9},{8,10},{9,11},{10,... | collective-permute-start | bytes 442376 | tf_op jit(solution)/shard_map/ppermute | solution.py:412
  32.0 13.3 %collective-permute-start.6 = (bf16[3,24,1024]{2,1,0:T(8,128)(2,1)S(1)}, bf16[3,24,1024]{2,1,0:T(8,128)(2,1)S(1)}, u32[]{:S(2)}, u32[]{:S(2)}) collective-permute-start(bf16[3,24,1024]{2,1,0:T(8,128)(2,1)S(1)} %collective-permute-done.4.refs_2_), channel_id=1, source_target_pairs={{0,30},{1,31},{2,0},{3,1},{4,2},{5,3},{6,4},{7,5},{8,6},{9,7},{10,... | collective-permute-start | bytes 442376 | tf_op jit(solution)/shard_map/ppermute | solution.py:412
  34.6 6.4 %collective-permute-start.7 = (bf16[24,1024]{1,0:T(8,128)(2,1)S(1)}, bf16[24,1024]{1,0:T(8,128)(2,1)S(1)}, u32[]{:S(2)}, u32[]{:S(2)}) collective-permute-start(bf16[24,1024]{1,0:T(8,128)(2,1)S(1)} %collective-permute-done.1.b_ref), channel_id=1, source_target_pairs={{0,6},{1,7},{2,8},{3,9},{4,10},{5,11},{6,12},{7,13},{8,14},{9,15},... | collective-permute-start | bytes 147464 | tf_op jit(solution)/shard_map/ppermute | solution.py:412
  41.0 3.7 %collective-permute-start.13 = (bf16[24,1024]{1,0:T(8,128)(2,1)S(1)}, bf16[24,1024]{1,0:T(8,128)(2,1)S(1)}, u32[]{:S(2)}, u32[]{:S(2)}) collective-permute-start(bf16[24,1024]{1,0:T(8,128)(2,1)S(1)} %collective-permute-done.7.refs_5_), channel_id=1, source_target_pairs={{0,1},{1,0},{2,3},{3,2},{4,5},{5,4},{6,7},{7,6},{8,9},{9,8},{10,11... | collective-permute-start | bytes 147464 | tf_op jit(solution)/shard_map/ppermute | solution.py:406
  43.8 1.8 %collective-permute-start.8 = (bf16[3,24,1024]{2,1,0:T(8,128)(2,1)S(1)}, bf16[3,24,1024]{2,1,0:T(8,128)(2,1)S(1)}, u32[]{:S(2)}, u32[]{:S(2)}) collective-permute-start(bf16[3,24,1024]{2,1,0:T(8,128)(2,1)S(1)} %shard_map.249.refs_0_), channel_id=1, source_target_pairs={{0,1},{1,0},{2,3},{3,2},{4,5},{5,4},{6,7},{7,6},{8,9},{9,8},{10,11... | collective-permute-start | bytes 442376 | tf_op jit(solution)/shard_map/ppermute | solution.py:406
  43.8 1.8 %collective-permute-start.10 = (bf16[3,24,1024]{2,1,0:T(8,128)(2,1)S(1)}, bf16[3,24,1024]{2,1,0:T(8,128)(2,1)S(1)}, u32[]{:S(2)}, u32[]{:S(2)}) collective-permute-start(bf16[3,24,1024]{2,1,0:T(8,128)(2,1)S(1)} %collective-permute-done.4.refs_2_), channel_id=1, source_target_pairs={{0,1},{1,0},{2,3},{3,2},{4,5},{5,4},{6,7},{7,6},{8,9},{9,8},{10,11... | collective-permute-start | bytes 442376 | tf_op jit(solution)/shard_map/ppermute | solution.py:406
  44.7 1.4 collective-permute-start.9
  45.1 1.4 collective-permute-start.11
  45.2 1.4 collective-permute-start.12
  69.7 4.2 %collective-permute-start.14 = (bf16[16,32,128]{2,1,0:T(8,128)(2,1)S(1)}, bf16[16,32,128]{2,1,0:T(8,128)(2,1)S(1)}, u32[]{:S(2)}, u32[]{:S(2)}) collective-permute-start(bf16[16,32,128]{2,1,0:T(8,128)(2,1)S(1)} %all_to_all.5.a_ref.refs_12_), channel_id=1, source_target_pairs={{0,1},{1,0},{2,3},{3,2},{4,5},{5,4},{6,7},{7,6},{8,9},{9,8},{10,11... | collective-permute-start | bytes 393224 | tf_op jit(solution)/shard_map/ppermute | solution.py:406
  73.9 40.5 %copy-start.3 = (bf16[1,512,2048]{2,1,0:T(8,128)(2,1)S(1)}, bf16[1,512,2048]{2,1,0:T(8,128)(2,1)}, u32[]{:S(2)}) copy-start(bf16[1,512,2048]{2,1,0:T(8,128)(2,1)} %refs_16_.1) | copy-start | bytes 6291460
  73.9 40.5 %copy-start.5 = (bf16[2048,256]{1,0:T(8,128)(2,1)S(1)}, bf16[2048,256]{1,0:T(8,128)(2,1)}, u32[]{:S(2)}) copy-start(bf16[2048,256]{1,0:T(8,128)(2,1)} %refs_18_.1) | copy-start | bytes 3145732
  78.4 34.9 %copy-start.8 = (bf16[2048]{0:T(1024)(128)(2,1)S(1)}, bf16[2048]{0:T(1024)(128)(2,1)}, u32[]{:S(2)}) copy-start(bf16[2048]{0:T(1024)(128)(2,1)} %param.45) | copy-start | bytes 12292
  78.4 36.0 %copy-start = (bf16[256,2048]{1,0:T(8,128)(2,1)S(1)}, bf16[256,2048]{1,0:T(8,128)(2,1)}, u32[]{:S(2)}) copy-start(bf16[256,2048]{1,0:T(8,128)(2,1)} %dd_ref.1) | copy-start | bytes 3145732
  78.4 36.0 %copy-start.1 = (bf16[1,2048,512]{2,1,0:T(8,128)(2,1)S(1)}, bf16[1,2048,512]{2,1,0:T(8,128)(2,1)}, u32[]{:S(2)}) copy-start(bf16[1,2048,512]{2,1,0:T(8,128)(2,1)} %refs_14_.1) | copy-start | bytes 6291460
  78.4 36.0 %copy-start.2 = (bf16[1,2048,512]{2,1,0:T(8,128)(2,1)S(1)}, bf16[1,2048,512]{2,1,0:T(8,128)(2,1)}, u32[]{:S(2)}) copy-start(bf16[1,2048,512]{2,1,0:T(8,128)(2,1)} %refs_15_.1) | copy-start | bytes 6291460
  78.4 36.0 %copy-start.4 = (bf16[2048,256]{1,0:T(8,128)(2,1)S(1)}, bf16[2048,256]{1,0:T(8,128)(2,1)}, u32[]{:S(2)}) copy-start(bf16[2048,256]{1,0:T(8,128)(2,1)} %refs_17_.1) | copy-start | bytes 3145732
  78.4 1.3 collective-permute-start.15
  79.8 13.1 %collective-permute-start.16 = (bf16[24,1024]{1,0:T(8,128)(2,1)S(1)}, bf16[24,1024]{1,0:T(8,128)(2,1)S(1)}, u32[]{:S(2)}, u32[]{:S(2)}) collective-permute-start(bf16[24,1024]{1,0:T(8,128)(2,1)S(1)} %shard_map.252.a_ref), channel_id=1, source_target_pairs={{0,10},{1,11},{2,12},{3,13},{4,14},{5,15},{6,16},{7,17},{8,18},{9,... | collective-permute-start | bytes 147464 | tf_op jit(solution)/shard_map/ppermute | solution.py:412
  82.2 11.0 %collective-permute-start.17 = (bf16[24,1024]{1,0:T(8,128)(2,1)S(1)}, bf16[24,1024]{1,0:T(8,128)(2,1)S(1)}, u32[]{:S(2)}, u32[]{:S(2)}) collective-permute-start(bf16[24,1024]{1,0:T(8,128)(2,1)S(1)} %shard_map.252.a_ref), channel_id=1, source_target_pairs={{0,22},{1,23},{2,24},{3,25},{4,26},{5,27},{6,28},{7,29},{8,30},{9,... | collective-permute-start | bytes 147464 | tf_op jit(solution)/shard_map/ppermute | solution.py:412
  93.2 5.9 %collective-permute-start.18 = (bf16[3,24,1024]{2,1,0:T(8,128)(2,1)S(1)}, bf16[3,24,1024]{2,1,0:T(8,128)(2,1)S(1)}, u32[]{:S(2)}, u32[]{:S(2)}) collective-permute-start(bf16[3,24,1024]{2,1,0:T(8,128)(2,1)S(1)} %shard_map.254.refs_0_), channel_id=1, source_target_pairs={{0,2},{1,3},{2,4},{3,5},{4,6},{5,7},{6,8},{7,9},{8,10},{9,11},{10,... | collective-permute-start | bytes 442376 | tf_op jit(solution)/shard_map/ppermute | solution.py:412
  93.3 5.8 %collective-permute-start.19 = (bf16[3,24,1024]{2,1,0:T(8,128)(2,1)S(1)}, bf16[3,24,1024]{2,1,0:T(8,128)(2,1)S(1)}, u32[]{:S(2)}, u32[]{:S(2)}) collective-permute-start(bf16[3,24,1024]{2,1,0:T(8,128)(2,1)S(1)} %shard_map.254.refs_0_), channel_id=1, source_target_pairs={{0,30},{1,31},{2,0},{3,1},{4,2},{5,3},{6,4},{7,5},{8,6},{9,7},{10,... | collective-permute-start | bytes 442376 | tf_op jit(solution)/shard_map/ppermute | solution.py:412
  99.1 13.7 %collective-permute-start.20 = (bf16[3,24,1024]{2,1,0:T(8,128)(2,1)S(1)}, bf16[3,24,1024]{2,1,0:T(8,128)(2,1)S(1)}, u32[]{:S(2)}, u32[]{:S(2)}) collective-permute-start(bf16[3,24,1024]{2,1,0:T(8,128)(2,1)S(1)} %collective-permute-done.18.refs_1_), channel_id=1, source_target_pairs={{0,2},{1,3},{2,4},{3,5},{4,6},{5,7},{6,8},{7,9},{8,10},{9,11},{10,... | collective-permute-start | bytes 442376 | tf_op jit(solution)/shard_map/ppermute | solution.py:412
  99.1 13.8 %collective-permute-start.21 = (bf16[3,24,1024]{2,1,0:T(8,128)(2,1)S(1)}, bf16[3,24,1024]{2,1,0:T(8,128)(2,1)S(1)}, u32[]{:S(2)}, u32[]{:S(2)}) collective-permute-start(bf16[3,24,1024]{2,1,0:T(8,128)(2,1)S(1)} %collective-permute-done.19.refs_2_), channel_id=1, source_target_pairs={{0,30},{1,31},{2,0},{3,1},{4,2},{5,3},{6,4},{7,5},{8,6},{9,7},{10,... | collective-permute-start | bytes 442376 | tf_op jit(solution)/shard_map/ppermute | solution.py:412
  101.8 7.2 %collective-permute-start.22 = (bf16[24,1024]{1,0:T(8,128)(2,1)S(1)}, bf16[24,1024]{1,0:T(8,128)(2,1)S(1)}, u32[]{:S(2)}, u32[]{:S(2)}) collective-permute-start(bf16[24,1024]{1,0:T(8,128)(2,1)S(1)} %collective-permute-done.16.b_ref), channel_id=1, source_target_pairs={{0,6},{1,7},{2,8},{3,9},{4,10},{5,11},{6,12},{7,13},{8,14},{9,15},... | collective-permute-start | bytes 147464 | tf_op jit(solution)/shard_map/ppermute | solution.py:412
  108.9 3.5 %collective-permute-start.28 = (bf16[24,1024]{1,0:T(8,128)(2,1)S(1)}, bf16[24,1024]{1,0:T(8,128)(2,1)S(1)}, u32[]{:S(2)}, u32[]{:S(2)}) collective-permute-start(bf16[24,1024]{1,0:T(8,128)(2,1)S(1)} %collective-permute-done.22.refs_5_), channel_id=1, source_target_pairs={{0,1},{1,0},{2,3},{3,2},{4,5},{5,4},{6,7},{7,6},{8,9},{9,8},{10,11... | collective-permute-start | bytes 147464 | tf_op jit(solution)/shard_map/ppermute | solution.py:406
  111.5 1.8 %collective-permute-start.23 = (bf16[3,24,1024]{2,1,0:T(8,128)(2,1)S(1)}, bf16[3,24,1024]{2,1,0:T(8,128)(2,1)S(1)}, u32[]{:S(2)}, u32[]{:S(2)}) collective-permute-start(bf16[3,24,1024]{2,1,0:T(8,128)(2,1)S(1)} %shard_map.254.refs_0_), channel_id=1, source_target_pairs={{0,1},{1,0},{2,3},{3,2},{4,5},{5,4},{6,7},{7,6},{8,9},{9,8},{10,11... | collective-permute-start | bytes 442376 | tf_op jit(solution)/shard_map/ppermute | solution.py:406
  111.6 1.8 %collective-permute-start.24 = (bf16[3,24,1024]{2,1,0:T(8,128)(2,1)S(1)}, bf16[3,24,1024]{2,1,0:T(8,128)(2,1)S(1)}, u32[]{:S(2)}, u32[]{:S(2)}) collective-permute-start(bf16[3,24,1024]{2,1,0:T(8,128)(2,1)S(1)} %collective-permute-done.18.refs_1_), channel_id=1, source_target_pairs={{0,1},{1,0},{2,3},{3,2},{4,5},{5,4},{6,7},{7,6},{8,9},{9,8},{10,11... | collective-permute-start | bytes 442376 | tf_op jit(solution)/shard_map/ppermute | solution.py:406
  112.4 1.4 collective-permute-start.25
  112.8 1.4 collective-permute-start.26
  112.9 1.4 collective-permute-start.27
  117.8 2.4 %collective-permute-start.29 = (bf16[384,1024]{1,0:T(8,128)(2,1)S(1)}, bf16[384,1024]{1,0:T(8,128)(2,1)S(1)}, u32[]{:S(2)}, u32[]{:S(2)}) collective-permute-start(bf16[384,1024]{1,0:T(8,128)(2,1)S(1)} %get-tuple-element.54), channel_id=1, source_target_pairs={{0,1},{1,0},{2,3},{3,2},{4,5},{5,4},{6,7},{7,6},{8,9},{9,8},{10,11... | collective-permute-start | bytes 2359304 | tf_op jit(solution)/shard_map/ppermute | solution.py:406
  120.3 5.2 %collective-permute-start.32 = (bf16[3,24,1024]{2,1,0:T(8,128)(2,1)S(1)}, bf16[3,24,1024]{2,1,0:T(8,128)(2,1)S(1)}, u32[]{:S(2)}, u32[]{:S(2)}) collective-permute-start(bf16[3,24,1024]{2,1,0:T(8,128)(2,1)S(1)} %get-tuple-element.59), channel_id=1, source_target_pairs={{0,30},{1,31},{2,0},{3,1},{4,2},{5,3},{6,4},{7,5},{8,6},{9,7},{10,... | collective-permute-start | bytes 442376 | tf_op jit(solution)/shard_map/ppermute | solution.py:412
  120.5 6.7 %collective-permute-start.30 = (bf16[3,24,1024]{2,1,0:T(8,128)(2,1)S(1)}, bf16[3,24,1024]{2,1,0:T(8,128)(2,1)S(1)}, u32[]{:S(2)}, u32[]{:S(2)}) collective-permute-start(bf16[3,24,1024]{2,1,0:T(8,128)(2,1)S(1)} %get-tuple-element.57), channel_id=1, source_target_pairs={{0,2},{1,3},{2,4},{3,5},{4,6},{5,7},{6,8},{7,9},{8,10},{9,11},{10,... | collective-permute-start | bytes 442376 | tf_op jit(solution)/shard_map/ppermute | solution.py:412
  125.6 8.3 %collective-permute-start.33 = (bf16[3,24,1024]{2,1,0:T(8,128)(2,1)S(1)}, bf16[3,24,1024]{2,1,0:T(8,128)(2,1)S(1)}, u32[]{:S(2)}, u32[]{:S(2)}) collective-permute-start(bf16[3,24,1024]{2,1,0:T(8,128)(2,1)S(1)} %shard_map.259), channel_id=1, source_target_pairs={{0,30},{1,31},{2,0},{3,1},{4,2},{5,3},{6,4},{7,5},{8,6},{9,7},{10,... | collective-permute-start | bytes 442376 | tf_op jit(solution)/shard_map/ppermute | solution.py:412
  127.1 7.1 %collective-permute-start.31 = (bf16[3,24,1024]{2,1,0:T(8,128)(2,1)S(1)}, bf16[3,24,1024]{2,1,0:T(8,128)(2,1)S(1)}, u32[]{:S(2)}, u32[]{:S(2)}) collective-permute-start(bf16[3,24,1024]{2,1,0:T(8,128)(2,1)S(1)} %shard_map.258), channel_id=1, source_target_pairs={{0,2},{1,3},{2,4},{3,5},{4,6},{5,7},{6,8},{7,9},{8,10},{9,11},{10,... | collective-permute-start | bytes 442376 | tf_op jit(solution)/shard_map/ppermute | solution.py:412
  127.3 6.6 %collective-permute-start.34 = (bf16[24,1024]{1,0:T(8,128)(2,1)S(1)}, bf16[24,1024]{1,0:T(8,128)(2,1)S(1)}, u32[]{:S(2)}, u32[]{:S(2)}) collective-permute-start(bf16[24,1024]{1,0:T(8,128)(2,1)S(1)} %get-tuple-element.60), channel_id=1, source_target_pairs={{0,6},{1,7},{2,8},{3,9},{4,10},{5,11},{6,12},{7,13},{8,14},{9,15},... | collective-permute-start | bytes 147464 | tf_op jit(solution)/shard_map/ppermute | solution.py:412
  134.3 10.2 %collective-permute-start.35 = (bf16[24,1024]{1,0:T(8,128)(2,1)S(1)}, bf16[24,1024]{1,0:T(8,128)(2,1)S(1)}, u32[]{:S(2)}, u32[]{:S(2)}) collective-permute-start(bf16[24,1024]{1,0:T(8,128)(2,1)S(1)} %get-tuple-element.62), channel_id=1, source_target_pairs={{0,10},{1,11},{2,12},{3,13},{4,14},{5,15},{6,16},{7,17},{8,18},{9,... | collective-permute-start | bytes 147464 | tf_op jit(solution)/shard_map/ppermute | solution.py:412
  135.1 11.1 %collective-permute-start.36 = (bf16[24,1024]{1,0:T(8,128)(2,1)S(1)}, bf16[24,1024]{1,0:T(8,128)(2,1)S(1)}, u32[]{:S(2)}, u32[]{:S(2)}) collective-permute-start(bf16[24,1024]{1,0:T(8,128)(2,1)S(1)} %get-tuple-element.63), channel_id=1, source_target_pairs={{0,22},{1,23},{2,24},{3,25},{4,26},{5,27},{6,28},{7,29},{8,30},{9,... | collective-permute-start | bytes 147464 | tf_op jit(solution)/shard_map/ppermute | solution.py:412
  146.3 4.0 %collective-permute-start.37 = (f32[12,1024]{1,0:T(8,128)S(1)}, f32[12,1024]{1,0:T(8,128)S(1)}, u32[]{:S(2)}, u32[]{:S(2)}) collective-permute-start(f32[12,1024]{1,0:T(8,128)S(1)} %get-tuple-element.65), channel_id=1, source_target_pairs={{0,1},{1,0},{2,3},{3,2},{4,5},{5,4},{6,7},{7,6},{8,9},{9,8},{10,11... | collective-permute-start | bytes 147464 | tf_op jit(solution)/shard_map/ppermute | solution.py:406

commit v5 on v4

--- a/solution.py
+++ b/solution.py
@@ -266,23 +266,14 @@
     return (gate * jax.nn.sigmoid(gate) * up).astype(BF16)
 
 
-def branch_kernel(*refs):
-    xs, ys = refs[:6], refs[6:12]
-    (a_ref, b_ref, eg_ref, eu_ref, ed_ref, dg_ref, du_ref, dd_ref, bw_ref,
-     send_ref, hidden_ref, made, placer_ref, gains_ref, table, x_scr, y_scr) = refs[12:]
+def route_kernel(a_ref, b_ref, picker_ref, placer_ref, weight_ref, table):
     c = core()
     me = lax.axis_index("ep").astype(F32)
     home = lax.div(lax.axis_index("ep"), 2)
     nz = a_ref.shape[0]
-    rows, h = x_scr.shape
+    slots, rows = picker_ref.shape
     r2 = rows // nz
     r = r2 // 2
-    slots = 2 * nz * CAP
-    at = pl.ds(pl.multiple_of(c * h, h), h)
-    to = pl.ds(pl.multiple_of((1 - c) * h, h), h)
-    collect(xs, x_scr)
-    collect(ys, y_scr)
-    x, y = x_scr[...], y_scr[...]
     low = lax.broadcasted_iota(jnp.int32, (r2, 128), 0) < r
     for k, offset in enumerate(offsets(nz)):
         z = lax.rem(home + offset, nz)
@@ -309,8 +300,24 @@
     rank = dot(earlier, jnp.broadcast_to(hit, (rows, 128)).astype(BF16))
     slot = block.astype(F32) * CAP + rank
     chosen = jnp.where((slot == lane.astype(F32)) & (hit > 0.5), 1.0, 0.0)
-    picker = chosen.T[:slots].astype(BF16)
-    placer = chosen[:, :slots].astype(BF16)
+    picker_ref[...] = chosen.T[:slots].astype(BF16)
+    placer_ref[...] = chosen[:, :slots].astype(BF16)
+    weight_ref[...] = jnp.broadcast_to(weight, weight_ref.shape)
+
+
+def branch_kernel(*refs):
+    xs, ys = refs[:6], refs[6:12]
+    (picker_ref, placer_ref, weight_ref, eg_ref, eu_ref, ed_ref, dg_ref, du_ref, dd_ref, bw_ref,
+     send_ref, hidden_ref, made, gains_ref, x_scr, y_scr) = refs[12:]
+    c = core()
+    rows, h = x_scr.shape
+    at = pl.ds(pl.multiple_of(c * h, h), h)
+    to = pl.ds(pl.multiple_of((1 - c) * h, h), h)
+    collect(xs, x_scr)
+    collect(ys, y_scr)
+    x, y = x_scr[...], y_scr[...]
+    lane = lax.broadcasted_iota(jnp.int32, (rows, 128), 1)
+    picker, weight = picker_ref[...], weight_ref[:, 0:1]
     px = dot(picker, x).astype(BF16)
     py = dot(picker, y).astype(BF16)
     gate = dot(px, eg_ref[0, at, :]) + dot(py, eg_ref[0, to, :])
@@ -324,10 +331,9 @@
     logit = logit + jnp.sum(y.astype(F32) * bw_ref[:, to].astype(F32), axis=1, keepdims=True)
     sig = jax.nn.sigmoid(logit)
     hidden_ref[...] = hidden
-    placer_ref[...] = placer
     gains_ref[...] = jnp.where(lane == 0, sig, weight)
     part = dot(hidden, dd_ref[:, to]) * sig
-    send_ref[...] = (part + dot(placer, made[:, to]) * weight).astype(BF16)
+    send_ref[...] = (part + dot(placer_ref[...], made[:, to]) * weight).astype(BF16)
 
 
 def rest_kernel(hidden_ref, made_ref, placer_ref, gains_ref, dd_ref, keep_ref):
@@ -460,13 +466,17 @@
         scratch=[(state_matrix.shape, F32)], sems=r,
         out_specs=[pl.BlockSpec(memory_space=pltpu.HBM), pl.BlockSpec(memory_space=pltpu.VMEM)])
     xs, ys = gather(chunk, token)
-    send, hidden, made, placer, scales = call(
+    picker, placer, weight = call(
+        route_kernel,
+        [((n * CAP, n * r), BF16), ((n * r, n * CAP), BF16), ((n * r, 128), F32)],
+        (a, b), scratch=[((4, n * r, 128), F32)])
+    send, hidden, made, scales = call(
         branch_kernel,
         [((n * r, h), BF16), ((n * r, dense_down.shape[0]), BF16), ((n * CAP, d), BF16),
-         ((n * r, n * CAP), BF16), ((n * r, 128), F32)],
-        (*xs, *ys, a, b, expert_gate, expert_up, expert_down, dense_gate, dense_up, dense_down,
-         branch_weight.reshape(1, d)),
-        scratch=[((4, n * r, 128), F32), ((n * r, h), BF16), ((n * r, h), BF16)], vmem=32)
+         ((n * r, 128), F32)],
+        (*xs, *ys, picker, placer, weight, expert_gate, expert_up, expert_down, dense_gate,
+         dense_up, dense_down, branch_weight.reshape(1, d)),
+        scratch=[((n * r, h), BF16), ((n * r, h), BF16)], vmem=32)
     got = swap(send)
     part, = call(rest_kernel, [((n * r, h), F32)], (hidden, made, placer, scales, dense_down),
                  flops=400000000)
@@ -474,8 +484,8 @@
     own, one, back, up, down, last = call(
         spread_kernel, [(three, F32)] * 3 + [(three, BF16)] * 2 + [(tile, BF16)],
         (part.reshape((nz,) + tile), got.reshape((nz,) + tile)))
+    last = shift(last, 8 - FAR)
     up, down = shift(up, 1), shift(down, -1)
-    last = shift(last, 8 - FAR)
     up, = call(relay_kernel, [(three, BF16)], (one, up))
     down, = call(relay_kernel, [(three, BF16)], (back, down))
     up, down = shift(up, 1), shift(down, -1)

time: 151 us -> 151 us (level)
  waiting for transfers between devices: 39.1 us -> 45.7 us
  blocking collectives: 22.4 us -> 18.1 us
  starting transfers between devices: 67.6 us -> 64.9 us
    ppermute x21, waiting for transfers between devices: 32 us -> 39 us  [shift(): lax.ppermute(x, 'ep', [(2 * z + c, 2 * ((z + offset) % nz) + c) for z in...]
    all_to_all x1, blocking collectives: 22.4 us -> 18.1 us  [exchange(): return lax.all_to_all(x, 'ep', 0, 0, axis_index_groups=groups)]
    ppermute x21, starting transfers between devices: 42.2 us -> 38.5 us  [shift(): lax.ppermute(x, 'ep', [(2 * z + c, 2 * ((z + offset) % nz) + c) for z in...]
    pallas_call x17 -> x18, Pallas kernels: 21 us -> 21.1 us  [call(): pl.pallas_call(kernel, out_shape=[pltpu.VMEM(s, d) if i in held and (not...]
  transfers between devices with their start and end apart: 38 -> 38, of which waited for: 24 -> 23; matrix products, arithmetic and copies ran while one was open for 0% -> 0% of each run, Pallas kernels for 8% -> 8%
where the time goes in v5:
time: 151 us
  starting transfers between devices  64.9 us (43%)
  waiting for transfers between devices  45.7 us (30%)
  Pallas kernels  21.1 us (14%)
  blocking collectives  18.1 us (12%)
    ppermute x21, waiting for transfers between devices, shift(): lax.ppermute(x, 'ep', [(2 * z + c, 2 * ((z + offset) % nz) + c) for z in...  39 us
    ppermute x21, starting transfers between devices, shift(): lax.ppermute(x, 'ep', [(2 * z + c, 2 * ((z + offset) % nz) + c) for z in...  38.5 us
    ppermute x17, starting transfers between devices, swap(): return lax.ppermute(x, 'ep', pairs)  26.4 us
    pallas_call x18, Pallas kernels, call(): pl.pallas_call(kernel, out_shape=[pltpu.VMEM(s, d) if i in held and (not...  21.1 us
    all_to_all x1, blocking collectives, exchange(): return lax.all_to_all(x, 'ep', 0, 0, axis_index_groups=groups)  18.1 us
    ppermute x17, waiting for transfers between devices, swap(): return lax.ppermute(x, 'ep', pairs)  6.63 us
  transfers between devices with their start and end apart: 38, of which 23 were waited for; matrix products, arithmetic and copies ran while one was open for 0% of the time, Pallas kernels for 8%

profile of v5, /device:TPU:69, one launch (start us, length us, event | category | flops | bytes accessed | tf_op | source)
XLA Modules:
  0.0 150.7 jit_solution(8035265908166442330)
XLA Ops:
  0.6 10.0 %collective-permute-start = (bf16[12,2048]{1,0:T(8,128)(2,1)}, bf16[12,2048]{1,0:T(8,128)(2,1)S(1)}, u32[]{:S(2)}, u32[]{:S(2)}) collective-permute-start(bf16[12,2048]{1,0:T(8,128)(2,1)} %resid_ref.1), channel_id=1, source_target_pairs={{0,1},{1,0},{2,3},{3,2},{4,5},{5,4},{6,7},{7,6},{8,9},{9,8},{10,11... | collective-permute-start | bytes 147464 | tf_op jit(solution)/shard_map/ppermute | solution.py:412
  10.6 1.0 shard_map.246
  11.9 6.1 %collective-permute-start.2 = (bf16[24,1024]{1,0:T(8,128)(2,1)S(1)}, bf16[24,1024]{1,0:T(8,128)(2,1)S(1)}, u32[]{:S(2)}, u32[]{:S(2)}) collective-permute-start(bf16[24,1024]{1,0:T(8,128)(2,1)S(1)} %shard_map.247.a_ref), channel_id=1, source_target_pairs={{0,22},{1,23},{2,24},{3,25},{4,26},{5,27},{6,28},{7,29},{8,30},{9,... | collective-permute-start | bytes 147464 | tf_op jit(solution)/shard_map/ppermute | solution.py:418
  18.3 5.1 %shard_map.248 = (f32[12,8]{1,0:T(8,128)S(1)}, f32[12,8]{1,0:T(8,128)S(1)}, f32[8,12]{1,0:T(8,128)}, bf16[8,128]{1,0:T(8,128)(2,1)S(1)}, bf16[128,2048]{1,0:T(8,...) custom-call(bf16[12,2048]{1,0:T(8,128)(2,1)S(1)} %get-tuple-element.39.own_ref.normed_ref, ...), custom_call_target="tpu_custom_call" | custom-call | flops 1000000 | bytes 1000000 | tf_op jit(solution)/shard_map/pallas_call | solution.py:25
  23.4 7.7 %collective-permute-done.1.b_ref = bf16[24,1024]{1,0:T(8,128)(2,1)S(1)} collective-permute-done((bf16[24,1024]{1,0:T(8,128)(2,1)S(1)}, bf16[24,1024]{1,0:T(8,128)(2,1)S(1)}, u32[]{:S(2)}, u32[]{:S(2)}) %collective-permute-start.1) | collective-permute-done | bytes 49184 | tf_op jit(solution)/shard_map/ppermute | solution.py:418
  31.2 1.4 collective-permute-start.3
  32.7 3.3 %collective-permute-done.4.refs_2_ = bf16[3,24,1024]{2,1,0:T(8,128)(2,1)S(1)} collective-permute-done((bf16[3,24,1024]{2,1,0:T(8,128)(2,1)S(1)}, bf16[3,24,1024]{2,1,0:T(8,128)(2,1)S(1)}, u32[]{:S(2)}, u32[]{:S(2)}) %collective-permute-start.4) | collective-permute-done | bytes 147488 | tf_op jit(solution)/shard_map/ppermute | solution.py:418
  36.0 1.4 collective-permute-start.6
  37.5 2.0 %collective-permute-start.7 = (bf16[24,1024]{1,0:T(8,128)(2,1)S(1)}, bf16[24,1024]{1,0:T(8,128)(2,1)S(1)}, u32[]{:S(2)}, u32[]{:S(2)}) collective-permute-start(bf16[24,1024]{1,0:T(8,128)(2,1)S(1)} %collective-permute-done.1.b_ref), channel_id=1, source_target_pairs={{0,6},{1,7},{2,8},{3,9},{4,10},{5,11},{6,12},{7,13},{8,14},{9,15},... | collective-permute-start | bytes 147464 | tf_op jit(solution)/shard_map/ppermute | solution.py:418
  39.5 4.0 %collective-permute-done.7.refs_5_ = bf16[24,1024]{1,0:T(8,128)(2,1)S(1)} collective-permute-done((bf16[24,1024]{1,0:T(8,128)(2,1)S(1)}, bf16[24,1024]{1,0:T(8,128)(2,1)S(1)}, u32[]{:S(2)}, u32[]{:S(2)}) %collective-permute-start.7) | collective-permute-done | bytes 49184 | tf_op jit(solution)/shard_map/ppermute | solution.py:418
  43.6 3.3 %collective-permute-start.13 = (bf16[24,1024]{1,0:T(8,128)(2,1)S(1)}, bf16[24,1024]{1,0:T(8,128)(2,1)S(1)}, u32[]{:S(2)}, u32[]{:S(2)}) collective-permute-start(bf16[24,1024]{1,0:T(8,128)(2,1)S(1)} %collective-permute-done.7.refs_5_), channel_id=1, source_target_pairs={{0,1},{1,0},{2,3},{3,2},{4,5},{5,4},{6,7},{7,6},{8,9},{9,8},{10,11... | collective-permute-start | bytes 147464 | tf_op jit(solution)/shard_map/ppermute | solution.py:412
  46.8 0.5 collective-permute-start.10
  48.6 0.5 collective-permute-done.9.refs_7_
  49.7 0.6 shard_map.250
  50.2 18.1 %all_to_all.5.a_ref = bf16[16,32,128]{2,1,0:T(8,128)(2,1)S(1)} all-to-all(bf16[16,32,128]{2,1,0:T(8,128)(2,1)S(1)} %shard_map.250), channel_id=1, replica_groups={{0,2,4,6,8,10,12,14,16,18,20,22,24,26,28,30},{1,3,5,7,9,11,13,15,17,19,..., dimensions={0} | all-to-all | bytes 262144 | tf_op jit(solution)/shard_map/all_to_all | solution.py:415
  68.4 3.3 %collective-permute-start.14 = (bf16[16,32,128]{2,1,0:T(8,128)(2,1)S(1)}, bf16[16,32,128]{2,1,0:T(8,128)(2,1)S(1)}, u32[]{:S(2)}, u32[]{:S(2)}) collective-permute-start(bf16[16,32,128]{2,1,0:T(8,128)(2,1)S(1)} %all_to_all.5.a_ref), channel_id=1, source_target_pairs={{0,1},{1,0},{2,3},{3,2},{4,5},{5,4},{6,7},{7,6},{8,9},{9,8},{10,11... | collective-permute-start | bytes 393224 | tf_op jit(solution)/shard_map/ppermute | solution.py:412
  71.6 1.0 collective-permute-done.14.b_ref
  72.6 4.5 %shard_map.251 = (f32[12,2048]{1,0:T(8,128)S(1)}, bf16[12,1024]{1,0:T(8,128)(2,1)S(1)}, bf16[12,1024]{1,0:T(8,128)(2,1)S(1)}, f32[12,8,128]{2,1,0:T(8,128)}, f32...) custom-call(bf16[16,32,128]{2,1,0:T(8,128)(2,1)S(1)} %all_to_all.5.a_ref, ...), custom_call_target="tpu_custom_call" | custom-call | flops 1000000 | bytes 1000000 | tf_op jit(solution)/shard_map/pallas_call | solution.py:25
  77.1 0.5 collective-permute-start.15
  77.6 0.9 collective-permute-done.15.got_ref
  78.5 2.2 %collective-permute-start.17 = (bf16[24,1024]{1,0:T(8,128)(2,1)S(1)}, bf16[24,1024]{1,0:T(8,128)(2,1)S(1)}, u32[]{:S(2)}, u32[]{:S(2)}) collective-permute-start(bf16[24,1024]{1,0:T(8,128)(2,1)S(1)} %shard_map.252.a_ref), channel_id=1, source_target_pairs={{0,22},{1,23},{2,24},{3,25},{4,26},{5,27},{6,28},{7,29},{8,30},{9,... | collective-permute-start | bytes 147464 | tf_op jit(solution)/shard_map/ppermute | solution.py:418
  80.7 4.2 %collective-permute-start.16 = (bf16[24,1024]{1,0:T(8,128)(2,1)S(1)}, bf16[24,1024]{1,0:T(8,128)(2,1)S(1)}, u32[]{:S(2)}, u32[]{:S(2)}) collective-permute-start(bf16[24,1024]{1,0:T(8,128)(2,1)S(1)} %shard_map.252.a_ref), channel_id=1, source_target_pairs={{0,10},{1,11},{2,12},{3,13},{4,14},{5,15},{6,16},{7,17},{8,18},{9,... | collective-permute-start | bytes 147464 | tf_op jit(solution)/shard_map/ppermute | solution.py:418
  84.9 4.7 %shard_map.253 = (f32[12,8,128,128]{3,2,1,0:T(8,128)}, f32[8,128]{1,0:T(8,128)S(1)}) custom-call(f32[12,8]{1,0:T(8,128)S(1)} %get-tuple-element.43.keep_ref, f32[8,16,128]{2,1,0:T(8,128)S(1)} %get-tuple-element.49.keys_ref, f32[128,128]{1,0:T(8,128)S(1)} %get-tuple-element.50.wvt_ref, f32[12,8,128,128]{3,2,1,0:T(8,128)S(1)} %get-tuple-element.45.m_ref), custom_call_target="tpu_custom_call" | custom-call | flops 1000000 | bytes 1000000 | tf_op jit(solution)/shard_map/pallas_call | solution.py:25
  89.6 3.3 %collective-permute-done.16.b_ref = bf16[24,1024]{1,0:T(8,128)(2,1)S(1)} collective-permute-done((bf16[24,1024]{1,0:T(8,128)(2,1)S(1)}, bf16[24,1024]{1,0:T(8,128)(2,1)S(1)}, u32[]{:S(2)}, u32[]{:S(2)}) %collective-permute-start.16) | collective-permute-done | bytes 49184 | tf_op jit(solution)/shard_map/ppermute | solution.py:418
  93.3 1.2 collective-permute-start.18
  94.5 3.4 %collective-permute-done.19.refs_2_ = bf16[3,24,1024]{2,1,0:T(8,128)(2,1)S(1)} collective-permute-done((bf16[3,24,1024]{2,1,0:T(8,128)(2,1)S(1)}, bf16[3,24,1024]{2,1,0:T(8,128)(2,1)S(1)}, u32[]{:S(2)}, u32[]{:S(2)}) %collective-permute-start.19) | collective-permute-done | bytes 147488 | tf_op jit(solution)/shard_map/ppermute | solution.py:418
  97.9 1.1 collective-permute-start.21
  99.4 3.6 %collective-permute-start.22 = (bf16[24,1024]{1,0:T(8,128)(2,1)S(1)}, bf16[24,1024]{1,0:T(8,128)(2,1)S(1)}, u32[]{:S(2)}, u32[]{:S(2)}) collective-permute-start(bf16[24,1024]{1,0:T(8,128)(2,1)S(1)} %collective-permute-done.16.b_ref), channel_id=1, source_target_pairs={{0,6},{1,7},{2,8},{3,9},{4,10},{5,11},{6,12},{7,13},{8,14},{9,15},... | collective-permute-start | bytes 147464 | tf_op jit(solution)/shard_map/ppermute | solution.py:418
  102.9 3.1 %collective-permute-done.22.refs_5_ = bf16[24,1024]{1,0:T(8,128)(2,1)S(1)} collective-permute-done((bf16[24,1024]{1,0:T(8,128)(2,1)S(1)}, bf16[24,1024]{1,0:T(8,128)(2,1)S(1)}, u32[]{:S(2)}, u32[]{:S(2)}) %collective-permute-start.22) | collective-permute-done | bytes 49184 | tf_op jit(solution)/shard_map/ppermute | solution.py:418
  106.1 2.4 %collective-permute-start.28 = (bf16[24,1024]{1,0:T(8,128)(2,1)S(1)}, bf16[24,1024]{1,0:T(8,128)(2,1)S(1)}, u32[]{:S(2)}, u32[]{:S(2)}) collective-permute-start(bf16[24,1024]{1,0:T(8,128)(2,1)S(1)} %collective-permute-done.22.refs_5_), channel_id=1, source_target_pairs={{0,1},{1,0},{2,3},{3,2},{4,5},{5,4},{6,7},{7,6},{8,9},{9,8},{10,11... | collective-permute-start | bytes 147464 | tf_op jit(solution)/shard_map/ppermute | solution.py:412
  108.4 0.5 collective-permute-start.25
  111.3 3.0 %shard_map.256 = (bf16[384,1024]{1,0:T(8,128)(2,1)S(1)}, bf16[384,256]{1,0:T(8,128)(2,1)S(1)}, bf16[64,2048]{1,0:T(8,128)(2,1)S(1)}, f32[384,128]{1,0:T(8,128)S(1)}) custom-call(bf16[3,24,1024]{2,1,0:T(8,128)(2,1)S(1)} %shard_map.254.refs_0_, bf16[3,24,1024]{2,1,0:T(8,128)(2,1)S(1)} %collective-permute-done.18.refs_1_, ...), custom_call_target="tpu_custom_call" | custom-call | flops 1000000 | bytes 1000000 | tf_op jit(solution)/shard_map/pallas_call | solution.py:25
  114.8 0.6 shard_map.257
  115.4 1.4 collective-permute-done.29
  116.9 1.4 collective-permute-start.30
  118.3 1.3 collective-permute-start.32
  119.6 3.6 %collective-permute-done.30.got_ref = bf16[3,24,1024]{2,1,0:T(8,128)(2,1)S(1)} collective-permute-done((bf16[3,24,1024]{2,1,0:T(8,128)(2,1)S(1)}, bf16[3,24,1024]{2,1,0:T(8,128)(2,1)S(1)}, u32[]{:S(2)}, u32[]{:S(2)}) %collective-permute-start.30) | collective-permute-done | bytes 147488 | tf_op jit(solution)/shard_map/ppermute | solution.py:418
  123.6 0.6 collective-permute-done.32.got_ref
  124.2 2.0 %collective-permute-start.33 = (bf16[3,24,1024]{2,1,0:T(8,128)(2,1)S(1)}, bf16[3,24,1024]{2,1,0:T(8,128)(2,1)S(1)}, u32[]{:S(2)}, u32[]{:S(2)}) collective-permute-start(bf16[3,24,1024]{2,1,0:T(8,128)(2,1)S(1)} %shard_map.260), channel_id=1, source_target_pairs={{0,30},{1,31},{2,0},{3,1},{4,2},{5,3},{6,4},{7,5},{8,6},{9,7},{10,... | collective-permute-start | bytes 442376 | tf_op jit(solution)/shard_map/ppermute | solution.py:418
  126.2 1.5 collective-permute-start.34
  127.7 5.1 %collective-permute-done.34.last_ref = bf16[24,1024]{1,0:T(8,128)(2,1)S(1)} collective-permute-done((bf16[24,1024]{1,0:T(8,128)(2,1)S(1)}, bf16[24,1024]{1,0:T(8,128)(2,1)S(1)}, u32[]{:S(2)}, u32[]{:S(2)}) %collective-permute-start.34) | collective-permute-done | bytes 49184 | tf_op jit(solution)/shard_map/ppermute | solution.py:418
  132.9 3.2 %collective-permute-start.35 = (bf16[24,1024]{1,0:T(8,128)(2,1)S(1)}, bf16[24,1024]{1,0:T(8,128)(2,1)S(1)}, u32[]{:S(2)}, u32[]{:S(2)}) collective-permute-start(bf16[24,1024]{1,0:T(8,128)(2,1)S(1)} %get-tuple-element.66), channel_id=1, source_target_pairs={{0,10},{1,11},{2,12},{3,13},{4,14},{5,15},{6,16},{7,17},{8,18},{9,... | collective-permute-start | bytes 147464 | tf_op jit(solution)/shard_map/ppermute | solution.py:418
  136.1 4.3 %collective-permute-start.36 = (bf16[24,1024]{1,0:T(8,128)(2,1)S(1)}, bf16[24,1024]{1,0:T(8,128)(2,1)S(1)}, u32[]{:S(2)}, u32[]{:S(2)}) collective-permute-start(bf16[24,1024]{1,0:T(8,128)(2,1)S(1)} %get-tuple-element.67), channel_id=1, source_target_pairs={{0,22},{1,23},{2,24},{3,25},{4,26},{5,27},{6,28},{7,29},{8,30},{9,... | collective-permute-start | bytes 147464 | tf_op jit(solution)/shard_map/ppermute | solution.py:418
  140.4 1.5 collective-permute-done.35.a_ref
  141.9 3.2 %collective-permute-done.36.b_ref = bf16[24,1024]{1,0:T(8,128)(2,1)S(1)} collective-permute-done((bf16[24,1024]{1,0:T(8,128)(2,1)S(1)}, bf16[24,1024]{1,0:T(8,128)(2,1)S(1)}, u32[]{:S(2)}, u32[]{:S(2)}) %collective-permute-start.36) | collective-permute-done | bytes 49184 | tf_op jit(solution)/shard_map/ppermute | solution.py:418
  145.2 3.9 %collective-permute-start.37 = (f32[12,1024]{1,0:T(8,128)S(1)}, f32[12,1024]{1,0:T(8,128)S(1)}, u32[]{:S(2)}, u32[]{:S(2)}) collective-permute-start(f32[12,1024]{1,0:T(8,128)S(1)} %get-tuple-element.69), channel_id=1, source_target_pairs={{0,1},{1,0},{2,3},{3,2},{4,5},{5,4},{6,7},{7,6},{8,9},{9,8},{10,11... | collective-permute-start | bytes 147464 | tf_op jit(solution)/shard_map/ppermute | solution.py:412
  149.1 0.9 collective-permute-done.37.got_ref
  150.0 0.7 shard_map.263
  (66 shorter events, 6.7 us)
Async XLA Ops:
  0.6 11.1 %collective-permute-start = (bf16[12,2048]{1,0:T(8,128)(2,1)}, bf16[12,2048]{1,0:T(8,128)(2,1)S(1)}, u32[]{:S(2)}, u32[]{:S(2)}) collective-permute-start(bf16[12,2048]{1,0:T(8,128)(2,1)} %resid_ref.1), channel_id=1, source_target_pairs={{0,1},{1,0},{2,3},{3,2},{4,5},{5,4},{6,7},{7,6},{8,9},{9,8},{10,11... | collective-permute-start | bytes 147464 | tf_op jit(solution)/shard_map/ppermute | solution.py:412
  11.9 11.5 %collective-permute-start.2 = (bf16[24,1024]{1,0:T(8,128)(2,1)S(1)}, bf16[24,1024]{1,0:T(8,128)(2,1)S(1)}, u32[]{:S(2)}, u32[]{:S(2)}) collective-permute-start(bf16[24,1024]{1,0:T(8,128)(2,1)S(1)} %shard_map.247.a_ref), channel_id=1, source_target_pairs={{0,22},{1,23},{2,24},{3,25},{4,26},{5,27},{6,28},{7,29},{8,30},{9,... | collective-permute-start | bytes 147464 | tf_op jit(solution)/shard_map/ppermute | solution.py:418
  17.9 13.2 %collective-permute-start.1 = (bf16[24,1024]{1,0:T(8,128)(2,1)S(1)}, bf16[24,1024]{1,0:T(8,128)(2,1)S(1)}, u32[]{:S(2)}, u32[]{:S(2)}) collective-permute-start(bf16[24,1024]{1,0:T(8,128)(2,1)S(1)} %shard_map.247.a_ref), channel_id=1, source_target_pairs={{0,10},{1,11},{2,12},{3,13},{4,14},{5,15},{6,16},{7,17},{8,18},{9,... | collective-permute-start | bytes 147464 | tf_op jit(solution)/shard_map/ppermute | solution.py:418
  18.3 54.3 %copy-start.6 = (bf16[12,2048]{1,0:T(8,128)(2,1)S(1)}, bf16[12,2048]{1,0:T(8,128)(2,1)}, u32[]{:S(2)}) copy-start(bf16[12,2048]{1,0:T(8,128)(2,1)} %resid_ref.1) | copy-start | bytes 147460
  18.3 54.3 %copy-start.7 = (f32[12,8,128]{2,1,0:T(8,128)S(1)}, f32[12,8,128]{2,1,0:T(8,128)}, u32[]{:S(2)}) copy-start(f32[12,8,128]{2,1,0:T(8,128)} %norm_ref.1) | copy-start | bytes 147460
  31.1 4.9 %collective-permute-start.4 = (bf16[3,24,1024]{2,1,0:T(8,128)(2,1)S(1)}, bf16[3,24,1024]{2,1,0:T(8,128)(2,1)S(1)}, u32[]{:S(2)}, u32[]{:S(2)}) collective-permute-start(bf16[3,24,1024]{2,1,0:T(8,128)(2,1)S(1)} %shard_map.249.refs_0_), channel_id=1, source_target_pairs={{0,30},{1,31},{2,0},{3,1},{4,2},{5,3},{6,4},{7,5},{8,6},{9,7},{10,... | collective-permute-start | bytes 442376 | tf_op jit(solution)/shard_map/ppermute | solution.py:418
  31.2 6.2 %collective-permute-start.3 = (bf16[3,24,1024]{2,1,0:T(8,128)(2,1)S(1)}, bf16[3,24,1024]{2,1,0:T(8,128)(2,1)S(1)}, u32[]{:S(2)}, u32[]{:S(2)}) collective-permute-start(bf16[3,24,1024]{2,1,0:T(8,128)(2,1)S(1)} %shard_map.249.refs_0_), channel_id=1, source_target_pairs={{0,2},{1,3},{2,4},{3,5},{4,6},{5,7},{6,8},{7,9},{8,10},{9,11},{10,... | collective-permute-start | bytes 442376 | tf_op jit(solution)/shard_map/ppermute | solution.py:418
  36.0 12.0 %collective-permute-start.6 = (bf16[3,24,1024]{2,1,0:T(8,128)(2,1)S(1)}, bf16[3,24,1024]{2,1,0:T(8,128)(2,1)S(1)}, u32[]{:S(2)}, u32[]{:S(2)}) collective-permute-start(bf16[3,24,1024]{2,1,0:T(8,128)(2,1)S(1)} %collective-permute-done.4.refs_2_), channel_id=1, source_target_pairs={{0,30},{1,31},{2,0},{3,1},{4,2},{5,3},{6,4},{7,5},{8,6},{9,7},{10,... | collective-permute-start | bytes 442376 | tf_op jit(solution)/shard_map/ppermute | solution.py:418
  37.4 10.8 %collective-permute-start.5 = (bf16[3,24,1024]{2,1,0:T(8,128)(2,1)S(1)}, bf16[3,24,1024]{2,1,0:T(8,128)(2,1)S(1)}, u32[]{:S(2)}, u32[]{:S(2)}) collective-permute-start(bf16[3,24,1024]{2,1,0:T(8,128)(2,1)S(1)} %collective-permute-done.3.refs_1_), channel_id=1, source_target_pairs={{0,2},{1,3},{2,4},{3,5},{4,6},{5,7},{6,8},{7,9},{8,10},{9,11},{10,... | collective-permute-start | bytes 442376 | tf_op jit(solution)/shard_map/ppermute | solution.py:418
  37.5 6.1 %collective-permute-start.7 = (bf16[24,1024]{1,0:T(8,128)(2,1)S(1)}, bf16[24,1024]{1,0:T(8,128)(2,1)S(1)}, u32[]{:S(2)}, u32[]{:S(2)}) collective-permute-start(bf16[24,1024]{1,0:T(8,128)(2,1)S(1)} %collective-permute-done.1.b_ref), channel_id=1, source_target_pairs={{0,6},{1,7},{2,8},{3,9},{4,10},{5,11},{6,12},{7,13},{8,14},{9,15},... | collective-permute-start | bytes 147464 | tf_op jit(solution)/shard_map/ppermute | solution.py:418
  43.6 4.2 %collective-permute-start.13 = (bf16[24,1024]{1,0:T(8,128)(2,1)S(1)}, bf16[24,1024]{1,0:T(8,128)(2,1)S(1)}, u32[]{:S(2)}, u32[]{:S(2)}) collective-permute-start(bf16[24,1024]{1,0:T(8,128)(2,1)S(1)} %collective-permute-done.7.refs_5_), channel_id=1, source_target_pairs={{0,1},{1,0},{2,3},{3,2},{4,5},{5,4},{6,7},{7,6},{8,9},{9,8},{10,11... | collective-permute-start | bytes 147464 | tf_op jit(solution)/shard_map/ppermute | solution.py:412
  46.8 1.8 %collective-permute-start.8 = (bf16[3,24,1024]{2,1,0:T(8,128)(2,1)S(1)}, bf16[3,24,1024]{2,1,0:T(8,128)(2,1)S(1)}, u32[]{:S(2)}, u32[]{:S(2)}) collective-permute-start(bf16[3,24,1024]{2,1,0:T(8,128)(2,1)S(1)} %shard_map.249.refs_0_), channel_id=1, source_target_pairs={{0,1},{1,0},{2,3},{3,2},{4,5},{5,4},{6,7},{7,6},{8,9},{9,8},{10,11... | collective-permute-start | bytes 442376 | tf_op jit(solution)/shard_map/ppermute | solution.py:412
  46.8 1.8 %collective-permute-start.10 = (bf16[3,24,1024]{2,1,0:T(8,128)(2,1)S(1)}, bf16[3,24,1024]{2,1,0:T(8,128)(2,1)S(1)}, u32[]{:S(2)}, u32[]{:S(2)}) collective-permute-start(bf16[3,24,1024]{2,1,0:T(8,128)(2,1)S(1)} %collective-permute-done.4.refs_2_), channel_id=1, source_target_pairs={{0,1},{1,0},{2,3},{3,2},{4,5},{5,4},{6,7},{7,6},{8,9},{9,8},{10,11... | collective-permute-start | bytes 442376 | tf_op jit(solution)/shard_map/ppermute | solution.py:412
  47.7 1.4 collective-permute-start.9
  48.1 1.4 collective-permute-start.12
  48.2 1.4 collective-permute-start.11
  68.4 4.2 %collective-permute-start.14 = (bf16[16,32,128]{2,1,0:T(8,128)(2,1)S(1)}, bf16[16,32,128]{2,1,0:T(8,128)(2,1)S(1)}, u32[]{:S(2)}, u32[]{:S(2)}) collective-permute-start(bf16[16,32,128]{2,1,0:T(8,128)(2,1)S(1)} %all_to_all.5.a_ref), channel_id=1, source_target_pairs={{0,1},{1,0},{2,3},{3,2},{4,5},{5,4},{6,7},{7,6},{8,9},{9,8},{10,11... | collective-permute-start | bytes 393224 | tf_op jit(solution)/shard_map/ppermute | solution.py:412
  72.6 38.6 %copy-start.3 = (bf16[1,512,2048]{2,1,0:T(8,128)(2,1)S(1)}, bf16[1,512,2048]{2,1,0:T(8,128)(2,1)}, u32[]{:S(2)}) copy-start(bf16[1,512,2048]{2,1,0:T(8,128)(2,1)} %refs_17_.1) | copy-start | bytes 6291460
  72.6 38.6 %copy-start.5 = (bf16[2048,256]{1,0:T(8,128)(2,1)S(1)}, bf16[2048,256]{1,0:T(8,128)(2,1)}, u32[]{:S(2)}) copy-start(bf16[2048,256]{1,0:T(8,128)(2,1)} %refs_19_.1) | copy-start | bytes 3145732
  77.1 33.1 %copy-start.8 = (bf16[2048]{0:T(1024)(128)(2,1)S(1)}, bf16[2048]{0:T(1024)(128)(2,1)}, u32[]{:S(2)}) copy-start(bf16[2048]{0:T(1024)(128)(2,1)} %param.45) | copy-start | bytes 12292
  77.1 34.1 %copy-start = (bf16[256,2048]{1,0:T(8,128)(2,1)S(1)}, bf16[256,2048]{1,0:T(8,128)(2,1)}, u32[]{:S(2)}) copy-start(bf16[256,2048]{1,0:T(8,128)(2,1)} %dd_ref.1) | copy-start | bytes 3145732
  77.1 34.1 %copy-start.1 = (bf16[1,2048,512]{2,1,0:T(8,128)(2,1)S(1)}, bf16[1,2048,512]{2,1,0:T(8,128)(2,1)}, u32[]{:S(2)}) copy-start(bf16[1,2048,512]{2,1,0:T(8,128)(2,1)} %refs_15_.1) | copy-start | bytes 6291460
  77.1 34.1 %copy-start.2 = (bf16[1,2048,512]{2,1,0:T(8,128)(2,1)S(1)}, bf16[1,2048,512]{2,1,0:T(8,128)(2,1)}, u32[]{:S(2)}) copy-start(bf16[1,2048,512]{2,1,0:T(8,128)(2,1)} %refs_16_.1) | copy-start | bytes 6291460
  77.1 34.1 %copy-start.4 = (bf16[2048,256]{1,0:T(8,128)(2,1)S(1)}, bf16[2048,256]{1,0:T(8,128)(2,1)}, u32[]{:S(2)}) copy-start(bf16[2048,256]{1,0:T(8,128)(2,1)} %refs_18_.1) | copy-start | bytes 3145732
  77.1 1.3 collective-permute-start.15
  78.5 11.0 %collective-permute-start.17 = (bf16[24,1024]{1,0:T(8,128)(2,1)S(1)}, bf16[24,1024]{1,0:T(8,128)(2,1)S(1)}, u32[]{:S(2)}, u32[]{:S(2)}) collective-permute-start(bf16[24,1024]{1,0:T(8,128)(2,1)S(1)} %shard_map.252.a_ref), channel_id=1, source_target_pairs={{0,22},{1,23},{2,24},{3,25},{4,26},{5,27},{6,28},{7,29},{8,30},{9,... | collective-permute-start | bytes 147464 | tf_op jit(solution)/shard_map/ppermute | solution.py:418
  80.7 12.1 %collective-permute-start.16 = (bf16[24,1024]{1,0:T(8,128)(2,1)S(1)}, bf16[24,1024]{1,0:T(8,128)(2,1)S(1)}, u32[]{:S(2)}, u32[]{:S(2)}) collective-permute-start(bf16[24,1024]{1,0:T(8,128)(2,1)S(1)} %shard_map.252.a_ref), channel_id=1, source_target_pairs={{0,10},{1,11},{2,12},{3,13},{4,14},{5,15},{6,16},{7,17},{8,18},{9,... | collective-permute-start | bytes 147464 | tf_op jit(solution)/shard_map/ppermute | solution.py:418
  92.9 5.0 %collective-permute-start.19 = (bf16[3,24,1024]{2,1,0:T(8,128)(2,1)S(1)}, bf16[3,24,1024]{2,1,0:T(8,128)(2,1)S(1)}, u32[]{:S(2)}, u32[]{:S(2)}) collective-permute-start(bf16[3,24,1024]{2,1,0:T(8,128)(2,1)S(1)} %shard_map.254.refs_0_), channel_id=1, source_target_pairs={{0,30},{1,31},{2,0},{3,1},{4,2},{5,3},{6,4},{7,5},{8,6},{9,7},{10,... | collective-permute-start | bytes 442376 | tf_op jit(solution)/shard_map/ppermute | solution.py:418
  93.3 5.7 %collective-permute-start.18 = (bf16[3,24,1024]{2,1,0:T(8,128)(2,1)S(1)}, bf16[3,24,1024]{2,1,0:T(8,128)(2,1)S(1)}, u32[]{:S(2)}, u32[]{:S(2)}) collective-permute-start(bf16[3,24,1024]{2,1,0:T(8,128)(2,1)S(1)} %shard_map.254.refs_0_), channel_id=1, source_target_pairs={{0,2},{1,3},{2,4},{3,5},{4,6},{5,7},{6,8},{7,9},{8,10},{9,11},{10,... | collective-permute-start | bytes 442376 | tf_op jit(solution)/shard_map/ppermute | solution.py:418
  97.9 11.8 %collective-permute-start.21 = (bf16[3,24,1024]{2,1,0:T(8,128)(2,1)S(1)}, bf16[3,24,1024]{2,1,0:T(8,128)(2,1)S(1)}, u32[]{:S(2)}, u32[]{:S(2)}) collective-permute-start(bf16[3,24,1024]{2,1,0:T(8,128)(2,1)S(1)} %collective-permute-done.19.refs_2_), channel_id=1, source_target_pairs={{0,30},{1,31},{2,0},{3,1},{4,2},{5,3},{6,4},{7,5},{8,6},{9,7},{10,... | collective-permute-start | bytes 442376 | tf_op jit(solution)/shard_map/ppermute | solution.py:418
  99.0 10.8 %collective-permute-start.20 = (bf16[3,24,1024]{2,1,0:T(8,128)(2,1)S(1)}, bf16[3,24,1024]{2,1,0:T(8,128)(2,1)S(1)}, u32[]{:S(2)}, u32[]{:S(2)}) collective-permute-start(bf16[3,24,1024]{2,1,0:T(8,128)(2,1)S(1)} %collective-permute-done.18.refs_1_), channel_id=1, source_target_pairs={{0,2},{1,3},{2,4},{3,5},{4,6},{5,7},{6,8},{7,9},{8,10},{9,11},{10,... | collective-permute-start | bytes 442376 | tf_op jit(solution)/shard_map/ppermute | solution.py:418
  99.4 6.7 %collective-permute-start.22 = (bf16[24,1024]{1,0:T(8,128)(2,1)S(1)}, bf16[24,1024]{1,0:T(8,128)(2,1)S(1)}, u32[]{:S(2)}, u32[]{:S(2)}) collective-permute-start(bf16[24,1024]{1,0:T(8,128)(2,1)S(1)} %collective-permute-done.16.b_ref), channel_id=1, source_target_pairs={{0,6},{1,7},{2,8},{3,9},{4,10},{5,11},{6,12},{7,13},{8,14},{9,15},... | collective-permute-start | bytes 147464 | tf_op jit(solution)/shard_map/ppermute | solution.py:418
  106.1 3.2 %collective-permute-start.28 = (bf16[24,1024]{1,0:T(8,128)(2,1)S(1)}, bf16[24,1024]{1,0:T(8,128)(2,1)S(1)}, u32[]{:S(2)}, u32[]{:S(2)}) collective-permute-start(bf16[24,1024]{1,0:T(8,128)(2,1)S(1)} %collective-permute-done.22.refs_5_), channel_id=1, source_target_pairs={{0,1},{1,0},{2,3},{3,2},{4,5},{5,4},{6,7},{7,6},{8,9},{9,8},{10,11... | collective-permute-start | bytes 147464 | tf_op jit(solution)/shard_map/ppermute | solution.py:412
  108.4 2.2 %collective-permute-start.23 = (bf16[3,24,1024]{2,1,0:T(8,128)(2,1)S(1)}, bf16[3,24,1024]{2,1,0:T(8,128)(2,1)S(1)}, u32[]{:S(2)}, u32[]{:S(2)}) collective-permute-start(bf16[3,24,1024]{2,1,0:T(8,128)(2,1)S(1)} %shard_map.254.refs_0_), channel_id=1, source_target_pairs={{0,1},{1,0},{2,3},{3,2},{4,5},{5,4},{6,7},{7,6},{8,9},{9,8},{10,11... | collective-permute-start | bytes 442376 | tf_op jit(solution)/shard_map/ppermute | solution.py:412
  108.4 2.2 %collective-permute-start.25 = (bf16[3,24,1024]{2,1,0:T(8,128)(2,1)S(1)}, bf16[3,24,1024]{2,1,0:T(8,128)(2,1)S(1)}, u32[]{:S(2)}, u32[]{:S(2)}) collective-permute-start(bf16[3,24,1024]{2,1,0:T(8,128)(2,1)S(1)} %collective-permute-done.19.refs_2_), channel_id=1, source_target_pairs={{0,1},{1,0},{2,3},{3,2},{4,5},{5,4},{6,7},{7,6},{8,9},{9,8},{10,11... | collective-permute-start | bytes 442376 | tf_op jit(solution)/shard_map/ppermute | solution.py:412
  109.3 1.4 collective-permute-start.24
  109.7 1.4 collective-permute-start.27
  109.8 1.4 collective-permute-start.26
  114.3 2.4 %collective-permute-start.29 = (bf16[384,1024]{1,0:T(8,128)(2,1)S(1)}, bf16[384,1024]{1,0:T(8,128)(2,1)S(1)}, u32[]{:S(2)}, u32[]{:S(2)}) collective-permute-start(bf16[384,1024]{1,0:T(8,128)(2,1)S(1)} %get-tuple-element.58), channel_id=1, source_target_pairs={{0,1},{1,0},{2,3},{3,2},{4,5},{5,4},{6,7},{7,6},{8,9},{9,8},{10,11... | collective-permute-start | bytes 2359304 | tf_op jit(solution)/shard_map/ppermute | solution.py:412
  116.9 6.4 %collective-permute-start.30 = (bf16[3,24,1024]{2,1,0:T(8,128)(2,1)S(1)}, bf16[3,24,1024]{2,1,0:T(8,128)(2,1)S(1)}, u32[]{:S(2)}, u32[]{:S(2)}) collective-permute-start(bf16[3,24,1024]{2,1,0:T(8,128)(2,1)S(1)} %get-tuple-element.61), channel_id=1, source_target_pairs={{0,2},{1,3},{2,4},{3,5},{4,6},{5,7},{6,8},{7,9},{8,10},{9,11},{10,... | collective-permute-start | bytes 442376 | tf_op jit(solution)/shard_map/ppermute | solution.py:418
  118.3 5.9 %collective-permute-start.32 = (bf16[3,24,1024]{2,1,0:T(8,128)(2,1)S(1)}, bf16[3,24,1024]{2,1,0:T(8,128)(2,1)S(1)}, u32[]{:S(2)}, u32[]{:S(2)}) collective-permute-start(bf16[3,24,1024]{2,1,0:T(8,128)(2,1)S(1)} %get-tuple-element.63), channel_id=1, source_target_pairs={{0,30},{1,31},{2,0},{3,1},{4,2},{5,3},{6,4},{7,5},{8,6},{9,7},{10,... | collective-permute-start | bytes 442376 | tf_op jit(solution)/shard_map/ppermute | solution.py:418
  123.3 9.5 %collective-permute-start.31 = (bf16[3,24,1024]{2,1,0:T(8,128)(2,1)S(1)}, bf16[3,24,1024]{2,1,0:T(8,128)(2,1)S(1)}, u32[]{:S(2)}, u32[]{:S(2)}) collective-permute-start(bf16[3,24,1024]{2,1,0:T(8,128)(2,1)S(1)} %shard_map.259), channel_id=1, source_target_pairs={{0,2},{1,3},{2,4},{3,5},{4,6},{5,7},{6,8},{7,9},{8,10},{9,11},{10,... | collective-permute-start | bytes 442376 | tf_op jit(solution)/shard_map/ppermute | solution.py:418
  124.2 8.6 %collective-permute-start.33 = (bf16[3,24,1024]{2,1,0:T(8,128)(2,1)S(1)}, bf16[3,24,1024]{2,1,0:T(8,128)(2,1)S(1)}, u32[]{:S(2)}, u32[]{:S(2)}) collective-permute-start(bf16[3,24,1024]{2,1,0:T(8,128)(2,1)S(1)} %shard_map.260), channel_id=1, source_target_pairs={{0,30},{1,31},{2,0},{3,1},{4,2},{5,3},{6,4},{7,5},{8,6},{9,7},{10,... | collective-permute-start | bytes 442376 | tf_op jit(solution)/shard_map/ppermute | solution.py:418
  126.2 6.6 %collective-permute-start.34 = (bf16[24,1024]{1,0:T(8,128)(2,1)S(1)}, bf16[24,1024]{1,0:T(8,128)(2,1)S(1)}, u32[]{:S(2)}, u32[]{:S(2)}) collective-permute-start(bf16[24,1024]{1,0:T(8,128)(2,1)S(1)} %get-tuple-element.64), channel_id=1, source_target_pairs={{0,6},{1,7},{2,8},{3,9},{4,10},{5,11},{6,12},{7,13},{8,14},{9,15},... | collective-permute-start | bytes 147464 | tf_op jit(solution)/shard_map/ppermute | solution.py:418
  132.9 9.1 %collective-permute-start.35 = (bf16[24,1024]{1,0:T(8,128)(2,1)S(1)}, bf16[24,1024]{1,0:T(8,128)(2,1)S(1)}, u32[]{:S(2)}, u32[]{:S(2)}) collective-permute-start(bf16[24,1024]{1,0:T(8,128)(2,1)S(1)} %get-tuple-element.66), channel_id=1, source_target_pairs={{0,10},{1,11},{2,12},{3,13},{4,14},{5,15},{6,16},{7,17},{8,18},{9,... | collective-permute-start | bytes 147464 | tf_op jit(solution)/shard_map/ppermute | solution.py:418
  136.1 9.1 %collective-permute-start.36 = (bf16[24,1024]{1,0:T(8,128)(2,1)S(1)}, bf16[24,1024]{1,0:T(8,128)(2,1)S(1)}, u32[]{:S(2)}, u32[]{:S(2)}) collective-permute-start(bf16[24,1024]{1,0:T(8,128)(2,1)S(1)} %get-tuple-element.67), channel_id=1, source_target_pairs={{0,22},{1,23},{2,24},{3,25},{4,26},{5,27},{6,28},{7,29},{8,30},{9,... | collective-permute-start | bytes 147464 | tf_op jit(solution)/shard_map/ppermute | solution.py:418
  145.2 4.8 %collective-permute-start.37 = (f32[12,1024]{1,0:T(8,128)S(1)}, f32[12,1024]{1,0:T(8,128)S(1)}, u32[]{:S(2)}, u32[]{:S(2)}) collective-permute-start(f32[12,1024]{1,0:T(8,128)S(1)} %get-tuple-element.69), channel_id=1, source_target_pairs={{0,1},{1,0},{2,3},{3,2},{4,5},{5,4},{6,7},{7,6},{8,9},{9,8},{10,11... | collective-permute-start | bytes 147464 | tf_op jit(solution)/shard_map/ppermute | solution.py:412

commit v6 on v5

--- a/solution.py
+++ b/solution.py
@@ -79,17 +79,21 @@
 def norm_kernel(own_ref, other_ref, gains_ref, out_ref, rows):
     c = core()
     r = own_ref.shape[0]
-    own = half_of(c, own_ref[...].astype(F32))
-    other = half_of(c, rms(other_ref[...].astype(F32), gains_ref[0:1, :]))
+    own = own_ref[...].astype(F32)
+    other = rms(other_ref[...].astype(F32), gains_ref[0:1, :])
     rows[:r] = jnp.where(c == 0, own, other)
     rows[r : 2 * r] = jnp.where(c == 0, other, own)
     out_ref[...] = rows[...].astype(BF16)
 
 
-def stack_kernel(a_ref, b_ref, c_ref, after_ref, out_ref):
-    out_ref[0] = a_ref[...]
-    out_ref[1] = b_ref[...]
-    out_ref[2] = c_ref[...]
+def stack_kernel(own_ref, far_ref, other_ref, after_ref, out_ref, half_ref):
+    c = core()
+    far, other = far_ref[...].astype(F32), other_ref[...].astype(F32)
+    minus = jnp.where(c == 0, far, other)
+    out_ref[0] = own_ref[...]
+    out_ref[1] = minus.astype(BF16)
+    out_ref[2] = jnp.where(c == 0, other, far).astype(BF16)
+    half_ref[...] = half_of(c, minus).astype(BF16)
 
 
 def gates_kernel(
@@ -140,27 +144,25 @@
 
 
 def collect(refs, out):
-    at = 0
-    for ref in refs:
-        size = 1
-        for extent in ref.shape[:-1]:
-            size *= extent
-        out[at : at + size] = ref[...].reshape(size, ref.shape[-1])
-        at += size
+    ring_ref, one_ref, one_swap, two_ref, two_swap, last_ref, last_swap = refs
+    c = core()
+    h = last_ref.shape[1]
+    out[0:3] = ring_ref[...]
+    out[pl.ds(3 + 3 * c, 3)] = one_ref[...]
+    out[pl.ds(6 - 3 * c, 3)] = one_swap[...]
+    out[pl.ds(9 + 3 * c, 3)] = two_ref[...]
+    out[pl.ds(12 - 3 * c, 3)] = two_swap[...]
+    mine, got = last_ref[...].astype(F32), last_swap[...].astype(F32)
+    out[15, :, :h] = jnp.where(c == 0, mine, got).astype(BF16)
+    out[15, :, h:] = jnp.where(c == 0, got, mine).astype(BF16)
 
 
 def proj_kernel(*refs):
-    xs, ys, (w_ref, info_ref, out_ref, x, y) = refs[:6], refs[6:12], refs[12:]
-    c = core()
+    pieces, (w_ref, info_ref, out_ref, x) = refs[:7], refs[7:]
     z = lax.div(lax.axis_index("ep"), 2)
-    nz = out_ref.shape[0]
-    h = x.shape[1]
-    r2 = x.shape[0] // nz
-    collect(xs, x)
-    collect(ys, y)
-    at = pl.ds(pl.multiple_of(c * h, h), h)
-    to = pl.ds(pl.multiple_of((1 - c) * h, h), h)
-    p = (dot_t(x[...], w_ref[:, at]) + dot_t(y[...], w_ref[:, to])).astype(BF16)
+    nz, r2, d = x.shape
+    collect(pieces, x)
+    p = dot_t(x[...].reshape(nz * r2, d), w_ref[...]).astype(BF16)
     for k, offset in enumerate(offsets(nz)):
         where = lax.rem(z + offset, nz)
         out_ref[where, :r2, :] = p[k * r2 : (k + 1) * r2]
@@ -169,7 +171,7 @@
 
 def cell_kernel(
     a_ref, b_ref, keep_ref, write_ref, m_ref, norm_ref, mix_ref, resid_ref, gains_ref,
-    middle_ref, mine_ref, send_ref, newnorm_ref, keys_ref, wvt_ref,
+    middle_ref, rows_ref, newnorm_ref, keys_ref, wvt_ref,
     p0, p1, q_scr, wv_scr, gated,
 ):
     c = core()
@@ -227,9 +229,7 @@
     mixed = dot(gated[...], mix_ref[...])
     middle = resid_ref[...].astype(F32) + rms(mixed, gains_ref[1:2, :])
     middle_ref[...] = middle
-    branch = rms(middle, gains_ref[2:3, :])
-    mine_ref[...] = half_of(c, branch).astype(BF16)
-    send_ref[...] = half_of(1 - c, branch).astype(BF16)
+    rows_ref[...] = rms(middle, gains_ref[2:3, :]).astype(BF16)
 
 
 def update_kernel(keep_ref, keys_ref, wvt_ref, m_ref, out_ref, token_ref, new, sems):
@@ -306,29 +306,23 @@
 
 
 def branch_kernel(*refs):
-    xs, ys = refs[:6], refs[6:12]
     (picker_ref, placer_ref, weight_ref, eg_ref, eu_ref, ed_ref, dg_ref, du_ref, dd_ref, bw_ref,
-     send_ref, hidden_ref, made, gains_ref, x_scr, y_scr) = refs[12:]
-    c = core()
-    rows, h = x_scr.shape
-    at = pl.ds(pl.multiple_of(c * h, h), h)
+     send_ref, hidden_ref, made, gains_ref, x_scr) = refs[7:]
+    c = core()
+    nz, r2, d = x_scr.shape
+    rows, h = nz * r2, d // 2
     to = pl.ds(pl.multiple_of((1 - c) * h, h), h)
-    collect(xs, x_scr)
-    collect(ys, y_scr)
-    x, y = x_scr[...], y_scr[...]
+    collect(refs[:7], x_scr)
+    x = x_scr[...].reshape(rows, d)
     lane = lax.broadcasted_iota(jnp.int32, (rows, 128), 1)
-    picker, weight = picker_ref[...], weight_ref[:, 0:1]
-    px = dot(picker, x).astype(BF16)
-    py = dot(picker, y).astype(BF16)
-    gate = dot(px, eg_ref[0, at, :]) + dot(py, eg_ref[0, to, :])
-    up = dot(px, eu_ref[0, at, :]) + dot(py, eu_ref[0, to, :])
+    weight = weight_ref[:, 0:1]
+    px = dot(picker_ref[...], x).astype(BF16)
+    gate = dot(px, eg_ref[0])
+    up = dot(px, eu_ref[0])
     made[...] = dot(silu_mul(gate, up), ed_ref[0]).astype(BF16)
 
-    gate = dot(x, dg_ref[at, :]) + dot(y, dg_ref[to, :])
-    up = dot(x, du_ref[at, :]) + dot(y, du_ref[to, :])
-    hidden = silu_mul(gate, up)
-    logit = jnp.sum(x.astype(F32) * bw_ref[:, at].astype(F32), axis=1, keepdims=True)
-    logit = logit + jnp.sum(y.astype(F32) * bw_ref[:, to].astype(F32), axis=1, keepdims=True)
+    hidden = silu_mul(dot(x, dg_ref[...]), dot(x, du_ref[...]))
+    logit = jnp.sum(x.astype(F32) * bw_ref[...].astype(F32), axis=1, keepdims=True)
     sig = jax.nn.sigmoid(logit)
     hidden_ref[...] = hidden
     gains_ref[...] = jnp.where(lane == 0, sig, weight)
@@ -420,13 +414,19 @@
 
     tile = (2 * r, h)
 
+    def apart(x, offset):
+        return lax.ppermute(
+            x, "ep", [(2 * z, 2 * ((z + offset) % nz)) for z in range(nz)]
+            + [(2 * z + 1, 2 * ((z - offset) % nz) + 1) for z in range(nz)])
+
     def gather(own, after):
-        plus, minus = shift(own, FAR), shift(own, -FAR)
-        ring, = call(stack_kernel, [((3,) + tile, BF16)], (own, plus, minus, after))
-        last = shift(plus, 8 - FAR)
-        up, down = shift(ring, 1), shift(ring, -1)
-        pieces = (ring, up, down, shift(up, 1), shift(down, -1), last)
-        return pieces, [swap(piece) for piece in pieces]
+        far = apart(own, FAR)
+        ring, half = call(stack_kernel, [((3, 2 * r, d), BF16), (tile, BF16)],
+                          (own, far, swap(far), after))
+        last = shift(half, 8 - FAR)
+        one = apart(ring, 1)
+        two = apart(one, 1)
+        return ring, one, swap(one), two, swap(two), last, swap(last)
 
     other = swap(resid)
     normed, gains = call(
@@ -443,29 +443,28 @@
                  ((heads, r), F32), ((2, r), jnp.int32),
                  ((2, r), BF16), ((128, 128), F32), ((8, 128), F32)],
         hbm=tuple(range(1, 14)), sems=12 + r, held=(4, 5, 6))
-    chunk, = call(norm_kernel, [(tile, BF16)], (normed, other, gains),
-                  scratch=[(tile, F32)])
-    xs, ys = gather(chunk, info)
+    chunk, = call(norm_kernel, [((2 * r, d), BF16)], (normed, other, gains),
+                  scratch=[((2 * r, d), F32)])
+    pieces = gather(chunk, info)
     projected, = call(
         proj_kernel, [((nz, 2 * r + 8, 4 * inner // n), BF16)],
-        (*xs, *ys, w_all, info), scratch=[((n * r, h), BF16)] * 2)
+        (*pieces, w_all, info), scratch=[((nz, 2 * r, d), BF16)])
     a = exchange(projected)
     b = swap(a)
-    middle, mine, send, new_norm, keys, wvt = call(
+    middle, rows, new_norm, keys, wvt = call(
         cell_kernel,
-        [((r, d), F32), ((r, h), BF16), ((r, h), BF16), ((r, heads, dh), F32),
+        [((r, d), F32), ((r, d), BF16), ((r, heads, dh), F32),
          ((heads, 16, dh), F32), ((dh, 128), F32)],
         (a, b, keep, write, state, state_norm, mix, resid, gains),
         scratch=[((nz, 16, dh), F32), ((nz, 16, dh), F32), ((heads, 16, dh), F32),
                  ((128, dh), F32), ((r, inner), BF16)])
-    got = swap(send)
-    chunk, = call(pair_kernel, [((2 * r, h), BF16)], (mine, got),
-                  scratch=[((2 * r, h), F32)])
+    chunk, = call(pair_kernel, [((2 * r, d), BF16)], (rows, swap(rows)),
+                  scratch=[((2 * r, d), F32)])
     new_matrix, token = call(
         update_kernel, [(state_matrix.shape, F32), ((8, 128), F32)], (keep, keys, wvt, state),
         scratch=[(state_matrix.shape, F32)], sems=r,
         out_specs=[pl.BlockSpec(memory_space=pltpu.HBM), pl.BlockSpec(memory_space=pltpu.VMEM)])
-    xs, ys = gather(chunk, token)
+    pieces = gather(chunk, token)
     picker, placer, weight = call(
         route_kernel,
         [((n * CAP, n * r), BF16), ((n * r, n * CAP), BF16), ((n * r, 128), F32)],
@@ -474,9 +473,9 @@
         branch_kernel,
         [((n * r, h), BF16), ((n * r, dense_down.shape[0]), BF16), ((n * CAP, d), BF16),
          ((n * r, 128), F32)],
-        (*xs, *ys, picker, placer, weight, expert_gate, expert_up, expert_down, dense_gate,
+        (*pieces, picker, placer, weight, expert_gate, expert_up, expert_down, dense_gate,
          dense_up, dense_down, branch_weight.reshape(1, d)),
-        scratch=[((n * r, h), BF16), ((n * r, h), BF16)], vmem=32)
+        scratch=[((nz, 2 * r, d), BF16)], vmem=32)
     got = swap(send)
     part, = call(rest_kernel, [((n * r, h), F32)], (hidden, made, placer, scales, dense_down),
                  flops=400000000)

time: 151 us -> 165 us (1.093)
  waiting for transfers between devices: 45.7 us -> 60.8 us
    ppermute x0 -> x6, waiting for transfers between devices: none -> 30.5 us  [apart(): lax.ppermute(x, 'ep', [(2 * z, 2 * ((z + offset) % nz)) for z in range(nz...]
    ppermute x21 -> x9, starting transfers between devices: 38.5 us -> 13.7 us  [shift(): lax.ppermute(x, 'ep', [(2 * z + c, 2 * ((z + offset) % nz) + c) for z in...]
    ppermute x0 -> x6, starting transfers between devices: none -> 20 us  [apart(): lax.ppermute(x, 'ep', [(2 * z, 2 * ((z + offset) % nz)) for z in range(nz...]
    ppermute x21 -> x9, waiting for transfers between devices: 39 us -> 24.7 us  [shift(): lax.ppermute(x, 'ep', [(2 * z + c, 2 * ((z + offset) % nz) + c) for z in...]
    ppermute x17 -> x13, starting transfers between devices: 26.4 us -> 30.2 us  [swap(): return lax.ppermute(x, 'ep', pairs)]
    ppermute x17 -> x13, waiting for transfers between devices: 6.63 us -> 5.58 us  [swap(): return lax.ppermute(x, 'ep', pairs)]
  transfers between devices with their start and end apart: 38 -> 28, of which waited for: 23 -> 19; matrix products, arithmetic and copies ran while one was open for 0% -> 0% of each run, Pallas kernels for 8% -> 7%
where the time goes in v6:
time: 165 us
  starting transfers between devices  63.9 us (39%)
  waiting for transfers between devices  60.8 us (37%)
  Pallas kernels  21.5 us (13%)
  blocking collectives  18 us (11%)
    ppermute x6, waiting for transfers between devices, apart(): lax.ppermute(x, 'ep', [(2 * z, 2 * ((z + offset) % nz)) for z in range(nz...  30.5 us
    ppermute x13, starting transfers between devices, swap(): return lax.ppermute(x, 'ep', pairs)  30.2 us
    ppermute x9, waiting for transfers between devices, shift(): lax.ppermute(x, 'ep', [(2 * z + c, 2 * ((z + offset) % nz) + c) for z in...  24.7 us
    pallas_call x18, Pallas kernels, call(): pl.pallas_call(kernel, out_shape=[pltpu.VMEM(s, d) if i in held and (not...  21.5 us
    ppermute x6, starting transfers between devices, apart(): lax.ppermute(x, 'ep', [(2 * z, 2 * ((z + offset) % nz)) for z in range(nz...  20 us
    all_to_all x1, blocking collectives, exchange(): return lax.all_to_all(x, 'ep', 0, 0, axis_index_groups=groups)  18 us
    ppermute x9, starting transfers between devices, shift(): lax.ppermute(x, 'ep', [(2 * z + c, 2 * ((z + offset) % nz) + c) for z in...  13.7 us
    ppermute x13, waiting for transfers between devices, swap(): return lax.ppermute(x, 'ep', pairs)  5.58 us
  transfers between devices with their start and end apart: 28, of which 19 were waited for; matrix products, arithmetic and copies ran while one was open for 0% of the time, Pallas kernels for 7%

profile of v6, /device:TPU:69, one launch (start us, length us, event | category | flops | bytes accessed | tf_op | source)
XLA Modules:
  0.0 165.1 jit_solution(8441076206298333593)
XLA Ops:
  0.6 10.0 %collective-permute-start = (bf16[12,2048]{1,0:T(8,128)(2,1)}, bf16[12,2048]{1,0:T(8,128)(2,1)S(1)}, u32[]{:S(2)}, u32[]{:S(2)}) collective-permute-start(bf16[12,2048]{1,0:T(8,128)(2,1)} %resid_ref.1), channel_id=1, source_target_pairs={{0,1},{1,0},{2,3},{3,2},{4,5},{5,4},{6,7},{7,6},{8,9},{9,8},{10,11... | collective-permute-start | bytes 147464 | tf_op jit(solution)/shard_map/ppermute | solution.py:406
  10.6 1.0 shard_map.246
  11.9 6.1 %collective-permute-start.1 = (bf16[24,2048]{1,0:T(8,128)(2,1)S(1)}, bf16[24,2048]{1,0:T(8,128)(2,1)S(1)}, u32[]{:S(2)}, u32[]{:S(2)}) collective-permute-start(bf16[24,2048]{1,0:T(8,128)(2,1)S(1)} %shard_map.247.own_ref), channel_id=1, source_target_pairs={{0,10},{2,12},{4,14},{6,16},{8,18},{10,20},{12,22},{14,24},{16,26}... | collective-permute-start | bytes 294920 | tf_op jit(solution)/shard_map/ppermute | solution.py:418
  18.0 4.1 %collective-permute-done.1.far_ref = bf16[24,2048]{1,0:T(8,128)(2,1)S(1)} collective-permute-done((bf16[24,2048]{1,0:T(8,128)(2,1)S(1)}, bf16[24,2048]{1,0:T(8,128)(2,1)S(1)}, u32[]{:S(2)}, u32[]{:S(2)}) %collective-permute-start.1) | collective-permute-done | bytes 98336 | tf_op jit(solution)/shard_map/ppermute | solution.py:418
  22.1 0.9 collective-permute-start.2
  23.0 5.1 %shard_map.248 = (f32[12,8]{1,0:T(8,128)S(1)}, f32[12,8]{1,0:T(8,128)S(1)}, f32[8,12]{1,0:T(8,128)}, bf16[8,128]{1,0:T(8,128)(2,1)S(1)}, bf16[128,2048]{1,0:T(8,...) custom-call(bf16[12,2048]{1,0:T(8,128)(2,1)S(1)} %get-tuple-element.42.own_ref.normed_ref, ...), custom_call_target="tpu_custom_call" | custom-call | flops 1000000 | bytes 1000000 | tf_op jit(solution)/shard_map/pallas_call | solution.py:25
  28.2 6.7 %collective-permute-start.3 = (bf16[3,24,2048]{2,1,0:T(8,128)(2,1)S(1)}, bf16[3,24,2048]{2,1,0:T(8,128)(2,1)S(1)}, u32[]{:S(2)}, u32[]{:S(2)}) collective-permute-start(bf16[3,24,2048]{2,1,0:T(8,128)(2,1)S(1)} %get-tuple-element.45.refs_0_), channel_id=1, source_target_pairs={{0,2},{2,4},{4,6},{6,8},{8,10},{10,12},{12,14},{14,16},{16,18},{18... | collective-permute-start | bytes 884744 | tf_op jit(solution)/shard_map/ppermute | solution.py:418
  34.9 3.7 %collective-permute-done.3.refs_1_ = bf16[3,24,2048]{2,1,0:T(8,128)(2,1)S(1)} collective-permute-done((bf16[3,24,2048]{2,1,0:T(8,128)(2,1)S(1)}, bf16[3,24,2048]{2,1,0:T(8,128)(2,1)S(1)}, u32[]{:S(2)}, u32[]{:S(2)}) %collective-permute-start.3) | collective-permute-done | bytes 294944 | tf_op jit(solution)/shard_map/ppermute | solution.py:418
  38.6 3.1 %collective-permute-start.5 = (bf16[3,24,2048]{2,1,0:T(8,128)(2,1)S(1)}, bf16[3,24,2048]{2,1,0:T(8,128)(2,1)S(1)}, u32[]{:S(2)}, u32[]{:S(2)}) collective-permute-start(bf16[3,24,2048]{2,1,0:T(8,128)(2,1)S(1)} %collective-permute-done.3.refs_1_), channel_id=1, source_target_pairs={{0,2},{2,4},{4,6},{6,8},{8,10},{10,12},{12,14},{14,16},{16,18},{18... | collective-permute-start | bytes 884744 | tf_op jit(solution)/shard_map/ppermute | solution.py:418
  41.7 3.7 %collective-permute-done.5.refs_3_ = bf16[3,24,2048]{2,1,0:T(8,128)(2,1)S(1)} collective-permute-done((bf16[3,24,2048]{2,1,0:T(8,128)(2,1)S(1)}, bf16[3,24,2048]{2,1,0:T(8,128)(2,1)S(1)}, u32[]{:S(2)}, u32[]{:S(2)}) %collective-permute-start.5) | collective-permute-done | bytes 294944 | tf_op jit(solution)/shard_map/ppermute | solution.py:418
  45.4 2.5 %collective-permute-start.6 = (bf16[3,24,2048]{2,1,0:T(8,128)(2,1)S(1)}, bf16[3,24,2048]{2,1,0:T(8,128)(2,1)S(1)}, u32[]{:S(2)}, u32[]{:S(2)}) collective-permute-start(bf16[3,24,2048]{2,1,0:T(8,128)(2,1)S(1)} %collective-permute-done.5.refs_3_), channel_id=1, source_target_pairs={{0,1},{1,0},{2,3},{3,2},{4,5},{5,4},{6,7},{7,6},{8,9},{9,8},{10,11... | collective-permute-start | bytes 884744 | tf_op jit(solution)/shard_map/ppermute | solution.py:406
  47.9 6.4 %collective-permute-done.7.refs_5_ = bf16[24,1024]{1,0:T(8,128)(2,1)S(1)} collective-permute-done((bf16[24,1024]{1,0:T(8,128)(2,1)S(1)}, bf16[24,1024]{1,0:T(8,128)(2,1)S(1)}, u32[]{:S(2)}, u32[]{:S(2)}) %collective-permute-start.7) | collective-permute-done | bytes 49184 | tf_op jit(solution)/shard_map/ppermute | solution.py:412
  54.2 0.8 collective-permute-start.8
  55.1 0.9 collective-permute-done.8.refs_6_
  56.0 0.6 shard_map.250
  56.6 18.0 %all_to_all.5.a_ref = bf16[16,32,128]{2,1,0:T(8,128)(2,1)S(1)} all-to-all(bf16[16,32,128]{2,1,0:T(8,128)(2,1)S(1)} %shard_map.250), channel_id=1, replica_groups={{0,2,4,6,8,10,12,14,16,18,20,22,24,26,28,30},{1,3,5,7,9,11,13,15,17,19,..., dimensions={0} | all-to-all | bytes 262144 | tf_op jit(solution)/shard_map/all_to_all | solution.py:409
  74.6 3.3 %collective-permute-start.9 = (bf16[16,32,128]{2,1,0:T(8,128)(2,1)S(1)}, bf16[16,32,128]{2,1,0:T(8,128)(2,1)S(1)}, u32[]{:S(2)}, u32[]{:S(2)}) collective-permute-start(bf16[16,32,128]{2,1,0:T(8,128)(2,1)S(1)} %all_to_all.5.a_ref), channel_id=1, source_target_pairs={{0,1},{1,0},{2,3},{3,2},{4,5},{5,4},{6,7},{7,6},{8,9},{9,8},{10,11... | collective-permute-start | bytes 393224 | tf_op jit(solution)/shard_map/ppermute | solution.py:406
  77.9 1.0 collective-permute-done.9.b_ref
  78.9 4.5 %shard_map.251 = (f32[12,2048]{1,0:T(8,128)S(1)}, bf16[12,2048]{1,0:T(8,128)(2,1)S(1)}, f32[12,8,128]{2,1,0:T(8,128)}, f32[8,16,128]{2,1,0:T(8,128)S(1)}, f32[128,128]{1,0:T(8,128)S(1)}) custom-call(bf16[16,32,128]{2,1,0:T(8,128)(2,1)S(1)} %all_to_all.5.a_ref, bf16[16,32,128]{2,1,0:T(8,128)(2,1)S(1)} %collective-permute-done.9.b_ref, ...), custom_call_target="tpu_custom_call" | custom-call | flops 1000000 | bytes 1000000 | tf_op jit(solution)/shard_map/pallas_call | solution.py:25
  83.5 0.5 collective-permute-start.10
  83.9 0.9 collective-permute-done.10.got_ref
  84.9 2.2 %collective-permute-start.11 = (bf16[24,2048]{1,0:T(8,128)(2,1)S(1)}, bf16[24,2048]{1,0:T(8,128)(2,1)S(1)}, u32[]{:S(2)}, u32[]{:S(2)}) collective-permute-start(bf16[24,2048]{1,0:T(8,128)(2,1)S(1)} %shard_map.252.own_ref), channel_id=1, source_target_pairs={{0,10},{2,12},{4,14},{6,16},{8,18},{10,20},{12,22},{14,24},{16,26}... | collective-permute-start | bytes 294920 | tf_op jit(solution)/shard_map/ppermute | solution.py:418
  87.1 10.1 %collective-permute-done.11.far_ref = bf16[24,2048]{1,0:T(8,128)(2,1)S(1)} collective-permute-done((bf16[24,2048]{1,0:T(8,128)(2,1)S(1)}, bf16[24,2048]{1,0:T(8,128)(2,1)S(1)}, u32[]{:S(2)}, u32[]{:S(2)}) %collective-permute-start.11) | collective-permute-done | bytes 98336 | tf_op jit(solution)/shard_map/ppermute | solution.py:418
  97.2 2.7 %collective-permute-start.12 = (bf16[24,2048]{1,0:T(8,128)(2,1)S(1)}, bf16[24,2048]{1,0:T(8,128)(2,1)S(1)}, u32[]{:S(2)}, u32[]{:S(2)}) collective-permute-start(bf16[24,2048]{1,0:T(8,128)(2,1)S(1)} %collective-permute-done.11.far_ref), channel_id=1, source_target_pairs={{0,1},{1,0},{2,3},{3,2},{4,5},{5,4},{6,7},{7,6},{8,9},{9,8},{10,11... | collective-permute-start | bytes 294920 | tf_op jit(solution)/shard_map/ppermute | solution.py:406
  99.9 4.7 %shard_map.253 = (f32[12,8,128,128]{3,2,1,0:T(8,128)}, f32[8,128]{1,0:T(8,128)S(1)}) custom-call(f32[12,8]{1,0:T(8,128)S(1)} %get-tuple-element.48.keep_ref, f32[8,16,128]{2,1,0:T(8,128)S(1)} %get-tuple-element.53.keys_ref, f32[128,128]{1,0:T(8,128)S(1)} %get-tuple-element.54.wvt_ref, f32[12,8,128,128]{3,2,1,0:T(8,128)S(1)} %get-tuple-element.50.m_ref), custom_call_target="tpu_custom_call" | custom-call | flops 1000000 | bytes 1000000 | tf_op jit(solution)/shard_map/pallas_call | solution.py:25
  104.6 0.6 collective-permute-start.13
  105.2 5.4 %collective-permute-done.13.refs_1_ = bf16[3,24,2048]{2,1,0:T(8,128)(2,1)S(1)} collective-permute-done((bf16[3,24,2048]{2,1,0:T(8,128)(2,1)S(1)}, bf16[3,24,2048]{2,1,0:T(8,128)(2,1)S(1)}, u32[]{:S(2)}, u32[]{:S(2)}) %collective-permute-start.13) | collective-permute-done | bytes 294944 | tf_op jit(solution)/shard_map/ppermute | solution.py:418
  110.6 1.4 collective-permute-start.15
  112.0 0.7 collective-permute-start.14
  112.7 3.5 %collective-permute-done.15.refs_3_ = bf16[3,24,2048]{2,1,0:T(8,128)(2,1)S(1)} collective-permute-done((bf16[3,24,2048]{2,1,0:T(8,128)(2,1)S(1)}, bf16[3,24,2048]{2,1,0:T(8,128)(2,1)S(1)}, u32[]{:S(2)}, u32[]{:S(2)}) %collective-permute-start.15) | collective-permute-done | bytes 294944 | tf_op jit(solution)/shard_map/ppermute | solution.py:418
  116.2 4.4 %collective-permute-start.16 = (bf16[3,24,2048]{2,1,0:T(8,128)(2,1)S(1)}, bf16[3,24,2048]{2,1,0:T(8,128)(2,1)S(1)}, u32[]{:S(2)}, u32[]{:S(2)}) collective-permute-start(bf16[3,24,2048]{2,1,0:T(8,128)(2,1)S(1)} %collective-permute-done.15.refs_3_), channel_id=1, source_target_pairs={{0,1},{1,0},{2,3},{3,2},{4,5},{5,4},{6,7},{7,6},{8,9},{9,8},{10,11... | collective-permute-start | bytes 884744 | tf_op jit(solution)/shard_map/ppermute | solution.py:406
  120.6 6.3 %collective-permute-done.17.refs_5_ = bf16[24,1024]{1,0:T(8,128)(2,1)S(1)} collective-permute-done((bf16[24,1024]{1,0:T(8,128)(2,1)S(1)}, bf16[24,1024]{1,0:T(8,128)(2,1)S(1)}, u32[]{:S(2)}, u32[]{:S(2)}) %collective-permute-start.17) | collective-permute-done | bytes 49184 | tf_op jit(solution)/shard_map/ppermute | solution.py:412
  126.9 0.9 collective-permute-start.18
  127.8 0.5 shard_map.255
  128.7 3.2 %shard_map.256 = (bf16[384,1024]{1,0:T(8,128)(2,1)S(1)}, bf16[384,256]{1,0:T(8,128)(2,1)S(1)}, bf16[64,2048]{1,0:T(8,128)(2,1)S(1)}, f32[384,128]{1,0:T(8,128)S(1)}) custom-call(bf16[3,24,2048]{2,1,0:T(8,128)(2,1)S(1)} %get-tuple-element.56.refs_0_, bf16[3,24,2048]{2,1,0:T(8,128)(2,1)S(1)} %collective-permute-done.13.refs_1_, ...), custom_call_target="tpu_custom_call" | custom-call | flops 1000000 | bytes 1000000 | tf_op jit(solution)/shard_map/pallas_call | solution.py:25
  132.0 0.4 collective-permute-start.19
  132.4 0.6 shard_map.257
  133.0 1.4 collective-permute-done.19
  134.6 2.6 %collective-permute-start.22 = (bf16[3,24,1024]{2,1,0:T(8,128)(2,1)S(1)}, bf16[3,24,1024]{2,1,0:T(8,128)(2,1)S(1)}, u32[]{:S(2)}, u32[]{:S(2)}) collective-permute-start(bf16[3,24,1024]{2,1,0:T(8,128)(2,1)S(1)} %get-tuple-element.69), channel_id=1, source_target_pairs={{0,30},{1,31},{2,0},{3,1},{4,2},{5,3},{6,4},{7,5},{8,6},{9,7},{10,... | collective-permute-start | bytes 442376 | tf_op jit(solution)/shard_map/ppermute | solution.py:412
  137.3 3.6 %collective-permute-done.20.got_ref = bf16[3,24,1024]{2,1,0:T(8,128)(2,1)S(1)} collective-permute-done((bf16[3,24,1024]{2,1,0:T(8,128)(2,1)S(1)}, bf16[3,24,1024]{2,1,0:T(8,128)(2,1)S(1)}, u32[]{:S(2)}, u32[]{:S(2)}) %collective-permute-start.20) | collective-permute-done | bytes 147488 | tf_op jit(solution)/shard_map/ppermute | solution.py:412
  141.1 2.7 %collective-permute-start.23 = (bf16[3,24,1024]{2,1,0:T(8,128)(2,1)S(1)}, bf16[3,24,1024]{2,1,0:T(8,128)(2,1)S(1)}, u32[]{:S(2)}, u32[]{:S(2)}) collective-permute-start(bf16[3,24,1024]{2,1,0:T(8,128)(2,1)S(1)} %shard_map.260), channel_id=1, source_target_pairs={{0,30},{1,31},{2,0},{3,1},{4,2},{5,3},{6,4},{7,5},{8,6},{9,7},{10,... | collective-permute-start | bytes 442376 | tf_op jit(solution)/shard_map/ppermute | solution.py:412
  144.3 6.3 %collective-permute-done.24.last_ref = bf16[24,1024]{1,0:T(8,128)(2,1)S(1)} collective-permute-done((bf16[24,1024]{1,0:T(8,128)(2,1)S(1)}, bf16[24,1024]{1,0:T(8,128)(2,1)S(1)}, u32[]{:S(2)}, u32[]{:S(2)}) %collective-permute-start.24) | collective-permute-done | bytes 49184 | tf_op jit(solution)/shard_map/ppermute | solution.py:412
  150.6 0.8 collective-permute-start.25
  151.4 6.8 %collective-permute-start.26 = (bf16[24,1024]{1,0:T(8,128)(2,1)S(1)}, bf16[24,1024]{1,0:T(8,128)(2,1)S(1)}, u32[]{:S(2)}, u32[]{:S(2)}) collective-permute-start(bf16[24,1024]{1,0:T(8,128)(2,1)S(1)} %get-tuple-element.73), channel_id=1, source_target_pairs={{0,22},{1,23},{2,24},{3,25},{4,26},{5,27},{6,28},{7,29},{8,30},{9,... | collective-permute-start | bytes 147464 | tf_op jit(solution)/shard_map/ppermute | solution.py:412
  158.2 1.7 %collective-permute-done.25.a_ref = bf16[24,1024]{1,0:T(8,128)(2,1)S(1)} collective-permute-done((bf16[24,1024]{1,0:T(8,128)(2,1)S(1)}, bf16[24,1024]{1,0:T(8,128)(2,1)S(1)}, u32[]{:S(2)}, u32[]{:S(2)}) %collective-permute-start.25) | collective-permute-done | bytes 49184 | tf_op jit(solution)/shard_map/ppermute | solution.py:412
  160.4 3.1 %collective-permute-start.27 = (f32[12,1024]{1,0:T(8,128)S(1)}, f32[12,1024]{1,0:T(8,128)S(1)}, u32[]{:S(2)}, u32[]{:S(2)}) collective-permute-start(f32[12,1024]{1,0:T(8,128)S(1)} %get-tuple-element.75), channel_id=1, source_target_pairs={{0,1},{1,0},{2,3},{3,2},{4,5},{5,4},{6,7},{7,6},{8,9},{9,8},{10,11... | collective-permute-start | bytes 147464 | tf_op jit(solution)/shard_map/ppermute | solution.py:406
  163.4 0.9 collective-permute-done.27.got_ref
  164.4 0.7 shard_map.263
  (46 shorter events, 2.3 us)
Async XLA Ops:
  0.6 11.1 %collective-permute-start = (bf16[12,2048]{1,0:T(8,128)(2,1)}, bf16[12,2048]{1,0:T(8,128)(2,1)S(1)}, u32[]{:S(2)}, u32[]{:S(2)}) collective-permute-start(bf16[12,2048]{1,0:T(8,128)(2,1)} %resid_ref.1), channel_id=1, source_target_pairs={{0,1},{1,0},{2,3},{3,2},{4,5},{5,4},{6,7},{7,6},{8,9},{9,8},{10,11... | collective-permute-start | bytes 147464 | tf_op jit(solution)/shard_map/ppermute | solution.py:406
  11.9 10.2 %collective-permute-start.1 = (bf16[24,2048]{1,0:T(8,128)(2,1)S(1)}, bf16[24,2048]{1,0:T(8,128)(2,1)S(1)}, u32[]{:S(2)}, u32[]{:S(2)}) collective-permute-start(bf16[24,2048]{1,0:T(8,128)(2,1)S(1)} %shard_map.247.own_ref), channel_id=1, source_target_pairs={{0,10},{2,12},{4,14},{6,16},{8,18},{10,20},{12,22},{14,24},{16,26}... | collective-permute-start | bytes 294920 | tf_op jit(solution)/shard_map/ppermute | solution.py:418
  22.1 6.1 %collective-permute-start.2 = (bf16[24,2048]{1,0:T(8,128)(2,1)S(1)}, bf16[24,2048]{1,0:T(8,128)(2,1)S(1)}, u32[]{:S(2)}, u32[]{:S(2)}) collective-permute-start(bf16[24,2048]{1,0:T(8,128)(2,1)S(1)} %collective-permute-done.1.far_ref), channel_id=1, source_target_pairs={{0,1},{1,0},{2,3},{3,2},{4,5},{5,4},{6,7},{7,6},{8,9},{9,8},{10,11... | collective-permute-start | bytes 294920 | tf_op jit(solution)/shard_map/ppermute | solution.py:406
  23.0 55.9 %copy-start.6 = (bf16[12,2048]{1,0:T(8,128)(2,1)S(1)}, bf16[12,2048]{1,0:T(8,128)(2,1)}, u32[]{:S(2)}) copy-start(bf16[12,2048]{1,0:T(8,128)(2,1)} %resid_ref.1) | copy-start | bytes 147460
  23.0 55.9 %copy-start.7 = (f32[12,8,128]{2,1,0:T(8,128)S(1)}, f32[12,8,128]{2,1,0:T(8,128)}, u32[]{:S(2)}) copy-start(f32[12,8,128]{2,1,0:T(8,128)} %norm_ref.1) | copy-start | bytes 147460
  28.2 10.3 %collective-permute-start.3 = (bf16[3,24,2048]{2,1,0:T(8,128)(2,1)S(1)}, bf16[3,24,2048]{2,1,0:T(8,128)(2,1)S(1)}, u32[]{:S(2)}, u32[]{:S(2)}) collective-permute-start(bf16[3,24,2048]{2,1,0:T(8,128)(2,1)S(1)} %get-tuple-element.45.refs_0_), channel_id=1, source_target_pairs={{0,2},{2,4},{4,6},{6,8},{8,10},{10,12},{12,14},{14,16},{16,18},{18... | collective-permute-start | bytes 884744 | tf_op jit(solution)/shard_map/ppermute | solution.py:418
  38.6 6.8 %collective-permute-start.5 = (bf16[3,24,2048]{2,1,0:T(8,128)(2,1)S(1)}, bf16[3,24,2048]{2,1,0:T(8,128)(2,1)S(1)}, u32[]{:S(2)}, u32[]{:S(2)}) collective-permute-start(bf16[3,24,2048]{2,1,0:T(8,128)(2,1)S(1)} %collective-permute-done.3.refs_1_), channel_id=1, source_target_pairs={{0,2},{2,4},{4,6},{6,8},{8,10},{10,12},{12,14},{14,16},{16,18},{18... | collective-permute-start | bytes 884744 | tf_op jit(solution)/shard_map/ppermute | solution.py:418
  41.7 14.3 %collective-permute-start.4 = (bf16[3,24,2048]{2,1,0:T(8,128)(2,1)S(1)}, bf16[3,24,2048]{2,1,0:T(8,128)(2,1)S(1)}, u32[]{:S(2)}, u32[]{:S(2)}) collective-permute-start(bf16[3,24,2048]{2,1,0:T(8,128)(2,1)S(1)} %collective-permute-done.3.refs_1_), channel_id=1, source_target_pairs={{0,1},{1,0},{2,3},{3,2},{4,5},{5,4},{6,7},{7,6},{8,9},{9,8},{10,11... | collective-permute-start | bytes 884744 | tf_op jit(solution)/shard_map/ppermute | solution.py:406
  45.4 10.6 %collective-permute-start.6 = (bf16[3,24,2048]{2,1,0:T(8,128)(2,1)S(1)}, bf16[3,24,2048]{2,1,0:T(8,128)(2,1)S(1)}, u32[]{:S(2)}, u32[]{:S(2)}) collective-permute-start(bf16[3,24,2048]{2,1,0:T(8,128)(2,1)S(1)} %collective-permute-done.5.refs_3_), channel_id=1, source_target_pairs={{0,1},{1,0},{2,3},{3,2},{4,5},{5,4},{6,7},{7,6},{8,9},{9,8},{10,11... | collective-permute-start | bytes 884744 | tf_op jit(solution)/shard_map/ppermute | solution.py:406
  47.9 6.4 %collective-permute-start.7 = (bf16[24,1024]{1,0:T(8,128)(2,1)S(1)}, bf16[24,1024]{1,0:T(8,128)(2,1)S(1)}, u32[]{:S(2)}, u32[]{:S(2)}) collective-permute-start(bf16[24,1024]{1,0:T(8,128)(2,1)S(1)} %get-tuple-element.46), channel_id=1, source_target_pairs={{0,6},{1,7},{2,8},{3,9},{4,10},{5,11},{6,12},{7,13},{8,14},{9,15},... | collective-permute-start | bytes 147464 | tf_op jit(solution)/shard_map/ppermute | solution.py:412
  54.2 1.7 %collective-permute-start.8 = (bf16[24,1024]{1,0:T(8,128)(2,1)S(1)}, bf16[24,1024]{1,0:T(8,128)(2,1)S(1)}, u32[]{:S(2)}, u32[]{:S(2)}) collective-permute-start(bf16[24,1024]{1,0:T(8,128)(2,1)S(1)} %collective-permute-done.7.refs_5_), channel_id=1, source_target_pairs={{0,1},{1,0},{2,3},{3,2},{4,5},{5,4},{6,7},{7,6},{8,9},{9,8},{10,11... | collective-permute-start | bytes 147464 | tf_op jit(solution)/shard_map/ppermute | solution.py:406
  74.6 4.3 %collective-permute-start.9 = (bf16[16,32,128]{2,1,0:T(8,128)(2,1)S(1)}, bf16[16,32,128]{2,1,0:T(8,128)(2,1)S(1)}, u32[]{:S(2)}, u32[]{:S(2)}) collective-permute-start(bf16[16,32,128]{2,1,0:T(8,128)(2,1)S(1)} %all_to_all.5.a_ref), channel_id=1, source_target_pairs={{0,1},{1,0},{2,3},{3,2},{4,5},{5,4},{6,7},{7,6},{8,9},{9,8},{10,11... | collective-permute-start | bytes 393224 | tf_op jit(solution)/shard_map/ppermute | solution.py:406
  78.9 49.8 %copy-start.3 = (bf16[1,512,2048]{2,1,0:T(8,128)(2,1)S(1)}, bf16[1,512,2048]{2,1,0:T(8,128)(2,1)}, u32[]{:S(2)}) copy-start(bf16[1,512,2048]{2,1,0:T(8,128)(2,1)} %refs_12_.1) | copy-start | bytes 6291460
  78.9 49.8 %copy-start.5 = (bf16[2048,256]{1,0:T(8,128)(2,1)S(1)}, bf16[2048,256]{1,0:T(8,128)(2,1)}, u32[]{:S(2)}) copy-start(bf16[2048,256]{1,0:T(8,128)(2,1)} %refs_14_.1) | copy-start | bytes 3145732
  83.4 44.4 %copy-start.8 = (bf16[2048]{0:T(1024)(128)(2,1)S(1)}, bf16[2048]{0:T(1024)(128)(2,1)}, u32[]{:S(2)}) copy-start(bf16[2048]{0:T(1024)(128)(2,1)} %param.45) | copy-start | bytes 12292
  83.4 45.3 %copy-start = (bf16[256,2048]{1,0:T(8,128)(2,1)S(1)}, bf16[256,2048]{1,0:T(8,128)(2,1)}, u32[]{:S(2)}) copy-start(bf16[256,2048]{1,0:T(8,128)(2,1)} %dd_ref.1) | copy-start | bytes 3145732
  83.4 45.3 %copy-start.1 = (bf16[1,2048,512]{2,1,0:T(8,128)(2,1)S(1)}, bf16[1,2048,512]{2,1,0:T(8,128)(2,1)}, u32[]{:S(2)}) copy-start(bf16[1,2048,512]{2,1,0:T(8,128)(2,1)} %refs_10_.1) | copy-start | bytes 6291460
  83.5 45.3 %copy-start.2 = (bf16[1,2048,512]{2,1,0:T(8,128)(2,1)S(1)}, bf16[1,2048,512]{2,1,0:T(8,128)(2,1)}, u32[]{:S(2)}) copy-start(bf16[1,2048,512]{2,1,0:T(8,128)(2,1)} %refs_11_.1) | copy-start | bytes 6291460
  83.5 45.3 %copy-start.4 = (bf16[2048,256]{1,0:T(8,128)(2,1)S(1)}, bf16[2048,256]{1,0:T(8,128)(2,1)}, u32[]{:S(2)}) copy-start(bf16[2048,256]{1,0:T(8,128)(2,1)} %refs_13_.1) | copy-start | bytes 3145732
  83.5 1.4 collective-permute-start.10
  84.9 12.3 %collective-permute-start.11 = (bf16[24,2048]{1,0:T(8,128)(2,1)S(1)}, bf16[24,2048]{1,0:T(8,128)(2,1)S(1)}, u32[]{:S(2)}, u32[]{:S(2)}) collective-permute-start(bf16[24,2048]{1,0:T(8,128)(2,1)S(1)} %shard_map.252.own_ref), channel_id=1, source_target_pairs={{0,10},{2,12},{4,14},{6,16},{8,18},{10,20},{12,22},{14,24},{16,26}... | collective-permute-start | bytes 294920 | tf_op jit(solution)/shard_map/ppermute | solution.py:418
  97.2 7.4 %collective-permute-start.12 = (bf16[24,2048]{1,0:T(8,128)(2,1)S(1)}, bf16[24,2048]{1,0:T(8,128)(2,1)S(1)}, u32[]{:S(2)}, u32[]{:S(2)}) collective-permute-start(bf16[24,2048]{1,0:T(8,128)(2,1)S(1)} %collective-permute-done.11.far_ref), channel_id=1, source_target_pairs={{0,1},{1,0},{2,3},{3,2},{4,5},{5,4},{6,7},{7,6},{8,9},{9,8},{10,11... | collective-permute-start | bytes 294920 | tf_op jit(solution)/shard_map/ppermute | solution.py:406
  104.6 6.0 %collective-permute-start.13 = (bf16[3,24,2048]{2,1,0:T(8,128)(2,1)S(1)}, bf16[3,24,2048]{2,1,0:T(8,128)(2,1)S(1)}, u32[]{:S(2)}, u32[]{:S(2)}) collective-permute-start(bf16[3,24,2048]{2,1,0:T(8,128)(2,1)S(1)} %get-tuple-element.56.refs_0_), channel_id=1, source_target_pairs={{0,2},{2,4},{4,6},{6,8},{8,10},{10,12},{12,14},{14,16},{16,18},{18... | collective-permute-start | bytes 884744 | tf_op jit(solution)/shard_map/ppermute | solution.py:418
  110.6 5.6 %collective-permute-start.15 = (bf16[3,24,2048]{2,1,0:T(8,128)(2,1)S(1)}, bf16[3,24,2048]{2,1,0:T(8,128)(2,1)S(1)}, u32[]{:S(2)}, u32[]{:S(2)}) collective-permute-start(bf16[3,24,2048]{2,1,0:T(8,128)(2,1)S(1)} %collective-permute-done.13.refs_1_), channel_id=1, source_target_pairs={{0,2},{2,4},{4,6},{6,8},{8,10},{10,12},{12,14},{14,16},{16,18},{18... | collective-permute-start | bytes 884744 | tf_op jit(solution)/shard_map/ppermute | solution.py:418
  112.0 16.7 %collective-permute-start.14 = (bf16[3,24,2048]{2,1,0:T(8,128)(2,1)S(1)}, bf16[3,24,2048]{2,1,0:T(8,128)(2,1)S(1)}, u32[]{:S(2)}, u32[]{:S(2)}) collective-permute-start(bf16[3,24,2048]{2,1,0:T(8,128)(2,1)S(1)} %collective-permute-done.13.refs_1_), channel_id=1, source_target_pairs={{0,1},{1,0},{2,3},{3,2},{4,5},{5,4},{6,7},{7,6},{8,9},{9,8},{10,11... | collective-permute-start | bytes 884744 | tf_op jit(solution)/shard_map/ppermute | solution.py:406
  116.2 12.5 %collective-permute-start.16 = (bf16[3,24,2048]{2,1,0:T(8,128)(2,1)S(1)}, bf16[3,24,2048]{2,1,0:T(8,128)(2,1)S(1)}, u32[]{:S(2)}, u32[]{:S(2)}) collective-permute-start(bf16[3,24,2048]{2,1,0:T(8,128)(2,1)S(1)} %collective-permute-done.15.refs_3_), channel_id=1, source_target_pairs={{0,1},{1,0},{2,3},{3,2},{4,5},{5,4},{6,7},{7,6},{8,9},{9,8},{10,11... | collective-permute-start | bytes 884744 | tf_op jit(solution)/shard_map/ppermute | solution.py:406
  120.6 6.3 %collective-permute-start.17 = (bf16[24,1024]{1,0:T(8,128)(2,1)S(1)}, bf16[24,1024]{1,0:T(8,128)(2,1)S(1)}, u32[]{:S(2)}, u32[]{:S(2)}) collective-permute-start(bf16[24,1024]{1,0:T(8,128)(2,1)S(1)} %get-tuple-element.57), channel_id=1, source_target_pairs={{0,6},{1,7},{2,8},{3,9},{4,10},{5,11},{6,12},{7,13},{8,14},{9,15},... | collective-permute-start | bytes 147464 | tf_op jit(solution)/shard_map/ppermute | solution.py:412
  126.9 1.7 %collective-permute-start.18 = (bf16[24,1024]{1,0:T(8,128)(2,1)S(1)}, bf16[24,1024]{1,0:T(8,128)(2,1)S(1)}, u32[]{:S(2)}, u32[]{:S(2)}) collective-permute-start(bf16[24,1024]{1,0:T(8,128)(2,1)S(1)} %collective-permute-done.17.refs_5_), channel_id=1, source_target_pairs={{0,1},{1,0},{2,3},{3,2},{4,5},{5,4},{6,7},{7,6},{8,9},{9,8},{10,11... | collective-permute-start | bytes 147464 | tf_op jit(solution)/shard_map/ppermute | solution.py:406
  132.0 2.4 %collective-permute-start.19 = (bf16[384,1024]{1,0:T(8,128)(2,1)S(1)}, bf16[384,1024]{1,0:T(8,128)(2,1)S(1)}, u32[]{:S(2)}, u32[]{:S(2)}) collective-permute-start(bf16[384,1024]{1,0:T(8,128)(2,1)S(1)} %get-tuple-element.64), channel_id=1, source_target_pairs={{0,1},{1,0},{2,3},{3,2},{4,5},{5,4},{6,7},{7,6},{8,9},{9,8},{10,11... | collective-permute-start | bytes 2359304 | tf_op jit(solution)/shard_map/ppermute | solution.py:406
  134.5 6.4 %collective-permute-start.20 = (bf16[3,24,1024]{2,1,0:T(8,128)(2,1)S(1)}, bf16[3,24,1024]{2,1,0:T(8,128)(2,1)S(1)}, u32[]{:S(2)}, u32[]{:S(2)}) collective-permute-start(bf16[3,24,1024]{2,1,0:T(8,128)(2,1)S(1)} %get-tuple-element.67), channel_id=1, source_target_pairs={{0,2},{1,3},{2,4},{3,5},{4,6},{5,7},{6,8},{7,9},{8,10},{9,11},{10,... | collective-permute-start | bytes 442376 | tf_op jit(solution)/shard_map/ppermute | solution.py:412
  134.6 6.4 %collective-permute-start.22 = (bf16[3,24,1024]{2,1,0:T(8,128)(2,1)S(1)}, bf16[3,24,1024]{2,1,0:T(8,128)(2,1)S(1)}, u32[]{:S(2)}, u32[]{:S(2)}) collective-permute-start(bf16[3,24,1024]{2,1,0:T(8,128)(2,1)S(1)} %get-tuple-element.69), channel_id=1, source_target_pairs={{0,30},{1,31},{2,0},{3,1},{4,2},{5,3},{6,4},{7,5},{8,6},{9,7},{10,... | collective-permute-start | bytes 442376 | tf_op jit(solution)/shard_map/ppermute | solution.py:412
  140.9 9.6 %collective-permute-start.21 = (bf16[3,24,1024]{2,1,0:T(8,128)(2,1)S(1)}, bf16[3,24,1024]{2,1,0:T(8,128)(2,1)S(1)}, u32[]{:S(2)}, u32[]{:S(2)}) collective-permute-start(bf16[3,24,1024]{2,1,0:T(8,128)(2,1)S(1)} %shard_map.259), channel_id=1, source_target_pairs={{0,2},{1,3},{2,4},{3,5},{4,6},{5,7},{6,8},{7,9},{8,10},{9,11},{10,... | collective-permute-start | bytes 442376 | tf_op jit(solution)/shard_map/ppermute | solution.py:412
  141.1 9.5 %collective-permute-start.23 = (bf16[3,24,1024]{2,1,0:T(8,128)(2,1)S(1)}, bf16[3,24,1024]{2,1,0:T(8,128)(2,1)S(1)}, u32[]{:S(2)}, u32[]{:S(2)}) collective-permute-start(bf16[3,24,1024]{2,1,0:T(8,128)(2,1)S(1)} %shard_map.260), channel_id=1, source_target_pairs={{0,30},{1,31},{2,0},{3,1},{4,2},{5,3},{6,4},{7,5},{8,6},{9,7},{10,... | collective-permute-start | bytes 442376 | tf_op jit(solution)/shard_map/ppermute | solution.py:412
  143.8 6.7 %collective-permute-start.24 = (bf16[24,1024]{1,0:T(8,128)(2,1)S(1)}, bf16[24,1024]{1,0:T(8,128)(2,1)S(1)}, u32[]{:S(2)}, u32[]{:S(2)}) collective-permute-start(bf16[24,1024]{1,0:T(8,128)(2,1)S(1)} %get-tuple-element.70), channel_id=1, source_target_pairs={{0,6},{1,7},{2,8},{3,9},{4,10},{5,11},{6,12},{7,13},{8,14},{9,15},... | collective-permute-start | bytes 147464 | tf_op jit(solution)/shard_map/ppermute | solution.py:412
  150.6 9.3 %collective-permute-start.25 = (bf16[24,1024]{1,0:T(8,128)(2,1)S(1)}, bf16[24,1024]{1,0:T(8,128)(2,1)S(1)}, u32[]{:S(2)}, u32[]{:S(2)}) collective-permute-start(bf16[24,1024]{1,0:T(8,128)(2,1)S(1)} %get-tuple-element.72), channel_id=1, source_target_pairs={{0,10},{1,11},{2,12},{3,13},{4,14},{5,15},{6,16},{7,17},{8,18},{9,... | collective-permute-start | bytes 147464 | tf_op jit(solution)/shard_map/ppermute | solution.py:412
  151.4 8.9 %collective-permute-start.26 = (bf16[24,1024]{1,0:T(8,128)(2,1)S(1)}, bf16[24,1024]{1,0:T(8,128)(2,1)S(1)}, u32[]{:S(2)}, u32[]{:S(2)}) collective-permute-start(bf16[24,1024]{1,0:T(8,128)(2,1)S(1)} %get-tuple-element.73), channel_id=1, source_target_pairs={{0,22},{1,23},{2,24},{3,25},{4,26},{5,27},{6,28},{7,29},{8,30},{9,... | collective-permute-start | bytes 147464 | tf_op jit(solution)/shard_map/ppermute | solution.py:412
  160.4 4.0 %collective-permute-start.27 = (f32[12,1024]{1,0:T(8,128)S(1)}, f32[12,1024]{1,0:T(8,128)S(1)}, u32[]{:S(2)}, u32[]{:S(2)}) collective-permute-start(f32[12,1024]{1,0:T(8,128)S(1)} %get-tuple-element.75), channel_id=1, source_target_pairs={{0,1},{1,0},{2,3},{3,2},{4,5},{5,4},{6,7},{7,6},{8,9},{9,8},{10,11... | collective-permute-start | bytes 147464 | tf_op jit(solution)/shard_map/ppermute | solution.py:406

commit v7 on v5

--- a/solution.py
+++ b/solution.py
@@ -365,13 +365,21 @@
     out_ref[...] = (own_ref[...] + got_ref[...].astype(F32)).astype(BF16)
 
 
-def fold_kernel(own_ref, a_ref, b_ref, last_ref, own_out, plus_ref, minus_ref):
+def fold_kernel(own_ref, a_ref, b_ref, own_out, minus_ref, plus_ref):
     def total(i):
         return own_ref[i] + a_ref[i].astype(F32) + b_ref[i].astype(F32)
 
+    minus_ref[...] = total(2).astype(BF16)
+    plus_ref[...] = total(1)
     own_out[...] = total(0)
-    plus_ref[...] = (total(1) + last_ref[...].astype(F32)).astype(BF16)
-    minus_ref[...] = total(2).astype(BF16)
+
+
+def mark_kernel(x_ref, out_ref):
+    out_ref[...] = x_ref[...]
+
+
+def join_kernel(plus_ref, last_ref, mark_ref, out_ref):
+    out_ref[...] = (plus_ref[...] + last_ref[...].astype(F32)).astype(BF16)
 
 
 def sum_kernel(own_ref, a_ref, b_ref, mine_ref, send_ref):
@@ -446,6 +454,7 @@
     chunk, = call(norm_kernel, [(tile, BF16)], (normed, other, gains),
                   scratch=[(tile, F32)])
     xs, ys = gather(chunk, info)
+    info, = call(mark_kernel, [(info.shape, BF16)], (info,))
     projected, = call(
         proj_kernel, [((nz, 2 * r + 8, 4 * inner // n), BF16)],
         (*xs, *ys, w_all, info), scratch=[((n * r, h), BF16)] * 2)
@@ -486,12 +495,15 @@
         (part.reshape((nz,) + tile), got.reshape((nz,) + tile)))
     last = shift(last, 8 - FAR)
     up, down = shift(up, 1), shift(down, -1)
+    mark, = call(mark_kernel, [(token.shape, F32)], (token,))
     up, = call(relay_kernel, [(three, BF16)], (one, up))
     down, = call(relay_kernel, [(three, BF16)], (back, down))
     up, down = shift(up, 1), shift(down, -1)
-    own, plus, minus = call(fold_kernel, [(tile, F32), (tile, BF16), (tile, BF16)],
-                            (own, up, down, last))
-    plus, minus = shift(plus, FAR), shift(minus, -FAR)
+    own, minus, plus = call(fold_kernel, [(tile, F32), (tile, BF16), (tile, F32)],
+                            (own, up, down))
+    minus = shift(minus, -FAR)
+    plus, = call(join_kernel, [(tile, BF16)], (plus, last, mark))
+    plus = shift(plus, FAR)
     mine, send = call(sum_kernel, [((r, h), F32), ((r, h), F32)], (own, plus, minus))
     got = swap(send)
     out, = call(final_kernel, [((r, d), BF16)], (mine, got, middle, gains))

time: 151 us -> 151 us (level)
    pallas_call x18 -> x21, Pallas kernels: 21.1 us -> 21.1 us  [call(): pl.pallas_call(kernel, out_shape=[pltpu.VMEM(s, d) if i in held and (not...]
  transfers between devices with their start and end apart: 38 -> 38, of which waited for: 23 -> 24; matrix products, arithmetic and copies ran while one was open for 0% -> 0% of each run, Pallas kernels for 8% -> 8%
where the time goes in v7:
time: 151 us
  starting transfers between devices  66.2 us (44%)
  waiting for transfers between devices  44.3 us (29%)
  Pallas kernels  21.1 us (14%)
  blocking collectives  18.1 us (12%)
    ppermute x21, starting transfers between devices, shift(): lax.ppermute(x, 'ep', [(2 * z + c, 2 * ((z + offset) % nz) + c) for z in...  38.5 us
    ppermute x21, waiting for transfers between devices, shift(): lax.ppermute(x, 'ep', [(2 * z + c, 2 * ((z + offset) % nz) + c) for z in...  37.7 us
    ppermute x17, starting transfers between devices, swap(): return lax.ppermute(x, 'ep', pairs)  27.7 us
    pallas_call x21, Pallas kernels, call(): pl.pallas_call(kernel, out_shape=[pltpu.VMEM(s, d) if i in held and (not...  21.1 us
    all_to_all x1, blocking collectives, exchange(): return lax.all_to_all(x, 'ep', 0, 0, axis_index_groups=groups)  18.1 us
    ppermute x17, waiting for transfers between devices, swap(): return lax.ppermute(x, 'ep', pairs)  6.63 us
  transfers between devices with their start and end apart: 38, of which 24 were waited for; matrix products, arithmetic and copies ran while one was open for 0% of the time, Pallas kernels for 8%

profile of v7, /device:TPU:69, one launch (start us, length us, event | category | flops | bytes accessed | tf_op | source)
XLA Modules:
  0.0 150.7 jit_solution(3444660225021264090)
XLA Ops:
  0.6 10.0 %collective-permute-start = (bf16[12,2048]{1,0:T(8,128)(2,1)}, bf16[12,2048]{1,0:T(8,128)(2,1)S(1)}, u32[]{:S(2)}, u32[]{:S(2)}) collective-permute-start(bf16[12,2048]{1,0:T(8,128)(2,1)} %resid_ref.1), channel_id=1, source_target_pairs={{0,1},{1,0},{2,3},{3,2},{4,5},{5,4},{6,7},{7,6},{8,9},{9,8},{10,11... | collective-permute-start | bytes 147464 | tf_op jit(solution)/shard_map/ppermute | solution.py:420
  10.6 1.0 shard_map.246
  11.9 6.1 %collective-permute-start.2 = (bf16[24,1024]{1,0:T(8,128)(2,1)S(1)}, bf16[24,1024]{1,0:T(8,128)(2,1)S(1)}, u32[]{:S(2)}, u32[]{:S(2)}) collective-permute-start(bf16[24,1024]{1,0:T(8,128)(2,1)S(1)} %shard_map.247.a_ref), channel_id=1, source_target_pairs={{0,22},{1,23},{2,24},{3,25},{4,26},{5,27},{6,28},{7,29},{8,30},{9,... | collective-permute-start | bytes 147464 | tf_op jit(solution)/shard_map/ppermute | solution.py:426
  18.3 5.1 %shard_map.248 = (f32[12,8]{1,0:T(8,128)S(1)}, f32[12,8]{1,0:T(8,128)S(1)}, f32[8,12]{1,0:T(8,128)}, bf16[8,128]{1,0:T(8,128)(2,1)S(1)}, bf16[128,2048]{1,0:T(8,...) custom-call(bf16[12,2048]{1,0:T(8,128)(2,1)S(1)} %get-tuple-element.39.own_ref.normed_ref, ...), custom_call_target="tpu_custom_call" | custom-call | flops 1000000 | bytes 1000000 | tf_op jit(solution)/shard_map/pallas_call | solution.py:25
  23.4 7.7 %collective-permute-done.1.b_ref = bf16[24,1024]{1,0:T(8,128)(2,1)S(1)} collective-permute-done((bf16[24,1024]{1,0:T(8,128)(2,1)S(1)}, bf16[24,1024]{1,0:T(8,128)(2,1)S(1)}, u32[]{:S(2)}, u32[]{:S(2)}) %collective-permute-start.1) | collective-permute-done | bytes 49184 | tf_op jit(solution)/shard_map/ppermute | solution.py:426
  31.2 1.4 collective-permute-start.3
  32.7 3.3 %collective-permute-done.4.refs_2_ = bf16[3,24,1024]{2,1,0:T(8,128)(2,1)S(1)} collective-permute-done((bf16[3,24,1024]{2,1,0:T(8,128)(2,1)S(1)}, bf16[3,24,1024]{2,1,0:T(8,128)(2,1)S(1)}, u32[]{:S(2)}, u32[]{:S(2)}) %collective-permute-start.4) | collective-permute-done | bytes 147488 | tf_op jit(solution)/shard_map/ppermute | solution.py:426
  36.0 1.4 collective-permute-start.6
  37.5 2.0 %collective-permute-start.7 = (bf16[24,1024]{1,0:T(8,128)(2,1)S(1)}, bf16[24,1024]{1,0:T(8,128)(2,1)S(1)}, u32[]{:S(2)}, u32[]{:S(2)}) collective-permute-start(bf16[24,1024]{1,0:T(8,128)(2,1)S(1)} %collective-permute-done.1.b_ref), channel_id=1, source_target_pairs={{0,6},{1,7},{2,8},{3,9},{4,10},{5,11},{6,12},{7,13},{8,14},{9,15},... | collective-permute-start | bytes 147464 | tf_op jit(solution)/shard_map/ppermute | solution.py:426
  39.5 4.0 %collective-permute-done.7.refs_5_ = bf16[24,1024]{1,0:T(8,128)(2,1)S(1)} collective-permute-done((bf16[24,1024]{1,0:T(8,128)(2,1)S(1)}, bf16[24,1024]{1,0:T(8,128)(2,1)S(1)}, u32[]{:S(2)}, u32[]{:S(2)}) %collective-permute-start.7) | collective-permute-done | bytes 49184 | tf_op jit(solution)/shard_map/ppermute | solution.py:426
  43.6 3.3 %collective-permute-start.13 = (bf16[24,1024]{1,0:T(8,128)(2,1)S(1)}, bf16[24,1024]{1,0:T(8,128)(2,1)S(1)}, u32[]{:S(2)}, u32[]{:S(2)}) collective-permute-start(bf16[24,1024]{1,0:T(8,128)(2,1)S(1)} %collective-permute-done.7.refs_5_), channel_id=1, source_target_pairs={{0,1},{1,0},{2,3},{3,2},{4,5},{5,4},{6,7},{7,6},{8,9},{9,8},{10,11... | collective-permute-start | bytes 147464 | tf_op jit(solution)/shard_map/ppermute | solution.py:420
  46.8 0.5 collective-permute-start.10
  48.6 0.5 collective-permute-done.9.refs_7_
  49.7 0.6 shard_map.251
  50.2 18.1 %all_to_all.5.a_ref = bf16[16,32,128]{2,1,0:T(8,128)(2,1)S(1)} all-to-all(bf16[16,32,128]{2,1,0:T(8,128)(2,1)S(1)} %shard_map.251), channel_id=1, replica_groups={{0,2,4,6,8,10,12,14,16,18,20,22,24,26,28,30},{1,3,5,7,9,11,13,15,17,19,..., dimensions={0} | all-to-all | bytes 262144 | tf_op jit(solution)/shard_map/all_to_all | solution.py:423
  68.4 3.3 %collective-permute-start.14 = (bf16[16,32,128]{2,1,0:T(8,128)(2,1)S(1)}, bf16[16,32,128]{2,1,0:T(8,128)(2,1)S(1)}, u32[]{:S(2)}, u32[]{:S(2)}) collective-permute-start(bf16[16,32,128]{2,1,0:T(8,128)(2,1)S(1)} %all_to_all.5.a_ref), channel_id=1, source_target_pairs={{0,1},{1,0},{2,3},{3,2},{4,5},{5,4},{6,7},{7,6},{8,9},{9,8},{10,11... | collective-permute-start | bytes 393224 | tf_op jit(solution)/shard_map/ppermute | solution.py:420
  71.6 1.0 collective-permute-done.14.b_ref
  72.6 4.5 %shard_map.252 = (f32[12,2048]{1,0:T(8,128)S(1)}, bf16[12,1024]{1,0:T(8,128)(2,1)S(1)}, bf16[12,1024]{1,0:T(8,128)(2,1)S(1)}, f32[12,8,128]{2,1,0:T(8,128)}, f32...) custom-call(bf16[16,32,128]{2,1,0:T(8,128)(2,1)S(1)} %all_to_all.5.a_ref, ...), custom_call_target="tpu_custom_call" | custom-call | flops 1000000 | bytes 1000000 | tf_op jit(solution)/shard_map/pallas_call | solution.py:25
  77.6 0.9 collective-permute-done.15.got_ref
  78.5 2.2 %collective-permute-start.17 = (bf16[24,1024]{1,0:T(8,128)(2,1)S(1)}, bf16[24,1024]{1,0:T(8,128)(2,1)S(1)}, u32[]{:S(2)}, u32[]{:S(2)}) collective-permute-start(bf16[24,1024]{1,0:T(8,128)(2,1)S(1)} %shard_map.253.a_ref), channel_id=1, source_target_pairs={{0,22},{1,23},{2,24},{3,25},{4,26},{5,27},{6,28},{7,29},{8,30},{9,... | collective-permute-start | bytes 147464 | tf_op jit(solution)/shard_map/ppermute | solution.py:426
  80.7 4.2 %collective-permute-start.16 = (bf16[24,1024]{1,0:T(8,128)(2,1)S(1)}, bf16[24,1024]{1,0:T(8,128)(2,1)S(1)}, u32[]{:S(2)}, u32[]{:S(2)}) collective-permute-start(bf16[24,1024]{1,0:T(8,128)(2,1)S(1)} %shard_map.253.a_ref), channel_id=1, source_target_pairs={{0,10},{1,11},{2,12},{3,13},{4,14},{5,15},{6,16},{7,17},{8,18},{9,... | collective-permute-start | bytes 147464 | tf_op jit(solution)/shard_map/ppermute | solution.py:426
  84.9 4.7 %shard_map.254 = (f32[12,8,128,128]{3,2,1,0:T(8,128)}, f32[8,128]{1,0:T(8,128)S(1)}) custom-call(f32[12,8]{1,0:T(8,128)S(1)} %get-tuple-element.43.keep_ref, f32[8,16,128]{2,1,0:T(8,128)S(1)} %get-tuple-element.49.keys_ref, f32[128,128]{1,0:T(8,128)S(1)} %get-tuple-element.50.wvt_ref, f32[12,8,128,128]{3,2,1,0:T(8,128)S(1)} %get-tuple-element.45.m_ref), custom_call_target="tpu_custom_call" | custom-call | flops 1000000 | bytes 1000000 | tf_op jit(solution)/shard_map/pallas_call | solution.py:25
  89.6 3.3 %collective-permute-done.16.b_ref = bf16[24,1024]{1,0:T(8,128)(2,1)S(1)} collective-permute-done((bf16[24,1024]{1,0:T(8,128)(2,1)S(1)}, bf16[24,1024]{1,0:T(8,128)(2,1)S(1)}, u32[]{:S(2)}, u32[]{:S(2)}) %collective-permute-start.16) | collective-permute-done | bytes 49184 | tf_op jit(solution)/shard_map/ppermute | solution.py:426
  93.3 1.2 collective-permute-start.18
  94.5 3.4 %collective-permute-done.19.refs_2_ = bf16[3,24,1024]{2,1,0:T(8,128)(2,1)S(1)} collective-permute-done((bf16[3,24,1024]{2,1,0:T(8,128)(2,1)S(1)}, bf16[3,24,1024]{2,1,0:T(8,128)(2,1)S(1)}, u32[]{:S(2)}, u32[]{:S(2)}) %collective-permute-start.19) | collective-permute-done | bytes 147488 | tf_op jit(solution)/shard_map/ppermute | solution.py:426
  97.9 1.1 collective-permute-start.21
  99.4 3.6 %collective-permute-start.22 = (bf16[24,1024]{1,0:T(8,128)(2,1)S(1)}, bf16[24,1024]{1,0:T(8,128)(2,1)S(1)}, u32[]{:S(2)}, u32[]{:S(2)}) collective-permute-start(bf16[24,1024]{1,0:T(8,128)(2,1)S(1)} %collective-permute-done.16.b_ref), channel_id=1, source_target_pairs={{0,6},{1,7},{2,8},{3,9},{4,10},{5,11},{6,12},{7,13},{8,14},{9,15},... | collective-permute-start | bytes 147464 | tf_op jit(solution)/shard_map/ppermute | solution.py:426
  102.9 3.1 %collective-permute-done.22.refs_5_ = bf16[24,1024]{1,0:T(8,128)(2,1)S(1)} collective-permute-done((bf16[24,1024]{1,0:T(8,128)(2,1)S(1)}, bf16[24,1024]{1,0:T(8,128)(2,1)S(1)}, u32[]{:S(2)}, u32[]{:S(2)}) %collective-permute-start.22) | collective-permute-done | bytes 49184 | tf_op jit(solution)/shard_map/ppermute | solution.py:426
  106.1 2.4 %collective-permute-start.28 = (bf16[24,1024]{1,0:T(8,128)(2,1)S(1)}, bf16[24,1024]{1,0:T(8,128)(2,1)S(1)}, u32[]{:S(2)}, u32[]{:S(2)}) collective-permute-start(bf16[24,1024]{1,0:T(8,128)(2,1)S(1)} %collective-permute-done.22.refs_5_), channel_id=1, source_target_pairs={{0,1},{1,0},{2,3},{3,2},{4,5},{5,4},{6,7},{7,6},{8,9},{9,8},{10,11... | collective-permute-start | bytes 147464 | tf_op jit(solution)/shard_map/ppermute | solution.py:420
  108.4 0.5 collective-permute-start.25
  111.3 3.0 %shard_map.257 = (bf16[384,1024]{1,0:T(8,128)(2,1)S(1)}, bf16[384,256]{1,0:T(8,128)(2,1)S(1)}, bf16[64,2048]{1,0:T(8,128)(2,1)S(1)}, f32[384,128]{1,0:T(8,128)S(1)}) custom-call(bf16[3,24,1024]{2,1,0:T(8,128)(2,1)S(1)} %shard_map.255.refs_0_, bf16[3,24,1024]{2,1,0:T(8,128)(2,1)S(1)} %collective-permute-done.18.refs_1_, ...), custom_call_target="tpu_custom_call" | custom-call | flops 1000000 | bytes 1000000 | tf_op jit(solution)/shard_map/pallas_call | solution.py:25
  114.8 0.6 shard_map.258
  115.4 1.4 collective-permute-done.29
  116.9 1.4 collective-permute-start.30
  118.3 1.3 collective-permute-start.32
  119.6 3.6 %collective-permute-done.30.got_ref = bf16[3,24,1024]{2,1,0:T(8,128)(2,1)S(1)} collective-permute-done((bf16[3,24,1024]{2,1,0:T(8,128)(2,1)S(1)}, bf16[3,24,1024]{2,1,0:T(8,128)(2,1)S(1)}, u32[]{:S(2)}, u32[]{:S(2)}) %collective-permute-start.30) | collective-permute-done | bytes 147488 | tf_op jit(solution)/shard_map/ppermute | solution.py:426
  123.6 0.6 collective-permute-done.32.got_ref
  124.2 2.0 %collective-permute-start.33 = (bf16[3,24,1024]{2,1,0:T(8,128)(2,1)S(1)}, bf16[3,24,1024]{2,1,0:T(8,128)(2,1)S(1)}, u32[]{:S(2)}, u32[]{:S(2)}) collective-permute-start(bf16[3,24,1024]{2,1,0:T(8,128)(2,1)S(1)} %shard_map.261), channel_id=1, source_target_pairs={{0,30},{1,31},{2,0},{3,1},{4,2},{5,3},{6,4},{7,5},{8,6},{9,7},{10,... | collective-permute-start | bytes 442376 | tf_op jit(solution)/shard_map/ppermute | solution.py:426
  126.2 1.5 collective-permute-start.34
  127.7 0.9 collective-permute-done.31.a_ref
  128.7 4.1 %collective-permute-done.34.last_ref = bf16[24,1024]{1,0:T(8,128)(2,1)S(1)} collective-permute-done((bf16[24,1024]{1,0:T(8,128)(2,1)S(1)}, bf16[24,1024]{1,0:T(8,128)(2,1)S(1)}, u32[]{:S(2)}, u32[]{:S(2)}) %collective-permute-start.34) | collective-permute-done | bytes 49184 | tf_op jit(solution)/shard_map/ppermute | solution.py:426
  132.8 3.2 %collective-permute-start.35 = (bf16[24,1024]{1,0:T(8,128)(2,1)S(1)}, bf16[24,1024]{1,0:T(8,128)(2,1)S(1)}, u32[]{:S(2)}, u32[]{:S(2)}) collective-permute-start(bf16[24,1024]{1,0:T(8,128)(2,1)S(1)} %shard_map.264), channel_id=1, source_target_pairs={{0,10},{1,11},{2,12},{3,13},{4,14},{5,15},{6,16},{7,17},{8,18},{9,... | collective-permute-start | bytes 147464 | tf_op jit(solution)/shard_map/ppermute | solution.py:426
  136.0 4.4 %collective-permute-start.36 = (bf16[24,1024]{1,0:T(8,128)(2,1)S(1)}, bf16[24,1024]{1,0:T(8,128)(2,1)S(1)}, u32[]{:S(2)}, u32[]{:S(2)}) collective-permute-start(bf16[24,1024]{1,0:T(8,128)(2,1)S(1)} %get-tuple-element.67), channel_id=1, source_target_pairs={{0,22},{1,23},{2,24},{3,25},{4,26},{5,27},{6,28},{7,29},{8,30},{9,... | collective-permute-start | bytes 147464 | tf_op jit(solution)/shard_map/ppermute | solution.py:426
  140.4 1.5 collective-permute-done.35.a_ref
  141.9 2.0 %collective-permute-done.36.b_ref = bf16[24,1024]{1,0:T(8,128)(2,1)S(1)} collective-permute-done((bf16[24,1024]{1,0:T(8,128)(2,1)S(1)}, bf16[24,1024]{1,0:T(8,128)(2,1)S(1)}, u32[]{:S(2)}, u32[]{:S(2)}) %collective-permute-start.36) | collective-permute-done | bytes 49184 | tf_op jit(solution)/shard_map/ppermute | solution.py:426
  143.9 5.1 %collective-permute-start.37 = (f32[12,1024]{1,0:T(8,128)S(1)}, f32[12,1024]{1,0:T(8,128)S(1)}, u32[]{:S(2)}, u32[]{:S(2)}) collective-permute-start(f32[12,1024]{1,0:T(8,128)S(1)} %get-tuple-element.69), channel_id=1, source_target_pairs={{0,1},{1,0},{2,3},{3,2},{4,5},{5,4},{6,7},{7,6},{8,9},{9,8},{10,11... | collective-permute-start | bytes 147464 | tf_op jit(solution)/shard_map/ppermute | solution.py:420
  149.0 0.9 collective-permute-done.37.got_ref
  149.9 0.7 shard_map.266
  (69 shorter events, 7.2 us)
Async XLA Ops:
  0.6 11.1 %collective-permute-start = (bf16[12,2048]{1,0:T(8,128)(2,1)}, bf16[12,2048]{1,0:T(8,128)(2,1)S(1)}, u32[]{:S(2)}, u32[]{:S(2)}) collective-permute-start(bf16[12,2048]{1,0:T(8,128)(2,1)} %resid_ref.1), channel_id=1, source_target_pairs={{0,1},{1,0},{2,3},{3,2},{4,5},{5,4},{6,7},{7,6},{8,9},{9,8},{10,11... | collective-permute-start | bytes 147464 | tf_op jit(solution)/shard_map/ppermute | solution.py:420
  11.9 11.5 %collective-permute-start.2 = (bf16[24,1024]{1,0:T(8,128)(2,1)S(1)}, bf16[24,1024]{1,0:T(8,128)(2,1)S(1)}, u32[]{:S(2)}, u32[]{:S(2)}) collective-permute-start(bf16[24,1024]{1,0:T(8,128)(2,1)S(1)} %shard_map.247.a_ref), channel_id=1, source_target_pairs={{0,22},{1,23},{2,24},{3,25},{4,26},{5,27},{6,28},{7,29},{8,30},{9,... | collective-permute-start | bytes 147464 | tf_op jit(solution)/shard_map/ppermute | solution.py:426
  17.9 13.2 %collective-permute-start.1 = (bf16[24,1024]{1,0:T(8,128)(2,1)S(1)}, bf16[24,1024]{1,0:T(8,128)(2,1)S(1)}, u32[]{:S(2)}, u32[]{:S(2)}) collective-permute-start(bf16[24,1024]{1,0:T(8,128)(2,1)S(1)} %shard_map.247.a_ref), channel_id=1, source_target_pairs={{0,10},{1,11},{2,12},{3,13},{4,14},{5,15},{6,16},{7,17},{8,18},{9,... | collective-permute-start | bytes 147464 | tf_op jit(solution)/shard_map/ppermute | solution.py:426
  18.3 54.3 %copy-start.6 = (bf16[12,2048]{1,0:T(8,128)(2,1)S(1)}, bf16[12,2048]{1,0:T(8,128)(2,1)}, u32[]{:S(2)}) copy-start(bf16[12,2048]{1,0:T(8,128)(2,1)} %resid_ref.1) | copy-start | bytes 147460
  18.3 54.3 %copy-start.7 = (f32[12,8,128]{2,1,0:T(8,128)S(1)}, f32[12,8,128]{2,1,0:T(8,128)}, u32[]{:S(2)}) copy-start(f32[12,8,128]{2,1,0:T(8,128)} %norm_ref.1) | copy-start | bytes 147460
  31.1 4.9 %collective-permute-start.4 = (bf16[3,24,1024]{2,1,0:T(8,128)(2,1)S(1)}, bf16[3,24,1024]{2,1,0:T(8,128)(2,1)S(1)}, u32[]{:S(2)}, u32[]{:S(2)}) collective-permute-start(bf16[3,24,1024]{2,1,0:T(8,128)(2,1)S(1)} %shard_map.249.refs_0_), channel_id=1, source_target_pairs={{0,30},{1,31},{2,0},{3,1},{4,2},{5,3},{6,4},{7,5},{8,6},{9,7},{10,... | collective-permute-start | bytes 442376 | tf_op jit(solution)/shard_map/ppermute | solution.py:426
  31.2 6.2 %collective-permute-start.3 = (bf16[3,24,1024]{2,1,0:T(8,128)(2,1)S(1)}, bf16[3,24,1024]{2,1,0:T(8,128)(2,1)S(1)}, u32[]{:S(2)}, u32[]{:S(2)}) collective-permute-start(bf16[3,24,1024]{2,1,0:T(8,128)(2,1)S(1)} %shard_map.249.refs_0_), channel_id=1, source_target_pairs={{0,2},{1,3},{2,4},{3,5},{4,6},{5,7},{6,8},{7,9},{8,10},{9,11},{10,... | collective-permute-start | bytes 442376 | tf_op jit(solution)/shard_map/ppermute | solution.py:426
  36.0 12.0 %collective-permute-start.6 = (bf16[3,24,1024]{2,1,0:T(8,128)(2,1)S(1)}, bf16[3,24,1024]{2,1,0:T(8,128)(2,1)S(1)}, u32[]{:S(2)}, u32[]{:S(2)}) collective-permute-start(bf16[3,24,1024]{2,1,0:T(8,128)(2,1)S(1)} %collective-permute-done.4.refs_2_), channel_id=1, source_target_pairs={{0,30},{1,31},{2,0},{3,1},{4,2},{5,3},{6,4},{7,5},{8,6},{9,7},{10,... | collective-permute-start | bytes 442376 | tf_op jit(solution)/shard_map/ppermute | solution.py:426
  37.4 10.8 %collective-permute-start.5 = (bf16[3,24,1024]{2,1,0:T(8,128)(2,1)S(1)}, bf16[3,24,1024]{2,1,0:T(8,128)(2,1)S(1)}, u32[]{:S(2)}, u32[]{:S(2)}) collective-permute-start(bf16[3,24,1024]{2,1,0:T(8,128)(2,1)S(1)} %collective-permute-done.3.refs_1_), channel_id=1, source_target_pairs={{0,2},{1,3},{2,4},{3,5},{4,6},{5,7},{6,8},{7,9},{8,10},{9,11},{10,... | collective-permute-start | bytes 442376 | tf_op jit(solution)/shard_map/ppermute | solution.py:426
  37.5 6.1 %collective-permute-start.7 = (bf16[24,1024]{1,0:T(8,128)(2,1)S(1)}, bf16[24,1024]{1,0:T(8,128)(2,1)S(1)}, u32[]{:S(2)}, u32[]{:S(2)}) collective-permute-start(bf16[24,1024]{1,0:T(8,128)(2,1)S(1)} %collective-permute-done.1.b_ref), channel_id=1, source_target_pairs={{0,6},{1,7},{2,8},{3,9},{4,10},{5,11},{6,12},{7,13},{8,14},{9,15},... | collective-permute-start | bytes 147464 | tf_op jit(solution)/shard_map/ppermute | solution.py:426
  43.6 4.2 %collective-permute-start.13 = (bf16[24,1024]{1,0:T(8,128)(2,1)S(1)}, bf16[24,1024]{1,0:T(8,128)(2,1)S(1)}, u32[]{:S(2)}, u32[]{:S(2)}) collective-permute-start(bf16[24,1024]{1,0:T(8,128)(2,1)S(1)} %collective-permute-done.7.refs_5_), channel_id=1, source_target_pairs={{0,1},{1,0},{2,3},{3,2},{4,5},{5,4},{6,7},{7,6},{8,9},{9,8},{10,11... | collective-permute-start | bytes 147464 | tf_op jit(solution)/shard_map/ppermute | solution.py:420
  46.8 1.8 %collective-permute-start.8 = (bf16[3,24,1024]{2,1,0:T(8,128)(2,1)S(1)}, bf16[3,24,1024]{2,1,0:T(8,128)(2,1)S(1)}, u32[]{:S(2)}, u32[]{:S(2)}) collective-permute-start(bf16[3,24,1024]{2,1,0:T(8,128)(2,1)S(1)} %shard_map.249.refs_0_), channel_id=1, source_target_pairs={{0,1},{1,0},{2,3},{3,2},{4,5},{5,4},{6,7},{7,6},{8,9},{9,8},{10,11... | collective-permute-start | bytes 442376 | tf_op jit(solution)/shard_map/ppermute | solution.py:420
  46.8 1.8 %collective-permute-start.10 = (bf16[3,24,1024]{2,1,0:T(8,128)(2,1)S(1)}, bf16[3,24,1024]{2,1,0:T(8,128)(2,1)S(1)}, u32[]{:S(2)}, u32[]{:S(2)}) collective-permute-start(bf16[3,24,1024]{2,1,0:T(8,128)(2,1)S(1)} %collective-permute-done.4.refs_2_), channel_id=1, source_target_pairs={{0,1},{1,0},{2,3},{3,2},{4,5},{5,4},{6,7},{7,6},{8,9},{9,8},{10,11... | collective-permute-start | bytes 442376 | tf_op jit(solution)/shard_map/ppermute | solution.py:420
  47.7 1.4 collective-permute-start.9
  48.1 1.4 collective-permute-start.12
  48.2 1.4 collective-permute-start.11
  68.4 4.2 %collective-permute-start.14 = (bf16[16,32,128]{2,1,0:T(8,128)(2,1)S(1)}, bf16[16,32,128]{2,1,0:T(8,128)(2,1)S(1)}, u32[]{:S(2)}, u32[]{:S(2)}) collective-permute-start(bf16[16,32,128]{2,1,0:T(8,128)(2,1)S(1)} %all_to_all.5.a_ref), channel_id=1, source_target_pairs={{0,1},{1,0},{2,3},{3,2},{4,5},{5,4},{6,7},{7,6},{8,9},{9,8},{10,11... | collective-permute-start | bytes 393224 | tf_op jit(solution)/shard_map/ppermute | solution.py:420
  72.6 38.6 %copy-start.3 = (bf16[1,512,2048]{2,1,0:T(8,128)(2,1)S(1)}, bf16[1,512,2048]{2,1,0:T(8,128)(2,1)}, u32[]{:S(2)}) copy-start(bf16[1,512,2048]{2,1,0:T(8,128)(2,1)} %refs_17_.1) | copy-start | bytes 6291460
  72.6 38.6 %copy-start.5 = (bf16[2048,256]{1,0:T(8,128)(2,1)S(1)}, bf16[2048,256]{1,0:T(8,128)(2,1)}, u32[]{:S(2)}) copy-start(bf16[2048,256]{1,0:T(8,128)(2,1)} %refs_19_.1) | copy-start | bytes 3145732
  77.1 33.1 %copy-start.8 = (bf16[2048]{0:T(1024)(128)(2,1)S(1)}, bf16[2048]{0:T(1024)(128)(2,1)}, u32[]{:S(2)}) copy-start(bf16[2048]{0:T(1024)(128)(2,1)} %param.45) | copy-start | bytes 12292
  77.1 34.1 %copy-start = (bf16[256,2048]{1,0:T(8,128)(2,1)S(1)}, bf16[256,2048]{1,0:T(8,128)(2,1)}, u32[]{:S(2)}) copy-start(bf16[256,2048]{1,0:T(8,128)(2,1)} %dd_ref.1) | copy-start | bytes 3145732
  77.1 34.1 %copy-start.1 = (bf16[1,2048,512]{2,1,0:T(8,128)(2,1)S(1)}, bf16[1,2048,512]{2,1,0:T(8,128)(2,1)}, u32[]{:S(2)}) copy-start(bf16[1,2048,512]{2,1,0:T(8,128)(2,1)} %refs_15_.1) | copy-start | bytes 6291460
  77.1 34.1 %copy-start.2 = (bf16[1,2048,512]{2,1,0:T(8,128)(2,1)S(1)}, bf16[1,2048,512]{2,1,0:T(8,128)(2,1)}, u32[]{:S(2)}) copy-start(bf16[1,2048,512]{2,1,0:T(8,128)(2,1)} %refs_16_.1) | copy-start | bytes 6291460
  77.1 34.1 %copy-start.4 = (bf16[2048,256]{1,0:T(8,128)(2,1)S(1)}, bf16[2048,256]{1,0:T(8,128)(2,1)}, u32[]{:S(2)}) copy-start(bf16[2048,256]{1,0:T(8,128)(2,1)} %refs_18_.1) | copy-start | bytes 3145732
  77.1 1.3 collective-permute-start.15
  78.5 11.0 %collective-permute-start.17 = (bf16[24,1024]{1,0:T(8,128)(2,1)S(1)}, bf16[24,1024]{1,0:T(8,128)(2,1)S(1)}, u32[]{:S(2)}, u32[]{:S(2)}) collective-permute-start(bf16[24,1024]{1,0:T(8,128)(2,1)S(1)} %shard_map.253.a_ref), channel_id=1, source_target_pairs={{0,22},{1,23},{2,24},{3,25},{4,26},{5,27},{6,28},{7,29},{8,30},{9,... | collective-permute-start | bytes 147464 | tf_op jit(solution)/shard_map/ppermute | solution.py:426
  80.7 12.1 %collective-permute-start.16 = (bf16[24,1024]{1,0:T(8,128)(2,1)S(1)}, bf16[24,1024]{1,0:T(8,128)(2,1)S(1)}, u32[]{:S(2)}, u32[]{:S(2)}) collective-permute-start(bf16[24,1024]{1,0:T(8,128)(2,1)S(1)} %shard_map.253.a_ref), channel_id=1, source_target_pairs={{0,10},{1,11},{2,12},{3,13},{4,14},{5,15},{6,16},{7,17},{8,18},{9,... | collective-permute-start | bytes 147464 | tf_op jit(solution)/shard_map/ppermute | solution.py:426
  92.9 5.0 %collective-permute-start.19 = (bf16[3,24,1024]{2,1,0:T(8,128)(2,1)S(1)}, bf16[3,24,1024]{2,1,0:T(8,128)(2,1)S(1)}, u32[]{:S(2)}, u32[]{:S(2)}) collective-permute-start(bf16[3,24,1024]{2,1,0:T(8,128)(2,1)S(1)} %shard_map.255.refs_0_), channel_id=1, source_target_pairs={{0,30},{1,31},{2,0},{3,1},{4,2},{5,3},{6,4},{7,5},{8,6},{9,7},{10,... | collective-permute-start | bytes 442376 | tf_op jit(solution)/shard_map/ppermute | solution.py:426
  93.3 5.7 %collective-permute-start.18 = (bf16[3,24,1024]{2,1,0:T(8,128)(2,1)S(1)}, bf16[3,24,1024]{2,1,0:T(8,128)(2,1)S(1)}, u32[]{:S(2)}, u32[]{:S(2)}) collective-permute-start(bf16[3,24,1024]{2,1,0:T(8,128)(2,1)S(1)} %shard_map.255.refs_0_), channel_id=1, source_target_pairs={{0,2},{1,3},{2,4},{3,5},{4,6},{5,7},{6,8},{7,9},{8,10},{9,11},{10,... | collective-permute-start | bytes 442376 | tf_op jit(solution)/shard_map/ppermute | solution.py:426
  97.9 11.8 %collective-permute-start.21 = (bf16[3,24,1024]{2,1,0:T(8,128)(2,1)S(1)}, bf16[3,24,1024]{2,1,0:T(8,128)(2,1)S(1)}, u32[]{:S(2)}, u32[]{:S(2)}) collective-permute-start(bf16[3,24,1024]{2,1,0:T(8,128)(2,1)S(1)} %collective-permute-done.19.refs_2_), channel_id=1, source_target_pairs={{0,30},{1,31},{2,0},{3,1},{4,2},{5,3},{6,4},{7,5},{8,6},{9,7},{10,... | collective-permute-start | bytes 442376 | tf_op jit(solution)/shard_map/ppermute | solution.py:426
  99.0 10.8 %collective-permute-start.20 = (bf16[3,24,1024]{2,1,0:T(8,128)(2,1)S(1)}, bf16[3,24,1024]{2,1,0:T(8,128)(2,1)S(1)}, u32[]{:S(2)}, u32[]{:S(2)}) collective-permute-start(bf16[3,24,1024]{2,1,0:T(8,128)(2,1)S(1)} %collective-permute-done.18.refs_1_), channel_id=1, source_target_pairs={{0,2},{1,3},{2,4},{3,5},{4,6},{5,7},{6,8},{7,9},{8,10},{9,11},{10,... | collective-permute-start | bytes 442376 | tf_op jit(solution)/shard_map/ppermute | solution.py:426
  99.4 6.7 %collective-permute-start.22 = (bf16[24,1024]{1,0:T(8,128)(2,1)S(1)}, bf16[24,1024]{1,0:T(8,128)(2,1)S(1)}, u32[]{:S(2)}, u32[]{:S(2)}) collective-permute-start(bf16[24,1024]{1,0:T(8,128)(2,1)S(1)} %collective-permute-done.16.b_ref), channel_id=1, source_target_pairs={{0,6},{1,7},{2,8},{3,9},{4,10},{5,11},{6,12},{7,13},{8,14},{9,15},... | collective-permute-start | bytes 147464 | tf_op jit(solution)/shard_map/ppermute | solution.py:426
  106.1 3.2 %collective-permute-start.28 = (bf16[24,1024]{1,0:T(8,128)(2,1)S(1)}, bf16[24,1024]{1,0:T(8,128)(2,1)S(1)}, u32[]{:S(2)}, u32[]{:S(2)}) collective-permute-start(bf16[24,1024]{1,0:T(8,128)(2,1)S(1)} %collective-permute-done.22.refs_5_), channel_id=1, source_target_pairs={{0,1},{1,0},{2,3},{3,2},{4,5},{5,4},{6,7},{7,6},{8,9},{9,8},{10,11... | collective-permute-start | bytes 147464 | tf_op jit(solution)/shard_map/ppermute | solution.py:420
  108.4 2.2 %collective-permute-start.23 = (bf16[3,24,1024]{2,1,0:T(8,128)(2,1)S(1)}, bf16[3,24,1024]{2,1,0:T(8,128)(2,1)S(1)}, u32[]{:S(2)}, u32[]{:S(2)}) collective-permute-start(bf16[3,24,1024]{2,1,0:T(8,128)(2,1)S(1)} %shard_map.255.refs_0_), channel_id=1, source_target_pairs={{0,1},{1,0},{2,3},{3,2},{4,5},{5,4},{6,7},{7,6},{8,9},{9,8},{10,11... | collective-permute-start | bytes 442376 | tf_op jit(solution)/shard_map/ppermute | solution.py:420
  108.4 2.2 %collective-permute-start.25 = (bf16[3,24,1024]{2,1,0:T(8,128)(2,1)S(1)}, bf16[3,24,1024]{2,1,0:T(8,128)(2,1)S(1)}, u32[]{:S(2)}, u32[]{:S(2)}) collective-permute-start(bf16[3,24,1024]{2,1,0:T(8,128)(2,1)S(1)} %collective-permute-done.19.refs_2_), channel_id=1, source_target_pairs={{0,1},{1,0},{2,3},{3,2},{4,5},{5,4},{6,7},{7,6},{8,9},{9,8},{10,11... | collective-permute-start | bytes 442376 | tf_op jit(solution)/shard_map/ppermute | solution.py:420
  109.3 1.4 collective-permute-start.24
  109.7 1.4 collective-permute-start.27
  109.8 1.4 collective-permute-start.26
  114.3 2.4 %collective-permute-start.29 = (bf16[384,1024]{1,0:T(8,128)(2,1)S(1)}, bf16[384,1024]{1,0:T(8,128)(2,1)S(1)}, u32[]{:S(2)}, u32[]{:S(2)}) collective-permute-start(bf16[384,1024]{1,0:T(8,128)(2,1)S(1)} %get-tuple-element.58), channel_id=1, source_target_pairs={{0,1},{1,0},{2,3},{3,2},{4,5},{5,4},{6,7},{7,6},{8,9},{9,8},{10,11... | collective-permute-start | bytes 2359304 | tf_op jit(solution)/shard_map/ppermute | solution.py:420
  116.9 6.4 %collective-permute-start.30 = (bf16[3,24,1024]{2,1,0:T(8,128)(2,1)S(1)}, bf16[3,24,1024]{2,1,0:T(8,128)(2,1)S(1)}, u32[]{:S(2)}, u32[]{:S(2)}) collective-permute-start(bf16[3,24,1024]{2,1,0:T(8,128)(2,1)S(1)} %get-tuple-element.61), channel_id=1, source_target_pairs={{0,2},{1,3},{2,4},{3,5},{4,6},{5,7},{6,8},{7,9},{8,10},{9,11},{10,... | collective-permute-start | bytes 442376 | tf_op jit(solution)/shard_map/ppermute | solution.py:426
  118.3 5.9 %collective-permute-start.32 = (bf16[3,24,1024]{2,1,0:T(8,128)(2,1)S(1)}, bf16[3,24,1024]{2,1,0:T(8,128)(2,1)S(1)}, u32[]{:S(2)}, u32[]{:S(2)}) collective-permute-start(bf16[3,24,1024]{2,1,0:T(8,128)(2,1)S(1)} %get-tuple-element.63), channel_id=1, source_target_pairs={{0,30},{1,31},{2,0},{3,1},{4,2},{5,3},{6,4},{7,5},{8,6},{9,7},{10,... | collective-permute-start | bytes 442376 | tf_op jit(solution)/shard_map/ppermute | solution.py:426
  123.3 5.3 %collective-permute-start.31 = (bf16[3,24,1024]{2,1,0:T(8,128)(2,1)S(1)}, bf16[3,24,1024]{2,1,0:T(8,128)(2,1)S(1)}, u32[]{:S(2)}, u32[]{:S(2)}) collective-permute-start(bf16[3,24,1024]{2,1,0:T(8,128)(2,1)S(1)} %shard_map.260), channel_id=1, source_target_pairs={{0,2},{1,3},{2,4},{3,5},{4,6},{5,7},{6,8},{7,9},{8,10},{9,11},{10,... | collective-permute-start | bytes 442376 | tf_op jit(solution)/shard_map/ppermute | solution.py:426
  124.2 4.4 %collective-permute-start.33 = (bf16[3,24,1024]{2,1,0:T(8,128)(2,1)S(1)}, bf16[3,24,1024]{2,1,0:T(8,128)(2,1)S(1)}, u32[]{:S(2)}, u32[]{:S(2)}) collective-permute-start(bf16[3,24,1024]{2,1,0:T(8,128)(2,1)S(1)} %shard_map.261), channel_id=1, source_target_pairs={{0,30},{1,31},{2,0},{3,1},{4,2},{5,3},{6,4},{7,5},{8,6},{9,7},{10,... | collective-permute-start | bytes 442376 | tf_op jit(solution)/shard_map/ppermute | solution.py:426
  126.2 6.6 %collective-permute-start.34 = (bf16[24,1024]{1,0:T(8,128)(2,1)S(1)}, bf16[24,1024]{1,0:T(8,128)(2,1)S(1)}, u32[]{:S(2)}, u32[]{:S(2)}) collective-permute-start(bf16[24,1024]{1,0:T(8,128)(2,1)S(1)} %get-tuple-element.66), channel_id=1, source_target_pairs={{0,6},{1,7},{2,8},{3,9},{4,10},{5,11},{6,12},{7,13},{8,14},{9,15},... | collective-permute-start | bytes 147464 | tf_op jit(solution)/shard_map/ppermute | solution.py:426
  132.8 9.1 %collective-permute-start.35 = (bf16[24,1024]{1,0:T(8,128)(2,1)S(1)}, bf16[24,1024]{1,0:T(8,128)(2,1)S(1)}, u32[]{:S(2)}, u32[]{:S(2)}) collective-permute-start(bf16[24,1024]{1,0:T(8,128)(2,1)S(1)} %shard_map.264), channel_id=1, source_target_pairs={{0,10},{1,11},{2,12},{3,13},{4,14},{5,15},{6,16},{7,17},{8,18},{9,... | collective-permute-start | bytes 147464 | tf_op jit(solution)/shard_map/ppermute | solution.py:426
  136.0 7.8 %collective-permute-start.36 = (bf16[24,1024]{1,0:T(8,128)(2,1)S(1)}, bf16[24,1024]{1,0:T(8,128)(2,1)S(1)}, u32[]{:S(2)}, u32[]{:S(2)}) collective-permute-start(bf16[24,1024]{1,0:T(8,128)(2,1)S(1)} %get-tuple-element.67), channel_id=1, source_target_pairs={{0,22},{1,23},{2,24},{3,25},{4,26},{5,27},{6,28},{7,29},{8,30},{9,... | collective-permute-start | bytes 147464 | tf_op jit(solution)/shard_map/ppermute | solution.py:426
  143.9 6.0 %collective-permute-start.37 = (f32[12,1024]{1,0:T(8,128)S(1)}, f32[12,1024]{1,0:T(8,128)S(1)}, u32[]{:S(2)}, u32[]{:S(2)}) collective-permute-start(f32[12,1024]{1,0:T(8,128)S(1)} %get-tuple-element.69), channel_id=1, source_target_pairs={{0,1},{1,0},{2,3},{3,2},{4,5},{5,4},{6,7},{7,6},{8,9},{9,8},{10,11... | collective-permute-start | bytes 147464 | tf_op jit(solution)/shard_map/ppermute | solution.py:420

commit v8 on v7

--- a/solution.py
+++ b/solution.py
@@ -308,7 +308,7 @@
 def branch_kernel(*refs):
     xs, ys = refs[:6], refs[6:12]
     (picker_ref, placer_ref, weight_ref, eg_ref, eu_ref, ed_ref, dg_ref, du_ref, dd_ref, bw_ref,
-     send_ref, hidden_ref, made, gains_ref, x_scr, y_scr) = refs[12:]
+     early_ref, late_ref, hidden_ref, made, gains_ref, x_scr, y_scr) = refs[12:]
     c = core()
     rows, h = x_scr.shape
     at = pl.ds(pl.multiple_of(c * h, h), h)
@@ -333,7 +333,11 @@
     hidden_ref[...] = hidden
     gains_ref[...] = jnp.where(lane == 0, sig, weight)
     part = dot(hidden, dd_ref[:, to]) * sig
-    send_ref[...] = (part + dot(placer_ref[...], made[:, to]) * weight).astype(BF16)
+    send = (part + dot(placer_ref[...], made[:, to]) * weight).astype(BF16)
+    size = rows // 16
+    early_ref[...] = send[9 * size : 15 * size]
+    late_ref[: 9 * size] = send[: 9 * size]
+    late_ref[9 * size :] = send[15 * size :]
 
 
 def rest_kernel(hidden_ref, made_ref, placer_ref, gains_ref, dd_ref, keep_ref):
@@ -344,20 +348,29 @@
     keep_ref[...] = part + dot(placer_ref[...], made_ref[:, at]) * gains_ref[:, 1:2]
 
 
-def spread_kernel(keep_ref, got_ref, zero_ref, one_ref, back_ref, up_ref, down_ref, last_ref):
-    nz = keep_ref.shape[0]
-    order = offsets(nz)
+def early_kernel(keep_ref, got_ref, up_ref, down_ref):
+    order = offsets(keep_ref.shape[0])
 
     def term(offset):
-        at = order.index(offset % nz)
-        return keep_ref[at] + got_ref[at].astype(F32)
+        at = order.index(offset % len(order))
+        return (keep_ref[at] + got_ref[at - 9].astype(F32)).astype(BF16)
+
+    for i, far in enumerate((0, FAR, -FAR)):
+        up_ref[i] = term(far + 2)
+        down_ref[i] = term(far - 2)
+
+
+def late_kernel(keep_ref, got_ref, zero_ref, one_ref, back_ref, last_ref):
+    order = offsets(keep_ref.shape[0])
+
+    def term(offset):
+        at = order.index(offset % len(order))
+        return keep_ref[at] + got_ref[at if at < 9 else 9].astype(F32)
 
     for i, far in enumerate((0, FAR, -FAR)):
         zero_ref[i] = term(far)
         one_ref[i] = term(far + 1)
         back_ref[i] = term(far - 1)
-        up_ref[i] = term(far + 2).astype(BF16)
-        down_ref[i] = term(far - 2).astype(BF16)
     last_ref[...] = term(8).astype(BF16)
 
 
@@ -454,7 +467,6 @@
     chunk, = call(norm_kernel, [(tile, BF16)], (normed, other, gains),
                   scratch=[(tile, F32)])
     xs, ys = gather(chunk, info)
-    info, = call(mark_kernel, [(info.shape, BF16)], (info,))
     projected, = call(
         proj_kernel, [((nz, 2 * r + 8, 4 * inner // n), BF16)],
         (*xs, *ys, w_all, info), scratch=[((n * r, h), BF16)] * 2)
@@ -479,20 +491,22 @@
         route_kernel,
         [((n * CAP, n * r), BF16), ((n * r, n * CAP), BF16), ((n * r, 128), F32)],
         (a, b), scratch=[((4, n * r, 128), F32)])
-    send, hidden, made, scales = call(
+    early, late, hidden, made, scales = call(
         branch_kernel,
-        [((n * r, h), BF16), ((n * r, dense_down.shape[0]), BF16), ((n * CAP, d), BF16),
+        [((6 * 2 * r, h), BF16), ((10 * 2 * r, h), BF16), ((n * r, dense_down.shape[0]), BF16),
+         ((n * CAP, d), BF16),
          ((n * r, 128), F32)],
         (*xs, *ys, picker, placer, weight, expert_gate, expert_up, expert_down, dense_gate,
          dense_up, dense_down, branch_weight.reshape(1, d)),
         scratch=[((n * r, h), BF16), ((n * r, h), BF16)], vmem=32)
-    got = swap(send)
+    early, late = swap(early), swap(late)
     part, = call(rest_kernel, [((n * r, h), F32)], (hidden, made, placer, scales, dense_down),
                  flops=400000000)
+    part = part.reshape((nz,) + tile)
     three = (3,) + tile
-    own, one, back, up, down, last = call(
-        spread_kernel, [(three, F32)] * 3 + [(three, BF16)] * 2 + [(tile, BF16)],
-        (part.reshape((nz,) + tile), got.reshape((nz,) + tile)))
+    up, down = call(early_kernel, [(three, BF16)] * 2, (part, early.reshape((6,) + tile)))
+    own, one, back, last = call(
+        late_kernel, [(three, F32)] * 3 + [(tile, BF16)], (part, late.reshape((10,) + tile)))
     last = shift(last, 8 - FAR)
     up, down = shift(up, 1), shift(down, -1)
     mark, = call(mark_kernel, [(token.shape, F32)], (token,))

time: 151 us -> 151 us (level)
    ppermute x17 -> x18, starting transfers between devices: 27.7 us -> 27.9 us  [swap(): return lax.ppermute(x, 'ep', pairs)]
    ppermute x17 -> x18, waiting for transfers between devices: 6.63 us -> 6.42 us  [swap(): return lax.ppermute(x, 'ep', pairs)]
  transfers between devices with their start and end apart: 38 -> 39, of which waited for: 24 -> 24; matrix products, arithmetic and copies ran while one was open for 0% -> 0% of each run, Pallas kernels for 8% -> 8%
where the time goes in v8:
time: 151 us
  starting transfers between devices  66.4 us (44%)
  waiting for transfers between devices  44 us (29%)
  Pallas kernels  21.2 us (14%)
  blocking collectives  18.1 us (12%)
    ppermute x21, starting transfers between devices, shift(): lax.ppermute(x, 'ep', [(2 * z + c, 2 * ((z + offset) % nz) + c) for z in...  38.5 us
    ppermute x21, waiting for transfers between devices, shift(): lax.ppermute(x, 'ep', [(2 * z + c, 2 * ((z + offset) % nz) + c) for z in...  37.6 us
    ppermute x18, starting transfers between devices, swap(): return lax.ppermute(x, 'ep', pairs)  27.9 us
    pallas_call x21, Pallas kernels, call(): pl.pallas_call(kernel, out_shape=[pltpu.VMEM(s, d) if i in held and (not...  21.2 us
    all_to_all x1, blocking collectives, exchange(): return lax.all_to_all(x, 'ep', 0, 0, axis_index_groups=groups)  18.1 us
    ppermute x18, waiting for transfers between devices, swap(): return lax.ppermute(x, 'ep', pairs)  6.42 us
  transfers between devices with their start and end apart: 39, of which 24 were waited for; matrix products, arithmetic and copies ran while one was open for 0% of the time, Pallas kernels for 8%

profile of v8, /device:TPU:69, one launch (start us, length us, event | category | flops | bytes accessed | tf_op | source)
XLA Modules:
  0.0 150.6 jit_solution(13937221240205041767)
XLA Ops:
  0.6 10.0 %collective-permute-start = (bf16[12,2048]{1,0:T(8,128)(2,1)}, bf16[12,2048]{1,0:T(8,128)(2,1)S(1)}, u32[]{:S(2)}, u32[]{:S(2)}) collective-permute-start(bf16[12,2048]{1,0:T(8,128)(2,1)} %resid_ref.1), channel_id=1, source_target_pairs={{0,1},{1,0},{2,3},{3,2},{4,5},{5,4},{6,7},{7,6},{8,9},{9,8},{10,11... | collective-permute-start | bytes 147464 | tf_op jit(solution)/shard_map/ppermute | solution.py:433
  10.6 1.0 shard_map.246
  11.9 6.1 %collective-permute-start.2 = (bf16[24,1024]{1,0:T(8,128)(2,1)S(1)}, bf16[24,1024]{1,0:T(8,128)(2,1)S(1)}, u32[]{:S(2)}, u32[]{:S(2)}) collective-permute-start(bf16[24,1024]{1,0:T(8,128)(2,1)S(1)} %shard_map.247.a_ref), channel_id=1, source_target_pairs={{0,22},{1,23},{2,24},{3,25},{4,26},{5,27},{6,28},{7,29},{8,30},{9,... | collective-permute-start | bytes 147464 | tf_op jit(solution)/shard_map/ppermute | solution.py:439
  18.3 5.1 %shard_map.248 = (f32[12,8]{1,0:T(8,128)S(1)}, f32[12,8]{1,0:T(8,128)S(1)}, f32[8,12]{1,0:T(8,128)}, bf16[8,128]{1,0:T(8,128)(2,1)S(1)}, bf16[128,2048]{1,0:T(8,...) custom-call(bf16[12,2048]{1,0:T(8,128)(2,1)S(1)} %get-tuple-element.40.own_ref.normed_ref, ...), custom_call_target="tpu_custom_call" | custom-call | flops 1000000 | bytes 1000000 | tf_op jit(solution)/shard_map/pallas_call | solution.py:25
  23.4 7.7 %collective-permute-done.1.b_ref = bf16[24,1024]{1,0:T(8,128)(2,1)S(1)} collective-permute-done((bf16[24,1024]{1,0:T(8,128)(2,1)S(1)}, bf16[24,1024]{1,0:T(8,128)(2,1)S(1)}, u32[]{:S(2)}, u32[]{:S(2)}) %collective-permute-start.1) | collective-permute-done | bytes 49184 | tf_op jit(solution)/shard_map/ppermute | solution.py:439
  31.2 1.4 collective-permute-start.3
  32.7 3.3 %collective-permute-done.4.refs_2_ = bf16[3,24,1024]{2,1,0:T(8,128)(2,1)S(1)} collective-permute-done((bf16[3,24,1024]{2,1,0:T(8,128)(2,1)S(1)}, bf16[3,24,1024]{2,1,0:T(8,128)(2,1)S(1)}, u32[]{:S(2)}, u32[]{:S(2)}) %collective-permute-start.4) | collective-permute-done | bytes 147488 | tf_op jit(solution)/shard_map/ppermute | solution.py:439
  36.0 1.4 collective-permute-start.6
  37.5 2.0 %collective-permute-start.7 = (bf16[24,1024]{1,0:T(8,128)(2,1)S(1)}, bf16[24,1024]{1,0:T(8,128)(2,1)S(1)}, u32[]{:S(2)}, u32[]{:S(2)}) collective-permute-start(bf16[24,1024]{1,0:T(8,128)(2,1)S(1)} %collective-permute-done.1.b_ref), channel_id=1, source_target_pairs={{0,6},{1,7},{2,8},{3,9},{4,10},{5,11},{6,12},{7,13},{8,14},{9,15},... | collective-permute-start | bytes 147464 | tf_op jit(solution)/shard_map/ppermute | solution.py:439
  39.5 4.0 %collective-permute-done.7.refs_5_ = bf16[24,1024]{1,0:T(8,128)(2,1)S(1)} collective-permute-done((bf16[24,1024]{1,0:T(8,128)(2,1)S(1)}, bf16[24,1024]{1,0:T(8,128)(2,1)S(1)}, u32[]{:S(2)}, u32[]{:S(2)}) %collective-permute-start.7) | collective-permute-done | bytes 49184 | tf_op jit(solution)/shard_map/ppermute | solution.py:439
  43.6 3.3 %collective-permute-start.13 = (bf16[24,1024]{1,0:T(8,128)(2,1)S(1)}, bf16[24,1024]{1,0:T(8,128)(2,1)S(1)}, u32[]{:S(2)}, u32[]{:S(2)}) collective-permute-start(bf16[24,1024]{1,0:T(8,128)(2,1)S(1)} %collective-permute-done.7.refs_5_), channel_id=1, source_target_pairs={{0,1},{1,0},{2,3},{3,2},{4,5},{5,4},{6,7},{7,6},{8,9},{9,8},{10,11... | collective-permute-start | bytes 147464 | tf_op jit(solution)/shard_map/ppermute | solution.py:433
  46.8 0.5 collective-permute-start.10
  48.6 0.5 collective-permute-done.9.refs_7_
  49.7 0.6 shard_map.250
  50.2 18.1 %all_to_all.5.a_ref = bf16[16,32,128]{2,1,0:T(8,128)(2,1)S(1)} all-to-all(bf16[16,32,128]{2,1,0:T(8,128)(2,1)S(1)} %shard_map.250), channel_id=1, replica_groups={{0,2,4,6,8,10,12,14,16,18,20,22,24,26,28,30},{1,3,5,7,9,11,13,15,17,19,..., dimensions={0} | all-to-all | bytes 262144 | tf_op jit(solution)/shard_map/all_to_all | solution.py:436
  68.4 3.3 %collective-permute-start.14 = (bf16[16,32,128]{2,1,0:T(8,128)(2,1)S(1)}, bf16[16,32,128]{2,1,0:T(8,128)(2,1)S(1)}, u32[]{:S(2)}, u32[]{:S(2)}) collective-permute-start(bf16[16,32,128]{2,1,0:T(8,128)(2,1)S(1)} %all_to_all.5.a_ref), channel_id=1, source_target_pairs={{0,1},{1,0},{2,3},{3,2},{4,5},{5,4},{6,7},{7,6},{8,9},{9,8},{10,11... | collective-permute-start | bytes 393224 | tf_op jit(solution)/shard_map/ppermute | solution.py:433
  71.6 1.0 collective-permute-done.14.b_ref
  72.6 4.5 %shard_map.251 = (f32[12,2048]{1,0:T(8,128)S(1)}, bf16[12,1024]{1,0:T(8,128)(2,1)S(1)}, bf16[12,1024]{1,0:T(8,128)(2,1)S(1)}, f32[12,8,128]{2,1,0:T(8,128)}, f32...) custom-call(bf16[16,32,128]{2,1,0:T(8,128)(2,1)S(1)} %all_to_all.5.a_ref, ...), custom_call_target="tpu_custom_call" | custom-call | flops 1000000 | bytes 1000000 | tf_op jit(solution)/shard_map/pallas_call | solution.py:25
  77.6 0.9 collective-permute-done.15.got_ref
  78.5 2.2 %collective-permute-start.17 = (bf16[24,1024]{1,0:T(8,128)(2,1)S(1)}, bf16[24,1024]{1,0:T(8,128)(2,1)S(1)}, u32[]{:S(2)}, u32[]{:S(2)}) collective-permute-start(bf16[24,1024]{1,0:T(8,128)(2,1)S(1)} %shard_map.252.a_ref), channel_id=1, source_target_pairs={{0,22},{1,23},{2,24},{3,25},{4,26},{5,27},{6,28},{7,29},{8,30},{9,... | collective-permute-start | bytes 147464 | tf_op jit(solution)/shard_map/ppermute | solution.py:439
  80.7 4.2 %collective-permute-start.16 = (bf16[24,1024]{1,0:T(8,128)(2,1)S(1)}, bf16[24,1024]{1,0:T(8,128)(2,1)S(1)}, u32[]{:S(2)}, u32[]{:S(2)}) collective-permute-start(bf16[24,1024]{1,0:T(8,128)(2,1)S(1)} %shard_map.252.a_ref), channel_id=1, source_target_pairs={{0,10},{1,11},{2,12},{3,13},{4,14},{5,15},{6,16},{7,17},{8,18},{9,... | collective-permute-start | bytes 147464 | tf_op jit(solution)/shard_map/ppermute | solution.py:439
  84.9 4.7 %shard_map.253 = (f32[12,8,128,128]{3,2,1,0:T(8,128)}, f32[8,128]{1,0:T(8,128)S(1)}) custom-call(f32[12,8]{1,0:T(8,128)S(1)} %get-tuple-element.44.keep_ref, f32[8,16,128]{2,1,0:T(8,128)S(1)} %get-tuple-element.50.keys_ref, f32[128,128]{1,0:T(8,128)S(1)} %get-tuple-element.51.wvt_ref, f32[12,8,128,128]{3,2,1,0:T(8,128)S(1)} %get-tuple-element.46.m_ref), custom_call_target="tpu_custom_call" | custom-call | flops 1000000 | bytes 1000000 | tf_op jit(solution)/shard_map/pallas_call | solution.py:25
  89.6 3.3 %collective-permute-done.16.b_ref = bf16[24,1024]{1,0:T(8,128)(2,1)S(1)} collective-permute-done((bf16[24,1024]{1,0:T(8,128)(2,1)S(1)}, bf16[24,1024]{1,0:T(8,128)(2,1)S(1)}, u32[]{:S(2)}, u32[]{:S(2)}) %collective-permute-start.16) | collective-permute-done | bytes 49184 | tf_op jit(solution)/shard_map/ppermute | solution.py:439
  93.3 1.2 collective-permute-start.18
  94.5 3.4 %collective-permute-done.19.refs_2_ = bf16[3,24,1024]{2,1,0:T(8,128)(2,1)S(1)} collective-permute-done((bf16[3,24,1024]{2,1,0:T(8,128)(2,1)S(1)}, bf16[3,24,1024]{2,1,0:T(8,128)(2,1)S(1)}, u32[]{:S(2)}, u32[]{:S(2)}) %collective-permute-start.19) | collective-permute-done | bytes 147488 | tf_op jit(solution)/shard_map/ppermute | solution.py:439
  97.9 1.1 collective-permute-start.21
  99.4 3.6 %collective-permute-start.22 = (bf16[24,1024]{1,0:T(8,128)(2,1)S(1)}, bf16[24,1024]{1,0:T(8,128)(2,1)S(1)}, u32[]{:S(2)}, u32[]{:S(2)}) collective-permute-start(bf16[24,1024]{1,0:T(8,128)(2,1)S(1)} %collective-permute-done.16.b_ref), channel_id=1, source_target_pairs={{0,6},{1,7},{2,8},{3,9},{4,10},{5,11},{6,12},{7,13},{8,14},{9,15},... | collective-permute-start | bytes 147464 | tf_op jit(solution)/shard_map/ppermute | solution.py:439
  102.9 3.1 %collective-permute-done.22.refs_5_ = bf16[24,1024]{1,0:T(8,128)(2,1)S(1)} collective-permute-done((bf16[24,1024]{1,0:T(8,128)(2,1)S(1)}, bf16[24,1024]{1,0:T(8,128)(2,1)S(1)}, u32[]{:S(2)}, u32[]{:S(2)}) %collective-permute-start.22) | collective-permute-done | bytes 49184 | tf_op jit(solution)/shard_map/ppermute | solution.py:439
  106.1 2.4 %collective-permute-start.28 = (bf16[24,1024]{1,0:T(8,128)(2,1)S(1)}, bf16[24,1024]{1,0:T(8,128)(2,1)S(1)}, u32[]{:S(2)}, u32[]{:S(2)}) collective-permute-start(bf16[24,1024]{1,0:T(8,128)(2,1)S(1)} %collective-permute-done.22.refs_5_), channel_id=1, source_target_pairs={{0,1},{1,0},{2,3},{3,2},{4,5},{5,4},{6,7},{7,6},{8,9},{9,8},{10,11... | collective-permute-start | bytes 147464 | tf_op jit(solution)/shard_map/ppermute | solution.py:433
  108.4 0.5 collective-permute-start.25
  111.3 3.0 %shard_map.256 = (bf16[144,1024]{1,0:T(8,128)(2,1)S(1)}, bf16[240,1024]{1,0:T(8,128)(2,1)S(1)}, bf16[384,256]{1,0:T(8,128)(2,1)S(1)}, bf16[64,2048]{1,0:T(8,128)(2,1)S(1)}, f32[384,128]{1,0:T(8,128)S(1)}) custom-call(bf16[3,24,1024]{2,1,0:T(8,128)(2,1)S(1)} %shard_map.254.refs_0_, bf16[3,24,1024]{2,1,0:T(8,128)(2,1)S(1)} %collective-permute-done.18.refs_1_, ...), custom_call_target="tpu_custom_call" | custom-call | flops 1000000 | bytes 1000000 | tf_op jit(solution)/shard_map/pallas_call | solution.py:25
  115.0 0.6 shard_map.257
  115.6 1.2 collective-permute-done.30
  116.8 1.4 collective-permute-start.31
  118.2 1.3 collective-permute-start.33
  119.7 3.5 %collective-permute-done.31.got_ref = bf16[3,24,1024]{2,1,0:T(8,128)(2,1)S(1)} collective-permute-done((bf16[3,24,1024]{2,1,0:T(8,128)(2,1)S(1)}, bf16[3,24,1024]{2,1,0:T(8,128)(2,1)S(1)}, u32[]{:S(2)}, u32[]{:S(2)}) %collective-permute-start.31) | collective-permute-done | bytes 147488 | tf_op jit(solution)/shard_map/ppermute | solution.py:439
  123.5 0.6 collective-permute-done.33.got_ref
  124.1 2.0 %collective-permute-start.34 = (bf16[3,24,1024]{2,1,0:T(8,128)(2,1)S(1)}, bf16[3,24,1024]{2,1,0:T(8,128)(2,1)S(1)}, u32[]{:S(2)}, u32[]{:S(2)}) collective-permute-start(bf16[3,24,1024]{2,1,0:T(8,128)(2,1)S(1)} %shard_map.261), channel_id=1, source_target_pairs={{0,30},{1,31},{2,0},{3,1},{4,2},{5,3},{6,4},{7,5},{8,6},{9,7},{10,... | collective-permute-start | bytes 442376 | tf_op jit(solution)/shard_map/ppermute | solution.py:439
  126.2 1.5 collective-permute-start.35
  127.6 0.9 collective-permute-done.32.a_ref
  128.6 4.1 %collective-permute-done.35.last_ref = bf16[24,1024]{1,0:T(8,128)(2,1)S(1)} collective-permute-done((bf16[24,1024]{1,0:T(8,128)(2,1)S(1)}, bf16[24,1024]{1,0:T(8,128)(2,1)S(1)}, u32[]{:S(2)}, u32[]{:S(2)}) %collective-permute-start.35) | collective-permute-done | bytes 49184 | tf_op jit(solution)/shard_map/ppermute | solution.py:439
  132.7 3.2 %collective-permute-start.36 = (bf16[24,1024]{1,0:T(8,128)(2,1)S(1)}, bf16[24,1024]{1,0:T(8,128)(2,1)S(1)}, u32[]{:S(2)}, u32[]{:S(2)}) collective-permute-start(bf16[24,1024]{1,0:T(8,128)(2,1)S(1)} %shard_map.264), channel_id=1, source_target_pairs={{0,10},{1,11},{2,12},{3,13},{4,14},{5,15},{6,16},{7,17},{8,18},{9,... | collective-permute-start | bytes 147464 | tf_op jit(solution)/shard_map/ppermute | solution.py:439
  136.0 4.4 %collective-permute-start.37 = (bf16[24,1024]{1,0:T(8,128)(2,1)S(1)}, bf16[24,1024]{1,0:T(8,128)(2,1)S(1)}, u32[]{:S(2)}, u32[]{:S(2)}) collective-permute-start(bf16[24,1024]{1,0:T(8,128)(2,1)S(1)} %get-tuple-element.69), channel_id=1, source_target_pairs={{0,22},{1,23},{2,24},{3,25},{4,26},{5,27},{6,28},{7,29},{8,30},{9,... | collective-permute-start | bytes 147464 | tf_op jit(solution)/shard_map/ppermute | solution.py:439
  140.3 1.5 collective-permute-done.36.a_ref
  141.8 2.0 %collective-permute-done.37.b_ref = bf16[24,1024]{1,0:T(8,128)(2,1)S(1)} collective-permute-done((bf16[24,1024]{1,0:T(8,128)(2,1)S(1)}, bf16[24,1024]{1,0:T(8,128)(2,1)S(1)}, u32[]{:S(2)}, u32[]{:S(2)}) %collective-permute-start.37) | collective-permute-done | bytes 49184 | tf_op jit(solution)/shard_map/ppermute | solution.py:439
  143.9 5.1 %collective-permute-start.38 = (f32[12,1024]{1,0:T(8,128)S(1)}, f32[12,1024]{1,0:T(8,128)S(1)}, u32[]{:S(2)}, u32[]{:S(2)}) collective-permute-start(f32[12,1024]{1,0:T(8,128)S(1)} %get-tuple-element.71), channel_id=1, source_target_pairs={{0,1},{1,0},{2,3},{3,2},{4,5},{5,4},{6,7},{7,6},{8,9},{9,8},{10,11... | collective-permute-start | bytes 147464 | tf_op jit(solution)/shard_map/ppermute | solution.py:433
  149.0 0.9 collective-permute-done.38.got_ref
  149.9 0.7 shard_map.266
  (71 shorter events, 7.4 us)
Async XLA Ops:
  0.6 11.1 %collective-permute-start = (bf16[12,2048]{1,0:T(8,128)(2,1)}, bf16[12,2048]{1,0:T(8,128)(2,1)S(1)}, u32[]{:S(2)}, u32[]{:S(2)}) collective-permute-start(bf16[12,2048]{1,0:T(8,128)(2,1)} %resid_ref.1), channel_id=1, source_target_pairs={{0,1},{1,0},{2,3},{3,2},{4,5},{5,4},{6,7},{7,6},{8,9},{9,8},{10,11... | collective-permute-start | bytes 147464 | tf_op jit(solution)/shard_map/ppermute | solution.py:433
  11.9 11.5 %collective-permute-start.2 = (bf16[24,1024]{1,0:T(8,128)(2,1)S(1)}, bf16[24,1024]{1,0:T(8,128)(2,1)S(1)}, u32[]{:S(2)}, u32[]{:S(2)}) collective-permute-start(bf16[24,1024]{1,0:T(8,128)(2,1)S(1)} %shard_map.247.a_ref), channel_id=1, source_target_pairs={{0,22},{1,23},{2,24},{3,25},{4,26},{5,27},{6,28},{7,29},{8,30},{9,... | collective-permute-start | bytes 147464 | tf_op jit(solution)/shard_map/ppermute | solution.py:439
  17.9 13.2 %collective-permute-start.1 = (bf16[24,1024]{1,0:T(8,128)(2,1)S(1)}, bf16[24,1024]{1,0:T(8,128)(2,1)S(1)}, u32[]{:S(2)}, u32[]{:S(2)}) collective-permute-start(bf16[24,1024]{1,0:T(8,128)(2,1)S(1)} %shard_map.247.a_ref), channel_id=1, source_target_pairs={{0,10},{1,11},{2,12},{3,13},{4,14},{5,15},{6,16},{7,17},{8,18},{9,... | collective-permute-start | bytes 147464 | tf_op jit(solution)/shard_map/ppermute | solution.py:439
  18.3 54.3 %copy-start.6 = (bf16[12,2048]{1,0:T(8,128)(2,1)S(1)}, bf16[12,2048]{1,0:T(8,128)(2,1)}, u32[]{:S(2)}) copy-start(bf16[12,2048]{1,0:T(8,128)(2,1)} %resid_ref.1) | copy-start | bytes 147460
  18.3 54.3 %copy-start.7 = (f32[12,8,128]{2,1,0:T(8,128)S(1)}, f32[12,8,128]{2,1,0:T(8,128)}, u32[]{:S(2)}) copy-start(f32[12,8,128]{2,1,0:T(8,128)} %norm_ref.1) | copy-start | bytes 147460
  31.1 4.9 %collective-permute-start.4 = (bf16[3,24,1024]{2,1,0:T(8,128)(2,1)S(1)}, bf16[3,24,1024]{2,1,0:T(8,128)(2,1)S(1)}, u32[]{:S(2)}, u32[]{:S(2)}) collective-permute-start(bf16[3,24,1024]{2,1,0:T(8,128)(2,1)S(1)} %shard_map.249.refs_0_), channel_id=1, source_target_pairs={{0,30},{1,31},{2,0},{3,1},{4,2},{5,3},{6,4},{7,5},{8,6},{9,7},{10,... | collective-permute-start | bytes 442376 | tf_op jit(solution)/shard_map/ppermute | solution.py:439
  31.2 6.2 %collective-permute-start.3 = (bf16[3,24,1024]{2,1,0:T(8,128)(2,1)S(1)}, bf16[3,24,1024]{2,1,0:T(8,128)(2,1)S(1)}, u32[]{:S(2)}, u32[]{:S(2)}) collective-permute-start(bf16[3,24,1024]{2,1,0:T(8,128)(2,1)S(1)} %shard_map.249.refs_0_), channel_id=1, source_target_pairs={{0,2},{1,3},{2,4},{3,5},{4,6},{5,7},{6,8},{7,9},{8,10},{9,11},{10,... | collective-permute-start | bytes 442376 | tf_op jit(solution)/shard_map/ppermute | solution.py:439
  36.0 12.0 %collective-permute-start.6 = (bf16[3,24,1024]{2,1,0:T(8,128)(2,1)S(1)}, bf16[3,24,1024]{2,1,0:T(8,128)(2,1)S(1)}, u32[]{:S(2)}, u32[]{:S(2)}) collective-permute-start(bf16[3,24,1024]{2,1,0:T(8,128)(2,1)S(1)} %collective-permute-done.4.refs_2_), channel_id=1, source_target_pairs={{0,30},{1,31},{2,0},{3,1},{4,2},{5,3},{6,4},{7,5},{8,6},{9,7},{10,... | collective-permute-start | bytes 442376 | tf_op jit(solution)/shard_map/ppermute | solution.py:439
  37.4 10.8 %collective-permute-start.5 = (bf16[3,24,1024]{2,1,0:T(8,128)(2,1)S(1)}, bf16[3,24,1024]{2,1,0:T(8,128)(2,1)S(1)}, u32[]{:S(2)}, u32[]{:S(2)}) collective-permute-start(bf16[3,24,1024]{2,1,0:T(8,128)(2,1)S(1)} %collective-permute-done.3.refs_1_), channel_id=1, source_target_pairs={{0,2},{1,3},{2,4},{3,5},{4,6},{5,7},{6,8},{7,9},{8,10},{9,11},{10,... | collective-permute-start | bytes 442376 | tf_op jit(solution)/shard_map/ppermute | solution.py:439
  37.5 6.1 %collective-permute-start.7 = (bf16[24,1024]{1,0:T(8,128)(2,1)S(1)}, bf16[24,1024]{1,0:T(8,128)(2,1)S(1)}, u32[]{:S(2)}, u32[]{:S(2)}) collective-permute-start(bf16[24,1024]{1,0:T(8,128)(2,1)S(1)} %collective-permute-done.1.b_ref), channel_id=1, source_target_pairs={{0,6},{1,7},{2,8},{3,9},{4,10},{5,11},{6,12},{7,13},{8,14},{9,15},... | collective-permute-start | bytes 147464 | tf_op jit(solution)/shard_map/ppermute | solution.py:439
  43.6 4.2 %collective-permute-start.13 = (bf16[24,1024]{1,0:T(8,128)(2,1)S(1)}, bf16[24,1024]{1,0:T(8,128)(2,1)S(1)}, u32[]{:S(2)}, u32[]{:S(2)}) collective-permute-start(bf16[24,1024]{1,0:T(8,128)(2,1)S(1)} %collective-permute-done.7.refs_5_), channel_id=1, source_target_pairs={{0,1},{1,0},{2,3},{3,2},{4,5},{5,4},{6,7},{7,6},{8,9},{9,8},{10,11... | collective-permute-start | bytes 147464 | tf_op jit(solution)/shard_map/ppermute | solution.py:433
  46.8 1.8 %collective-permute-start.8 = (bf16[3,24,1024]{2,1,0:T(8,128)(2,1)S(1)}, bf16[3,24,1024]{2,1,0:T(8,128)(2,1)S(1)}, u32[]{:S(2)}, u32[]{:S(2)}) collective-permute-start(bf16[3,24,1024]{2,1,0:T(8,128)(2,1)S(1)} %shard_map.249.refs_0_), channel_id=1, source_target_pairs={{0,1},{1,0},{2,3},{3,2},{4,5},{5,4},{6,7},{7,6},{8,9},{9,8},{10,11... | collective-permute-start | bytes 442376 | tf_op jit(solution)/shard_map/ppermute | solution.py:433
  46.8 1.8 %collective-permute-start.10 = (bf16[3,24,1024]{2,1,0:T(8,128)(2,1)S(1)}, bf16[3,24,1024]{2,1,0:T(8,128)(2,1)S(1)}, u32[]{:S(2)}, u32[]{:S(2)}) collective-permute-start(bf16[3,24,1024]{2,1,0:T(8,128)(2,1)S(1)} %collective-permute-done.4.refs_2_), channel_id=1, source_target_pairs={{0,1},{1,0},{2,3},{3,2},{4,5},{5,4},{6,7},{7,6},{8,9},{9,8},{10,11... | collective-permute-start | bytes 442376 | tf_op jit(solution)/shard_map/ppermute | solution.py:433
  47.7 1.4 collective-permute-start.9
  48.1 1.4 collective-permute-start.12
  48.2 1.4 collective-permute-start.11
  68.4 4.2 %collective-permute-start.14 = (bf16[16,32,128]{2,1,0:T(8,128)(2,1)S(1)}, bf16[16,32,128]{2,1,0:T(8,128)(2,1)S(1)}, u32[]{:S(2)}, u32[]{:S(2)}) collective-permute-start(bf16[16,32,128]{2,1,0:T(8,128)(2,1)S(1)} %all_to_all.5.a_ref), channel_id=1, source_target_pairs={{0,1},{1,0},{2,3},{3,2},{4,5},{5,4},{6,7},{7,6},{8,9},{9,8},{10,11... | collective-permute-start | bytes 393224 | tf_op jit(solution)/shard_map/ppermute | solution.py:433
  72.6 38.6 %copy-start.3 = (bf16[1,512,2048]{2,1,0:T(8,128)(2,1)S(1)}, bf16[1,512,2048]{2,1,0:T(8,128)(2,1)}, u32[]{:S(2)}) copy-start(bf16[1,512,2048]{2,1,0:T(8,128)(2,1)} %refs_17_.1) | copy-start | bytes 6291460
  72.6 38.6 %copy-start.5 = (bf16[2048,256]{1,0:T(8,128)(2,1)S(1)}, bf16[2048,256]{1,0:T(8,128)(2,1)}, u32[]{:S(2)}) copy-start(bf16[2048,256]{1,0:T(8,128)(2,1)} %refs_19_.1) | copy-start | bytes 3145732
  77.1 33.1 %copy-start.8 = (bf16[2048]{0:T(1024)(128)(2,1)S(1)}, bf16[2048]{0:T(1024)(128)(2,1)}, u32[]{:S(2)}) copy-start(bf16[2048]{0:T(1024)(128)(2,1)} %param.45) | copy-start | bytes 12292
  77.1 34.1 %copy-start = (bf16[256,2048]{1,0:T(8,128)(2,1)S(1)}, bf16[256,2048]{1,0:T(8,128)(2,1)}, u32[]{:S(2)}) copy-start(bf16[256,2048]{1,0:T(8,128)(2,1)} %dd_ref.1) | copy-start | bytes 3145732
  77.1 34.1 %copy-start.1 = (bf16[1,2048,512]{2,1,0:T(8,128)(2,1)S(1)}, bf16[1,2048,512]{2,1,0:T(8,128)(2,1)}, u32[]{:S(2)}) copy-start(bf16[1,2048,512]{2,1,0:T(8,128)(2,1)} %refs_15_.1) | copy-start | bytes 6291460
  77.1 34.1 %copy-start.2 = (bf16[1,2048,512]{2,1,0:T(8,128)(2,1)S(1)}, bf16[1,2048,512]{2,1,0:T(8,128)(2,1)}, u32[]{:S(2)}) copy-start(bf16[1,2048,512]{2,1,0:T(8,128)(2,1)} %refs_16_.1) | copy-start | bytes 6291460
  77.1 34.1 %copy-start.4 = (bf16[2048,256]{1,0:T(8,128)(2,1)S(1)}, bf16[2048,256]{1,0:T(8,128)(2,1)}, u32[]{:S(2)}) copy-start(bf16[2048,256]{1,0:T(8,128)(2,1)} %refs_18_.1) | copy-start | bytes 3145732
  77.1 1.3 collective-permute-start.15
  78.5 11.0 %collective-permute-start.17 = (bf16[24,1024]{1,0:T(8,128)(2,1)S(1)}, bf16[24,1024]{1,0:T(8,128)(2,1)S(1)}, u32[]{:S(2)}, u32[]{:S(2)}) collective-permute-start(bf16[24,1024]{1,0:T(8,128)(2,1)S(1)} %shard_map.252.a_ref), channel_id=1, source_target_pairs={{0,22},{1,23},{2,24},{3,25},{4,26},{5,27},{6,28},{7,29},{8,30},{9,... | collective-permute-start | bytes 147464 | tf_op jit(solution)/shard_map/ppermute | solution.py:439
  80.7 12.1 %collective-permute-start.16 = (bf16[24,1024]{1,0:T(8,128)(2,1)S(1)}, bf16[24,1024]{1,0:T(8,128)(2,1)S(1)}, u32[]{:S(2)}, u32[]{:S(2)}) collective-permute-start(bf16[24,1024]{1,0:T(8,128)(2,1)S(1)} %shard_map.252.a_ref), channel_id=1, source_target_pairs={{0,10},{1,11},{2,12},{3,13},{4,14},{5,15},{6,16},{7,17},{8,18},{9,... | collective-permute-start | bytes 147464 | tf_op jit(solution)/shard_map/ppermute | solution.py:439
  92.9 5.0 %collective-permute-start.19 = (bf16[3,24,1024]{2,1,0:T(8,128)(2,1)S(1)}, bf16[3,24,1024]{2,1,0:T(8,128)(2,1)S(1)}, u32[]{:S(2)}, u32[]{:S(2)}) collective-permute-start(bf16[3,24,1024]{2,1,0:T(8,128)(2,1)S(1)} %shard_map.254.refs_0_), channel_id=1, source_target_pairs={{0,30},{1,31},{2,0},{3,1},{4,2},{5,3},{6,4},{7,5},{8,6},{9,7},{10,... | collective-permute-start | bytes 442376 | tf_op jit(solution)/shard_map/ppermute | solution.py:439
  93.3 5.7 %collective-permute-start.18 = (bf16[3,24,1024]{2,1,0:T(8,128)(2,1)S(1)}, bf16[3,24,1024]{2,1,0:T(8,128)(2,1)S(1)}, u32[]{:S(2)}, u32[]{:S(2)}) collective-permute-start(bf16[3,24,1024]{2,1,0:T(8,128)(2,1)S(1)} %shard_map.254.refs_0_), channel_id=1, source_target_pairs={{0,2},{1,3},{2,4},{3,5},{4,6},{5,7},{6,8},{7,9},{8,10},{9,11},{10,... | collective-permute-start | bytes 442376 | tf_op jit(solution)/shard_map/ppermute | solution.py:439
  97.9 11.8 %collective-permute-start.21 = (bf16[3,24,1024]{2,1,0:T(8,128)(2,1)S(1)}, bf16[3,24,1024]{2,1,0:T(8,128)(2,1)S(1)}, u32[]{:S(2)}, u32[]{:S(2)}) collective-permute-start(bf16[3,24,1024]{2,1,0:T(8,128)(2,1)S(1)} %collective-permute-done.19.refs_2_), channel_id=1, source_target_pairs={{0,30},{1,31},{2,0},{3,1},{4,2},{5,3},{6,4},{7,5},{8,6},{9,7},{10,... | collective-permute-start | bytes 442376 | tf_op jit(solution)/shard_map/ppermute | solution.py:439
  99.0 10.8 %collective-permute-start.20 = (bf16[3,24,1024]{2,1,0:T(8,128)(2,1)S(1)}, bf16[3,24,1024]{2,1,0:T(8,128)(2,1)S(1)}, u32[]{:S(2)}, u32[]{:S(2)}) collective-permute-start(bf16[3,24,1024]{2,1,0:T(8,128)(2,1)S(1)} %collective-permute-done.18.refs_1_), channel_id=1, source_target_pairs={{0,2},{1,3},{2,4},{3,5},{4,6},{5,7},{6,8},{7,9},{8,10},{9,11},{10,... | collective-permute-start | bytes 442376 | tf_op jit(solution)/shard_map/ppermute | solution.py:439
  99.4 6.7 %collective-permute-start.22 = (bf16[24,1024]{1,0:T(8,128)(2,1)S(1)}, bf16[24,1024]{1,0:T(8,128)(2,1)S(1)}, u32[]{:S(2)}, u32[]{:S(2)}) collective-permute-start(bf16[24,1024]{1,0:T(8,128)(2,1)S(1)} %collective-permute-done.16.b_ref), channel_id=1, source_target_pairs={{0,6},{1,7},{2,8},{3,9},{4,10},{5,11},{6,12},{7,13},{8,14},{9,15},... | collective-permute-start | bytes 147464 | tf_op jit(solution)/shard_map/ppermute | solution.py:439
  106.1 3.2 %collective-permute-start.28 = (bf16[24,1024]{1,0:T(8,128)(2,1)S(1)}, bf16[24,1024]{1,0:T(8,128)(2,1)S(1)}, u32[]{:S(2)}, u32[]{:S(2)}) collective-permute-start(bf16[24,1024]{1,0:T(8,128)(2,1)S(1)} %collective-permute-done.22.refs_5_), channel_id=1, source_target_pairs={{0,1},{1,0},{2,3},{3,2},{4,5},{5,4},{6,7},{7,6},{8,9},{9,8},{10,11... | collective-permute-start | bytes 147464 | tf_op jit(solution)/shard_map/ppermute | solution.py:433
  108.4 2.2 %collective-permute-start.23 = (bf16[3,24,1024]{2,1,0:T(8,128)(2,1)S(1)}, bf16[3,24,1024]{2,1,0:T(8,128)(2,1)S(1)}, u32[]{:S(2)}, u32[]{:S(2)}) collective-permute-start(bf16[3,24,1024]{2,1,0:T(8,128)(2,1)S(1)} %shard_map.254.refs_0_), channel_id=1, source_target_pairs={{0,1},{1,0},{2,3},{3,2},{4,5},{5,4},{6,7},{7,6},{8,9},{9,8},{10,11... | collective-permute-start | bytes 442376 | tf_op jit(solution)/shard_map/ppermute | solution.py:433
  108.4 2.2 %collective-permute-start.25 = (bf16[3,24,1024]{2,1,0:T(8,128)(2,1)S(1)}, bf16[3,24,1024]{2,1,0:T(8,128)(2,1)S(1)}, u32[]{:S(2)}, u32[]{:S(2)}) collective-permute-start(bf16[3,24,1024]{2,1,0:T(8,128)(2,1)S(1)} %collective-permute-done.19.refs_2_), channel_id=1, source_target_pairs={{0,1},{1,0},{2,3},{3,2},{4,5},{5,4},{6,7},{7,6},{8,9},{9,8},{10,11... | collective-permute-start | bytes 442376 | tf_op jit(solution)/shard_map/ppermute | solution.py:433
  109.3 1.4 collective-permute-start.24
  109.7 1.4 collective-permute-start.27
  109.8 1.4 collective-permute-start.26
  114.3 5.2 %collective-permute-start.29 = (bf16[240,1024]{1,0:T(8,128)(2,1)S(1)}, bf16[240,1024]{1,0:T(8,128)(2,1)S(1)}, u32[]{:S(2)}, u32[]{:S(2)}) collective-permute-start(bf16[240,1024]{1,0:T(8,128)(2,1)S(1)} %get-tuple-element.59), channel_id=1, source_target_pairs={{0,1},{1,0},{2,3},{3,2},{4,5},{5,4},{6,7},{7,6},{8,9},{9,8},{10,11... | collective-permute-start | bytes 1474568 | tf_op jit(solution)/shard_map/ppermute | solution.py:433
  114.8 2.0 %collective-permute-start.30 = (bf16[144,1024]{1,0:T(8,128)(2,1)S(1)}, bf16[144,1024]{1,0:T(8,128)(2,1)S(1)}, u32[]{:S(2)}, u32[]{:S(2)}) collective-permute-start(bf16[144,1024]{1,0:T(8,128)(2,1)S(1)} %get-tuple-element.62), channel_id=1, source_target_pairs={{0,1},{1,0},{2,3},{3,2},{4,5},{5,4},{6,7},{7,6},{8,9},{9,8},{10,11... | collective-permute-start | bytes 884744 | tf_op jit(solution)/shard_map/ppermute | solution.py:433
  116.8 6.4 %collective-permute-start.31 = (bf16[3,24,1024]{2,1,0:T(8,128)(2,1)S(1)}, bf16[3,24,1024]{2,1,0:T(8,128)(2,1)S(1)}, u32[]{:S(2)}, u32[]{:S(2)}) collective-permute-start(bf16[3,24,1024]{2,1,0:T(8,128)(2,1)S(1)} %get-tuple-element.63), channel_id=1, source_target_pairs={{0,2},{1,3},{2,4},{3,5},{4,6},{5,7},{6,8},{7,9},{8,10},{9,11},{10,... | collective-permute-start | bytes 442376 | tf_op jit(solution)/shard_map/ppermute | solution.py:439
  118.2 5.9 %collective-permute-start.33 = (bf16[3,24,1024]{2,1,0:T(8,128)(2,1)S(1)}, bf16[3,24,1024]{2,1,0:T(8,128)(2,1)S(1)}, u32[]{:S(2)}, u32[]{:S(2)}) collective-permute-start(bf16[3,24,1024]{2,1,0:T(8,128)(2,1)S(1)} %get-tuple-element.65), channel_id=1, source_target_pairs={{0,30},{1,31},{2,0},{3,1},{4,2},{5,3},{6,4},{7,5},{8,6},{9,7},{10,... | collective-permute-start | bytes 442376 | tf_op jit(solution)/shard_map/ppermute | solution.py:439
  123.2 5.3 %collective-permute-start.32 = (bf16[3,24,1024]{2,1,0:T(8,128)(2,1)S(1)}, bf16[3,24,1024]{2,1,0:T(8,128)(2,1)S(1)}, u32[]{:S(2)}, u32[]{:S(2)}) collective-permute-start(bf16[3,24,1024]{2,1,0:T(8,128)(2,1)S(1)} %shard_map.260), channel_id=1, source_target_pairs={{0,2},{1,3},{2,4},{3,5},{4,6},{5,7},{6,8},{7,9},{8,10},{9,11},{10,... | collective-permute-start | bytes 442376 | tf_op jit(solution)/shard_map/ppermute | solution.py:439
  124.1 4.4 %collective-permute-start.34 = (bf16[3,24,1024]{2,1,0:T(8,128)(2,1)S(1)}, bf16[3,24,1024]{2,1,0:T(8,128)(2,1)S(1)}, u32[]{:S(2)}, u32[]{:S(2)}) collective-permute-start(bf16[3,24,1024]{2,1,0:T(8,128)(2,1)S(1)} %shard_map.261), channel_id=1, source_target_pairs={{0,30},{1,31},{2,0},{3,1},{4,2},{5,3},{6,4},{7,5},{8,6},{9,7},{10,... | collective-permute-start | bytes 442376 | tf_op jit(solution)/shard_map/ppermute | solution.py:439
  126.2 6.6 %collective-permute-start.35 = (bf16[24,1024]{1,0:T(8,128)(2,1)S(1)}, bf16[24,1024]{1,0:T(8,128)(2,1)S(1)}, u32[]{:S(2)}, u32[]{:S(2)}) collective-permute-start(bf16[24,1024]{1,0:T(8,128)(2,1)S(1)} %get-tuple-element.68), channel_id=1, source_target_pairs={{0,6},{1,7},{2,8},{3,9},{4,10},{5,11},{6,12},{7,13},{8,14},{9,15},... | collective-permute-start | bytes 147464 | tf_op jit(solution)/shard_map/ppermute | solution.py:439
  132.7 9.1 %collective-permute-start.36 = (bf16[24,1024]{1,0:T(8,128)(2,1)S(1)}, bf16[24,1024]{1,0:T(8,128)(2,1)S(1)}, u32[]{:S(2)}, u32[]{:S(2)}) collective-permute-start(bf16[24,1024]{1,0:T(8,128)(2,1)S(1)} %shard_map.264), channel_id=1, source_target_pairs={{0,10},{1,11},{2,12},{3,13},{4,14},{5,15},{6,16},{7,17},{8,18},{9,... | collective-permute-start | bytes 147464 | tf_op jit(solution)/shard_map/ppermute | solution.py:439
  136.0 7.8 %collective-permute-start.37 = (bf16[24,1024]{1,0:T(8,128)(2,1)S(1)}, bf16[24,1024]{1,0:T(8,128)(2,1)S(1)}, u32[]{:S(2)}, u32[]{:S(2)}) collective-permute-start(bf16[24,1024]{1,0:T(8,128)(2,1)S(1)} %get-tuple-element.69), channel_id=1, source_target_pairs={{0,22},{1,23},{2,24},{3,25},{4,26},{5,27},{6,28},{7,29},{8,30},{9,... | collective-permute-start | bytes 147464 | tf_op jit(solution)/shard_map/ppermute | solution.py:439
  143.9 6.0 %collective-permute-start.38 = (f32[12,1024]{1,0:T(8,128)S(1)}, f32[12,1024]{1,0:T(8,128)S(1)}, u32[]{:S(2)}, u32[]{:S(2)}) collective-permute-start(f32[12,1024]{1,0:T(8,128)S(1)} %get-tuple-element.71), channel_id=1, source_target_pairs={{0,1},{1,0},{2,3},{3,2},{4,5},{5,4},{6,7},{7,6},{8,9},{9,8},{10,11... | collective-permute-start | bytes 147464 | tf_op jit(solution)/shard_map/ppermute | solution.py:433
